TPU v7x, 256 devices: a whole 4x4x8 slice. The times are simulated.
256 devices in a mesh: sp: 16 (over y, x), tp: 16 (over z, core).
Axes of the slice: x: 4, y: 4, z: 8, core: 2. Of those that a mesh axis runs over, the one named last changes fastest.
Arguments:
- queries: bfloat16 [8192, 2048], P('sp', 'tp'), may hold values from -16 to 16
- key_vectors: bfloat16 [8192, 2048], P('sp', 'tp'), may hold values from -4 to 4
- value_vectors: bfloat16 [8192, 2048], P('sp', 'tp'), may hold values from -5 to 5
- forget_totals: float32 [8192, 16], P('sp', 'tp'), may hold values from -1368 to 0, as said below
- head_gain: float32 [2048], P('tp'), may hold values from 0.1 to 1.9
- stream: bfloat16 [8192, 2048], P(('sp', 'tp')), may hold values from -6 to 6
- out_weight: bfloat16 [2048, 2048], replicated, may hold values from -0.125 to 0.125
- norm_gain: float32 [2048], replicated, may hold values from 0.1 to 1.9
- routing: int32 [8192, 2], P(('sp', 'tp')), may hold values from 0 to 15, all different within a row; in each aligned block of 32 rows (0 to 31, 32 to 63, ...) at most 8 rows name the same one
- route_weights: float32 [8192, 2], P(('sp', 'tp')), may hold values from 0.2 to 1
- gate_weight: bfloat16 [16, 2048, 4096], P('sp', None, 'tp'), may hold values from -0.125 to 0.125
- up_weight: bfloat16 [16, 2048, 4096], P('sp', None, 'tp'), may hold values from -0.125 to 0.125
- down_weight: bfloat16 [16, 4096, 2048], P('sp', 'tp'), may hold values from -0.09375 to 0.09375
Outputs:
- layer_out: bfloat16 [8192, 2048], P(('sp', 'tp'))
Inputs may be any that keep to these rules, and one draw needn't show every extreme that they name: `forget_totals`: along the positions, the values of each head never rise. `routing`: A token's 2 experts differ. Within the tokens of one device (aligned blocks of 32 rows) no expert is named more than 8 times.
All inputs are finite; a program needn't handle non-finite values.
Results may differ from a plain program's by a relative error of at most 0.01145.
Values may be sent and summed in bfloat16 or wider, within the bound.
No kernel may reach another device: no remote copies, remote signals or barrier semaphores. Data moves between devices by JAX's collectives and lax.ppermute only.
A program may use at most 128 MiB of HBM per device.

v0:
```python
from functools import partial

import jax
import jax.numpy as jnp
from jax import lax
from jax.experimental import pallas as pl
from jax.experimental.pallas import tpu as pltpu
from jax.sharding import PartitionSpec as P


HD = 128
TOP = 2
LOG2E = 1.4426950408889634
low_score = -1e30
GATE_ROWS = 16
KEYS = 256
PIECE = KEYS + GATE_ROWS
BLOCK = 2 * PIECE
PACK = HD + GATE_ROWS


def sp_perm(dy, dx, needed):
    pairs = []
    for y in range(4):
        for x in range(4):
            into = (y + dy) % 4, (x + dx) % 4
            if needed(*into):
                pairs.append((y * 4 + x, into[0] * 4 + into[1]))
    return pairs


def z_perm(dz):
    return [(z * 2 + c, ((z + dz) % 8) * 2 + c) for z in range(8) for c in range(2)]


core_swap = [(i, i ^ 1) for i in range(16)]


vmem = pl.BlockSpec(memory_space=pltpu.VMEM)


def three_parts(wide):
    first = wide.astype(jnp.bfloat16)
    rest = wide - first.astype(jnp.float32)
    second = rest.astype(jnp.bfloat16)
    third = (rest - second.astype(jnp.float32)).astype(jnp.bfloat16)
    return first, second, third


def piece_kernel(*refs):
    sources, outs, staged, sems = refs[:4], refs[4:6], refs[6:10], refs[10]
    copies = [
        pltpu.make_async_copy(source, into, sems.at[i])
        for i, (source, into) in enumerate(zip(sources, staged))
    ]
    for copy in copies:
        copy.start()
    for copy in copies:
        copy.wait()
    queries, keys, values, gates = staged
    keys_own, query_pack = outs
    stretched = gates[...] * HD**0.5
    tok_count = stretched.shape[1]
    row = lax.broadcasted_iota(jnp.int32, (GATE_ROWS, KEYS), 0)
    for i in range(2):
        at_row = i * PIECE
        rows = slice(i * KEYS, (i + 1) * KEYS)
        keys_own[at_row : at_row + HD, :] = jnp.transpose(values[rows, :])
        keys_own[at_row + HD : at_row + KEYS, 0:HD] = keys[i * KEYS : i * KEYS + HD, :]
        keys_own[at_row + HD : at_row + KEYS, HD:KEYS] = keys[i * KEYS + HD : (i + 1) * KEYS, :]
        parts = [part.astype(jnp.float32) for part in three_parts(-stretched[:, rows])]
        block = jnp.where((row >= 3) & (row < 6), 1.0, 0.0)
        for at, part in enumerate(parts):
            block = jnp.where(row == at, part, block)
        keys_own[at_row + KEYS : at_row + PIECE, :] = block.astype(jnp.bfloat16)
    wide_row = lax.broadcasted_iota(jnp.int32, (GATE_ROWS, tok_count), 0)
    mix = jnp.where(wide_row < 3, 1.0, 0.0)
    parts = [part.astype(jnp.float32) for part in three_parts(stretched[:, 0:1])]
    for at, part in enumerate(parts):
        mix = jnp.where(wide_row == 3 + at, part, mix)
    mix = jnp.where(wide_row == 6, low_score, mix)
    query_pack[HD:PACK, :] = mix.astype(jnp.bfloat16)
    query_pack[0:HD, :] = jnp.transpose(queries[...])


def make_pieces(queries, keys, values, gates):
    tok_count = queries.shape[0]
    return pl.pallas_call(
        piece_kernel,
        out_shape=(
            jax.ShapeDtypeStruct((BLOCK, 2 * HD), jnp.bfloat16),
            jax.ShapeDtypeStruct((PACK, tok_count), jnp.bfloat16),
        ),
        in_specs=[pl.BlockSpec(memory_space=pltpu.HBM)] * 4,
        out_specs=(vmem,) * 2,
        scratch_shapes=[pltpu.VMEM((tok_count, HD), jnp.bfloat16)] * 3
        + [pltpu.VMEM((1, tok_count), jnp.float32), pltpu.SemaphoreType.DMA((4,))],
        compiler_params=pltpu.CompilerParams(vmem_limit_bytes=6 << 20),
        name="make_pieces",
    )(queries, keys, values, gates.reshape(1, tok_count))


def fold(query_pack, state, pieces, own_block=False):
    run_max, run_sum, run_acc = state
    tok_count = query_pack.shape[1]
    scale = HD ** (-0.5) * LOG2E
    scores = []
    for i, (keys_in, at) in enumerate(pieces):
        bias = lax.dot_general(
            keys_in[pl.ds(at + KEYS, GATE_ROWS), :],
            query_pack[HD:PACK, :],
            (((0,), (0,)), ((), ())),
            preferred_element_type=jnp.float32,
        )
        for part in range(KEYS // HD):
            keys = keys_in[pl.ds(at + HD, HD), part * HD : (part + 1) * HD]
            score = jnp.dot(keys, query_pack[0:HD, :], preferred_element_type=jnp.float32)
            score = score + bias[part * HD : (part + 1) * HD]
            if own_block:
                key_at = lax.broadcasted_iota(jnp.int32, score.shape, 0)
                key_at = key_at + (i * KEYS + part * HD)
                query_at = lax.broadcasted_iota(jnp.int32, score.shape, 1)
                score = jnp.where(key_at <= query_at, score, low_score)
            scores.append(score)
    old_max = run_max[0:1, :]
    peak = scores[0]
    for score in scores[1:]:
        peak = jnp.maximum(peak, score)
    new_max = jnp.maximum(old_max, jnp.max(peak, axis=0, keepdims=True))
    rescale = jnp.exp2((old_max - new_max) * scale)
    scaled_max = new_max * scale
    total = run_sum[...] * rescale
    acc = run_acc[...] * rescale
    for i, (keys_in, at) in enumerate(pieces):
        rounded = []
        for score in scores[2 * i : 2 * i + 2]:
            lifted = jnp.exp2(score * scale - scaled_max)
            total = total + jnp.sum(lifted.reshape(HD // 8, 8, tok_count), axis=0)
            rounded.append(lifted.astype(jnp.bfloat16))
        acc = acc + jnp.dot(
            keys_in[pl.ds(at, HD), :],
            jnp.concatenate(rounded, axis=0),
            preferred_element_type=jnp.float32,
        )
    run_sum[...] = total
    run_acc[...] = acc
    run_max[...] = jnp.broadcast_to(new_max, run_max.shape)


def clear(state):
    run_max, run_sum, run_acc = state
    run_max[...] = jnp.full_like(run_max, low_score)
    run_sum[...] = jnp.zeros_like(run_sum)
    run_acc[...] = jnp.zeros_like(run_acc)


def fold_blocks(query_pack, state, stack, first, count, seen=None):
    def block(i, carry):
        at = pl.multiple_of(i * BLOCK, 32)

        def run():
            fold(query_pack, state, [(stack, at), (stack, at + PIECE)])

        if seen is None:
            run()
        else:
            pl.when(seen(i))(run)
        return carry

    lax.fori_loop(first, first + count, block, 0)


def pack_result(state, out):
    run_max, run_sum, run_acc = state
    total = jnp.sum(run_sum[...], axis=0, keepdims=True)
    out[0:HD, :] = (run_acc[...] / total).astype(jnp.bfloat16)
    row = lax.broadcasted_iota(jnp.int32, (GATE_ROWS, total.shape[1]), 0)
    block = jnp.zeros(row.shape, jnp.float32)
    for at, part in enumerate(three_parts(run_max[0:1, :]) + three_parts(total)):
        block = jnp.where(row == at, part.astype(jnp.float32), block)
    out[HD:PACK, :] = block.astype(jnp.bfloat16)


def fill(stack, parts):
    at = 0
    for part in parts:
        stack[at : at + part.shape[0], :] = part[...]
        at += part.shape[0]


def distant_kernel(*refs):
    packs, keys, states, stack = refs[:2], refs[2:5], (refs[5:8], refs[8:11]), refs[11]
    own_y = lax.axis_index("sp") >> 2
    fill(stack, keys)
    for pack, state, above in zip(packs, states, (3, 2)):

        @pl.when(own_y + above <= 3)
        def _():
            clear(state)
            fold_blocks(pack, state, stack, 0, 3)


def distant_end_kernel(*refs):
    packs, far, states_in, outs = refs[:2], refs[2:4], (refs[4:7], refs[7:10]), refs[10:12]
    state = refs[12:15]
    own_y = lax.axis_index("sp") >> 2
    for pack, state_in, out, above in zip(packs, states_in, outs, (3, 2)):

        @pl.when(own_y + above <= 3)
        def _():
            for into, came in zip(state, state_in):
                into[...] = came[...]
            fold(pack, state, [(far[0], 0), (far[1], 0)])
            pack_result(state, out)


def close_kernel(*refs):
    next_pack, own_pack = refs[:2]
    keys, out, own_state = refs[2:7], refs[7], refs[8:11]
    state, stack = refs[11:14], refs[14]
    own = lax.axis_index("sp")
    own_x = own & 3
    fill(stack, keys)

    @pl.when(own < 12)
    def _():
        clear(state)
        fold_blocks(next_pack, state, stack, 0, 4)
        pack_result(state, out)

    clear(own_state)
    fold(own_pack, own_state, [(keys[0], 0), (keys[0], PIECE)], own_block=True)

    def seen(i):
        move = jnp.where(i == 1, -1, jnp.where(i == 2, 1, 2))
        return ((own_x + move) & 3) < own_x

    fold_blocks(own_pack, own_state, stack, 1, 3, seen)


def merge_kernel(*refs):
    came, own_state, gain, head_out = refs[:3], refs[3:6], refs[6], refs[7]
    own_y = lax.axis_index("sp") >> 2
    scale = HD ** (-0.5) * LOG2E
    peaks = [own_state[0][0:1, :]]
    totals = [jnp.sum(own_state[1][...], axis=0, keepdims=True)]
    for above, pack in enumerate(came):
        rows = pack[HD:PACK, :].astype(jnp.float32)
        parts = [rows[at : at + 1, :] for at in range(6)]
        valid = own_y > above
        peaks.append(jnp.where(valid, parts[0] + parts[1] + parts[2], low_score))
        totals.append(jnp.where(valid, parts[3] + parts[4] + parts[5], 0.0))
    top = peaks[0]
    for peak in peaks[1:]:
        top = jnp.maximum(top, peak)
    weight = jnp.exp2((peaks[0] - top) * scale)
    total = totals[0] * weight
    acc = own_state[2][...] * weight
    for pack, peak, share in zip(came, peaks[1:], totals[1:]):
        weight = share * jnp.exp2((peak - top) * scale)
        total = total + weight
        acc = acc + pack[0:HD, :].astype(jnp.float32) * weight
    attended = acc / total
    mean_square = jnp.mean(attended * attended, axis=0, keepdims=True)
    normed = jnp.transpose(attended * lax.rsqrt(mean_square + 1e-06))
    head_out[...] = (normed * gain[...]).astype(jnp.bfloat16)


def attend(kernel, operands, outs, scratch, folds):
    tok_count = 2 * KEYS
    return pl.pallas_call(
        kernel,
        out_shape=tuple(jax.ShapeDtypeStruct(*out) for out in outs),
        in_specs=[vmem] * len(operands),
        out_specs=(vmem,) * len(outs),
        scratch_shapes=[pltpu.VMEM(*shape) for shape in scratch],
        compiler_params=pltpu.CompilerParams(vmem_limit_bytes=12 << 20),
        cost_estimate=pl.CostEstimate(
            flops=8 * tok_count * tok_count * HD * folds,
            transcendentals=tok_count * tok_count * folds,
            bytes_accessed=1 << 20,
        ),
    )(*operands)


def attention(queries, key_vectors, value_vectors, forget_totals, head_gain, early):
    tok_count = queries.shape[0]

    def shift(array, dy, dx, needed):
        return lax.ppermute(array, "sp", sp_perm(dy, dx, needed))

    keys_own, own_pack = make_pieces(queries, key_vectors, value_vectors, forget_totals)
    low = shift(keys_own, 0, 1, lambda y, x: y < 3 or x > 0)
    high = shift(keys_own, 0, -1, lambda y, x: y < 3 or x in (0, 3))
    pack3 = shift(own_pack, 1, 0, lambda y, x: y == 0)
    pack2 = shift(own_pack, 2, 0, lambda y, x: y < 2)
    pack1 = shift(own_pack, -1, 0, lambda y, x: y < 3)
    far_a = shift(low[:PIECE], 0, 1, lambda y, x: y < 3 or x > 1)
    far_b = shift(high[PIECE:], 0, -1, lambda y, x: y < 3 or x > 1)

    narrow = ((8, tok_count), jnp.float32)
    state = [narrow, narrow, ((HD, tok_count), jnp.float32)]
    result = ((PACK, tok_count), jnp.bfloat16)

    def stack(count):
        return ((count * BLOCK, 2 * HD), jnp.bfloat16)

    near = attend(distant_kernel, [pack3, pack2, keys_own, low, high], state * 2, [stack(3)], 6)
    far_a, far_b, near, early = lax.optimization_barrier((far_a, far_b, near, early))
    part3, part2 = attend(
        distant_end_kernel, [pack3, pack2, far_a, far_b, *near], [result] * 2, state, 2
    )
    part3, part2, pack1 = lax.optimization_barrier((part3, part2, pack1))
    back3 = shift(part3, -1, 0, lambda y, x: y == 3)
    back2 = shift(part2, 2, 0, lambda y, x: y > 1)
    part1, *own_state = attend(
        close_kernel,
        [pack1, own_pack, keys_own, low, high, far_a, far_b],
        [result] + state,
        state + [stack(4)],
        8,
    )
    back1 = shift(part1, 1, 0, lambda y, x: y > 0)
    (head_out,) = attend(
        merge_kernel,
        [back1, back2, back3, *own_state, head_gain.reshape(1, HD)],
        [((tok_count, HD), jnp.bfloat16)],
        [],
        0,
    )
    return head_out, early


def expert_kernel(*refs, count):
    rows = refs[:count]
    gate_a, gate_b, up_a, up_b, down_a, down_b = refs[count : count + 6]
    outs = refs[count + 6 : 2 * count + 6]
    joined, made = refs[2 * count + 6 :]
    each = rows[0].shape[0]
    for i, part in enumerate(rows):
        joined[i * each : (i + 1) * each, :] = part[...]
    tall, wide = 128, 512

    def block(i, carry):
        spot = pl.ds(pl.multiple_of(i * tall, tall), tall)
        mine = joined[spot, :]
        hidden = []
        for gate, up in ((gate_a, up_a), (gate_b, up_b)):
            gate_pre = jnp.dot(mine, gate[...], preferred_element_type=jnp.float32)
            up_pre = jnp.dot(mine, up[...], preferred_element_type=jnp.float32)
            silu = gate_pre / (1.0 + jnp.exp(-gate_pre))
            hidden.append((silu * up_pre).astype(jnp.bfloat16))

        def column(j, inner):
            cols = pl.ds(pl.multiple_of(j * wide, wide), wide)
            part = jnp.dot(
                hidden[0], down_a[:, cols], preferred_element_type=jnp.float32
            ) + jnp.dot(hidden[1], down_b[:, cols], preferred_element_type=jnp.float32)
            made[spot, cols] = part.astype(jnp.bfloat16)
            return inner

        return lax.fori_loop(0, made.shape[1] // wide, column, carry)

    lax.fori_loop(0, joined.shape[0] // tall, block, 0)
    for i, out in enumerate(outs):
        out[...] = made[i * each : (i + 1) * each, :]


def expert_rows(rows, weights):
    count = len(rows)
    each, width = rows[0].shape
    hidden = weights[0].shape[1] * 2
    flops = 2 * count * each * width * hidden * 3
    joined = pltpu.VMEM((count * each, width), jnp.bfloat16)
    return pl.pallas_call(
        partial(expert_kernel, count=count),
        out_shape=tuple(jax.ShapeDtypeStruct((each, width), jnp.bfloat16) for _ in rows),
        in_specs=[vmem] * (count + 6),
        out_specs=(vmem,) * count,
        scratch_shapes=[joined, joined],
        compiler_params=pltpu.CompilerParams(vmem_limit_bytes=16 << 20),
        cost_estimate=pl.CostEstimate(flops=flops, transcendentals=0, bytes_accessed=6 << 20),
    )(*rows, *weights)


def added(left, right):
    return (left.astype(jnp.float32) + right.astype(jnp.float32)).astype(jnp.bfloat16)


def expert_sum(own, weights):
    def up(array):
        return lax.ppermute(array, "tp", z_perm(1))

    def down(array):
        return lax.ppermute(array, "tp", z_perm(-1))

    half = own.shape[0] // 2
    top, end = own[:half], own[half:]
    up_top, down_end, up_end, down_top = [up(top)], [down(end)], [up(end)], [down(top)]
    for _ in range(2):
        up_top.append(up(up_top[-1]))
        down_end.append(down(down_end[-1]))
        up_end.append(up(up_end[-1]))
        down_top.append(down(down_top[-1]))
    up_top.append(up(up_top[-1]))
    down_end.append(down(down_end[-1]))
    chains = (up_top, up_end, down_top, down_end)
    near = expert_rows([top, end] + [chain[0] for chain in chains], weights)
    mid = expert_rows([chain[i] for i in (1, 2) for chain in chains], weights)
    far_top, far_end = expert_rows([up_top[3], down_end[3]], weights)
    done = [near[2:], mid[:4], mid[4:]]

    low_top, high_end = down(done[2][0]), up(done[2][3])
    high_top, low_end = up(far_top), down(far_end)
    high_top = up(added(high_top, done[2][2]))
    low_end = down(added(low_end, done[2][1]))
    for i in (1, 0):
        low_top = down(added(low_top, done[i][0]))
        high_end = up(added(high_end, done[i][3]))
        high_top = up(added(high_top, done[i][2]))
        low_end = down(added(low_end, done[i][1]))
    sums = []
    for parts in ((low_top, high_top, near[0]), (low_end, high_end, near[1])):
        low, high, mine = (part.astype(jnp.float32) for part in parts)
        sums.append((low + high + mine).astype(jnp.bfloat16))
    return jnp.concatenate(sums)


def place_rows(routing, slot_count, capacity):
    expert_count, row_count = slot_count // capacity, routing.shape[1]
    expert_id = lax.broadcasted_iota(jnp.int32, (expert_count, row_count), 0)
    chosen = [(routing[k : k + 1, :] == expert_id).astype(jnp.float32) for k in range(TOP)]
    before = lax.broadcasted_iota(jnp.int32, (row_count, row_count), 0)
    before = before < lax.broadcasted_iota(jnp.int32, (row_count, row_count), 1)
    before = before.astype(jnp.float32).astype(jnp.bfloat16)
    counts = jnp.dot(
        sum(chosen).astype(jnp.bfloat16), before, preferred_element_type=jnp.float32
    )
    slot_id = lax.broadcasted_iota(jnp.int32, (slot_count, row_count), 0)
    here = []
    for k in range(TOP):
        rank = jnp.sum(counts * chosen[k], axis=0, keepdims=True).astype(jnp.int32)
        here.append(slot_id == routing[k : k + 1, :] * capacity + rank)
    return here


def project_kernel(
    heads, out_weight, stream, norm_gain, routing, route_weights, resid_sum, outgoing, mixing, joined
):
    for head in range(heads.shape[0]):
        joined[:, head * HD : (head + 1) * HD] = heads[head]
    slot_count = mixing.shape[0]
    experts = slot_count // max(2, 2 * TOP * stream.shape[0] // lax.axis_size("sp"))
    here = place_rows(routing[...], slot_count, slot_count // experts)
    mix = jnp.zeros(mixing.shape, jnp.float32)
    place = jnp.zeros(mixing.shape, jnp.float32)
    for k in range(TOP):
        mix = jnp.where(here[k], route_weights[k : k + 1, :], mix)
        place = jnp.where(here[k], 1.0, place)
    mixing[...] = mix
    wide = 512

    def column(j, carry):
        cols = pl.ds(pl.multiple_of(j * wide, wide), wide)
        mixed_rows = jnp.dot(joined[...], out_weight[:, cols], preferred_element_type=jnp.float32)
        resid_sum[:, cols] = stream[:, cols].astype(jnp.float32) + mixed_rows
        return carry

    lax.fori_loop(0, resid_sum.shape[1] // wide, column, 0)
    resid = resid_sum[...]
    center = resid - jnp.mean(resid, axis=1, keepdims=True)
    spread = jnp.mean(center * center, axis=1, keepdims=True)
    normed = (center * lax.rsqrt(spread + 1e-05) * norm_gain[...]).astype(jnp.bfloat16)
    outgoing[...] = jnp.dot(
        place.astype(jnp.bfloat16), normed, preferred_element_type=jnp.float32
    ).astype(jnp.bfloat16)


def project(heads, out_weight, stream, norm_gain, routing, route_weights, slot_count):
    rows, width = stream.shape
    return pl.pallas_call(
        project_kernel,
        out_shape=(
            jax.ShapeDtypeStruct((rows, width), jnp.float32),
            jax.ShapeDtypeStruct((slot_count, width), jnp.bfloat16),
            jax.ShapeDtypeStruct((slot_count, rows), jnp.float32),
        ),
        in_specs=[vmem] * 6,
        out_specs=(vmem,) * 3,
        scratch_shapes=[pltpu.VMEM((rows, heads.shape[0] * HD), jnp.bfloat16)],
        compiler_params=pltpu.CompilerParams(vmem_limit_bytes=14 << 20),
        name="project",
    )(
        heads,
        out_weight,
        stream,
        norm_gain.reshape(1, width),
        jnp.transpose(routing),
        jnp.transpose(route_weights),
    )


def combine_kernel(resid_sum, returned, mixing, out):
    total = resid_sum[...]
    for part in three_parts(mixing[...]):
        total = total + lax.dot_general(
            part, returned[...], (((0,), (0,)), ((), ())), preferred_element_type=jnp.float32
        )
    out[...] = total.astype(jnp.bfloat16)


def combine(resid_sum, returned, mixing):
    return pl.pallas_call(
        combine_kernel,
        out_shape=jax.ShapeDtypeStruct(resid_sum.shape, jnp.bfloat16),
        in_specs=[vmem] * 3,
        out_specs=vmem,
        compiler_params=pltpu.CompilerParams(vmem_limit_bytes=6 << 20),
        name="combine",
    )(resid_sum, returned, mixing)


def on_device(
    queries,
    key_vectors,
    value_vectors,
    forget_totals,
    head_gain,
    stream,
    out_weight,
    norm_gain,
    routing,
    route_weights,
    gate_weight,
    up_weight,
    down_weight,
):
    sp_count = lax.axis_size("sp")
    own_weights = (gate_weight[0], up_weight[0], down_weight[0])
    other_weights = tuple(lax.ppermute(weight, "tp", core_swap) for weight in own_weights)
    head_out, other_weights = attention(
        queries, key_vectors, value_vectors, forget_totals, head_gain, other_weights
    )
    weights = []
    for mine, other in zip(own_weights, other_weights):
        weights += [mine, other]
    row_count, width = stream.shape
    capacity = max(2, 2 * TOP * row_count // sp_count)
    heads = head_out.reshape(-1, row_count, HD)
    heads = lax.all_to_all(heads, "tp", split_axis=0, concat_axis=0, tiled=True)
    resid_sum, outgoing, mixing = project(
        heads, out_weight, stream, norm_gain, routing, route_weights, sp_count * capacity
    )
    outgoing = outgoing.reshape(sp_count, capacity, width)
    arrived = lax.all_to_all(outgoing, "sp", split_axis=0, concat_axis=0, tiled=True)
    summed = expert_sum(arrived.reshape(-1, width), weights)
    expert_out = summed.reshape(sp_count, capacity, width)
    returned = lax.all_to_all(expert_out, "sp", split_axis=0, concat_axis=0, tiled=True)
    return combine(resid_sum, returned.reshape(-1, width), mixing)


def solution(mesh):
    in_specs = (
        P("sp", "tp"),
        P("sp", "tp"),
        P("sp", "tp"),
        P("sp", "tp"),
        P("tp"),
        P(("sp", "tp"), None),
        P(),
        P(),
        P(("sp", "tp"), None),
        P(("sp", "tp"), None),
        P("sp", None, "tp"),
        P("sp", None, "tp"),
        P("sp", "tp", None),
    )
    out_specs = P(("sp", "tp"), None)
    return jax.shard_map(
        on_device, mesh=mesh, in_specs=in_specs, out_specs=out_specs, check_vma=False
    )
```

profile of v0, /device:TPU:2, one launch (start us, length us, event | category | flops | bytes accessed | tf_op | source)
XLA Modules:
  0.0 215.8 jit_solution(16146746950186118525)
XLA Ops:
  5.9 3.4 %collective-permute-start.2 = (bf16[544,256]{1,0:T(8,128)(2,1)S(1)}, bf16[544,256]{1,0:T(8,128)(2,1)S(1)}, u32[]{:S(2)}, u32[]{:S(2)}) collective-permute-start(bf16[544,256]{1,0:T(8,128)(2,1)S(1)} %get-tuple-element.53.refs_2_), channel_id=1, source_target_pairs={{0,16},{16,32},{32,48},{48,0},{64,80},{80,96},{96,112},{112,64},{1... | collective-permute-start | bytes 835592 | tf_op jit(solution)/shard_map/ppermute | solution.py:290
  9.3 4.7 %collective-permute-done.refs_0_ = bf16[144,512]{1,0:T(8,128)(2,1)S(1)} collective-permute-done((bf16[144,512]{1,0:T(8,128)(2,1)S(1)}, bf16[144,512]{1,0:T(8,128)(2,1)S(1)}, u32[]{:S(2)}, u32[]{:S(2)}) %collective-permute-start) | collective-permute-done | bytes 147488 | tf_op jit(solution)/shard_map/ppermute | solution.py:290
  14.0 4.1 %collective-permute-start.4 = (bf16[544,256]{1,0:T(8,128)(2,1)S(1)}, bf16[544,256]{1,0:T(8,128)(2,1)S(1)}, u32[]{:S(2)}, u32[]{:S(2)}) collective-permute-start(bf16[544,256]{1,0:T(8,128)(2,1)S(1)} %get-tuple-element.53.refs_2_), channel_id=1, source_target_pairs={{0,48},{16,0},{32,16},{48,32},{64,112},{80,64},{96,80},{112,96},{1... | collective-permute-start | bytes 835592 | tf_op jit(solution)/shard_map/ppermute | solution.py:290
  18.1 1.3 collective-permute-start.1
  19.4 4.6 %collective-permute-done.4.refs_4_ = bf16[544,256]{1,0:T(8,128)(2,1)S(1)} collective-permute-done((bf16[544,256]{1,0:T(8,128)(2,1)S(1)}, bf16[544,256]{1,0:T(8,128)(2,1)S(1)}, u32[]{:S(2)}, u32[]{:S(2)}) %collective-permute-start.4) | collective-permute-done | bytes 278560 | tf_op jit(solution)/shard_map/ppermute | solution.py:290
  24.1 3.4 %collective-permute-start.3 = (bf16[272,256]{1,0:T(8,128)(2,1)S(1)}, bf16[272,256]{1,0:T(8,128)(2,1)S(1)}, u32[]{:S(2)}, u32[]{:S(2)}) collective-permute-start(bf16[272,256]{1,0:T(8,128)(2,1)S(1)} %slice.24), channel_id=1, source_target_pairs={{0,16},{16,32},{32,48},{48,0},{64,80},{80,96},{96,112},{112,64},{1... | collective-permute-start | bytes 417800 | tf_op jit(solution)/shard_map/ppermute | solution.py:290
  27.5 1.6 collective-permute-start.9
  29.1 2.1 collective-permute-done.3.refs_2_.refs_5_
  31.2 5.1 %collective-permute-start.5 = (bf16[272,256]{1,0:T(8,128)(2,1)S(1)}, bf16[272,256]{1,0:T(8,128)(2,1)S(1)}, u32[]{:S(2)}, u32[]{:S(2)}) collective-permute-start(bf16[272,256]{1,0:T(8,128)(2,1)S(1)} %slice.25), channel_id=1, source_target_pairs={{0,48},{16,0},{32,16},{48,32},{64,112},{80,64},{96,80},{112,96},{1... | collective-permute-start | bytes 417800 | tf_op jit(solution)/shard_map/ppermute | solution.py:290
  36.3 5.1 %shard_map.127 = (f32[8,512]{1,0:T(8,128)S(1)}, f32[8,512]{1,0:T(8,128)S(1)}, f32[128,512]{1,0:T(8,128)S(1)}, f32[8,512]{1,0:T(8,128)S(1)}, f32[8,512]{1,0:T(8,128)S(1)}, /*index=5*/f32[128,512]{1,0:T(8,128)S(1)}) custom-call(bf16[144,512]{1,0:T(8,128)(2,1)S(1)} %collective-permute-done.refs_0_, bf16[144,512]{1,0:T(8,128)(2,1)S(1)} %collective-permute-done.1.refs_1_, ...), custom_call_target="tpu_custom_call" | custom-call | flops 1610612736 | bytes 1048576 | tf_op jit(solution)/shard_map/pallas_call | solution.py:271
  41.5 1.7 shard_map.128
  43.3 5.1 %shard_map.129 = (bf16[144,512]{1,0:T(8,128)(2,1)S(1)}, f32[8,512]{1,0:T(8,128)S(1)}, f32[8,512]{1,0:T(8,128)S(1)}, f32[128,512]{1,0:T(8,128)S(1)}) custom-call(bf16[144,512]{1,0:T(8,128)(2,1)S(1)} %collective-permute-done.9.refs_0_, bf16[144,512]{1,0:T(8,128)(2,1)S(1)} %get-tuple-element.52.refs_1_, bf16[544,256]{1,0:T(8,128)(2,1)S(1)} %get-tuple-element.53.refs_2_, ...), custom_call_target="tpu_custom_call" | custom-call | flops 2147483648 | bytes 1048576 | tf_op jit(solution)/shard_map/pallas_call | solution.py:271
  48.4 1.3 collective-permute-start.10
  49.7 1.3 collective-permute-start.11
  51.0 1.3 collective-permute-start.12
  52.3 1.6 collective-permute-done.11.refs_1_
  55.3 16.1 %all_to_all.15.heads = bf16[16,32,128]{2,1,0:T(8,128)(2,1)S(1)} all-to-all(bf16[16,32,128]{2,1,0:T(8,128)(2,1)S(1)} %bitcast.33), channel_id=1, replica_groups=mesh['sp'=16,'tp'=16] {'tp'}, dimensions={0} | all-to-all | bytes 262144 | tf_op jit(solution)/shard_map/all_to_all | solution.py:550
  71.4 2.5 %project.1 = (f32[32,2048]{1,0:T(8,128)S(1)}, bf16[128,2048]{1,0:T(8,128)(2,1)S(1)}, f32[128,32]{1,0:T(8,128)S(1)}) custom-call(bf16[16,32,128]{2,1,0:T(8,128)(2,1)S(1)} %all_to_all.15.heads, bf16[2048,2048]{1,0:T(8,128)(2,1)S(1)} %bitcast.18, bf16[32,2048]{1,0:T(8,128)(2,1)S(1)} %copy-done.3, f32[1,2048]{1,0:T(1,128)S(1)} %bitcast.34, ...), custom_call_target="tpu_custom_call" | custom-call | tf_op jit(solution)/shard_map/project/pallas_call | solution.py:481
  73.9 20.0 %all_to_all.16 = bf16[16,8,2048]{2,1,0:T(8,128)(2,1)S(1)} all-to-all(bf16[16,8,2048]{2,1,0:T(8,128)(2,1)S(1)} %bitcast.32), channel_id=1, replica_groups=mesh['sp'=16,'tp'=16] {'sp'}, dimensions={0} | all-to-all | bytes 1048576 | tf_op jit(solution)/shard_map/all_to_all | solution.py:555
  95.3 2.5 %collective-permute-start.17 = (bf16[64,2048]{1,0:T(8,128)(2,1)S(1)}, bf16[64,2048]{1,0:T(8,128)(2,1)S(1)}, u32[]{:S(2)}, u32[]{:S(2)}) collective-permute-start(bf16[64,2048]{1,0:T(8,128)(2,1)S(1)} %get-tuple-element.100.refs_0_), channel_id=1, source_target_pairs={{0,14},{1,15},{2,0},{3,1},{4,2},{5,3},{6,4},{7,5},{8,6},{9,7},{10,... | collective-permute-start | bytes 786440 | tf_op jit(solution)/shard_map/ppermute | solution.py:395
  97.8 1.5 collective-permute-start.19
  99.3 5.1 %collective-permute-done.13.refs_2_ = bf16[64,2048]{1,0:T(8,128)(2,1)S(1)} collective-permute-done((bf16[64,2048]{1,0:T(8,128)(2,1)S(1)}, bf16[64,2048]{1,0:T(8,128)(2,1)S(1)}, u32[]{:S(2)}, u32[]{:S(2)}) %collective-permute-start.13) | collective-permute-done | bytes 262176 | tf_op jit(solution)/shard_map/ppermute | solution.py:392
  104.4 5.6 %collective-permute-done.15.refs_3_ = bf16[64,2048]{1,0:T(8,128)(2,1)S(1)} collective-permute-done((bf16[64,2048]{1,0:T(8,128)(2,1)S(1)}, bf16[64,2048]{1,0:T(8,128)(2,1)S(1)}, u32[]{:S(2)}, u32[]{:S(2)}) %collective-permute-start.15) | collective-permute-done | bytes 262176 | tf_op jit(solution)/shard_map/ppermute | solution.py:392
  110.0 3.2 %collective-permute-start.18 = (bf16[64,2048]{1,0:T(8,128)(2,1)S(1)}, bf16[64,2048]{1,0:T(8,128)(2,1)S(1)}, u32[]{:S(2)}, u32[]{:S(2)}) collective-permute-start(bf16[64,2048]{1,0:T(8,128)(2,1)S(1)} %collective-permute-done.17.refs_4_), channel_id=1, source_target_pairs={{0,14},{1,15},{2,0},{3,1},{4,2},{5,3},{6,4},{7,5},{8,6},{9,7},{10,... | collective-permute-start | bytes 786440 | tf_op jit(solution)/shard_map/ppermute | solution.py:395
  113.3 2.3 %collective-permute-done.14.refs_0_ = bf16[64,2048]{1,0:T(8,128)(2,1)S(1)} collective-permute-done((bf16[64,2048]{1,0:T(8,128)(2,1)S(1)}, bf16[64,2048]{1,0:T(8,128)(2,1)S(1)}, u32[]{:S(2)}, u32[]{:S(2)}) %collective-permute-start.14) | collective-permute-done | bytes 262176 | tf_op jit(solution)/shard_map/ppermute | solution.py:392
  115.6 5.6 %collective-permute-done.16.refs_1_ = bf16[64,2048]{1,0:T(8,128)(2,1)S(1)} collective-permute-done((bf16[64,2048]{1,0:T(8,128)(2,1)S(1)}, bf16[64,2048]{1,0:T(8,128)(2,1)S(1)}, u32[]{:S(2)}, u32[]{:S(2)}) %collective-permute-start.16) | collective-permute-done | bytes 262176 | tf_op jit(solution)/shard_map/ppermute | solution.py:392
  121.3 3.2 %collective-permute-start.23 = (bf16[64,2048]{1,0:T(8,128)(2,1)S(1)}, bf16[64,2048]{1,0:T(8,128)(2,1)S(1)}, u32[]{:S(2)}, u32[]{:S(2)}) collective-permute-start(bf16[64,2048]{1,0:T(8,128)(2,1)S(1)} %collective-permute-done.18.refs_2_), channel_id=1, source_target_pairs={{0,14},{1,15},{2,0},{3,1},{4,2},{5,3},{6,4},{7,5},{8,6},{9,7},{10,... | collective-permute-start | bytes 786440 | tf_op jit(solution)/shard_map/ppermute | solution.py:395
  124.6 2.3 %collective-permute-done.21.refs_4_ = bf16[64,2048]{1,0:T(8,128)(2,1)S(1)} collective-permute-done((bf16[64,2048]{1,0:T(8,128)(2,1)S(1)}, bf16[64,2048]{1,0:T(8,128)(2,1)S(1)}, u32[]{:S(2)}, u32[]{:S(2)}) %collective-permute-start.21) | collective-permute-done | bytes 262176 | tf_op jit(solution)/shard_map/ppermute | solution.py:392
  126.9 3.9 %collective-permute-done.22.refs_5_ = bf16[64,2048]{1,0:T(8,128)(2,1)S(1)} collective-permute-done((bf16[64,2048]{1,0:T(8,128)(2,1)S(1)}, bf16[64,2048]{1,0:T(8,128)(2,1)S(1)}, u32[]{:S(2)}, u32[]{:S(2)}) %collective-permute-start.22) | collective-permute-done | bytes 262176 | tf_op jit(solution)/shard_map/ppermute | solution.py:392
  130.7 1.4 collective-permute-done.24.refs_7_
  132.2 7.0 %shard_map.131 = (bf16[64,2048]{1,0:T(8,128)(2,1)S(1)}, bf16[64,2048]{1,0:T(8,128)(2,1)S(1)}, bf16[64,2048]{1,0:T(8,128)(2,1)S(1)}, bf16[64,2048]{1,0:T(8,128)(2...) custom-call(bf16[64,2048]{1,0:T(8,128)(2,1)S(1)} %collective-permute, ...), custom_call_target="tpu_custom_call" | custom-call | flops 3221225472 | bytes 6291456 | tf_op jit(solution)/shard_map/pallas_call | solution.py:375
  139.2 3.8 %collective-permute-start.25 = (bf16[64,2048]{1,0:T(8,128)(2,1)S(1)}, bf16[64,2048]{1,0:T(8,128)(2,1)S(1)}, u32[]{:S(2)}, u32[]{:S(2)}) collective-permute-start(bf16[64,2048]{1,0:T(8,128)(2,1)S(1)} %get-tuple-element.82), channel_id=1, source_target_pairs={{0,14},{1,15},{2,0},{3,1},{4,2},{5,3},{6,4},{7,5},{8,6},{9,7},{10,... | collective-permute-start | bytes 786440 | tf_op jit(solution)/shard_map/ppermute | solution.py:395
  143.0 5.3 %shard_map.132 = (bf16[64,2048]{1,0:T(8,128)(2,1)S(1)}, bf16[64,2048]{1,0:T(8,128)(2,1)S(1)}, bf16[64,2048]{1,0:T(8,128)(2,1)S(1)}, bf16[64,2048]{1,0:T(8,128)(2...) custom-call(bf16[64,2048]{1,0:T(8,128)(2,1)S(1)} %get-tuple-element.100.refs_0_, ...), custom_call_target="tpu_custom_call" | custom-call | flops 2415919104 | bytes 6291456 | tf_op jit(solution)/shard_map/pallas_call | solution.py:375
  148.4 3.2 %collective-permute-start.29 = (bf16[64,2048]{1,0:T(8,128)(2,1)S(1)}, bf16[64,2048]{1,0:T(8,128)(2,1)S(1)}, u32[]{:S(2)}, u32[]{:S(2)}) collective-permute-start(bf16[64,2048]{1,0:T(8,128)(2,1)S(1)} %collective-permute-done.24.refs_7_), channel_id=1, source_target_pairs={{0,14},{1,15},{2,0},{3,1},{4,2},{5,3},{6,4},{7,5},{8,6},{9,7},{10,... | collective-permute-start | bytes 786440 | tf_op jit(solution)/shard_map/ppermute | solution.py:395
  151.7 2.0 collective-permute-start.26
  153.7 5.3 %collective-permute-done.28.refs_0_ = bf16[64,2048]{1,0:T(8,128)(2,1)S(1)} collective-permute-done((bf16[64,2048]{1,0:T(8,128)(2,1)S(1)}, bf16[64,2048]{1,0:T(8,128)(2,1)S(1)}, u32[]{:S(2)}, u32[]{:S(2)}) %collective-permute-start.28) | collective-permute-done | bytes 262176 | tf_op jit(solution)/shard_map/ppermute | solution.py:392
  159.1 1.7 shard_map.133
  160.9 3.2 %collective-permute-start.34 = (bf16[64,2048]{1,0:T(8,128)(2,1)S(1)}, bf16[64,2048]{1,0:T(8,128)(2,1)S(1)}, u32[]{:S(2)}, u32[]{:S(2)}) collective-permute-start(bf16[64,2048]{1,0:T(8,128)(2,1)S(1)} %get-tuple-element.90), channel_id=1, source_target_pairs={{0,14},{1,15},{2,0},{3,1},{4,2},{5,3},{6,4},{7,5},{8,6},{9,7},{10,... | collective-permute-start | bytes 786440 | tf_op jit(solution)/shard_map/ppermute | solution.py:395
  164.4 3.3 %collective-permute-start.27 = (bf16[64,2048]{1,0:T(8,128)(2,1)S(1)}, bf16[64,2048]{1,0:T(8,128)(2,1)S(1)}, u32[]{:S(2)}, u32[]{:S(2)}) collective-permute-start(bf16[64,2048]{1,0:T(8,128)(2,1)S(1)} %add_convert_fusion.10), channel_id=1, source_target_pairs={{0,14},{1,15},{2,0},{3,1},{4,2},{5,3},{6,4},{7,5},{8,6},{9,7},{10,... | collective-permute-start | bytes 786440 | tf_op jit(solution)/shard_map/ppermute | solution.py:395
  167.6 3.6 %collective-permute-done.30 = bf16[64,2048]{1,0:T(8,128)(2,1)S(1)} collective-permute-done((bf16[64,2048]{1,0:T(8,128)(2,1)S(1)}, bf16[64,2048]{1,0:T(8,128)(2,1)S(1)}, u32[]{:S(2)}, u32[]{:S(2)}) %collective-permute-start.30) | collective-permute-done | bytes 262176 | tf_op jit(solution)/shard_map/ppermute | solution.py:392
  171.5 3.3 %collective-permute-start.35 = (bf16[64,2048]{1,0:T(8,128)(2,1)S(1)}, bf16[64,2048]{1,0:T(8,128)(2,1)S(1)}, u32[]{:S(2)}, u32[]{:S(2)}) collective-permute-start(bf16[64,2048]{1,0:T(8,128)(2,1)S(1)} %add_convert_fusion.5), channel_id=1, source_target_pairs={{0,14},{1,15},{2,0},{3,1},{4,2},{5,3},{6,4},{7,5},{8,6},{9,7},{10,... | collective-permute-start | bytes 786440 | tf_op jit(solution)/shard_map/ppermute | solution.py:395
  174.8 2.1 collective-permute-done.39
  177.0 5.1 %collective-permute-done.31 = bf16[64,2048]{1,0:T(8,128)(2,1)S(1)} collective-permute-done((bf16[64,2048]{1,0:T(8,128)(2,1)S(1)}, bf16[64,2048]{1,0:T(8,128)(2,1)S(1)}, u32[]{:S(2)}, u32[]{:S(2)}) %collective-permute-start.31) | collective-permute-done | bytes 262176 | tf_op jit(solution)/shard_map/ppermute | solution.py:392
  182.4 3.3 %collective-permute-start.36 = (bf16[64,2048]{1,0:T(8,128)(2,1)S(1)}, bf16[64,2048]{1,0:T(8,128)(2,1)S(1)}, u32[]{:S(2)}, u32[]{:S(2)}) collective-permute-start(bf16[64,2048]{1,0:T(8,128)(2,1)S(1)} %add_convert_fusion.4), channel_id=1, source_target_pairs={{0,14},{1,15},{2,0},{3,1},{4,2},{5,3},{6,4},{7,5},{8,6},{9,7},{10,... | collective-permute-start | bytes 786440 | tf_op jit(solution)/shard_map/ppermute | solution.py:395
  185.7 5.8 %collective-permute-done.32 = bf16[64,2048]{1,0:T(8,128)(2,1)S(1)} collective-permute-done((bf16[64,2048]{1,0:T(8,128)(2,1)S(1)}, bf16[64,2048]{1,0:T(8,128)(2,1)S(1)}, u32[]{:S(2)}, u32[]{:S(2)}) %collective-permute-start.32) | collective-permute-done | bytes 262176 | tf_op jit(solution)/shard_map/ppermute | solution.py:392
  191.7 3.3 %collective-permute-start.37 = (bf16[64,2048]{1,0:T(8,128)(2,1)S(1)}, bf16[64,2048]{1,0:T(8,128)(2,1)S(1)}, u32[]{:S(2)}, u32[]{:S(2)}) collective-permute-start(bf16[64,2048]{1,0:T(8,128)(2,1)S(1)} %add_convert_fusion.3), channel_id=1, source_target_pairs={{0,14},{1,15},{2,0},{3,1},{4,2},{5,3},{6,4},{7,5},{8,6},{9,7},{10,... | collective-permute-start | bytes 786440 | tf_op jit(solution)/shard_map/ppermute | solution.py:395
  195.0 4.2 %collective-permute-done.33 = bf16[64,2048]{1,0:T(8,128)(2,1)S(1)} collective-permute-done((bf16[64,2048]{1,0:T(8,128)(2,1)S(1)}, bf16[64,2048]{1,0:T(8,128)(2,1)S(1)}, u32[]{:S(2)}, u32[]{:S(2)}) %collective-permute-start.33) | collective-permute-done | bytes 262176 | tf_op jit(solution)/shard_map/ppermute | solution.py:392
  199.5 15.3 %all_to_all.17 = bf16[16,8,2048]{2,1,0:T(8,128)(2,1)S(1)} all-to-all(bf16[16,8,2048]{2,1,0:T(8,128)(2,1)S(1)} %maximum_bitcast_fusion), channel_id=1, replica_groups=mesh['sp'=16,'tp'=16] {'sp'}, dimensions={0} | all-to-all | bytes 1048576 | tf_op jit(solution)/shard_map/all_to_all | solution.py:558
  (92 shorter events, 11.6 us)
Async XLA Ops:
  0.0 41.5 %collective-permute-start.6 = (bf16[2048,256]{1,0:T(8,128)(2,1)}, bf16[2048,256]{1,0:T(8,128)(2,1)S(1)}, u32[]{:S(2)}, u32[]{:S(2)}) collective-permute-start(bf16[2048,256]{1,0:T(8,128)(2,1)} %bitcast.20), channel_id=1, source_target_pairs={{0,1},{1,0},{2,3},{3,2},{4,5},{5,4},{6,7},{7,6},{8,9},{9,8},{10,11... | collective-permute-start | bytes 3145736 | tf_op jit(solution)/shard_map/ppermute | solution.py:540
  0.0 41.5 %collective-permute-start.7 = (bf16[2048,256]{1,0:T(8,128)(2,1)}, bf16[2048,256]{1,0:T(8,128)(2,1)S(1)}, u32[]{:S(2)}, u32[]{:S(2)}) collective-permute-start(bf16[2048,256]{1,0:T(8,128)(2,1)} %bitcast.24), channel_id=1, source_target_pairs={{0,1},{1,0},{2,3},{3,2},{4,5},{5,4},{6,7},{7,6},{8,9},{9,8},{10,11... | collective-permute-start | bytes 3145736 | tf_op jit(solution)/shard_map/ppermute | solution.py:540
  0.5 41.0 %collective-permute-start.8 = (bf16[256,2048]{1,0:T(8,128)(2,1)}, bf16[256,2048]{1,0:T(8,128)(2,1)S(1)}, u32[]{:S(2)}, u32[]{:S(2)}) collective-permute-start(bf16[256,2048]{1,0:T(8,128)(2,1)} %bitcast.28), channel_id=1, source_target_pairs={{0,1},{1,0},{2,3},{3,2},{4,5},{5,4},{6,7},{7,6},{8,9},{9,8},{10,11... | collective-permute-start | bytes 3145736 | tf_op jit(solution)/shard_map/ppermute | solution.py:540
  3.9 51.1 %copy-start.11 = (f32[128]{0:T(128)S(1)}, f32[128]{0:T(128)}, u32[]{:S(2)}) copy-start(f32[128]{0:T(128)} %param.17) | copy-start | bytes 1540
  4.6 9.4 %collective-permute-start = (bf16[144,512]{1,0:T(8,128)(2,1)S(1)}, bf16[144,512]{1,0:T(8,128)(2,1)S(1)}, u32[]{:S(2)}, u32[]{:S(2)}) collective-permute-start(bf16[144,512]{1,0:T(8,128)(2,1)S(1)} %get-tuple-element.52.refs_1_), channel_id=1, source_target_pairs={{192,0},{208,16},{224,32},{240,48},{193,1},{209,17},{225,33},{241,... | collective-permute-start | bytes 442376 | tf_op jit(solution)/shard_map/ppermute | solution.py:290
  5.9 12.2 %collective-permute-start.2 = (bf16[544,256]{1,0:T(8,128)(2,1)S(1)}, bf16[544,256]{1,0:T(8,128)(2,1)S(1)}, u32[]{:S(2)}, u32[]{:S(2)}) collective-permute-start(bf16[544,256]{1,0:T(8,128)(2,1)S(1)} %get-tuple-element.53.refs_2_), channel_id=1, source_target_pairs={{0,16},{16,32},{32,48},{48,0},{64,80},{80,96},{96,112},{112,64},{1... | collective-permute-start | bytes 835592 | tf_op jit(solution)/shard_map/ppermute | solution.py:290
  14.0 10.1 %collective-permute-start.4 = (bf16[544,256]{1,0:T(8,128)(2,1)S(1)}, bf16[544,256]{1,0:T(8,128)(2,1)S(1)}, u32[]{:S(2)}, u32[]{:S(2)}) collective-permute-start(bf16[544,256]{1,0:T(8,128)(2,1)S(1)} %get-tuple-element.53.refs_2_), channel_id=1, source_target_pairs={{0,48},{16,0},{32,16},{48,32},{64,112},{80,64},{96,80},{112,96},{1... | collective-permute-start | bytes 835592 | tf_op jit(solution)/shard_map/ppermute | solution.py:290
  18.1 9.4 %collective-permute-start.1 = (bf16[144,512]{1,0:T(8,128)(2,1)S(1)}, bf16[144,512]{1,0:T(8,128)(2,1)S(1)}, u32[]{:S(2)}, u32[]{:S(2)}) collective-permute-start(bf16[144,512]{1,0:T(8,128)(2,1)S(1)} %get-tuple-element.52.refs_1_), channel_id=1, source_target_pairs={{128,0},{144,16},{160,32},{176,48},{192,64},{208,80},{224,96},{240... | collective-permute-start | bytes 442376 | tf_op jit(solution)/shard_map/ppermute | solution.py:290
  24.1 7.2 %collective-permute-start.3 = (bf16[272,256]{1,0:T(8,128)(2,1)S(1)}, bf16[272,256]{1,0:T(8,128)(2,1)S(1)}, u32[]{:S(2)}, u32[]{:S(2)}) collective-permute-start(bf16[272,256]{1,0:T(8,128)(2,1)S(1)} %slice.24), channel_id=1, source_target_pairs={{0,16},{16,32},{32,48},{48,0},{64,80},{80,96},{96,112},{112,64},{1... | collective-permute-start | bytes 417800 | tf_op jit(solution)/shard_map/ppermute | solution.py:290
  27.5 43.9 %slice-start = ((s8[8388608]{0:T(1024)(128)(4,1)}), s8[4194304]{0:T(1024)(128)(4,1)S(1)}, s32[]{:S(2)}) async-start(s8[8388608]{0:T(1024)(128)(4,1)} %bitcast.17), calls=%async_computation.3 | async-start | bytes 8388608
  27.5 43.8 %copy-start.3 = (bf16[32,2048]{1,0:T(8,128)(2,1)S(1)}, bf16[32,2048]{1,0:T(8,128)(2,1)}, u32[]{:S(2)}) copy-start(bf16[32,2048]{1,0:T(8,128)(2,1)} %stream.1) | copy-start | bytes 393220
  27.5 43.8 %copy-start.7 = (f32[2048]{0:T(1024)S(1)}, f32[2048]{0:T(1024)}, u32[]{:S(2)}) copy-start(f32[2048]{0:T(1024)} %param.20) | copy-start | bytes 24580
  27.5 15.7 %collective-permute-start.9 = (bf16[144,512]{1,0:T(8,128)(2,1)S(1)}, bf16[144,512]{1,0:T(8,128)(2,1)S(1)}, u32[]{:S(2)}, u32[]{:S(2)}) collective-permute-start(bf16[144,512]{1,0:T(8,128)(2,1)S(1)} %get-tuple-element.52.refs_1_), channel_id=1, source_target_pairs={{64,0},{80,16},{96,32},{112,48},{128,64},{144,80},{160,96},{176,11... | collective-permute-start | bytes 442376 | tf_op jit(solution)/shard_map/ppermute | solution.py:290
  31.2 10.2 %collective-permute-start.5 = (bf16[272,256]{1,0:T(8,128)(2,1)S(1)}, bf16[272,256]{1,0:T(8,128)(2,1)S(1)}, u32[]{:S(2)}, u32[]{:S(2)}) collective-permute-start(bf16[272,256]{1,0:T(8,128)(2,1)S(1)} %slice.25), channel_id=1, source_target_pairs={{0,48},{16,0},{32,16},{48,32},{64,112},{80,64},{96,80},{112,96},{1... | collective-permute-start | bytes 417800 | tf_op jit(solution)/shard_map/ppermute | solution.py:290
  43.2 88.9 %copy-start = (bf16[1,2048,256]{2,1,0:T(8,128)(2,1)S(1)}, bf16[1,2048,256]{2,1,0:T(8,128)(2,1)}, u32[]{:S(2)}) copy-start(bf16[1,2048,256]{2,1,0:T(8,128)(2,1)} %param.23) | copy-start | bytes 3145732
  43.2 88.9 %copy-start.1 = (bf16[1,2048,256]{2,1,0:T(8,128)(2,1)S(1)}, bf16[1,2048,256]{2,1,0:T(8,128)(2,1)}, u32[]{:S(2)}) copy-start(bf16[1,2048,256]{2,1,0:T(8,128)(2,1)} %param.24) | copy-start | bytes 3145732
  43.2 88.9 %copy-start.2 = (bf16[1,256,2048]{2,1,0:T(8,128)(2,1)S(1)}, bf16[1,256,2048]{2,1,0:T(8,128)(2,1)}, u32[]{:S(2)}) copy-start(bf16[1,256,2048]{2,1,0:T(8,128)(2,1)} %param.25) | copy-start | bytes 3145732
  48.4 4.0 %collective-permute-start.10 = (bf16[144,512]{1,0:T(8,128)(2,1)S(1)}, bf16[144,512]{1,0:T(8,128)(2,1)S(1)}, u32[]{:S(2)}, u32[]{:S(2)}) collective-permute-start(bf16[144,512]{1,0:T(8,128)(2,1)S(1)} %get-tuple-element.71), channel_id=1, source_target_pairs={{0,64},{16,80},{32,96},{48,112},{64,128},{80,144},{96,160},{112,17... | collective-permute-start | bytes 442376 | tf_op jit(solution)/shard_map/ppermute | solution.py:290
  49.7 4.2 %collective-permute-start.11 = (bf16[144,512]{1,0:T(8,128)(2,1)S(1)}, bf16[144,512]{1,0:T(8,128)(2,1)S(1)}, u32[]{:S(2)}, u32[]{:S(2)}) collective-permute-start(bf16[144,512]{1,0:T(8,128)(2,1)S(1)} %get-tuple-element.72), channel_id=1, source_target_pairs={{0,128},{16,144},{32,160},{48,176},{64,192},{80,208},{96,224},{112... | collective-permute-start | bytes 442376 | tf_op jit(solution)/shard_map/ppermute | solution.py:290
  51.0 4.0 %collective-permute-start.12 = (bf16[144,512]{1,0:T(8,128)(2,1)S(1)}, bf16[144,512]{1,0:T(8,128)(2,1)S(1)}, u32[]{:S(2)}, u32[]{:S(2)}) collective-permute-start(bf16[144,512]{1,0:T(8,128)(2,1)S(1)} %get-tuple-element.73), channel_id=1, source_target_pairs={{0,192},{16,208},{32,224},{48,240},{1,193},{17,209},{33,225},{49,2... | collective-permute-start | bytes 442376 | tf_op jit(solution)/shard_map/ppermute | solution.py:290
  93.9 10.5 %collective-permute-start.13 = (bf16[64,2048]{1,0:T(8,128)(2,1)S(1)}, bf16[64,2048]{1,0:T(8,128)(2,1)S(1)}, u32[]{:S(2)}, u32[]{:S(2)}) collective-permute-start(bf16[64,2048]{1,0:T(8,128)(2,1)S(1)} %get-tuple-element.100.refs_0_), channel_id=1, source_target_pairs={{0,2},{1,3},{2,4},{3,5},{4,6},{5,7},{6,8},{7,9},{8,10},{9,11},{10,... | collective-permute-start | bytes 786440 | tf_op jit(solution)/shard_map/ppermute | solution.py:392
  94.6 15.5 %collective-permute-start.15 = (bf16[64,2048]{1,0:T(8,128)(2,1)S(1)}, bf16[64,2048]{1,0:T(8,128)(2,1)S(1)}, u32[]{:S(2)}, u32[]{:S(2)}) collective-permute-start(bf16[64,2048]{1,0:T(8,128)(2,1)S(1)} %get-tuple-element.99.refs_1_), channel_id=1, source_target_pairs={{0,2},{1,3},{2,4},{3,5},{4,6},{5,7},{6,8},{7,9},{8,10},{9,11},{10,... | collective-permute-start | bytes 786440 | tf_op jit(solution)/shard_map/ppermute | solution.py:392
  95.3 14.7 %collective-permute-start.17 = (bf16[64,2048]{1,0:T(8,128)(2,1)S(1)}, bf16[64,2048]{1,0:T(8,128)(2,1)S(1)}, u32[]{:S(2)}, u32[]{:S(2)}) collective-permute-start(bf16[64,2048]{1,0:T(8,128)(2,1)S(1)} %get-tuple-element.100.refs_0_), channel_id=1, source_target_pairs={{0,14},{1,15},{2,0},{3,1},{4,2},{5,3},{6,4},{7,5},{8,6},{9,7},{10,... | collective-permute-start | bytes 786440 | tf_op jit(solution)/shard_map/ppermute | solution.py:395
  97.8 15.5 %collective-permute-start.19 = (bf16[64,2048]{1,0:T(8,128)(2,1)S(1)}, bf16[64,2048]{1,0:T(8,128)(2,1)S(1)}, u32[]{:S(2)}, u32[]{:S(2)}) collective-permute-start(bf16[64,2048]{1,0:T(8,128)(2,1)S(1)} %get-tuple-element.99.refs_1_), channel_id=1, source_target_pairs={{0,14},{1,15},{2,0},{3,1},{4,2},{5,3},{6,4},{7,5},{8,6},{9,7},{10,... | collective-permute-start | bytes 786440 | tf_op jit(solution)/shard_map/ppermute | solution.py:395
  104.4 11.2 %collective-permute-start.14 = (bf16[64,2048]{1,0:T(8,128)(2,1)S(1)}, bf16[64,2048]{1,0:T(8,128)(2,1)S(1)}, u32[]{:S(2)}, u32[]{:S(2)}) collective-permute-start(bf16[64,2048]{1,0:T(8,128)(2,1)S(1)} %collective-permute-done.13.refs_2_), channel_id=1, source_target_pairs={{0,2},{1,3},{2,4},{3,5},{4,6},{5,7},{6,8},{7,9},{8,10},{9,11},{10,... | collective-permute-start | bytes 786440 | tf_op jit(solution)/shard_map/ppermute | solution.py:392
  110.0 11.2 %collective-permute-start.16 = (bf16[64,2048]{1,0:T(8,128)(2,1)S(1)}, bf16[64,2048]{1,0:T(8,128)(2,1)S(1)}, u32[]{:S(2)}, u32[]{:S(2)}) collective-permute-start(bf16[64,2048]{1,0:T(8,128)(2,1)S(1)} %collective-permute-done.15.refs_3_), channel_id=1, source_target_pairs={{0,2},{1,3},{2,4},{3,5},{4,6},{5,7},{6,8},{7,9},{8,10},{9,11},{10,... | collective-permute-start | bytes 786440 | tf_op jit(solution)/shard_map/ppermute | solution.py:392
  110.0 11.2 %collective-permute-start.18 = (bf16[64,2048]{1,0:T(8,128)(2,1)S(1)}, bf16[64,2048]{1,0:T(8,128)(2,1)S(1)}, u32[]{:S(2)}, u32[]{:S(2)}) collective-permute-start(bf16[64,2048]{1,0:T(8,128)(2,1)S(1)} %collective-permute-done.17.refs_4_), channel_id=1, source_target_pairs={{0,14},{1,15},{2,0},{3,1},{4,2},{5,3},{6,4},{7,5},{8,6},{9,7},{10,... | collective-permute-start | bytes 786440 | tf_op jit(solution)/shard_map/ppermute | solution.py:395
  113.3 11.2 %collective-permute-start.20 = (bf16[64,2048]{1,0:T(8,128)(2,1)S(1)}, bf16[64,2048]{1,0:T(8,128)(2,1)S(1)}, u32[]{:S(2)}, u32[]{:S(2)}) collective-permute-start(bf16[64,2048]{1,0:T(8,128)(2,1)S(1)} %collective-permute-done.19.refs_5_), channel_id=1, source_target_pairs={{0,14},{1,15},{2,0},{3,1},{4,2},{5,3},{6,4},{7,5},{8,6},{9,7},{10,... | collective-permute-start | bytes 786440 | tf_op jit(solution)/shard_map/ppermute | solution.py:395
  115.6 11.2 %collective-permute-start.21 = (bf16[64,2048]{1,0:T(8,128)(2,1)S(1)}, bf16[64,2048]{1,0:T(8,128)(2,1)S(1)}, u32[]{:S(2)}, u32[]{:S(2)}) collective-permute-start(bf16[64,2048]{1,0:T(8,128)(2,1)S(1)} %collective-permute-done.14.refs_0_), channel_id=1, source_target_pairs={{0,2},{1,3},{2,4},{3,5},{4,6},{5,7},{6,8},{7,9},{8,10},{9,11},{10,... | collective-permute-start | bytes 786440 | tf_op jit(solution)/shard_map/ppermute | solution.py:392
  121.2 9.5 %collective-permute-start.22 = (bf16[64,2048]{1,0:T(8,128)(2,1)S(1)}, bf16[64,2048]{1,0:T(8,128)(2,1)S(1)}, u32[]{:S(2)}, u32[]{:S(2)}) collective-permute-start(bf16[64,2048]{1,0:T(8,128)(2,1)S(1)} %collective-permute-done.16.refs_1_), channel_id=1, source_target_pairs={{0,2},{1,3},{2,4},{3,5},{4,6},{5,7},{6,8},{7,9},{8,10},{9,11},{10,... | collective-permute-start | bytes 786440 | tf_op jit(solution)/shard_map/ppermute | solution.py:392
  121.3 9.5 %collective-permute-start.23 = (bf16[64,2048]{1,0:T(8,128)(2,1)S(1)}, bf16[64,2048]{1,0:T(8,128)(2,1)S(1)}, u32[]{:S(2)}, u32[]{:S(2)}) collective-permute-start(bf16[64,2048]{1,0:T(8,128)(2,1)S(1)} %collective-permute-done.18.refs_2_), channel_id=1, source_target_pairs={{0,14},{1,15},{2,0},{3,1},{4,2},{5,3},{6,4},{7,5},{8,6},{9,7},{10,... | collective-permute-start | bytes 786440 | tf_op jit(solution)/shard_map/ppermute | solution.py:395
  124.5 7.7 %collective-permute-start.24 = (bf16[64,2048]{1,0:T(8,128)(2,1)S(1)}, bf16[64,2048]{1,0:T(8,128)(2,1)S(1)}, u32[]{:S(2)}, u32[]{:S(2)}) collective-permute-start(bf16[64,2048]{1,0:T(8,128)(2,1)S(1)} %collective-permute-done.20.refs_3_), channel_id=1, source_target_pairs={{0,14},{1,15},{2,0},{3,1},{4,2},{5,3},{6,4},{7,5},{8,6},{9,7},{10,... | collective-permute-start | bytes 786440 | tf_op jit(solution)/shard_map/ppermute | solution.py:395
  139.2 12.5 %collective-permute-start.25 = (bf16[64,2048]{1,0:T(8,128)(2,1)S(1)}, bf16[64,2048]{1,0:T(8,128)(2,1)S(1)}, u32[]{:S(2)}, u32[]{:S(2)}) collective-permute-start(bf16[64,2048]{1,0:T(8,128)(2,1)S(1)} %get-tuple-element.82), channel_id=1, source_target_pairs={{0,14},{1,15},{2,0},{3,1},{4,2},{5,3},{6,4},{7,5},{8,6},{9,7},{10,... | collective-permute-start | bytes 786440 | tf_op jit(solution)/shard_map/ppermute | solution.py:395
  148.2 15.9 %collective-permute-start.38 = (bf16[64,2048]{1,0:T(8,128)(2,1)S(1)}, bf16[64,2048]{1,0:T(8,128)(2,1)S(1)}, u32[]{:S(2)}, u32[]{:S(2)}) collective-permute-start(bf16[64,2048]{1,0:T(8,128)(2,1)S(1)} %get-tuple-element.94), channel_id=1, source_target_pairs={{0,2},{1,3},{2,4},{3,5},{4,6},{5,7},{6,8},{7,9},{8,10},{9,11},{10,... | collective-permute-start | bytes 786440 | tf_op jit(solution)/shard_map/ppermute | solution.py:392
  148.3 10.7 %collective-permute-start.28 = (bf16[64,2048]{1,0:T(8,128)(2,1)S(1)}, bf16[64,2048]{1,0:T(8,128)(2,1)S(1)}, u32[]{:S(2)}, u32[]{:S(2)}) collective-permute-start(bf16[64,2048]{1,0:T(8,128)(2,1)S(1)} %collective-permute-done.21.refs_4_), channel_id=1, source_target_pairs={{0,2},{1,3},{2,4},{3,5},{4,6},{5,7},{6,8},{7,9},{8,10},{9,11},{10,... | collective-permute-start | bytes 786440 | tf_op jit(solution)/shard_map/ppermute | solution.py:392
  148.4 10.7 %collective-permute-start.29 = (bf16[64,2048]{1,0:T(8,128)(2,1)S(1)}, bf16[64,2048]{1,0:T(8,128)(2,1)S(1)}, u32[]{:S(2)}, u32[]{:S(2)}) collective-permute-start(bf16[64,2048]{1,0:T(8,128)(2,1)S(1)} %collective-permute-done.24.refs_7_), channel_id=1, source_target_pairs={{0,14},{1,15},{2,0},{3,1},{4,2},{5,3},{6,4},{7,5},{8,6},{9,7},{10,... | collective-permute-start | bytes 786440 | tf_op jit(solution)/shard_map/ppermute | solution.py:395
  151.7 12.6 %collective-permute-start.26 = (bf16[64,2048]{1,0:T(8,128)(2,1)S(1)}, bf16[64,2048]{1,0:T(8,128)(2,1)S(1)}, u32[]{:S(2)}, u32[]{:S(2)}) collective-permute-start(bf16[64,2048]{1,0:T(8,128)(2,1)S(1)} %add_convert_fusion.11), channel_id=1, source_target_pairs={{0,14},{1,15},{2,0},{3,1},{4,2},{5,3},{6,4},{7,5},{8,6},{9,7},{10,... | collective-permute-start | bytes 786440 | tf_op jit(solution)/shard_map/ppermute | solution.py:395
  160.8 10.5 %collective-permute-start.30 = (bf16[64,2048]{1,0:T(8,128)(2,1)S(1)}, bf16[64,2048]{1,0:T(8,128)(2,1)S(1)}, u32[]{:S(2)}, u32[]{:S(2)}) collective-permute-start(bf16[64,2048]{1,0:T(8,128)(2,1)S(1)} %get-tuple-element.85), channel_id=1, source_target_pairs={{0,2},{1,3},{2,4},{3,5},{4,6},{5,7},{6,8},{7,9},{8,10},{9,11},{10,... | collective-permute-start | bytes 786440 | tf_op jit(solution)/shard_map/ppermute | solution.py:392
  160.9 10.5 %collective-permute-start.34 = (bf16[64,2048]{1,0:T(8,128)(2,1)S(1)}, bf16[64,2048]{1,0:T(8,128)(2,1)S(1)}, u32[]{:S(2)}, u32[]{:S(2)}) collective-permute-start(bf16[64,2048]{1,0:T(8,128)(2,1)S(1)} %get-tuple-element.90), channel_id=1, source_target_pairs={{0,14},{1,15},{2,0},{3,1},{4,2},{5,3},{6,4},{7,5},{8,6},{9,7},{10,... | collective-permute-start | bytes 786440 | tf_op jit(solution)/shard_map/ppermute | solution.py:395
  164.2 12.7 %collective-permute-start.39 = (bf16[64,2048]{1,0:T(8,128)(2,1)S(1)}, bf16[64,2048]{1,0:T(8,128)(2,1)S(1)}, u32[]{:S(2)}, u32[]{:S(2)}) collective-permute-start(bf16[64,2048]{1,0:T(8,128)(2,1)S(1)} %add_convert_fusion.2), channel_id=1, source_target_pairs={{0,2},{1,3},{2,4},{3,5},{4,6},{5,7},{6,8},{7,9},{8,10},{9,11},{10,... | collective-permute-start | bytes 786440 | tf_op jit(solution)/shard_map/ppermute | solution.py:392
  164.4 30.6 %collective-permute-start.27 = (bf16[64,2048]{1,0:T(8,128)(2,1)S(1)}, bf16[64,2048]{1,0:T(8,128)(2,1)S(1)}, u32[]{:S(2)}, u32[]{:S(2)}) collective-permute-start(bf16[64,2048]{1,0:T(8,128)(2,1)S(1)} %add_convert_fusion.10), channel_id=1, source_target_pairs={{0,14},{1,15},{2,0},{3,1},{4,2},{5,3},{6,4},{7,5},{8,6},{9,7},{10,... | collective-permute-start | bytes 786440 | tf_op jit(solution)/shard_map/ppermute | solution.py:395
  171.3 10.8 %collective-permute-start.31 = (bf16[64,2048]{1,0:T(8,128)(2,1)S(1)}, bf16[64,2048]{1,0:T(8,128)(2,1)S(1)}, u32[]{:S(2)}, u32[]{:S(2)}) collective-permute-start(bf16[64,2048]{1,0:T(8,128)(2,1)S(1)} %add_convert_fusion.9), channel_id=1, source_target_pairs={{0,2},{1,3},{2,4},{3,5},{4,6},{5,7},{6,8},{7,9},{8,10},{9,11},{10,... | collective-permute-start | bytes 786440 | tf_op jit(solution)/shard_map/ppermute | solution.py:392
  171.5 10.8 %collective-permute-start.35 = (bf16[64,2048]{1,0:T(8,128)(2,1)S(1)}, bf16[64,2048]{1,0:T(8,128)(2,1)S(1)}, u32[]{:S(2)}, u32[]{:S(2)}) collective-permute-start(bf16[64,2048]{1,0:T(8,128)(2,1)S(1)} %add_convert_fusion.5), channel_id=1, source_target_pairs={{0,14},{1,15},{2,0},{3,1},{4,2},{5,3},{6,4},{7,5},{8,6},{9,7},{10,... | collective-permute-start | bytes 786440 | tf_op jit(solution)/shard_map/ppermute | solution.py:395
  176.9 22.4 %collective-permute-start.40 = (bf16[64,2048]{1,0:T(8,128)(2,1)S(1)}, bf16[64,2048]{1,0:T(8,128)(2,1)S(1)}, u32[]{:S(2)}, u32[]{:S(2)}) collective-permute-start(bf16[64,2048]{1,0:T(8,128)(2,1)S(1)} %add_convert_fusion.1), channel_id=1, source_target_pairs={{0,2},{1,3},{2,4},{3,5},{4,6},{5,7},{6,8},{7,9},{8,10},{9,11},{10,... | collective-permute-start | bytes 786440 | tf_op jit(solution)/shard_map/ppermute | solution.py:392
  182.2 9.3 %collective-permute-start.32 = (bf16[64,2048]{1,0:T(8,128)(2,1)S(1)}, bf16[64,2048]{1,0:T(8,128)(2,1)S(1)}, u32[]{:S(2)}, u32[]{:S(2)}) collective-permute-start(bf16[64,2048]{1,0:T(8,128)(2,1)S(1)} %add_convert_fusion.8), channel_id=1, source_target_pairs={{0,2},{1,3},{2,4},{3,5},{4,6},{5,7},{6,8},{7,9},{8,10},{9,11},{10,... | collective-permute-start | bytes 786440 | tf_op jit(solution)/shard_map/ppermute | solution.py:392
  182.4 9.2 %collective-permute-start.36 = (bf16[64,2048]{1,0:T(8,128)(2,1)S(1)}, bf16[64,2048]{1,0:T(8,128)(2,1)S(1)}, u32[]{:S(2)}, u32[]{:S(2)}) collective-permute-start(bf16[64,2048]{1,0:T(8,128)(2,1)S(1)} %add_convert_fusion.4), channel_id=1, source_target_pairs={{0,14},{1,15},{2,0},{3,1},{4,2},{5,3},{6,4},{7,5},{8,6},{9,7},{10,... | collective-permute-start | bytes 786440 | tf_op jit(solution)/shard_map/ppermute | solution.py:395
  191.5 7.7 %collective-permute-start.33 = (bf16[64,2048]{1,0:T(8,128)(2,1)S(1)}, bf16[64,2048]{1,0:T(8,128)(2,1)S(1)}, u32[]{:S(2)}, u32[]{:S(2)}) collective-permute-start(bf16[64,2048]{1,0:T(8,128)(2,1)S(1)} %add_convert_fusion.7), channel_id=1, source_target_pairs={{0,2},{1,3},{2,4},{3,5},{4,6},{5,7},{6,8},{7,9},{8,10},{9,11},{10,... | collective-permute-start | bytes 786440 | tf_op jit(solution)/shard_map/ppermute | solution.py:392
  191.7 7.6 %collective-permute-start.37 = (bf16[64,2048]{1,0:T(8,128)(2,1)S(1)}, bf16[64,2048]{1,0:T(8,128)(2,1)S(1)}, u32[]{:S(2)}, u32[]{:S(2)}) collective-permute-start(bf16[64,2048]{1,0:T(8,128)(2,1)S(1)} %add_convert_fusion.3), channel_id=1, source_target_pairs={{0,14},{1,15},{2,0},{3,1},{4,2},{5,3},{6,4},{7,5},{8,6},{9,7},{10,... | collective-permute-start | bytes 786440 | tf_op jit(solution)/shard_map/ppermute | solution.py:395
  (7 other events, 119.2 us)
where the time goes:
time: 216 us
  waiting for transfers between devices  66.4 us (31%)
  starting transfers between devices  62.7 us (29%)
  blocking collectives  51.3 us (24%)
  Pallas kernels  30.5 us (14%)
  local copies, waits for them, and re-layouts  3.52 us (2%)
    ppermute x14, waiting for transfers between devices, up(): return lax.ppermute(array, 'tp', z_perm(1))  50.9 us
    ppermute x14, starting transfers between devices, down(): return lax.ppermute(array, 'tp', z_perm(-1))  36 us
    ppermute x10, starting transfers between devices, shift(): return lax.ppermute(array, 'sp', sp_perm(dy, dx, needed))  24.1 us
    all_to_all x1, blocking collectives, on_device(): lax.all_to_all(outgoing, 'sp', split_axis=0, concat_axis=0, tiled=True)  20 us
    all_to_all x1, blocking collectives, on_device(): heads = lax.all_to_all(heads, 'tp', split_axis=0, concat_axis=0, tiled=True)  16.1 us
    all_to_all x1, blocking collectives, on_device(): lax.all_to_all(expert_out, 'sp', split_axis=0, concat_axis=0, tiled=True)  15.3 us
    ppermute x10, waiting for transfers between devices, shift(): return lax.ppermute(array, 'sp', sp_perm(dy, dx, needed))  14 us
    pallas_call x3, Pallas kernels, expert_rows(): pl.pallas_call(partial(expert_kernel, count=count), out_shape=tuple((jax....  14 us
  transfers between devices with their start and end apart: 41, of which 18 were waited for; matrix products, arithmetic and copies ran while one was open for 0% of the time, Pallas kernels for 7%

commit v1 on v0

--- a/solution.py
+++ b/solution.py
@@ -37,6 +37,10 @@
 
 
 vmem = pl.BlockSpec(memory_space=pltpu.VMEM)
+
+
+def in_hbm(*arrays):
+    return [pltpu.with_memory_space_constraint(array, pltpu.HBM) for array in arrays]
 
 
 def three_parts(wide):
@@ -97,7 +101,7 @@
         + [pltpu.VMEM((1, tok_count), jnp.float32), pltpu.SemaphoreType.DMA((4,))],
         compiler_params=pltpu.CompilerParams(vmem_limit_bytes=6 << 20),
         name="make_pieces",
-    )(queries, keys, values, gates.reshape(1, tok_count))
+    )(*in_hbm(queries, keys, values, gates.reshape(1, tok_count)))
 
 
 def fold(query_pack, state, pieces, own_block=False):
@@ -283,7 +287,7 @@
     )(*operands)
 
 
-def attention(queries, key_vectors, value_vectors, forget_totals, head_gain, early):
+def attention(queries, key_vectors, value_vectors, forget_totals, head_gain, weights):
     tok_count = queries.shape[0]
 
     def shift(array, dy, dx, needed):
@@ -306,7 +310,7 @@
         return ((count * BLOCK, 2 * HD), jnp.bfloat16)
 
     near = attend(distant_kernel, [pack3, pack2, keys_own, low, high], state * 2, [stack(3)], 6)
-    far_a, far_b, near, early = lax.optimization_barrier((far_a, far_b, near, early))
+    far_a, far_b, near = lax.optimization_barrier((far_a, far_b, near))
     part3, part2 = attend(
         distant_end_kernel, [pack3, pack2, far_a, far_b, *near], [result] * 2, state, 2
     )
@@ -321,6 +325,8 @@
         8,
     )
     back1 = shift(part1, 1, 0, lambda y, x: y > 0)
+    part1, weights = lax.optimization_barrier((part1, weights))
+    staged = stage_weights(*weights)
     (head_out,) = attend(
         merge_kernel,
         [back1, back2, back3, *own_state, head_gain.reshape(1, HD)],
@@ -328,59 +334,87 @@
         [],
         0,
     )
-    return head_out, early
+    return head_out, staged
+
+
+def staging_kernel(gate, up, down, out, sems):
+    tall, wide = gate.shape
+    copies = [
+        pltpu.make_async_copy(gate, out.at[pl.ds(0, tall)], sems.at[0]),
+        pltpu.make_async_copy(up, out.at[pl.ds(tall, tall)], sems.at[1]),
+    ]
+    for i in range(down.shape[1] // wide):
+        source = down.at[:, pl.ds(i * wide, wide)]
+        into = out.at[pl.ds(2 * tall + i * down.shape[0], down.shape[0])]
+        copies.append(pltpu.make_async_copy(source, into, sems.at[2 + i]))
+    for copy in copies:
+        copy.start()
+    for copy in copies:
+        copy.wait()
+
+
+def stage_weights(gate, up, down):
+    blocks = down.shape[1] // gate.shape[1]
+    rows = 2 * gate.shape[0] + blocks * down.shape[0]
+    return pl.pallas_call(
+        staging_kernel,
+        out_shape=jax.ShapeDtypeStruct((rows, gate.shape[1]), jnp.bfloat16),
+        in_specs=[pl.BlockSpec(memory_space=pltpu.HBM)] * 3,
+        out_specs=vmem,
+        scratch_shapes=[pltpu.SemaphoreType.DMA((2 + blocks,))],
+        compiler_params=pltpu.CompilerParams(vmem_limit_bytes=4 << 20),
+        name="stage_weights",
+    )(*in_hbm(gate, up, down))
 
 
 def expert_kernel(*refs, count):
-    rows = refs[:count]
-    gate_a, gate_b, up_a, up_b, down_a, down_b = refs[count : count + 6]
-    outs = refs[count + 6 : 2 * count + 6]
-    joined, made = refs[2 * count + 6 :]
-    each = rows[0].shape[0]
+    rows, halves = refs[:count], refs[count : count + 2]
+    outs = refs[count + 2 : 2 * count + 2]
+    joined, made = refs[2 * count + 2 :]
+    each, width = rows[0].shape
+    units = halves[0].shape[1]
     for i, part in enumerate(rows):
         joined[i * each : (i + 1) * each, :] = part[...]
-    tall, wide = 128, 512
+    tall = 128
 
     def block(i, carry):
         spot = pl.ds(pl.multiple_of(i * tall, tall), tall)
         mine = joined[spot, :]
         hidden = []
-        for gate, up in ((gate_a, up_a), (gate_b, up_b)):
-            gate_pre = jnp.dot(mine, gate[...], preferred_element_type=jnp.float32)
-            up_pre = jnp.dot(mine, up[...], preferred_element_type=jnp.float32)
+        for half in halves:
+            gate_pre = jnp.dot(mine, half[0:width, :], preferred_element_type=jnp.float32)
+            up_pre = jnp.dot(mine, half[width : 2 * width, :], preferred_element_type=jnp.float32)
             silu = gate_pre / (1.0 + jnp.exp(-gate_pre))
             hidden.append((silu * up_pre).astype(jnp.bfloat16))
-
-        def column(j, inner):
-            cols = pl.ds(pl.multiple_of(j * wide, wide), wide)
+        for col in range(0, width, units):
+            at = 2 * width + col
             part = jnp.dot(
-                hidden[0], down_a[:, cols], preferred_element_type=jnp.float32
-            ) + jnp.dot(hidden[1], down_b[:, cols], preferred_element_type=jnp.float32)
-            made[spot, cols] = part.astype(jnp.bfloat16)
-            return inner
-
-        return lax.fori_loop(0, made.shape[1] // wide, column, carry)
+                hidden[0], halves[0][at : at + units, :], preferred_element_type=jnp.float32
+            ) + jnp.dot(
+                hidden[1], halves[1][at : at + units, :], preferred_element_type=jnp.float32
+            )
+            made[spot, col : col + units] = part.astype(jnp.bfloat16)
+        return carry
 
     lax.fori_loop(0, joined.shape[0] // tall, block, 0)
     for i, out in enumerate(outs):
         out[...] = made[i * each : (i + 1) * each, :]
 
 
-def expert_rows(rows, weights):
+def expert_rows(rows, halves):
     count = len(rows)
     each, width = rows[0].shape
-    hidden = weights[0].shape[1] * 2
-    flops = 2 * count * each * width * hidden * 3
+    flops = 2 * count * each * width * halves[0].shape[1] * 2 * 3
     joined = pltpu.VMEM((count * each, width), jnp.bfloat16)
     return pl.pallas_call(
         partial(expert_kernel, count=count),
         out_shape=tuple(jax.ShapeDtypeStruct((each, width), jnp.bfloat16) for _ in rows),
-        in_specs=[vmem] * (count + 6),
+        in_specs=[vmem] * (count + 2),
         out_specs=(vmem,) * count,
         scratch_shapes=[joined, joined],
         compiler_params=pltpu.CompilerParams(vmem_limit_bytes=16 << 20),
         cost_estimate=pl.CostEstimate(flops=flops, transcendentals=0, bytes_accessed=6 << 20),
-    )(*rows, *weights)
+    )(*rows, *halves)
 
 
 def added(left, right):
@@ -396,8 +430,8 @@
 
     half = own.shape[0] // 2
     top, end = own[:half], own[half:]
-    up_top, down_end, up_end, down_top = [up(top)], [down(end)], [up(end)], [down(top)]
-    for _ in range(2):
+    up_top, down_end, up_end, down_top = [top], [end], [end], [top]
+    for _ in range(1, 4):
         up_top.append(up(up_top[-1]))
         down_end.append(down(down_end[-1]))
         up_end.append(up(up_end[-1]))
@@ -405,10 +439,12 @@
     up_top.append(up(up_top[-1]))
     down_end.append(down(down_end[-1]))
     chains = (up_top, up_end, down_top, down_end)
-    near = expert_rows([top, end] + [chain[0] for chain in chains], weights)
-    mid = expert_rows([chain[i] for i in (1, 2) for chain in chains], weights)
-    far_top, far_end = expert_rows([up_top[3], down_end[3]], weights)
-    done = [near[2:], mid[:4], mid[4:]]
+    made = []
+    for i in range(1, 4):
+        rows = [chain[i] for chain in chains]
+        made.append(expert_rows(([top, end] if i == 1 else []) + rows, weights))
+    mine, done = made[0][:2], [made[0][2:], made[1], made[2]]
+    far_top, far_end = expert_rows([up_top[4], down_end[4]], weights)
 
     low_top, high_end = down(done[2][0]), up(done[2][3])
     high_top, low_end = up(far_top), down(far_end)
@@ -420,9 +456,9 @@
         high_top = up(added(high_top, done[i][2]))
         low_end = down(added(low_end, done[i][1]))
     sums = []
-    for parts in ((low_top, high_top, near[0]), (low_end, high_end, near[1])):
-        low, high, mine = (part.astype(jnp.float32) for part in parts)
-        sums.append((low + high + mine).astype(jnp.bfloat16))
+    for parts in ((low_top, high_top, mine[0]), (low_end, high_end, mine[1])):
+        low, high, own_part = (part.astype(jnp.float32) for part in parts)
+        sums.append((low + high + own_part).astype(jnp.bfloat16))
     return jnp.concatenate(sums)
 
 
@@ -536,14 +572,15 @@
     down_weight,
 ):
     sp_count = lax.axis_size("sp")
-    own_weights = (gate_weight[0], up_weight[0], down_weight[0])
-    other_weights = tuple(lax.ppermute(weight, "tp", core_swap) for weight in own_weights)
-    head_out, other_weights = attention(
-        queries, key_vectors, value_vectors, forget_totals, head_gain, other_weights
-    )
-    weights = []
-    for mine, other in zip(own_weights, other_weights):
-        weights += [mine, other]
+    head_out, own_half = attention(
+        queries,
+        key_vectors,
+        value_vectors,
+        forget_totals,
+        head_gain,
+        (gate_weight[0], up_weight[0], down_weight[0]),
+    )
+    weights = own_half, lax.ppermute(own_half, "tp", core_swap)
     row_count, width = stream.shape
     capacity = max(2, 2 * TOP * row_count // sp_count)
     heads = head_out.reshape(-1, row_count, HD)

time: 216 us -> 188 us (0.87)
  waiting for transfers between devices: 66.4 us -> 37.7 us
  starting transfers between devices: 62.7 us -> 68.4 us
  local copies, waits for them, and re-layouts: 3.52 us -> 0.1 us
    ppermute x14, waiting for transfers between devices: 50.9 us -> 27.4 us  [up(): return lax.ppermute(array, 'tp', z_perm(1))]
    ppermute x10, waiting for transfers between devices: 14 us -> 4.73 us  [shift(): return lax.ppermute(array, 'sp', sp_perm(dy, dx, needed))]
    ppermute x14, starting transfers between devices: 36 us -> 44.2 us  [down(): return lax.ppermute(array, 'tp', z_perm(-1))]
    pallas_call x3 -> x4, Pallas kernels: 14 us -> 9.44 us  [expert_rows(): pl.pallas_call(partial(expert_kernel, count=count), out_shape=tuple((jax....]
    ppermute x14, waiting for transfers between devices: 1.46 us -> 5.53 us  [down(): return lax.ppermute(array, 'tp', z_perm(-1))]
    unnamed x28 -> x14, local copies, waits for them, and re-layouts: 3.46 us -> 0.04 us
  transfers between devices with their start and end apart: 41 -> 39, of which waited for: 18 -> 15; matrix products, arithmetic and copies ran while one was open for 0% -> 0% of each run, Pallas kernels for 7% -> 10%
where the time goes in v1:
time: 188 us
  starting transfers between devices  68.4 us (36%)
  blocking collectives  52.1 us (28%)
  waiting for transfers between devices  37.7 us (20%)
  Pallas kernels  28.4 us (15%)
    ppermute x14, starting transfers between devices, down(): return lax.ppermute(array, 'tp', z_perm(-1))  44.2 us
    ppermute x14, waiting for transfers between devices, up(): return lax.ppermute(array, 'tp', z_perm(1))  27.4 us
    ppermute x10, starting transfers between devices, shift(): return lax.ppermute(array, 'sp', sp_perm(dy, dx, needed))  22.8 us
    all_to_all x1, blocking collectives, on_device(): lax.all_to_all(outgoing, 'sp', split_axis=0, concat_axis=0, tiled=True)  21.5 us
    all_to_all x1, blocking collectives, on_device(): heads = lax.all_to_all(heads, 'tp', split_axis=0, concat_axis=0, tiled=True)  17 us
    all_to_all x1, blocking collectives, on_device(): lax.all_to_all(expert_out, 'sp', split_axis=0, concat_axis=0, tiled=True)  13.5 us
    pallas_call x4, Pallas kernels, attend(): pl.pallas_call(kernel, out_shape=tuple((jax.ShapeDtypeStruct(*out) for ou...  12.2 us
    pallas_call x4, Pallas kernels, expert_rows(): pl.pallas_call(partial(expert_kernel, count=count), out_shape=tuple((jax....  9.44 us
  transfers between devices with their start and end apart: 39, of which 15 were waited for; matrix products, arithmetic and copies ran while one was open for 0% of the time, Pallas kernels for 10%

profile of v1, /device:TPU:2, one launch (start us, length us, event | category | flops | bytes accessed | tf_op | source)
XLA Modules:
  0.0 188.0 jit_solution(7460344302084786474)
XLA Ops:
  1.2 3.4 %collective-permute-start.2 = (bf16[544,256]{1,0:T(8,128)(2,1)S(1)}, bf16[544,256]{1,0:T(8,128)(2,1)S(1)}, u32[]{:S(2)}, u32[]{:S(2)}) collective-permute-start(bf16[544,256]{1,0:T(8,128)(2,1)S(1)} %get-tuple-element.53.refs_2_), channel_id=1, source_target_pairs={{0,16},{16,32},{32,48},{48,0},{64,80},{80,96},{96,112},{112,64},{1... | collective-permute-start | bytes 835592 | tf_op jit(solution)/shard_map/ppermute | solution.py:294
  4.6 2.7 %collective-permute-start.4 = (bf16[544,256]{1,0:T(8,128)(2,1)S(1)}, bf16[544,256]{1,0:T(8,128)(2,1)S(1)}, u32[]{:S(2)}, u32[]{:S(2)}) collective-permute-start(bf16[544,256]{1,0:T(8,128)(2,1)S(1)} %get-tuple-element.53.refs_2_), channel_id=1, source_target_pairs={{0,48},{16,0},{32,16},{48,32},{64,112},{80,64},{96,80},{112,96},{1... | collective-permute-start | bytes 835592 | tf_op jit(solution)/shard_map/ppermute | solution.py:294
  7.3 1.3 collective-permute-start
  8.6 1.3 collective-permute-start.1
  11.5 3.4 %collective-permute-start.3 = (bf16[272,256]{1,0:T(8,128)(2,1)S(1)}, bf16[272,256]{1,0:T(8,128)(2,1)S(1)}, u32[]{:S(2)}, u32[]{:S(2)}) collective-permute-start(bf16[272,256]{1,0:T(8,128)(2,1)S(1)} %slice.24), channel_id=1, source_target_pairs={{0,16},{16,32},{32,48},{48,0},{64,80},{80,96},{96,112},{112,64},{1... | collective-permute-start | bytes 417800 | tf_op jit(solution)/shard_map/ppermute | solution.py:294
  15.0 3.4 %collective-permute-start.5 = (bf16[272,256]{1,0:T(8,128)(2,1)S(1)}, bf16[272,256]{1,0:T(8,128)(2,1)S(1)}, u32[]{:S(2)}, u32[]{:S(2)}) collective-permute-start(bf16[272,256]{1,0:T(8,128)(2,1)S(1)} %slice.25), channel_id=1, source_target_pairs={{0,48},{16,0},{32,16},{48,32},{64,112},{80,64},{96,80},{112,96},{1... | collective-permute-start | bytes 417800 | tf_op jit(solution)/shard_map/ppermute | solution.py:294
  18.4 5.1 %shard_map.127 = (f32[8,512]{1,0:T(8,128)S(1)}, f32[8,512]{1,0:T(8,128)S(1)}, f32[128,512]{1,0:T(8,128)S(1)}, f32[8,512]{1,0:T(8,128)S(1)}, f32[8,512]{1,0:T(8,128)S(1)}, /*index=5*/f32[128,512]{1,0:T(8,128)S(1)}) custom-call(bf16[144,512]{1,0:T(8,128)(2,1)S(1)} %collective-permute-done.refs_0_, bf16[144,512]{1,0:T(8,128)(2,1)S(1)} %collective-permute-done.1.refs_1_, ...), custom_call_target="tpu_custom_call" | custom-call | flops 1610612736 | bytes 1048576 | tf_op jit(solution)/shard_map/pallas_call | solution.py:275
  23.5 1.7 shard_map.128
  25.3 5.1 %shard_map.129 = (bf16[144,512]{1,0:T(8,128)(2,1)S(1)}, f32[8,512]{1,0:T(8,128)S(1)}, f32[8,512]{1,0:T(8,128)S(1)}, f32[128,512]{1,0:T(8,128)S(1)}) custom-call(bf16[144,512]{1,0:T(8,128)(2,1)S(1)} %collective-permute-done.6.refs_0_, bf16[144,512]{1,0:T(8,128)(2,1)S(1)} %get-tuple-element.52.refs_1_, bf16[544,256]{1,0:T(8,128)(2,1)S(1)} %get-tuple-element.53.refs_2_, ...), custom_call_target="tpu_custom_call" | custom-call | flops 2147483648 | bytes 1048576 | tf_op jit(solution)/shard_map/pallas_call | solution.py:275
  30.5 2.0 %stage_weights.1.refs_4_.refs_6_.refs_2_ = bf16[6144,256]{1,0:T(8,128)(2,1)S(1)} custom-call(bf16[2048,256]{1,0:T(8,128)(2,1)} %bitcast.26, bf16[2048,256]{1,0:T(8,128)(2,1)} %bitcast.27, bf16[256,2048]{1,0:T(8,128)(2,1)} %bitcast.28), custom_call_target="tpu_custom_call" | custom-call | tf_op jit(solution)/shard_map/stage_weights/pallas_call | solution.py:359
  32.5 1.6 collective-permute-start.7
  34.1 3.2 %collective-permute-start.8 = (bf16[144,512]{1,0:T(8,128)(2,1)S(1)}, bf16[144,512]{1,0:T(8,128)(2,1)S(1)}, u32[]{:S(2)}, u32[]{:S(2)}) collective-permute-start(bf16[144,512]{1,0:T(8,128)(2,1)S(1)} %get-tuple-element.72), channel_id=1, source_target_pairs={{0,128},{16,144},{32,160},{48,176},{64,192},{80,208},{96,224},{112... | collective-permute-start | bytes 442376 | tf_op jit(solution)/shard_map/ppermute | solution.py:294
  37.3 1.3 collective-permute-start.9
  38.6 2.4 %collective-permute-done.8.refs_1_ = bf16[144,512]{1,0:T(8,128)(2,1)S(1)} collective-permute-done((bf16[144,512]{1,0:T(8,128)(2,1)S(1)}, bf16[144,512]{1,0:T(8,128)(2,1)S(1)}, u32[]{:S(2)}, u32[]{:S(2)}) %collective-permute-start.8) | collective-permute-done | bytes 147488 | tf_op jit(solution)/shard_map/ppermute | solution.py:294
  41.1 2.0 %collective-permute-done.9.refs_2_ = bf16[144,512]{1,0:T(8,128)(2,1)S(1)} collective-permute-done((bf16[144,512]{1,0:T(8,128)(2,1)S(1)}, bf16[144,512]{1,0:T(8,128)(2,1)S(1)}, u32[]{:S(2)}, u32[]{:S(2)}) %collective-permute-start.9) | collective-permute-done | bytes 147488 | tf_op jit(solution)/shard_map/ppermute | solution.py:294
  43.3 17.0 %all_to_all.15.heads = bf16[16,32,128]{2,1,0:T(8,128)(2,1)S(1)} all-to-all(bf16[16,32,128]{2,1,0:T(8,128)(2,1)S(1)} %bitcast.21), channel_id=1, replica_groups=mesh['sp'=16,'tp'=16] {'tp'}, dimensions={0} | all-to-all | bytes 262144 | tf_op jit(solution)/shard_map/all_to_all | solution.py:587
  60.4 2.5 %project.1 = (f32[32,2048]{1,0:T(8,128)S(1)}, bf16[128,2048]{1,0:T(8,128)(2,1)S(1)}, f32[128,32]{1,0:T(8,128)S(1)}) custom-call(bf16[16,32,128]{2,1,0:T(8,128)(2,1)S(1)} %all_to_all.15.heads, bf16[2048,2048]{1,0:T(8,128)(2,1)S(1)} %bitcast.18, bf16[32,2048]{1,0:T(8,128)(2,1)S(1)} %copy-done, f32[1,2048]{1,0:T(1,128)S(1)} %bitcast.22, s32[2,32]{1,0:T(2,128)S(1)} %bitcast.23, ...), custom_call_target="tpu_custom_call" | custom-call | tf_op jit(solution)/shard_map/project/pallas_call | solution.py:517
  62.9 21.5 %all_to_all.16 = bf16[16,8,2048]{2,1,0:T(8,128)(2,1)S(1)} all-to-all(bf16[16,8,2048]{2,1,0:T(8,128)(2,1)S(1)} %bitcast.20), channel_id=1, replica_groups=mesh['sp'=16,'tp'=16] {'sp'}, dimensions={0} | all-to-all | bytes 1048576 | tf_op jit(solution)/shard_map/all_to_all | solution.py:592
  85.1 2.7 %collective-permute-start.19 = (bf16[64,2048]{1,0:T(8,128)(2,1)S(1)}, bf16[64,2048]{1,0:T(8,128)(2,1)S(1)}, u32[]{:S(2)}, u32[]{:S(2)}) collective-permute-start(bf16[64,2048]{1,0:T(8,128)(2,1)S(1)} %get-tuple-element.99.refs_1_), channel_id=1, source_target_pairs={{0,14},{1,15},{2,0},{3,1},{4,2},{5,3},{6,4},{7,5},{8,6},{9,7},{10,... | collective-permute-start | bytes 786440 | tf_op jit(solution)/shard_map/ppermute | solution.py:429
  87.8 3.2 %collective-permute-start.16 = (bf16[64,2048]{1,0:T(8,128)(2,1)S(1)}, bf16[64,2048]{1,0:T(8,128)(2,1)S(1)}, u32[]{:S(2)}, u32[]{:S(2)}) collective-permute-start(bf16[64,2048]{1,0:T(8,128)(2,1)S(1)} %get-tuple-element.100.refs_0_), channel_id=1, source_target_pairs={{0,14},{1,15},{2,0},{3,1},{4,2},{5,3},{6,4},{7,5},{8,6},{9,7},{10,... | collective-permute-start | bytes 786440 | tf_op jit(solution)/shard_map/ppermute | solution.py:429
  91.1 3.9 %collective-permute-done.10.refs_2_ = bf16[64,2048]{1,0:T(8,128)(2,1)S(1)} collective-permute-done((bf16[64,2048]{1,0:T(8,128)(2,1)S(1)}, bf16[64,2048]{1,0:T(8,128)(2,1)S(1)}, u32[]{:S(2)}, u32[]{:S(2)}) %collective-permute-start.10) | collective-permute-done | bytes 262176 | tf_op jit(solution)/shard_map/ppermute | solution.py:426
  95.0 3.2 %collective-permute-start.20 = (bf16[64,2048]{1,0:T(8,128)(2,1)S(1)}, bf16[64,2048]{1,0:T(8,128)(2,1)S(1)}, u32[]{:S(2)}, u32[]{:S(2)}) collective-permute-start(bf16[64,2048]{1,0:T(8,128)(2,1)S(1)} %collective-permute-done.19.refs_5_), channel_id=1, source_target_pairs={{0,14},{1,15},{2,0},{3,1},{4,2},{5,3},{6,4},{7,5},{8,6},{9,7},{10,... | collective-permute-start | bytes 786440 | tf_op jit(solution)/shard_map/ppermute | solution.py:429
  98.2 2.4 %collective-permute-done.13.refs_3_ = bf16[64,2048]{1,0:T(8,128)(2,1)S(1)} collective-permute-done((bf16[64,2048]{1,0:T(8,128)(2,1)S(1)}, bf16[64,2048]{1,0:T(8,128)(2,1)S(1)}, u32[]{:S(2)}, u32[]{:S(2)}) %collective-permute-start.13) | collective-permute-done | bytes 262176 | tf_op jit(solution)/shard_map/ppermute | solution.py:426
  100.6 3.2 %collective-permute-start.17 = (bf16[64,2048]{1,0:T(8,128)(2,1)S(1)}, bf16[64,2048]{1,0:T(8,128)(2,1)S(1)}, u32[]{:S(2)}, u32[]{:S(2)}) collective-permute-start(bf16[64,2048]{1,0:T(8,128)(2,1)S(1)} %collective-permute-done.16.refs_4_), channel_id=1, source_target_pairs={{0,14},{1,15},{2,0},{3,1},{4,2},{5,3},{6,4},{7,5},{8,6},{9,7},{10,... | collective-permute-start | bytes 786440 | tf_op jit(solution)/shard_map/ppermute | solution.py:429
  103.8 2.4 %collective-permute-done.11.refs_0_ = bf16[64,2048]{1,0:T(8,128)(2,1)S(1)} collective-permute-done((bf16[64,2048]{1,0:T(8,128)(2,1)S(1)}, bf16[64,2048]{1,0:T(8,128)(2,1)S(1)}, u32[]{:S(2)}, u32[]{:S(2)}) %collective-permute-start.11) | collective-permute-done | bytes 262176 | tf_op jit(solution)/shard_map/ppermute | solution.py:426
  106.2 3.2 %collective-permute-start.21 = (bf16[64,2048]{1,0:T(8,128)(2,1)S(1)}, bf16[64,2048]{1,0:T(8,128)(2,1)S(1)}, u32[]{:S(2)}, u32[]{:S(2)}) collective-permute-start(bf16[64,2048]{1,0:T(8,128)(2,1)S(1)} %collective-permute-done.20.refs_3_), channel_id=1, source_target_pairs={{0,14},{1,15},{2,0},{3,1},{4,2},{5,3},{6,4},{7,5},{8,6},{9,7},{10,... | collective-permute-start | bytes 786440 | tf_op jit(solution)/shard_map/ppermute | solution.py:429
  109.4 2.4 %collective-permute-done.14.refs_1_ = bf16[64,2048]{1,0:T(8,128)(2,1)S(1)} collective-permute-done((bf16[64,2048]{1,0:T(8,128)(2,1)S(1)}, bf16[64,2048]{1,0:T(8,128)(2,1)S(1)}, u32[]{:S(2)}, u32[]{:S(2)}) %collective-permute-start.14) | collective-permute-done | bytes 262176 | tf_op jit(solution)/shard_map/ppermute | solution.py:426
  111.8 3.2 %collective-permute-start.18 = (bf16[64,2048]{1,0:T(8,128)(2,1)S(1)}, bf16[64,2048]{1,0:T(8,128)(2,1)S(1)}, u32[]{:S(2)}, u32[]{:S(2)}) collective-permute-start(bf16[64,2048]{1,0:T(8,128)(2,1)S(1)} %collective-permute-done.17.refs_2_), channel_id=1, source_target_pairs={{0,14},{1,15},{2,0},{3,1},{4,2},{5,3},{6,4},{7,5},{8,6},{9,7},{10,... | collective-permute-start | bytes 786440 | tf_op jit(solution)/shard_map/ppermute | solution.py:429
  115.1 2.4 %collective-permute-done.12.refs_0_ = bf16[64,2048]{1,0:T(8,128)(2,1)S(1)} collective-permute-done((bf16[64,2048]{1,0:T(8,128)(2,1)S(1)}, bf16[64,2048]{1,0:T(8,128)(2,1)S(1)}, u32[]{:S(2)}, u32[]{:S(2)}) %collective-permute-start.12) | collective-permute-done | bytes 262176 | tf_op jit(solution)/shard_map/ppermute | solution.py:426
  117.4 3.2 %collective-permute-start.27 = (bf16[64,2048]{1,0:T(8,128)(2,1)S(1)}, bf16[64,2048]{1,0:T(8,128)(2,1)S(1)}, u32[]{:S(2)}, u32[]{:S(2)}) collective-permute-start(bf16[64,2048]{1,0:T(8,128)(2,1)S(1)} %collective-permute-done.21.refs_3_), channel_id=1, source_target_pairs={{0,14},{1,15},{2,0},{3,1},{4,2},{5,3},{6,4},{7,5},{8,6},{9,7},{10,... | collective-permute-start | bytes 786440 | tf_op jit(solution)/shard_map/ppermute | solution.py:429
  120.7 2.4 %collective-permute-done.15.refs_1_ = bf16[64,2048]{1,0:T(8,128)(2,1)S(1)} collective-permute-done((bf16[64,2048]{1,0:T(8,128)(2,1)S(1)}, bf16[64,2048]{1,0:T(8,128)(2,1)S(1)}, u32[]{:S(2)}, u32[]{:S(2)}) %collective-permute-start.15) | collective-permute-done | bytes 262176 | tf_op jit(solution)/shard_map/ppermute | solution.py:426
  123.1 2.4 %shard_map.131 = (bf16[64,2048]{1,0:T(8,128)(2,1)S(1)}, bf16[64,2048]{1,0:T(8,128)(2,1)S(1)}, bf16[64,2048]{1,0:T(8,128)(2,1)S(1)}, bf16[64,2048]{1,0:T(8,128)(2,1)S(1)}) custom-call(bf16[64,2048]{1,0:T(8,128)(2,1)S(1)} %collective-permute-done.12.refs_0_, bf16[64,2048]{1,0:T(8,128)(2,1)S(1)} %collective-permute-done.15.refs_1_, ...), custom_call_target="tpu_custom_call" | custom-call | flops 1610612736 | bytes 6291456 | tf_op jit(solution)/shard_map/pallas_call | solution.py:409
  125.6 2.3 %collective-permute-done.26.refs_0_ = bf16[64,2048]{1,0:T(8,128)(2,1)S(1)} collective-permute-done((bf16[64,2048]{1,0:T(8,128)(2,1)S(1)}, bf16[64,2048]{1,0:T(8,128)(2,1)S(1)}, u32[]{:S(2)}, u32[]{:S(2)}) %collective-permute-start.26) | collective-permute-done | bytes 262176 | tf_op jit(solution)/shard_map/ppermute | solution.py:426
  129.0 2.1 %collective-permute-start.32 = (bf16[64,2048]{1,0:T(8,128)(2,1)S(1)}, bf16[64,2048]{1,0:T(8,128)(2,1)S(1)}, u32[]{:S(2)}, u32[]{:S(2)}) collective-permute-start(bf16[64,2048]{1,0:T(8,128)(2,1)S(1)} %get-tuple-element.90), channel_id=1, source_target_pairs={{0,14},{1,15},{2,0},{3,1},{4,2},{5,3},{6,4},{7,5},{8,6},{9,7},{10,... | collective-permute-start | bytes 786440 | tf_op jit(solution)/shard_map/ppermute | solution.py:429
  131.1 3.2 %collective-permute-start.23 = (bf16[64,2048]{1,0:T(8,128)(2,1)S(1)}, bf16[64,2048]{1,0:T(8,128)(2,1)S(1)}, u32[]{:S(2)}, u32[]{:S(2)}) collective-permute-start(bf16[64,2048]{1,0:T(8,128)(2,1)S(1)} %get-tuple-element.82), channel_id=1, source_target_pairs={{0,14},{1,15},{2,0},{3,1},{4,2},{5,3},{6,4},{7,5},{8,6},{9,7},{10,... | collective-permute-start | bytes 786440 | tf_op jit(solution)/shard_map/ppermute | solution.py:429
  134.3 2.4 %shard_map.132 = (bf16[64,2048]{1,0:T(8,128)(2,1)S(1)}, bf16[64,2048]{1,0:T(8,128)(2,1)S(1)}, bf16[64,2048]{1,0:T(8,128)(2,1)S(1)}, bf16[64,2048]{1,0:T(8,128)(2,1)S(1)}) custom-call(bf16[64,2048]{1,0:T(8,128)(2,1)S(1)} %collective-permute-done.11.refs_0_, bf16[64,2048]{1,0:T(8,128)(2,1)S(1)} %collective-permute-done.14.refs_1_, ...), custom_call_target="tpu_custom_call" | custom-call | flops 1610612736 | bytes 6291456 | tf_op jit(solution)/shard_map/pallas_call | solution.py:409
  136.7 3.6 %shard_map.133 = (bf16[64,2048]{1,0:T(8,128)(2,1)S(1)}, bf16[64,2048]{1,0:T(8,128)(2,1)S(1)}, bf16[64,2048]{1,0:T(8,128)(2,1)S(1)}, bf16[64,2048]{1,0:T(8,128)(2...) custom-call(bf16[64,2048]{1,0:T(8,128)(2,1)S(1)} %get-tuple-element.100.refs_0_, ...), custom_call_target="tpu_custom_call" | custom-call | flops 2415919104 | bytes 6291456 | tf_op jit(solution)/shard_map/pallas_call | solution.py:409
  140.5 3.3 %collective-permute-start.33 = (bf16[64,2048]{1,0:T(8,128)(2,1)S(1)}, bf16[64,2048]{1,0:T(8,128)(2,1)S(1)}, u32[]{:S(2)}, u32[]{:S(2)}) collective-permute-start(bf16[64,2048]{1,0:T(8,128)(2,1)S(1)} %add_convert_fusion.5), channel_id=1, source_target_pairs={{0,14},{1,15},{2,0},{3,1},{4,2},{5,3},{6,4},{7,5},{8,6},{9,7},{10,... | collective-permute-start | bytes 786440 | tf_op jit(solution)/shard_map/ppermute | solution.py:429
  144.1 3.3 %collective-permute-start.24 = (bf16[64,2048]{1,0:T(8,128)(2,1)S(1)}, bf16[64,2048]{1,0:T(8,128)(2,1)S(1)}, u32[]{:S(2)}, u32[]{:S(2)}) collective-permute-start(bf16[64,2048]{1,0:T(8,128)(2,1)S(1)} %add_convert_fusion.11), channel_id=1, source_target_pairs={{0,14},{1,15},{2,0},{3,1},{4,2},{5,3},{6,4},{7,5},{8,6},{9,7},{10,... | collective-permute-start | bytes 786440 | tf_op jit(solution)/shard_map/ppermute | solution.py:429
  147.4 3.5 %collective-permute-done.37 = bf16[64,2048]{1,0:T(8,128)(2,1)S(1)} collective-permute-done((bf16[64,2048]{1,0:T(8,128)(2,1)S(1)}, bf16[64,2048]{1,0:T(8,128)(2,1)S(1)}, u32[]{:S(2)}, u32[]{:S(2)}) %collective-permute-start.37) | collective-permute-done | bytes 262176 | tf_op jit(solution)/shard_map/ppermute | solution.py:426
  151.1 3.3 %collective-permute-start.34 = (bf16[64,2048]{1,0:T(8,128)(2,1)S(1)}, bf16[64,2048]{1,0:T(8,128)(2,1)S(1)}, u32[]{:S(2)}, u32[]{:S(2)}) collective-permute-start(bf16[64,2048]{1,0:T(8,128)(2,1)S(1)} %add_convert_fusion.4), channel_id=1, source_target_pairs={{0,14},{1,15},{2,0},{3,1},{4,2},{5,3},{6,4},{7,5},{8,6},{9,7},{10,... | collective-permute-start | bytes 786440 | tf_op jit(solution)/shard_map/ppermute | solution.py:429
  154.4 2.1 %collective-permute-done.29 = bf16[64,2048]{1,0:T(8,128)(2,1)S(1)} collective-permute-done((bf16[64,2048]{1,0:T(8,128)(2,1)S(1)}, bf16[64,2048]{1,0:T(8,128)(2,1)S(1)}, u32[]{:S(2)}, u32[]{:S(2)}) %collective-permute-start.29) | collective-permute-done | bytes 262176 | tf_op jit(solution)/shard_map/ppermute | solution.py:426
  156.7 3.3 %collective-permute-start.25 = (bf16[64,2048]{1,0:T(8,128)(2,1)S(1)}, bf16[64,2048]{1,0:T(8,128)(2,1)S(1)}, u32[]{:S(2)}, u32[]{:S(2)}) collective-permute-start(bf16[64,2048]{1,0:T(8,128)(2,1)S(1)} %add_convert_fusion.10), channel_id=1, source_target_pairs={{0,14},{1,15},{2,0},{3,1},{4,2},{5,3},{6,4},{7,5},{8,6},{9,7},{10,... | collective-permute-start | bytes 786440 | tf_op jit(solution)/shard_map/ppermute | solution.py:429
  160.0 1.8 collective-permute-done.34
  161.8 3.8 %collective-permute-start.35 = (bf16[64,2048]{1,0:T(8,128)(2,1)S(1)}, bf16[64,2048]{1,0:T(8,128)(2,1)S(1)}, u32[]{:S(2)}, u32[]{:S(2)}) collective-permute-start(bf16[64,2048]{1,0:T(8,128)(2,1)S(1)} %add_convert_fusion.3), channel_id=1, source_target_pairs={{0,14},{1,15},{2,0},{3,1},{4,2},{5,3},{6,4},{7,5},{8,6},{9,7},{10,... | collective-permute-start | bytes 786440 | tf_op jit(solution)/shard_map/ppermute | solution.py:429
  165.8 3.7 %collective-permute-done.35 = bf16[64,2048]{1,0:T(8,128)(2,1)S(1)} collective-permute-done((bf16[64,2048]{1,0:T(8,128)(2,1)S(1)}, bf16[64,2048]{1,0:T(8,128)(2,1)S(1)}, u32[]{:S(2)}, u32[]{:S(2)}) %collective-permute-start.35) | collective-permute-done | bytes 262176 | tf_op jit(solution)/shard_map/ppermute | solution.py:429
  169.6 3.7 %collective-permute-done.31 = bf16[64,2048]{1,0:T(8,128)(2,1)S(1)} collective-permute-done((bf16[64,2048]{1,0:T(8,128)(2,1)S(1)}, bf16[64,2048]{1,0:T(8,128)(2,1)S(1)}, u32[]{:S(2)}, u32[]{:S(2)}) %collective-permute-start.31) | collective-permute-done | bytes 262176 | tf_op jit(solution)/shard_map/ppermute | solution.py:426
  173.5 13.5 %all_to_all.17 = bf16[16,8,2048]{2,1,0:T(8,128)(2,1)S(1)} all-to-all(bf16[16,8,2048]{2,1,0:T(8,128)(2,1)S(1)} %maximum_bitcast_fusion), channel_id=1, replica_groups=mesh['sp'=16,'tp'=16] {'sp'}, dimensions={0} | all-to-all | bytes 1048576 | tf_op jit(solution)/shard_map/all_to_all | solution.py:595
  (76 shorter events, 7.7 us)
Async XLA Ops:
  1.2 10.3 %collective-permute-start.2 = (bf16[544,256]{1,0:T(8,128)(2,1)S(1)}, bf16[544,256]{1,0:T(8,128)(2,1)S(1)}, u32[]{:S(2)}, u32[]{:S(2)}) collective-permute-start(bf16[544,256]{1,0:T(8,128)(2,1)S(1)} %get-tuple-element.53.refs_2_), channel_id=1, source_target_pairs={{0,16},{16,32},{32,48},{48,0},{64,80},{80,96},{96,112},{112,64},{1... | collective-permute-start | bytes 835592 | tf_op jit(solution)/shard_map/ppermute | solution.py:294
  4.6 10.3 %collective-permute-start.4 = (bf16[544,256]{1,0:T(8,128)(2,1)S(1)}, bf16[544,256]{1,0:T(8,128)(2,1)S(1)}, u32[]{:S(2)}, u32[]{:S(2)}) collective-permute-start(bf16[544,256]{1,0:T(8,128)(2,1)S(1)} %get-tuple-element.53.refs_2_), channel_id=1, source_target_pairs={{0,48},{16,0},{32,16},{48,32},{64,112},{80,64},{96,80},{112,96},{1... | collective-permute-start | bytes 835592 | tf_op jit(solution)/shard_map/ppermute | solution.py:294
  7.3 11.1 %collective-permute-start = (bf16[144,512]{1,0:T(8,128)(2,1)S(1)}, bf16[144,512]{1,0:T(8,128)(2,1)S(1)}, u32[]{:S(2)}, u32[]{:S(2)}) collective-permute-start(bf16[144,512]{1,0:T(8,128)(2,1)S(1)} %get-tuple-element.52.refs_1_), channel_id=1, source_target_pairs={{192,0},{208,16},{224,32},{240,48},{193,1},{209,17},{225,33},{241,... | collective-permute-start | bytes 442376 | tf_op jit(solution)/shard_map/ppermute | solution.py:294
  8.6 9.8 %collective-permute-start.1 = (bf16[144,512]{1,0:T(8,128)(2,1)S(1)}, bf16[144,512]{1,0:T(8,128)(2,1)S(1)}, u32[]{:S(2)}, u32[]{:S(2)}) collective-permute-start(bf16[144,512]{1,0:T(8,128)(2,1)S(1)} %get-tuple-element.52.refs_1_), channel_id=1, source_target_pairs={{128,0},{144,16},{160,32},{176,48},{192,64},{208,80},{224,96},{240... | collective-permute-start | bytes 442376 | tf_op jit(solution)/shard_map/ppermute | solution.py:294
  9.9 15.3 %collective-permute-start.6 = (bf16[144,512]{1,0:T(8,128)(2,1)S(1)}, bf16[144,512]{1,0:T(8,128)(2,1)S(1)}, u32[]{:S(2)}, u32[]{:S(2)}) collective-permute-start(bf16[144,512]{1,0:T(8,128)(2,1)S(1)} %get-tuple-element.52.refs_1_), channel_id=1, source_target_pairs={{64,0},{80,16},{96,32},{112,48},{128,64},{144,80},{160,96},{176,11... | collective-permute-start | bytes 442376 | tf_op jit(solution)/shard_map/ppermute | solution.py:294
  11.5 12.0 %collective-permute-start.3 = (bf16[272,256]{1,0:T(8,128)(2,1)S(1)}, bf16[272,256]{1,0:T(8,128)(2,1)S(1)}, u32[]{:S(2)}, u32[]{:S(2)}) collective-permute-start(bf16[272,256]{1,0:T(8,128)(2,1)S(1)} %slice.24), channel_id=1, source_target_pairs={{0,16},{16,32},{32,48},{48,0},{64,80},{80,96},{96,112},{112,64},{1... | collective-permute-start | bytes 417800 | tf_op jit(solution)/shard_map/ppermute | solution.py:294
  15.0 8.5 %collective-permute-start.5 = (bf16[272,256]{1,0:T(8,128)(2,1)S(1)}, bf16[272,256]{1,0:T(8,128)(2,1)S(1)}, u32[]{:S(2)}, u32[]{:S(2)}) collective-permute-start(bf16[272,256]{1,0:T(8,128)(2,1)S(1)} %slice.25), channel_id=1, source_target_pairs={{0,48},{16,0},{32,16},{48,32},{64,112},{80,64},{96,80},{112,96},{1... | collective-permute-start | bytes 417800 | tf_op jit(solution)/shard_map/ppermute | solution.py:294
  25.2 35.1 %slice-start = ((s8[8388608]{0:T(1024)(128)(4,1)}), s8[4194304]{0:T(1024)(128)(4,1)S(1)}, s32[]{:S(2)}) async-start(s8[8388608]{0:T(1024)(128)(4,1)} %bitcast.17), calls=%async_computation.3 | async-start | bytes 8388608
  25.2 35.1 %slice-start.1 = ((s8[8388608]{0:T(1024)(128)(4,1)}), s8[4194304]{0:T(1024)(128)(4,1)S(1)}, s32[]{:S(2)}) async-start(s8[8388608]{0:T(1024)(128)(4,1)} %bitcast.17), calls=%async_computation.4 | async-start | bytes 8388608
  30.4 12.6 %copy-start.4 = (f32[128]{0:T(128)S(1)}, f32[128]{0:T(128)}, u32[]{:S(2)}) copy-start(f32[128]{0:T(128)} %param.17) | copy-start | bytes 1540
  30.4 29.9 %copy-start = (bf16[32,2048]{1,0:T(8,128)(2,1)S(1)}, bf16[32,2048]{1,0:T(8,128)(2,1)}, u32[]{:S(2)}) copy-start(bf16[32,2048]{1,0:T(8,128)(2,1)} %stream.1) | copy-start | bytes 393220
  30.4 29.9 %copy-start.1 = (f32[2048]{0:T(1024)S(1)}, f32[2048]{0:T(1024)}, u32[]{:S(2)}) copy-start(f32[2048]{0:T(1024)} %param.20) | copy-start | bytes 24580
  30.4 29.9 %copy-start.2 = (s32[32,2]{0,1:T(2,128)S(1)}, s32[32,2]{0,1:T(2,128)}, u32[]{:S(2)}) copy-start(s32[32,2]{0,1:T(2,128)} %param.21) | copy-start | bytes 772
  30.4 29.9 %copy-start.3 = (f32[32,2]{0,1:T(2,128)S(1)}, f32[32,2]{0,1:T(2,128)}, u32[]{:S(2)}) copy-start(f32[32,2]{0,1:T(2,128)} %param.22) | copy-start | bytes 772
  32.4 90.6 %collective-permute-start.22 = (bf16[6144,256]{1,0:T(8,128)(2,1)S(1)}, bf16[6144,256]{1,0:T(8,128)(2,1)S(1)}, u32[]{:S(2)}, u32[]{:S(2)}) collective-permute-start(bf16[6144,256]{1,0:T(8,128)(2,1)S(1)} %stage_weights.1.refs_4_.refs_6_.refs_2_), channel_id=1, source_target_pairs={{0,1},{1,0},{2,3},{3,2},{4,5},{5,4},{6,7},{7,6},{8,9},{9,8},{10,11... | collective-permute-start | bytes 9437192 | tf_op jit(solution)/shard_map/ppermute | solution.py:583
  32.5 6.1 %collective-permute-start.7 = (bf16[144,512]{1,0:T(8,128)(2,1)S(1)}, bf16[144,512]{1,0:T(8,128)(2,1)S(1)}, u32[]{:S(2)}, u32[]{:S(2)}) collective-permute-start(bf16[144,512]{1,0:T(8,128)(2,1)S(1)} %get-tuple-element.71), channel_id=1, source_target_pairs={{0,64},{16,80},{32,96},{48,112},{64,128},{80,144},{96,160},{112,17... | collective-permute-start | bytes 442376 | tf_op jit(solution)/shard_map/ppermute | solution.py:294
  34.1 6.9 %collective-permute-start.8 = (bf16[144,512]{1,0:T(8,128)(2,1)S(1)}, bf16[144,512]{1,0:T(8,128)(2,1)S(1)}, u32[]{:S(2)}, u32[]{:S(2)}) collective-permute-start(bf16[144,512]{1,0:T(8,128)(2,1)S(1)} %get-tuple-element.72), channel_id=1, source_target_pairs={{0,128},{16,144},{32,160},{48,176},{64,192},{80,208},{96,224},{112... | collective-permute-start | bytes 442376 | tf_op jit(solution)/shard_map/ppermute | solution.py:294
  37.3 5.7 %collective-permute-start.9 = (bf16[144,512]{1,0:T(8,128)(2,1)S(1)}, bf16[144,512]{1,0:T(8,128)(2,1)S(1)}, u32[]{:S(2)}, u32[]{:S(2)}) collective-permute-start(bf16[144,512]{1,0:T(8,128)(2,1)S(1)} %get-tuple-element.73), channel_id=1, source_target_pairs={{0,192},{16,208},{32,224},{48,240},{1,193},{17,209},{33,225},{49,2... | collective-permute-start | bytes 442376 | tf_op jit(solution)/shard_map/ppermute | solution.py:294
  84.5 10.5 %collective-permute-start.10 = (bf16[64,2048]{1,0:T(8,128)(2,1)S(1)}, bf16[64,2048]{1,0:T(8,128)(2,1)S(1)}, u32[]{:S(2)}, u32[]{:S(2)}) collective-permute-start(bf16[64,2048]{1,0:T(8,128)(2,1)S(1)} %get-tuple-element.100.refs_0_), channel_id=1, source_target_pairs={{0,2},{1,3},{2,4},{3,5},{4,6},{5,7},{6,8},{7,9},{8,10},{9,11},{10,... | collective-permute-start | bytes 786440 | tf_op jit(solution)/shard_map/ppermute | solution.py:426
  85.1 9.8 %collective-permute-start.19 = (bf16[64,2048]{1,0:T(8,128)(2,1)S(1)}, bf16[64,2048]{1,0:T(8,128)(2,1)S(1)}, u32[]{:S(2)}, u32[]{:S(2)}) collective-permute-start(bf16[64,2048]{1,0:T(8,128)(2,1)S(1)} %get-tuple-element.99.refs_1_), channel_id=1, source_target_pairs={{0,14},{1,15},{2,0},{3,1},{4,2},{5,3},{6,4},{7,5},{8,6},{9,7},{10,... | collective-permute-start | bytes 786440 | tf_op jit(solution)/shard_map/ppermute | solution.py:429
  87.8 12.8 %collective-permute-start.13 = (bf16[64,2048]{1,0:T(8,128)(2,1)S(1)}, bf16[64,2048]{1,0:T(8,128)(2,1)S(1)}, u32[]{:S(2)}, u32[]{:S(2)}) collective-permute-start(bf16[64,2048]{1,0:T(8,128)(2,1)S(1)} %get-tuple-element.99.refs_1_), channel_id=1, source_target_pairs={{0,2},{1,3},{2,4},{3,5},{4,6},{5,7},{6,8},{7,9},{8,10},{9,11},{10,... | collective-permute-start | bytes 786440 | tf_op jit(solution)/shard_map/ppermute | solution.py:426
  87.8 12.8 %collective-permute-start.16 = (bf16[64,2048]{1,0:T(8,128)(2,1)S(1)}, bf16[64,2048]{1,0:T(8,128)(2,1)S(1)}, u32[]{:S(2)}, u32[]{:S(2)}) collective-permute-start(bf16[64,2048]{1,0:T(8,128)(2,1)S(1)} %get-tuple-element.100.refs_0_), channel_id=1, source_target_pairs={{0,14},{1,15},{2,0},{3,1},{4,2},{5,3},{6,4},{7,5},{8,6},{9,7},{10,... | collective-permute-start | bytes 786440 | tf_op jit(solution)/shard_map/ppermute | solution.py:429
  95.0 11.2 %collective-permute-start.11 = (bf16[64,2048]{1,0:T(8,128)(2,1)S(1)}, bf16[64,2048]{1,0:T(8,128)(2,1)S(1)}, u32[]{:S(2)}, u32[]{:S(2)}) collective-permute-start(bf16[64,2048]{1,0:T(8,128)(2,1)S(1)} %collective-permute-done.10.refs_2_), channel_id=1, source_target_pairs={{0,2},{1,3},{2,4},{3,5},{4,6},{5,7},{6,8},{7,9},{8,10},{9,11},{10,... | collective-permute-start | bytes 786440 | tf_op jit(solution)/shard_map/ppermute | solution.py:426
  95.0 11.2 %collective-permute-start.20 = (bf16[64,2048]{1,0:T(8,128)(2,1)S(1)}, bf16[64,2048]{1,0:T(8,128)(2,1)S(1)}, u32[]{:S(2)}, u32[]{:S(2)}) collective-permute-start(bf16[64,2048]{1,0:T(8,128)(2,1)S(1)} %collective-permute-done.19.refs_5_), channel_id=1, source_target_pairs={{0,14},{1,15},{2,0},{3,1},{4,2},{5,3},{6,4},{7,5},{8,6},{9,7},{10,... | collective-permute-start | bytes 786440 | tf_op jit(solution)/shard_map/ppermute | solution.py:429
  100.6 11.2 %collective-permute-start.14 = (bf16[64,2048]{1,0:T(8,128)(2,1)S(1)}, bf16[64,2048]{1,0:T(8,128)(2,1)S(1)}, u32[]{:S(2)}, u32[]{:S(2)}) collective-permute-start(bf16[64,2048]{1,0:T(8,128)(2,1)S(1)} %collective-permute-done.13.refs_3_), channel_id=1, source_target_pairs={{0,2},{1,3},{2,4},{3,5},{4,6},{5,7},{6,8},{7,9},{8,10},{9,11},{10,... | collective-permute-start | bytes 786440 | tf_op jit(solution)/shard_map/ppermute | solution.py:426
  100.6 11.2 %collective-permute-start.17 = (bf16[64,2048]{1,0:T(8,128)(2,1)S(1)}, bf16[64,2048]{1,0:T(8,128)(2,1)S(1)}, u32[]{:S(2)}, u32[]{:S(2)}) collective-permute-start(bf16[64,2048]{1,0:T(8,128)(2,1)S(1)} %collective-permute-done.16.refs_4_), channel_id=1, source_target_pairs={{0,14},{1,15},{2,0},{3,1},{4,2},{5,3},{6,4},{7,5},{8,6},{9,7},{10,... | collective-permute-start | bytes 786440 | tf_op jit(solution)/shard_map/ppermute | solution.py:429
  106.2 11.2 %collective-permute-start.12 = (bf16[64,2048]{1,0:T(8,128)(2,1)S(1)}, bf16[64,2048]{1,0:T(8,128)(2,1)S(1)}, u32[]{:S(2)}, u32[]{:S(2)}) collective-permute-start(bf16[64,2048]{1,0:T(8,128)(2,1)S(1)} %collective-permute-done.11.refs_0_), channel_id=1, source_target_pairs={{0,2},{1,3},{2,4},{3,5},{4,6},{5,7},{6,8},{7,9},{8,10},{9,11},{10,... | collective-permute-start | bytes 786440 | tf_op jit(solution)/shard_map/ppermute | solution.py:426
  106.2 11.2 %collective-permute-start.21 = (bf16[64,2048]{1,0:T(8,128)(2,1)S(1)}, bf16[64,2048]{1,0:T(8,128)(2,1)S(1)}, u32[]{:S(2)}, u32[]{:S(2)}) collective-permute-start(bf16[64,2048]{1,0:T(8,128)(2,1)S(1)} %collective-permute-done.20.refs_3_), channel_id=1, source_target_pairs={{0,14},{1,15},{2,0},{3,1},{4,2},{5,3},{6,4},{7,5},{8,6},{9,7},{10,... | collective-permute-start | bytes 786440 | tf_op jit(solution)/shard_map/ppermute | solution.py:429
  111.8 11.2 %collective-permute-start.15 = (bf16[64,2048]{1,0:T(8,128)(2,1)S(1)}, bf16[64,2048]{1,0:T(8,128)(2,1)S(1)}, u32[]{:S(2)}, u32[]{:S(2)}) collective-permute-start(bf16[64,2048]{1,0:T(8,128)(2,1)S(1)} %collective-permute-done.14.refs_1_), channel_id=1, source_target_pairs={{0,2},{1,3},{2,4},{3,5},{4,6},{5,7},{6,8},{7,9},{8,10},{9,11},{10,... | collective-permute-start | bytes 786440 | tf_op jit(solution)/shard_map/ppermute | solution.py:426
  111.8 11.2 %collective-permute-start.18 = (bf16[64,2048]{1,0:T(8,128)(2,1)S(1)}, bf16[64,2048]{1,0:T(8,128)(2,1)S(1)}, u32[]{:S(2)}, u32[]{:S(2)}) collective-permute-start(bf16[64,2048]{1,0:T(8,128)(2,1)S(1)} %collective-permute-done.17.refs_2_), channel_id=1, source_target_pairs={{0,14},{1,15},{2,0},{3,1},{4,2},{5,3},{6,4},{7,5},{8,6},{9,7},{10,... | collective-permute-start | bytes 786440 | tf_op jit(solution)/shard_map/ppermute | solution.py:429
  117.4 10.5 %collective-permute-start.26 = (bf16[64,2048]{1,0:T(8,128)(2,1)S(1)}, bf16[64,2048]{1,0:T(8,128)(2,1)S(1)}, u32[]{:S(2)}, u32[]{:S(2)}) collective-permute-start(bf16[64,2048]{1,0:T(8,128)(2,1)S(1)} %collective-permute-done.12.refs_0_), channel_id=1, source_target_pairs={{0,2},{1,3},{2,4},{3,5},{4,6},{5,7},{6,8},{7,9},{8,10},{9,11},{10,... | collective-permute-start | bytes 786440 | tf_op jit(solution)/shard_map/ppermute | solution.py:426
  117.4 10.5 %collective-permute-start.27 = (bf16[64,2048]{1,0:T(8,128)(2,1)S(1)}, bf16[64,2048]{1,0:T(8,128)(2,1)S(1)}, u32[]{:S(2)}, u32[]{:S(2)}) collective-permute-start(bf16[64,2048]{1,0:T(8,128)(2,1)S(1)} %collective-permute-done.21.refs_3_), channel_id=1, source_target_pairs={{0,14},{1,15},{2,0},{3,1},{4,2},{5,3},{6,4},{7,5},{8,6},{9,7},{10,... | collective-permute-start | bytes 786440 | tf_op jit(solution)/shard_map/ppermute | solution.py:429
  125.5 14.8 %collective-permute-start.36 = (bf16[64,2048]{1,0:T(8,128)(2,1)S(1)}, bf16[64,2048]{1,0:T(8,128)(2,1)S(1)}, u32[]{:S(2)}, u32[]{:S(2)}) collective-permute-start(bf16[64,2048]{1,0:T(8,128)(2,1)S(1)} %get-tuple-element.94), channel_id=1, source_target_pairs={{0,2},{1,3},{2,4},{3,5},{4,6},{5,7},{6,8},{7,9},{8,10},{9,11},{10,... | collective-permute-start | bytes 786440 | tf_op jit(solution)/shard_map/ppermute | solution.py:426
  129.0 11.4 %collective-permute-start.32 = (bf16[64,2048]{1,0:T(8,128)(2,1)S(1)}, bf16[64,2048]{1,0:T(8,128)(2,1)S(1)}, u32[]{:S(2)}, u32[]{:S(2)}) collective-permute-start(bf16[64,2048]{1,0:T(8,128)(2,1)S(1)} %get-tuple-element.90), channel_id=1, source_target_pairs={{0,14},{1,15},{2,0},{3,1},{4,2},{5,3},{6,4},{7,5},{8,6},{9,7},{10,... | collective-permute-start | bytes 786440 | tf_op jit(solution)/shard_map/ppermute | solution.py:429
  131.1 12.7 %collective-permute-start.28 = (bf16[64,2048]{1,0:T(8,128)(2,1)S(1)}, bf16[64,2048]{1,0:T(8,128)(2,1)S(1)}, u32[]{:S(2)}, u32[]{:S(2)}) collective-permute-start(bf16[64,2048]{1,0:T(8,128)(2,1)S(1)} %get-tuple-element.85), channel_id=1, source_target_pairs={{0,2},{1,3},{2,4},{3,5},{4,6},{5,7},{6,8},{7,9},{8,10},{9,11},{10,... | collective-permute-start | bytes 786440 | tf_op jit(solution)/shard_map/ppermute | solution.py:426
  131.1 12.9 %collective-permute-start.23 = (bf16[64,2048]{1,0:T(8,128)(2,1)S(1)}, bf16[64,2048]{1,0:T(8,128)(2,1)S(1)}, u32[]{:S(2)}, u32[]{:S(2)}) collective-permute-start(bf16[64,2048]{1,0:T(8,128)(2,1)S(1)} %get-tuple-element.82), channel_id=1, source_target_pairs={{0,14},{1,15},{2,0},{3,1},{4,2},{5,3},{6,4},{7,5},{8,6},{9,7},{10,... | collective-permute-start | bytes 786440 | tf_op jit(solution)/shard_map/ppermute | solution.py:429
  140.4 10.5 %collective-permute-start.37 = (bf16[64,2048]{1,0:T(8,128)(2,1)S(1)}, bf16[64,2048]{1,0:T(8,128)(2,1)S(1)}, u32[]{:S(2)}, u32[]{:S(2)}) collective-permute-start(bf16[64,2048]{1,0:T(8,128)(2,1)S(1)} %add_convert_fusion.2), channel_id=1, source_target_pairs={{0,2},{1,3},{2,4},{3,5},{4,6},{5,7},{6,8},{7,9},{8,10},{9,11},{10,... | collective-permute-start | bytes 786440 | tf_op jit(solution)/shard_map/ppermute | solution.py:426
  140.5 10.5 %collective-permute-start.33 = (bf16[64,2048]{1,0:T(8,128)(2,1)S(1)}, bf16[64,2048]{1,0:T(8,128)(2,1)S(1)}, u32[]{:S(2)}, u32[]{:S(2)}) collective-permute-start(bf16[64,2048]{1,0:T(8,128)(2,1)S(1)} %add_convert_fusion.5), channel_id=1, source_target_pairs={{0,14},{1,15},{2,0},{3,1},{4,2},{5,3},{6,4},{7,5},{8,6},{9,7},{10,... | collective-permute-start | bytes 786440 | tf_op jit(solution)/shard_map/ppermute | solution.py:429
  143.9 12.6 %collective-permute-start.29 = (bf16[64,2048]{1,0:T(8,128)(2,1)S(1)}, bf16[64,2048]{1,0:T(8,128)(2,1)S(1)}, u32[]{:S(2)}, u32[]{:S(2)}) collective-permute-start(bf16[64,2048]{1,0:T(8,128)(2,1)S(1)} %add_convert_fusion.9), channel_id=1, source_target_pairs={{0,2},{1,3},{2,4},{3,5},{4,6},{5,7},{6,8},{7,9},{8,10},{9,11},{10,... | collective-permute-start | bytes 786440 | tf_op jit(solution)/shard_map/ppermute | solution.py:426
  144.1 12.5 %collective-permute-start.24 = (bf16[64,2048]{1,0:T(8,128)(2,1)S(1)}, bf16[64,2048]{1,0:T(8,128)(2,1)S(1)}, u32[]{:S(2)}, u32[]{:S(2)}) collective-permute-start(bf16[64,2048]{1,0:T(8,128)(2,1)S(1)} %add_convert_fusion.11), channel_id=1, source_target_pairs={{0,14},{1,15},{2,0},{3,1},{4,2},{5,3},{6,4},{7,5},{8,6},{9,7},{10,... | collective-permute-start | bytes 786440 | tf_op jit(solution)/shard_map/ppermute | solution.py:429
  150.9 14.9 %collective-permute-start.38 = (bf16[64,2048]{1,0:T(8,128)(2,1)S(1)}, bf16[64,2048]{1,0:T(8,128)(2,1)S(1)}, u32[]{:S(2)}, u32[]{:S(2)}) collective-permute-start(bf16[64,2048]{1,0:T(8,128)(2,1)S(1)} %add_convert_fusion.1), channel_id=1, source_target_pairs={{0,2},{1,3},{2,4},{3,5},{4,6},{5,7},{6,8},{7,9},{8,10},{9,11},{10,... | collective-permute-start | bytes 786440 | tf_op jit(solution)/shard_map/ppermute | solution.py:426
  151.1 10.7 %collective-permute-start.34 = (bf16[64,2048]{1,0:T(8,128)(2,1)S(1)}, bf16[64,2048]{1,0:T(8,128)(2,1)S(1)}, u32[]{:S(2)}, u32[]{:S(2)}) collective-permute-start(bf16[64,2048]{1,0:T(8,128)(2,1)S(1)} %add_convert_fusion.4), channel_id=1, source_target_pairs={{0,14},{1,15},{2,0},{3,1},{4,2},{5,3},{6,4},{7,5},{8,6},{9,7},{10,... | collective-permute-start | bytes 786440 | tf_op jit(solution)/shard_map/ppermute | solution.py:429
  156.5 9.1 %collective-permute-start.30 = (bf16[64,2048]{1,0:T(8,128)(2,1)S(1)}, bf16[64,2048]{1,0:T(8,128)(2,1)S(1)}, u32[]{:S(2)}, u32[]{:S(2)}) collective-permute-start(bf16[64,2048]{1,0:T(8,128)(2,1)S(1)} %add_convert_fusion.8), channel_id=1, source_target_pairs={{0,2},{1,3},{2,4},{3,5},{4,6},{5,7},{6,8},{7,9},{8,10},{9,11},{10,... | collective-permute-start | bytes 786440 | tf_op jit(solution)/shard_map/ppermute | solution.py:426
  156.7 12.9 %collective-permute-start.25 = (bf16[64,2048]{1,0:T(8,128)(2,1)S(1)}, bf16[64,2048]{1,0:T(8,128)(2,1)S(1)}, u32[]{:S(2)}, u32[]{:S(2)}) collective-permute-start(bf16[64,2048]{1,0:T(8,128)(2,1)S(1)} %add_convert_fusion.10), channel_id=1, source_target_pairs={{0,14},{1,15},{2,0},{3,1},{4,2},{5,3},{6,4},{7,5},{8,6},{9,7},{10,... | collective-permute-start | bytes 786440 | tf_op jit(solution)/shard_map/ppermute | solution.py:429
  161.8 7.7 %collective-permute-start.35 = (bf16[64,2048]{1,0:T(8,128)(2,1)S(1)}, bf16[64,2048]{1,0:T(8,128)(2,1)S(1)}, u32[]{:S(2)}, u32[]{:S(2)}) collective-permute-start(bf16[64,2048]{1,0:T(8,128)(2,1)S(1)} %add_convert_fusion.3), channel_id=1, source_target_pairs={{0,14},{1,15},{2,0},{3,1},{4,2},{5,3},{6,4},{7,5},{8,6},{9,7},{10,... | collective-permute-start | bytes 786440 | tf_op jit(solution)/shard_map/ppermute | solution.py:429
  165.7 7.7 %collective-permute-start.31 = (bf16[64,2048]{1,0:T(8,128)(2,1)S(1)}, bf16[64,2048]{1,0:T(8,128)(2,1)S(1)}, u32[]{:S(2)}, u32[]{:S(2)}) collective-permute-start(bf16[64,2048]{1,0:T(8,128)(2,1)S(1)} %add_convert_fusion.7), channel_id=1, source_target_pairs={{0,2},{1,3},{2,4},{3,5},{4,6},{5,7},{6,8},{7,9},{8,10},{9,11},{10,... | collective-permute-start | bytes 786440 | tf_op jit(solution)/shard_map/ppermute | solution.py:426

commit v2 on v1

--- a/solution.py
+++ b/solution.py
@@ -104,28 +104,21 @@
     )(*in_hbm(queries, keys, values, gates.reshape(1, tok_count)))
 
 
-def fold(query_pack, state, pieces, own_block=False):
+def fold(query_wide, state, stack, keys_wide, block, own_block=False):
     run_max, run_sum, run_acc = state
-    tok_count = query_pack.shape[1]
+    tok_count = query_wide.shape[1]
     scale = HD ** (-0.5) * LOG2E
     scores = []
-    for i, (keys_in, at) in enumerate(pieces):
-        bias = lax.dot_general(
-            keys_in[pl.ds(at + KEYS, GATE_ROWS), :],
-            query_pack[HD:PACK, :],
-            (((0,), (0,)), ((), ())),
-            preferred_element_type=jnp.float32,
+    for part in range(2 * KEYS // HD):
+        spot = pl.ds(pl.multiple_of(block * (2 * KEYS) + part * HD, HD), HD)
+        score = jnp.dot(
+            keys_wide[spot, :], query_wide[...], preferred_element_type=jnp.float32
         )
-        for part in range(KEYS // HD):
-            keys = keys_in[pl.ds(at + HD, HD), part * HD : (part + 1) * HD]
-            score = jnp.dot(keys, query_pack[0:HD, :], preferred_element_type=jnp.float32)
-            score = score + bias[part * HD : (part + 1) * HD]
-            if own_block:
-                key_at = lax.broadcasted_iota(jnp.int32, score.shape, 0)
-                key_at = key_at + (i * KEYS + part * HD)
-                query_at = lax.broadcasted_iota(jnp.int32, score.shape, 1)
-                score = jnp.where(key_at <= query_at, score, low_score)
-            scores.append(score)
+        if own_block:
+            key_at = lax.broadcasted_iota(jnp.int32, score.shape, 0) + part * HD
+            query_at = lax.broadcasted_iota(jnp.int32, score.shape, 1)
+            score = jnp.where(key_at <= query_at, score, low_score)
+        scores.append(score)
     old_max = run_max[0:1, :]
     peak = scores[0]
     for score in scores[1:]:
@@ -135,14 +128,15 @@
     scaled_max = new_max * scale
     total = run_sum[...] * rescale
     acc = run_acc[...] * rescale
-    for i, (keys_in, at) in enumerate(pieces):
+    for i in range(2):
+        at = pl.multiple_of(block * BLOCK + i * PIECE, GATE_ROWS)
         rounded = []
         for score in scores[2 * i : 2 * i + 2]:
             lifted = jnp.exp2(score * scale - scaled_max)
             total = total + jnp.sum(lifted.reshape(HD // 8, 8, tok_count), axis=0)
             rounded.append(lifted.astype(jnp.bfloat16))
         acc = acc + jnp.dot(
-            keys_in[pl.ds(at, HD), :],
+            stack[pl.ds(at, HD), :],
             jnp.concatenate(rounded, axis=0),
             preferred_element_type=jnp.float32,
         )
@@ -153,18 +147,22 @@
 
 def clear(state):
     run_max, run_sum, run_acc = state
-    run_max[...] = jnp.full_like(run_max, low_score)
-    run_sum[...] = jnp.zeros_like(run_sum)
-    run_acc[...] = jnp.zeros_like(run_acc)
-
-
-def fold_blocks(query_pack, state, stack, first, count, seen=None):
+    run_max[...] = jnp.full(run_max.shape, low_score, jnp.float32)
+    run_sum[...] = jnp.zeros(run_sum.shape, jnp.float32)
+    run_acc[...] = jnp.zeros(run_acc.shape, jnp.float32)
+
+
+def nth_state(state, i):
+    found = []
+    for ref in state:
+        rows = ref.shape[0] // 2
+        found.append(ref.at[pl.ds(pl.multiple_of(i * rows, 8), rows)])
+    return found
+
+
+def fold_blocks(query_wide, state, stack, keys_wide, first, count, seen=None):
     def block(i, carry):
-        at = pl.multiple_of(i * BLOCK, 32)
-
-        def run():
-            fold(query_pack, state, [(stack, at), (stack, at + PIECE)])
-
+        run = partial(fold, query_wide, state, stack, keys_wide, i)
         if seen is None:
             run()
         else:
@@ -172,6 +170,28 @@
         return carry
 
     lax.fori_loop(first, first + count, block, 0)
+
+
+def load_blocks(stack, keys_wide, parts):
+    at = 0
+    for part in parts:
+        stack[at : at + part.shape[0], :] = part[...]
+        at += part.shape[0]
+    for piece in range(at // PIECE):
+        row, at = piece * KEYS, piece * PIECE
+        for half in range(KEYS // HD):
+            keys_wide[row + half * HD : row + (half + 1) * HD, 0:HD] = stack[
+                at + HD : at + 2 * HD, half * HD : (half + 1) * HD
+            ]
+        gates = stack[at + KEYS : at + PIECE, :].astype(jnp.float32)
+        rest = jnp.zeros((HD - GATE_ROWS, KEYS), jnp.float32)
+        columns = jnp.transpose(jnp.concatenate([gates, rest], axis=0))
+        keys_wide[row : row + KEYS, HD : 2 * HD] = columns.astype(jnp.bfloat16)
+
+
+def load_query(query_wide, pack):
+    query_wide[0:PACK, :] = pack[...]
+    query_wide[PACK : 2 * HD, :] = jnp.zeros((2 * HD - PACK, pack.shape[1]), jnp.bfloat16)
 
 
 def pack_result(state, out):
@@ -185,61 +205,81 @@
     out[HD:PACK, :] = block.astype(jnp.bfloat16)
 
 
-def fill(stack, parts):
-    at = 0
-    for part in parts:
-        stack[at : at + part.shape[0], :] = part[...]
-        at += part.shape[0]
-
-
 def distant_kernel(*refs):
-    packs, keys, states, stack = refs[:2], refs[2:5], (refs[5:8], refs[8:11]), refs[11]
+    packs, keys, states = refs[:2], refs[2:5], refs[5:8]
+    stack, keys_wide, query_wide = refs[8:]
     own_y = lax.axis_index("sp") >> 2
-    fill(stack, keys)
-    for pack, state, above in zip(packs, states, (3, 2)):
-
-        @pl.when(own_y + above <= 3)
+
+    @pl.when(own_y < 2)
+    def _():
+        load_blocks(stack, keys_wide, keys)
+
+    def each(i, carry):
+        @pl.when(own_y <= i)
         def _():
+            for at, pack in enumerate(packs):
+                pl.when(i == at)(partial(load_query, query_wide, pack))
+            state = nth_state(states, i)
             clear(state)
-            fold_blocks(pack, state, stack, 0, 3)
+            fold_blocks(query_wide, state, stack, keys_wide, 0, 3)
+
+        return carry
+
+    lax.fori_loop(0, 2, each, 0)
 
 
 def distant_end_kernel(*refs):
-    packs, far, states_in, outs = refs[:2], refs[2:4], (refs[4:7], refs[7:10]), refs[10:12]
-    state = refs[12:15]
+    packs, far, states, outs = refs[:2], refs[2:4], refs[4:7], refs[7:9]
+    state, (stack, keys_wide, query_wide) = refs[9:12], refs[12:]
     own_y = lax.axis_index("sp") >> 2
-    for pack, state_in, out, above in zip(packs, states_in, outs, (3, 2)):
-
-        @pl.when(own_y + above <= 3)
+
+    @pl.when(own_y < 2)
+    def _():
+        load_blocks(stack, keys_wide, far)
+
+    def each(i, carry):
+        @pl.when(own_y <= i)
         def _():
-            for into, came in zip(state, state_in):
+            for into, came in zip(state, nth_state(states, i)):
                 into[...] = came[...]
-            fold(pack, state, [(far[0], 0), (far[1], 0)])
-            pack_result(state, out)
-
-
-def close_kernel(*refs):
-    next_pack, own_pack = refs[:2]
-    keys, out, own_state = refs[2:7], refs[7], refs[8:11]
-    state, stack = refs[11:14], refs[14]
-    own = lax.axis_index("sp")
-    own_x = own & 3
-    fill(stack, keys)
-
-    @pl.when(own < 12)
+            for at, pack in enumerate(packs):
+                pl.when(i == at)(partial(load_query, query_wide, pack))
+            fold(query_wide, state, stack, keys_wide, 0)
+            for at, out in enumerate(outs):
+                pl.when(i == at)(partial(pack_result, state, out))
+
+        return carry
+
+    lax.fori_loop(0, 2, each, 0)
+
+
+def next_kernel(*refs):
+    pack, keys, out, state = refs[0], refs[1:6], refs[6], refs[7:10]
+    stack, keys_wide, query_wide = refs[10:]
+
+    @pl.when(lax.axis_index("sp") < 12)
     def _():
+        load_blocks(stack, keys_wide, keys)
+        load_query(query_wide, pack)
         clear(state)
-        fold_blocks(next_pack, state, stack, 0, 4)
+        fold_blocks(query_wide, state, stack, keys_wide, 0, 4)
         pack_result(state, out)
 
-    clear(own_state)
-    fold(own_pack, own_state, [(keys[0], 0), (keys[0], PIECE)], own_block=True)
+
+def own_kernel(*refs):
+    pack, keys, state = refs[0], refs[1:6], refs[6:9]
+    stack, keys_wide, query_wide = refs[9:]
+    own_x = lax.axis_index("sp") & 3
+    load_blocks(stack, keys_wide, keys)
+    load_query(query_wide, pack)
+    clear(state)
+    fold(query_wide, state, stack, keys_wide, 0, own_block=True)
 
     def seen(i):
         move = jnp.where(i == 1, -1, jnp.where(i == 2, 1, 2))
         return ((own_x + move) & 3) < own_x
 
-    fold_blocks(own_pack, own_state, stack, 1, 3, seen)
+    fold_blocks(query_wide, state, stack, keys_wide, 1, 3, seen)
 
 
 def merge_kernel(*refs):
@@ -304,28 +344,26 @@
 
     narrow = ((8, tok_count), jnp.float32)
     state = [narrow, narrow, ((HD, tok_count), jnp.float32)]
+    both = [((2 * shape[0], tok_count), kind) for shape, kind in state]
     result = ((PACK, tok_count), jnp.bfloat16)
 
-    def stack(count):
-        return ((count * BLOCK, 2 * HD), jnp.bfloat16)
-
-    near = attend(distant_kernel, [pack3, pack2, keys_own, low, high], state * 2, [stack(3)], 6)
+    def loaded(count):
+        shapes = (count * BLOCK, 2 * HD), (count * 2 * KEYS, 2 * HD), (2 * HD, tok_count)
+        return [(shape, jnp.bfloat16) for shape in shapes]
+
+    near = attend(distant_kernel, [pack3, pack2, keys_own, low, high], both, loaded(3), 6)
     far_a, far_b, near = lax.optimization_barrier((far_a, far_b, near))
     part3, part2 = attend(
-        distant_end_kernel, [pack3, pack2, far_a, far_b, *near], [result] * 2, state, 2
+        distant_end_kernel, [pack3, pack2, far_a, far_b, *near], [result] * 2, state + loaded(1), 2
     )
     part3, part2, pack1 = lax.optimization_barrier((part3, part2, pack1))
     back3 = shift(part3, -1, 0, lambda y, x: y == 3)
     back2 = shift(part2, 2, 0, lambda y, x: y > 1)
-    part1, *own_state = attend(
-        close_kernel,
-        [pack1, own_pack, keys_own, low, high, far_a, far_b],
-        [result] + state,
-        state + [stack(4)],
-        8,
-    )
+    keys = [keys_own, low, high, far_a, far_b]
+    (part1,) = attend(next_kernel, [pack1, *keys], [result], state + loaded(4), 4)
+    part1, own_pack, keys, weights = lax.optimization_barrier((part1, own_pack, keys, weights))
     back1 = shift(part1, 1, 0, lambda y, x: y > 0)
-    part1, weights = lax.optimization_barrier((part1, weights))
+    own_state = attend(own_kernel, [own_pack, *keys], state, loaded(4), 4)
     staged = stage_weights(*weights)
     (head_out,) = attend(
         merge_kernel,

time: 188 us -> 185 us (0.984)
    pallas_call x4 -> x5, Pallas kernels: 12.2 us -> 10.9 us  [attend(): pl.pallas_call(kernel, out_shape=tuple((jax.ShapeDtypeStruct(*out) for ou...]
  transfers between devices with their start and end apart: 39 -> 39, of which waited for: 15 -> 15; matrix products, arithmetic and copies ran while one was open for 0% -> 0% of each run, Pallas kernels for 10% -> 11%
where the time goes in v2:
time: 185 us; the launch traced here: 184 us
  starting transfers between devices  69.2 us (37%)
  blocking collectives  50.4 us (27%)
  waiting for transfers between devices  36.1 us (20%)
  Pallas kernels  27.2 us (15%)
    ppermute x14, starting transfers between devices, down(): return lax.ppermute(array, 'tp', z_perm(-1))  44.2 us
    ppermute x14, waiting for transfers between devices, up(): return lax.ppermute(array, 'tp', z_perm(1))  27.4 us
    ppermute x10, starting transfers between devices, shift(): return lax.ppermute(array, 'sp', sp_perm(dy, dx, needed))  23.6 us
    all_to_all x1, blocking collectives, on_device(): lax.all_to_all(outgoing, 'sp', split_axis=0, concat_axis=0, tiled=True)  19.9 us
    all_to_all x1, blocking collectives, on_device(): heads = lax.all_to_all(heads, 'tp', split_axis=0, concat_axis=0, tiled=True)  17 us
    all_to_all x1, blocking collectives, on_device(): lax.all_to_all(expert_out, 'sp', split_axis=0, concat_axis=0, tiled=True)  13.5 us
    pallas_call x5, Pallas kernels, attend(): pl.pallas_call(kernel, out_shape=tuple((jax.ShapeDtypeStruct(*out) for ou...  10.9 us
    pallas_call x4, Pallas kernels, expert_rows(): pl.pallas_call(partial(expert_kernel, count=count), out_shape=tuple((jax....  9.44 us
  transfers between devices with their start and end apart: 39, of which 15 were waited for; matrix products, arithmetic and copies ran while one was open for 0% of the time, Pallas kernels for 11%

profile of v2, /device:TPU:2, one launch (start us, length us, event | category | flops | bytes accessed | tf_op | source)
XLA Modules:
  0.0 184.4 jit_solution(6892912568239042770)
XLA Ops:
  1.2 3.4 %collective-permute-start.2 = (bf16[544,256]{1,0:T(8,128)(2,1)S(1)}, bf16[544,256]{1,0:T(8,128)(2,1)S(1)}, u32[]{:S(2)}, u32[]{:S(2)}) collective-permute-start(bf16[544,256]{1,0:T(8,128)(2,1)S(1)} %get-tuple-element.69.refs_2_.refs_1_), channel_id=1, source_target_pairs={{0,16},{16,32},{32,48},{48,0},{64,80},{80,96},{96,112},{112,64},{1... | collective-permute-start | bytes 835592 | tf_op jit(solution)/shard_map/ppermute | solution.py:334
  4.6 2.7 %collective-permute-start.4 = (bf16[544,256]{1,0:T(8,128)(2,1)S(1)}, bf16[544,256]{1,0:T(8,128)(2,1)S(1)}, u32[]{:S(2)}, u32[]{:S(2)}) collective-permute-start(bf16[544,256]{1,0:T(8,128)(2,1)S(1)} %get-tuple-element.69.refs_2_.refs_1_), channel_id=1, source_target_pairs={{0,48},{16,0},{32,16},{48,32},{64,112},{80,64},{96,80},{112,96},{1... | collective-permute-start | bytes 835592 | tf_op jit(solution)/shard_map/ppermute | solution.py:334
  7.3 1.3 collective-permute-start
  8.6 1.3 collective-permute-start.1
  11.5 3.4 %collective-permute-start.3 = (bf16[272,256]{1,0:T(8,128)(2,1)S(1)}, bf16[272,256]{1,0:T(8,128)(2,1)S(1)}, u32[]{:S(2)}, u32[]{:S(2)}) collective-permute-start(bf16[272,256]{1,0:T(8,128)(2,1)S(1)} %slice.24), channel_id=1, source_target_pairs={{0,16},{16,32},{32,48},{48,0},{64,80},{80,96},{96,112},{112,64},{1... | collective-permute-start | bytes 417800 | tf_op jit(solution)/shard_map/ppermute | solution.py:334
  15.0 3.4 %collective-permute-start.5 = (bf16[272,256]{1,0:T(8,128)(2,1)S(1)}, bf16[272,256]{1,0:T(8,128)(2,1)S(1)}, u32[]{:S(2)}, u32[]{:S(2)}) collective-permute-start(bf16[272,256]{1,0:T(8,128)(2,1)S(1)} %slice.25), channel_id=1, source_target_pairs={{0,48},{16,0},{32,16},{48,32},{64,112},{80,64},{96,80},{112,96},{1... | collective-permute-start | bytes 417800 | tf_op jit(solution)/shard_map/ppermute | solution.py:334
  18.4 4.4 %shard_map.127 = (f32[16,512]{1,0:T(8,128)S(1)}, f32[16,512]{1,0:T(8,128)S(1)}, f32[256,512]{1,0:T(8,128)S(1)}) custom-call(bf16[144,512]{1,0:T(8,128)(2,1)S(1)} %collective-permute-done.refs_0_, bf16[144,512]{1,0:T(8,128)(2,1)S(1)} %collective-permute-done.1.refs_1_, bf16[544,256]{1,0:T(8,128)(2,1)S(1)} %get-tuple-element.69.refs_2_.refs_1_, ...), custom_call_target="tpu_custom_call" | custom-call | flops 1610612736 | bytes 1048576 | tf_op jit(solution)/shard_map/pallas_call | solution.py:315
  22.8 1.7 shard_map.128
  24.5 3.1 %shard_map.129 = bf16[144,512]{1,0:T(8,128)(2,1)S(1)} custom-call(bf16[144,512]{1,0:T(8,128)(2,1)S(1)} %collective-permute-done.6.refs_0_, bf16[544,256]{1,0:T(8,128)(2,1)S(1)} %get-tuple-element.69.refs_2_.refs_1_, bf16[544,256]{1,0:T(8,128)(2,1)S(1)} %collective-permute-done.2.refs_3_.refs_2_, bf16[544,256]{1,0:T(8,128)(2,1)S(1)} %collective-permute-done.4.refs_4_.refs_3_, ...), custom_call_target="tpu_custom_call" | custom-call | flops 1073741824 | bytes 1048576 | tf_op jit(solution)/shard_map/pallas_call | solution.py:315
  27.7 2.1 %stage_weights.1.refs_4_.refs_6_.refs_2_ = bf16[6144,256]{1,0:T(8,128)(2,1)S(1)} custom-call(bf16[2048,256]{1,0:T(8,128)(2,1)} %bitcast.26, bf16[2048,256]{1,0:T(8,128)(2,1)} %bitcast.27, bf16[256,2048]{1,0:T(8,128)(2,1)} %bitcast.28), custom_call_target="tpu_custom_call" | custom-call | tf_op jit(solution)/shard_map/stage_weights/pallas_call | solution.py:397
  29.9 2.5 %collective-permute-start.7 = (bf16[144,512]{1,0:T(8,128)(2,1)S(1)}, bf16[144,512]{1,0:T(8,128)(2,1)S(1)}, u32[]{:S(2)}, u32[]{:S(2)}) collective-permute-start(bf16[144,512]{1,0:T(8,128)(2,1)S(1)} %shard_map.129), channel_id=1, source_target_pairs={{0,64},{16,80},{32,96},{48,112},{64,128},{80,144},{96,160},{112,17... | collective-permute-start | bytes 442376 | tf_op jit(solution)/shard_map/ppermute | solution.py:334
  32.4 3.1 %collective-permute-start.8 = (bf16[144,512]{1,0:T(8,128)(2,1)S(1)}, bf16[144,512]{1,0:T(8,128)(2,1)S(1)}, u32[]{:S(2)}, u32[]{:S(2)}) collective-permute-start(bf16[144,512]{1,0:T(8,128)(2,1)S(1)} %get-tuple-element.66), channel_id=1, source_target_pairs={{0,128},{16,144},{32,160},{48,176},{64,192},{80,208},{96,224},{112... | collective-permute-start | bytes 442376 | tf_op jit(solution)/shard_map/ppermute | solution.py:334
  35.5 1.3 collective-permute-start.9
  36.8 1.5 shard_map.130
  39.1 1.9 %collective-permute-done.9.refs_2_ = bf16[144,512]{1,0:T(8,128)(2,1)S(1)} collective-permute-done((bf16[144,512]{1,0:T(8,128)(2,1)S(1)}, bf16[144,512]{1,0:T(8,128)(2,1)S(1)}, u32[]{:S(2)}, u32[]{:S(2)}) %collective-permute-start.9) | collective-permute-done | bytes 147488 | tf_op jit(solution)/shard_map/ppermute | solution.py:334
  41.4 17.0 %all_to_all.15.heads = bf16[16,32,128]{2,1,0:T(8,128)(2,1)S(1)} all-to-all(bf16[16,32,128]{2,1,0:T(8,128)(2,1)S(1)} %bitcast.21), channel_id=1, replica_groups=mesh['sp'=16,'tp'=16] {'tp'}, dimensions={0} | all-to-all | bytes 262144 | tf_op jit(solution)/shard_map/all_to_all | solution.py:625
  58.4 2.5 %project.1 = (f32[32,2048]{1,0:T(8,128)S(1)}, bf16[128,2048]{1,0:T(8,128)(2,1)S(1)}, f32[128,32]{1,0:T(8,128)S(1)}) custom-call(bf16[16,32,128]{2,1,0:T(8,128)(2,1)S(1)} %all_to_all.15.heads, bf16[2048,2048]{1,0:T(8,128)(2,1)S(1)} %bitcast.18, bf16[32,2048]{1,0:T(8,128)(2,1)S(1)} %copy-done, f32[1,2048]{1,0:T(1,128)S(1)} %bitcast.22, s32[2,32]{1,0:T(2,128)S(1)} %bitcast.23, ...), custom_call_target="tpu_custom_call" | custom-call | tf_op jit(solution)/shard_map/project/pallas_call | solution.py:555
  61.0 19.9 %all_to_all.16 = bf16[16,8,2048]{2,1,0:T(8,128)(2,1)S(1)} all-to-all(bf16[16,8,2048]{2,1,0:T(8,128)(2,1)S(1)} %bitcast.20), channel_id=1, replica_groups=mesh['sp'=16,'tp'=16] {'sp'}, dimensions={0} | all-to-all | bytes 1048576 | tf_op jit(solution)/shard_map/all_to_all | solution.py:630
  81.5 2.7 %collective-permute-start.19 = (bf16[64,2048]{1,0:T(8,128)(2,1)S(1)}, bf16[64,2048]{1,0:T(8,128)(2,1)S(1)}, u32[]{:S(2)}, u32[]{:S(2)}) collective-permute-start(bf16[64,2048]{1,0:T(8,128)(2,1)S(1)} %get-tuple-element.99.refs_1_), channel_id=1, source_target_pairs={{0,14},{1,15},{2,0},{3,1},{4,2},{5,3},{6,4},{7,5},{8,6},{9,7},{10,... | collective-permute-start | bytes 786440 | tf_op jit(solution)/shard_map/ppermute | solution.py:467
  84.2 3.2 %collective-permute-start.16 = (bf16[64,2048]{1,0:T(8,128)(2,1)S(1)}, bf16[64,2048]{1,0:T(8,128)(2,1)S(1)}, u32[]{:S(2)}, u32[]{:S(2)}) collective-permute-start(bf16[64,2048]{1,0:T(8,128)(2,1)S(1)} %get-tuple-element.100.refs_0_), channel_id=1, source_target_pairs={{0,14},{1,15},{2,0},{3,1},{4,2},{5,3},{6,4},{7,5},{8,6},{9,7},{10,... | collective-permute-start | bytes 786440 | tf_op jit(solution)/shard_map/ppermute | solution.py:467
  87.5 3.9 %collective-permute-done.10.refs_2_ = bf16[64,2048]{1,0:T(8,128)(2,1)S(1)} collective-permute-done((bf16[64,2048]{1,0:T(8,128)(2,1)S(1)}, bf16[64,2048]{1,0:T(8,128)(2,1)S(1)}, u32[]{:S(2)}, u32[]{:S(2)}) %collective-permute-start.10) | collective-permute-done | bytes 262176 | tf_op jit(solution)/shard_map/ppermute | solution.py:464
  91.4 3.2 %collective-permute-start.20 = (bf16[64,2048]{1,0:T(8,128)(2,1)S(1)}, bf16[64,2048]{1,0:T(8,128)(2,1)S(1)}, u32[]{:S(2)}, u32[]{:S(2)}) collective-permute-start(bf16[64,2048]{1,0:T(8,128)(2,1)S(1)} %collective-permute-done.19.refs_5_), channel_id=1, source_target_pairs={{0,14},{1,15},{2,0},{3,1},{4,2},{5,3},{6,4},{7,5},{8,6},{9,7},{10,... | collective-permute-start | bytes 786440 | tf_op jit(solution)/shard_map/ppermute | solution.py:467
  94.6 2.4 %collective-permute-done.13.refs_3_ = bf16[64,2048]{1,0:T(8,128)(2,1)S(1)} collective-permute-done((bf16[64,2048]{1,0:T(8,128)(2,1)S(1)}, bf16[64,2048]{1,0:T(8,128)(2,1)S(1)}, u32[]{:S(2)}, u32[]{:S(2)}) %collective-permute-start.13) | collective-permute-done | bytes 262176 | tf_op jit(solution)/shard_map/ppermute | solution.py:464
  97.0 3.2 %collective-permute-start.17 = (bf16[64,2048]{1,0:T(8,128)(2,1)S(1)}, bf16[64,2048]{1,0:T(8,128)(2,1)S(1)}, u32[]{:S(2)}, u32[]{:S(2)}) collective-permute-start(bf16[64,2048]{1,0:T(8,128)(2,1)S(1)} %collective-permute-done.16.refs_4_), channel_id=1, source_target_pairs={{0,14},{1,15},{2,0},{3,1},{4,2},{5,3},{6,4},{7,5},{8,6},{9,7},{10,... | collective-permute-start | bytes 786440 | tf_op jit(solution)/shard_map/ppermute | solution.py:467
  100.2 2.4 %collective-permute-done.11.refs_0_ = bf16[64,2048]{1,0:T(8,128)(2,1)S(1)} collective-permute-done((bf16[64,2048]{1,0:T(8,128)(2,1)S(1)}, bf16[64,2048]{1,0:T(8,128)(2,1)S(1)}, u32[]{:S(2)}, u32[]{:S(2)}) %collective-permute-start.11) | collective-permute-done | bytes 262176 | tf_op jit(solution)/shard_map/ppermute | solution.py:464
  102.6 3.2 %collective-permute-start.21 = (bf16[64,2048]{1,0:T(8,128)(2,1)S(1)}, bf16[64,2048]{1,0:T(8,128)(2,1)S(1)}, u32[]{:S(2)}, u32[]{:S(2)}) collective-permute-start(bf16[64,2048]{1,0:T(8,128)(2,1)S(1)} %collective-permute-done.20.refs_3_), channel_id=1, source_target_pairs={{0,14},{1,15},{2,0},{3,1},{4,2},{5,3},{6,4},{7,5},{8,6},{9,7},{10,... | collective-permute-start | bytes 786440 | tf_op jit(solution)/shard_map/ppermute | solution.py:467
  105.9 2.4 %collective-permute-done.14.refs_1_ = bf16[64,2048]{1,0:T(8,128)(2,1)S(1)} collective-permute-done((bf16[64,2048]{1,0:T(8,128)(2,1)S(1)}, bf16[64,2048]{1,0:T(8,128)(2,1)S(1)}, u32[]{:S(2)}, u32[]{:S(2)}) %collective-permute-start.14) | collective-permute-done | bytes 262176 | tf_op jit(solution)/shard_map/ppermute | solution.py:464
  108.2 3.2 %collective-permute-start.18 = (bf16[64,2048]{1,0:T(8,128)(2,1)S(1)}, bf16[64,2048]{1,0:T(8,128)(2,1)S(1)}, u32[]{:S(2)}, u32[]{:S(2)}) collective-permute-start(bf16[64,2048]{1,0:T(8,128)(2,1)S(1)} %collective-permute-done.17.refs_2_), channel_id=1, source_target_pairs={{0,14},{1,15},{2,0},{3,1},{4,2},{5,3},{6,4},{7,5},{8,6},{9,7},{10,... | collective-permute-start | bytes 786440 | tf_op jit(solution)/shard_map/ppermute | solution.py:467
  111.5 2.4 %collective-permute-done.12.refs_0_ = bf16[64,2048]{1,0:T(8,128)(2,1)S(1)} collective-permute-done((bf16[64,2048]{1,0:T(8,128)(2,1)S(1)}, bf16[64,2048]{1,0:T(8,128)(2,1)S(1)}, u32[]{:S(2)}, u32[]{:S(2)}) %collective-permute-start.12) | collective-permute-done | bytes 262176 | tf_op jit(solution)/shard_map/ppermute | solution.py:464
  113.9 3.2 %collective-permute-start.27 = (bf16[64,2048]{1,0:T(8,128)(2,1)S(1)}, bf16[64,2048]{1,0:T(8,128)(2,1)S(1)}, u32[]{:S(2)}, u32[]{:S(2)}) collective-permute-start(bf16[64,2048]{1,0:T(8,128)(2,1)S(1)} %collective-permute-done.21.refs_3_), channel_id=1, source_target_pairs={{0,14},{1,15},{2,0},{3,1},{4,2},{5,3},{6,4},{7,5},{8,6},{9,7},{10,... | collective-permute-start | bytes 786440 | tf_op jit(solution)/shard_map/ppermute | solution.py:467
  117.1 2.4 %collective-permute-done.15.refs_1_ = bf16[64,2048]{1,0:T(8,128)(2,1)S(1)} collective-permute-done((bf16[64,2048]{1,0:T(8,128)(2,1)S(1)}, bf16[64,2048]{1,0:T(8,128)(2,1)S(1)}, u32[]{:S(2)}, u32[]{:S(2)}) %collective-permute-start.15) | collective-permute-done | bytes 262176 | tf_op jit(solution)/shard_map/ppermute | solution.py:464
  119.5 2.4 %shard_map.132 = (bf16[64,2048]{1,0:T(8,128)(2,1)S(1)}, bf16[64,2048]{1,0:T(8,128)(2,1)S(1)}, bf16[64,2048]{1,0:T(8,128)(2,1)S(1)}, bf16[64,2048]{1,0:T(8,128)(2,1)S(1)}) custom-call(bf16[64,2048]{1,0:T(8,128)(2,1)S(1)} %collective-permute-done.12.refs_0_, bf16[64,2048]{1,0:T(8,128)(2,1)S(1)} %collective-permute-done.15.refs_1_, ...), custom_call_target="tpu_custom_call" | custom-call | flops 1610612736 | bytes 6291456 | tf_op jit(solution)/shard_map/pallas_call | solution.py:447
  122.0 2.3 %collective-permute-done.26.refs_0_ = bf16[64,2048]{1,0:T(8,128)(2,1)S(1)} collective-permute-done((bf16[64,2048]{1,0:T(8,128)(2,1)S(1)}, bf16[64,2048]{1,0:T(8,128)(2,1)S(1)}, u32[]{:S(2)}, u32[]{:S(2)}) %collective-permute-start.26) | collective-permute-done | bytes 262176 | tf_op jit(solution)/shard_map/ppermute | solution.py:464
  125.5 2.0 %collective-permute-start.32 = (bf16[64,2048]{1,0:T(8,128)(2,1)S(1)}, bf16[64,2048]{1,0:T(8,128)(2,1)S(1)}, u32[]{:S(2)}, u32[]{:S(2)}) collective-permute-start(bf16[64,2048]{1,0:T(8,128)(2,1)S(1)} %get-tuple-element.90), channel_id=1, source_target_pairs={{0,14},{1,15},{2,0},{3,1},{4,2},{5,3},{6,4},{7,5},{8,6},{9,7},{10,... | collective-permute-start | bytes 786440 | tf_op jit(solution)/shard_map/ppermute | solution.py:467
  127.6 3.2 %collective-permute-start.23 = (bf16[64,2048]{1,0:T(8,128)(2,1)S(1)}, bf16[64,2048]{1,0:T(8,128)(2,1)S(1)}, u32[]{:S(2)}, u32[]{:S(2)}) collective-permute-start(bf16[64,2048]{1,0:T(8,128)(2,1)S(1)} %get-tuple-element.82), channel_id=1, source_target_pairs={{0,14},{1,15},{2,0},{3,1},{4,2},{5,3},{6,4},{7,5},{8,6},{9,7},{10,... | collective-permute-start | bytes 786440 | tf_op jit(solution)/shard_map/ppermute | solution.py:467
  130.7 2.4 %shard_map.133 = (bf16[64,2048]{1,0:T(8,128)(2,1)S(1)}, bf16[64,2048]{1,0:T(8,128)(2,1)S(1)}, bf16[64,2048]{1,0:T(8,128)(2,1)S(1)}, bf16[64,2048]{1,0:T(8,128)(2,1)S(1)}) custom-call(bf16[64,2048]{1,0:T(8,128)(2,1)S(1)} %collective-permute-done.11.refs_0_, bf16[64,2048]{1,0:T(8,128)(2,1)S(1)} %collective-permute-done.14.refs_1_, ...), custom_call_target="tpu_custom_call" | custom-call | flops 1610612736 | bytes 6291456 | tf_op jit(solution)/shard_map/pallas_call | solution.py:447
  133.1 3.6 %shard_map.134 = (bf16[64,2048]{1,0:T(8,128)(2,1)S(1)}, bf16[64,2048]{1,0:T(8,128)(2,1)S(1)}, bf16[64,2048]{1,0:T(8,128)(2,1)S(1)}, bf16[64,2048]{1,0:T(8,128)(2...) custom-call(bf16[64,2048]{1,0:T(8,128)(2,1)S(1)} %get-tuple-element.100.refs_0_, ...), custom_call_target="tpu_custom_call" | custom-call | flops 2415919104 | bytes 6291456 | tf_op jit(solution)/shard_map/pallas_call | solution.py:447
  136.9 3.3 %collective-permute-start.33 = (bf16[64,2048]{1,0:T(8,128)(2,1)S(1)}, bf16[64,2048]{1,0:T(8,128)(2,1)S(1)}, u32[]{:S(2)}, u32[]{:S(2)}) collective-permute-start(bf16[64,2048]{1,0:T(8,128)(2,1)S(1)} %add_convert_fusion.5), channel_id=1, source_target_pairs={{0,14},{1,15},{2,0},{3,1},{4,2},{5,3},{6,4},{7,5},{8,6},{9,7},{10,... | collective-permute-start | bytes 786440 | tf_op jit(solution)/shard_map/ppermute | solution.py:467
  140.5 3.3 %collective-permute-start.24 = (bf16[64,2048]{1,0:T(8,128)(2,1)S(1)}, bf16[64,2048]{1,0:T(8,128)(2,1)S(1)}, u32[]{:S(2)}, u32[]{:S(2)}) collective-permute-start(bf16[64,2048]{1,0:T(8,128)(2,1)S(1)} %add_convert_fusion.11), channel_id=1, source_target_pairs={{0,14},{1,15},{2,0},{3,1},{4,2},{5,3},{6,4},{7,5},{8,6},{9,7},{10,... | collective-permute-start | bytes 786440 | tf_op jit(solution)/shard_map/ppermute | solution.py:467
  143.8 3.5 %collective-permute-done.37 = bf16[64,2048]{1,0:T(8,128)(2,1)S(1)} collective-permute-done((bf16[64,2048]{1,0:T(8,128)(2,1)S(1)}, bf16[64,2048]{1,0:T(8,128)(2,1)S(1)}, u32[]{:S(2)}, u32[]{:S(2)}) %collective-permute-start.37) | collective-permute-done | bytes 262176 | tf_op jit(solution)/shard_map/ppermute | solution.py:464
  147.5 3.3 %collective-permute-start.34 = (bf16[64,2048]{1,0:T(8,128)(2,1)S(1)}, bf16[64,2048]{1,0:T(8,128)(2,1)S(1)}, u32[]{:S(2)}, u32[]{:S(2)}) collective-permute-start(bf16[64,2048]{1,0:T(8,128)(2,1)S(1)} %add_convert_fusion.4), channel_id=1, source_target_pairs={{0,14},{1,15},{2,0},{3,1},{4,2},{5,3},{6,4},{7,5},{8,6},{9,7},{10,... | collective-permute-start | bytes 786440 | tf_op jit(solution)/shard_map/ppermute | solution.py:467
  150.8 2.1 %collective-permute-done.29 = bf16[64,2048]{1,0:T(8,128)(2,1)S(1)} collective-permute-done((bf16[64,2048]{1,0:T(8,128)(2,1)S(1)}, bf16[64,2048]{1,0:T(8,128)(2,1)S(1)}, u32[]{:S(2)}, u32[]{:S(2)}) %collective-permute-start.29) | collective-permute-done | bytes 262176 | tf_op jit(solution)/shard_map/ppermute | solution.py:464
  153.1 3.3 %collective-permute-start.25 = (bf16[64,2048]{1,0:T(8,128)(2,1)S(1)}, bf16[64,2048]{1,0:T(8,128)(2,1)S(1)}, u32[]{:S(2)}, u32[]{:S(2)}) collective-permute-start(bf16[64,2048]{1,0:T(8,128)(2,1)S(1)} %add_convert_fusion.10), channel_id=1, source_target_pairs={{0,14},{1,15},{2,0},{3,1},{4,2},{5,3},{6,4},{7,5},{8,6},{9,7},{10,... | collective-permute-start | bytes 786440 | tf_op jit(solution)/shard_map/ppermute | solution.py:467
  156.4 1.8 collective-permute-done.34
  158.2 3.8 %collective-permute-start.35 = (bf16[64,2048]{1,0:T(8,128)(2,1)S(1)}, bf16[64,2048]{1,0:T(8,128)(2,1)S(1)}, u32[]{:S(2)}, u32[]{:S(2)}) collective-permute-start(bf16[64,2048]{1,0:T(8,128)(2,1)S(1)} %add_convert_fusion.3), channel_id=1, source_target_pairs={{0,14},{1,15},{2,0},{3,1},{4,2},{5,3},{6,4},{7,5},{8,6},{9,7},{10,... | collective-permute-start | bytes 786440 | tf_op jit(solution)/shard_map/ppermute | solution.py:467
  162.2 3.7 %collective-permute-done.35 = bf16[64,2048]{1,0:T(8,128)(2,1)S(1)} collective-permute-done((bf16[64,2048]{1,0:T(8,128)(2,1)S(1)}, bf16[64,2048]{1,0:T(8,128)(2,1)S(1)}, u32[]{:S(2)}, u32[]{:S(2)}) %collective-permute-start.35) | collective-permute-done | bytes 262176 | tf_op jit(solution)/shard_map/ppermute | solution.py:467
  166.0 3.7 %collective-permute-done.31 = bf16[64,2048]{1,0:T(8,128)(2,1)S(1)} collective-permute-done((bf16[64,2048]{1,0:T(8,128)(2,1)S(1)}, bf16[64,2048]{1,0:T(8,128)(2,1)S(1)}, u32[]{:S(2)}, u32[]{:S(2)}) %collective-permute-start.31) | collective-permute-done | bytes 262176 | tf_op jit(solution)/shard_map/ppermute | solution.py:464
  169.9 13.5 %all_to_all.17 = bf16[16,8,2048]{2,1,0:T(8,128)(2,1)S(1)} all-to-all(bf16[16,8,2048]{2,1,0:T(8,128)(2,1)S(1)} %maximum_bitcast_fusion), channel_id=1, replica_groups=mesh['sp'=16,'tp'=16] {'sp'}, dimensions={0} | all-to-all | bytes 1048576 | tf_op jit(solution)/shard_map/all_to_all | solution.py:633
  (77 shorter events, 8.6 us)
Async XLA Ops:
  1.2 10.3 %collective-permute-start.2 = (bf16[544,256]{1,0:T(8,128)(2,1)S(1)}, bf16[544,256]{1,0:T(8,128)(2,1)S(1)}, u32[]{:S(2)}, u32[]{:S(2)}) collective-permute-start(bf16[544,256]{1,0:T(8,128)(2,1)S(1)} %get-tuple-element.69.refs_2_.refs_1_), channel_id=1, source_target_pairs={{0,16},{16,32},{32,48},{48,0},{64,80},{80,96},{96,112},{112,64},{1... | collective-permute-start | bytes 835592 | tf_op jit(solution)/shard_map/ppermute | solution.py:334
  4.6 10.3 %collective-permute-start.4 = (bf16[544,256]{1,0:T(8,128)(2,1)S(1)}, bf16[544,256]{1,0:T(8,128)(2,1)S(1)}, u32[]{:S(2)}, u32[]{:S(2)}) collective-permute-start(bf16[544,256]{1,0:T(8,128)(2,1)S(1)} %get-tuple-element.69.refs_2_.refs_1_), channel_id=1, source_target_pairs={{0,48},{16,0},{32,16},{48,32},{64,112},{80,64},{96,80},{112,96},{1... | collective-permute-start | bytes 835592 | tf_op jit(solution)/shard_map/ppermute | solution.py:334
  7.3 11.1 %collective-permute-start = (bf16[144,512]{1,0:T(8,128)(2,1)S(1)}, bf16[144,512]{1,0:T(8,128)(2,1)S(1)}, u32[]{:S(2)}, u32[]{:S(2)}) collective-permute-start(bf16[144,512]{1,0:T(8,128)(2,1)S(1)} %get-tuple-element.68.refs_0_), channel_id=1, source_target_pairs={{192,0},{208,16},{224,32},{240,48},{193,1},{209,17},{225,33},{241,... | collective-permute-start | bytes 442376 | tf_op jit(solution)/shard_map/ppermute | solution.py:334
  8.6 9.8 %collective-permute-start.1 = (bf16[144,512]{1,0:T(8,128)(2,1)S(1)}, bf16[144,512]{1,0:T(8,128)(2,1)S(1)}, u32[]{:S(2)}, u32[]{:S(2)}) collective-permute-start(bf16[144,512]{1,0:T(8,128)(2,1)S(1)} %get-tuple-element.68.refs_0_), channel_id=1, source_target_pairs={{128,0},{144,16},{160,32},{176,48},{192,64},{208,80},{224,96},{240... | collective-permute-start | bytes 442376 | tf_op jit(solution)/shard_map/ppermute | solution.py:334
  9.9 14.6 %collective-permute-start.6 = (bf16[144,512]{1,0:T(8,128)(2,1)S(1)}, bf16[144,512]{1,0:T(8,128)(2,1)S(1)}, u32[]{:S(2)}, u32[]{:S(2)}) collective-permute-start(bf16[144,512]{1,0:T(8,128)(2,1)S(1)} %get-tuple-element.68.refs_0_), channel_id=1, source_target_pairs={{64,0},{80,16},{96,32},{112,48},{128,64},{144,80},{160,96},{176,11... | collective-permute-start | bytes 442376 | tf_op jit(solution)/shard_map/ppermute | solution.py:334
  11.5 11.3 %collective-permute-start.3 = (bf16[272,256]{1,0:T(8,128)(2,1)S(1)}, bf16[272,256]{1,0:T(8,128)(2,1)S(1)}, u32[]{:S(2)}, u32[]{:S(2)}) collective-permute-start(bf16[272,256]{1,0:T(8,128)(2,1)S(1)} %slice.24), channel_id=1, source_target_pairs={{0,16},{16,32},{32,48},{48,0},{64,80},{80,96},{96,112},{112,64},{1... | collective-permute-start | bytes 417800 | tf_op jit(solution)/shard_map/ppermute | solution.py:334
  15.0 7.9 %collective-permute-start.5 = (bf16[272,256]{1,0:T(8,128)(2,1)S(1)}, bf16[272,256]{1,0:T(8,128)(2,1)S(1)}, u32[]{:S(2)}, u32[]{:S(2)}) collective-permute-start(bf16[272,256]{1,0:T(8,128)(2,1)S(1)} %slice.25), channel_id=1, source_target_pairs={{0,48},{16,0},{32,16},{48,32},{64,112},{80,64},{96,80},{112,96},{1... | collective-permute-start | bytes 417800 | tf_op jit(solution)/shard_map/ppermute | solution.py:334
  24.5 33.9 %slice-start = ((s8[8388608]{0:T(1024)(128)(4,1)}), s8[4194304]{0:T(1024)(128)(4,1)S(1)}, s32[]{:S(2)}) async-start(s8[8388608]{0:T(1024)(128)(4,1)} %bitcast.17), calls=%async_computation.3 | async-start | bytes 8388608
  27.6 30.8 %slice-start.1 = ((s8[8388608]{0:T(1024)(128)(4,1)}), s8[4194304]{0:T(1024)(128)(4,1)S(1)}, s32[]{:S(2)}) async-start(s8[8388608]{0:T(1024)(128)(4,1)} %bitcast.17), calls=%async_computation.4 | async-start | bytes 8388608
  29.7 11.4 %copy-start.4 = (f32[128]{0:T(128)S(1)}, f32[128]{0:T(128)}, u32[]{:S(2)}) copy-start(f32[128]{0:T(128)} %param.17) | copy-start | bytes 1540
  29.7 28.7 %copy-start = (bf16[32,2048]{1,0:T(8,128)(2,1)S(1)}, bf16[32,2048]{1,0:T(8,128)(2,1)}, u32[]{:S(2)}) copy-start(bf16[32,2048]{1,0:T(8,128)(2,1)} %stream.1) | copy-start | bytes 393220
  29.7 28.7 %copy-start.1 = (f32[2048]{0:T(1024)S(1)}, f32[2048]{0:T(1024)}, u32[]{:S(2)}) copy-start(f32[2048]{0:T(1024)} %param.20) | copy-start | bytes 24580
  29.8 28.7 %copy-start.2 = (s32[32,2]{0,1:T(2,128)S(1)}, s32[32,2]{0,1:T(2,128)}, u32[]{:S(2)}) copy-start(s32[32,2]{0,1:T(2,128)} %param.21) | copy-start | bytes 772
  29.8 28.7 %copy-start.3 = (f32[32,2]{0,1:T(2,128)S(1)}, f32[32,2]{0,1:T(2,128)}, u32[]{:S(2)}) copy-start(f32[32,2]{0,1:T(2,128)} %param.22) | copy-start | bytes 772
  29.8 89.7 %collective-permute-start.22 = (bf16[6144,256]{1,0:T(8,128)(2,1)S(1)}, bf16[6144,256]{1,0:T(8,128)(2,1)S(1)}, u32[]{:S(2)}, u32[]{:S(2)}) collective-permute-start(bf16[6144,256]{1,0:T(8,128)(2,1)S(1)} %stage_weights.1.refs_4_.refs_6_.refs_2_), channel_id=1, source_target_pairs={{0,1},{1,0},{2,3},{3,2},{4,5},{5,4},{6,7},{7,6},{8,9},{9,8},{10,11... | collective-permute-start | bytes 9437192 | tf_op jit(solution)/shard_map/ppermute | solution.py:621
  29.9 8.4 %collective-permute-start.7 = (bf16[144,512]{1,0:T(8,128)(2,1)S(1)}, bf16[144,512]{1,0:T(8,128)(2,1)S(1)}, u32[]{:S(2)}, u32[]{:S(2)}) collective-permute-start(bf16[144,512]{1,0:T(8,128)(2,1)S(1)} %shard_map.129), channel_id=1, source_target_pairs={{0,64},{16,80},{32,96},{48,112},{64,128},{80,144},{96,160},{112,17... | collective-permute-start | bytes 442376 | tf_op jit(solution)/shard_map/ppermute | solution.py:334
  32.4 6.8 %collective-permute-start.8 = (bf16[144,512]{1,0:T(8,128)(2,1)S(1)}, bf16[144,512]{1,0:T(8,128)(2,1)S(1)}, u32[]{:S(2)}, u32[]{:S(2)}) collective-permute-start(bf16[144,512]{1,0:T(8,128)(2,1)S(1)} %get-tuple-element.66), channel_id=1, source_target_pairs={{0,128},{16,144},{32,160},{48,176},{64,192},{80,208},{96,224},{112... | collective-permute-start | bytes 442376 | tf_op jit(solution)/shard_map/ppermute | solution.py:334
  35.5 5.5 %collective-permute-start.9 = (bf16[144,512]{1,0:T(8,128)(2,1)S(1)}, bf16[144,512]{1,0:T(8,128)(2,1)S(1)}, u32[]{:S(2)}, u32[]{:S(2)}) collective-permute-start(bf16[144,512]{1,0:T(8,128)(2,1)S(1)} %get-tuple-element.67), channel_id=1, source_target_pairs={{0,192},{16,208},{32,224},{48,240},{1,193},{17,209},{33,225},{49,2... | collective-permute-start | bytes 442376 | tf_op jit(solution)/shard_map/ppermute | solution.py:334
  80.9 10.5 %collective-permute-start.10 = (bf16[64,2048]{1,0:T(8,128)(2,1)S(1)}, bf16[64,2048]{1,0:T(8,128)(2,1)S(1)}, u32[]{:S(2)}, u32[]{:S(2)}) collective-permute-start(bf16[64,2048]{1,0:T(8,128)(2,1)S(1)} %get-tuple-element.100.refs_0_), channel_id=1, source_target_pairs={{0,2},{1,3},{2,4},{3,5},{4,6},{5,7},{6,8},{7,9},{8,10},{9,11},{10,... | collective-permute-start | bytes 786440 | tf_op jit(solution)/shard_map/ppermute | solution.py:464
  81.5 9.8 %collective-permute-start.19 = (bf16[64,2048]{1,0:T(8,128)(2,1)S(1)}, bf16[64,2048]{1,0:T(8,128)(2,1)S(1)}, u32[]{:S(2)}, u32[]{:S(2)}) collective-permute-start(bf16[64,2048]{1,0:T(8,128)(2,1)S(1)} %get-tuple-element.99.refs_1_), channel_id=1, source_target_pairs={{0,14},{1,15},{2,0},{3,1},{4,2},{5,3},{6,4},{7,5},{8,6},{9,7},{10,... | collective-permute-start | bytes 786440 | tf_op jit(solution)/shard_map/ppermute | solution.py:467
  84.2 12.8 %collective-permute-start.13 = (bf16[64,2048]{1,0:T(8,128)(2,1)S(1)}, bf16[64,2048]{1,0:T(8,128)(2,1)S(1)}, u32[]{:S(2)}, u32[]{:S(2)}) collective-permute-start(bf16[64,2048]{1,0:T(8,128)(2,1)S(1)} %get-tuple-element.99.refs_1_), channel_id=1, source_target_pairs={{0,2},{1,3},{2,4},{3,5},{4,6},{5,7},{6,8},{7,9},{8,10},{9,11},{10,... | collective-permute-start | bytes 786440 | tf_op jit(solution)/shard_map/ppermute | solution.py:464
  84.2 12.8 %collective-permute-start.16 = (bf16[64,2048]{1,0:T(8,128)(2,1)S(1)}, bf16[64,2048]{1,0:T(8,128)(2,1)S(1)}, u32[]{:S(2)}, u32[]{:S(2)}) collective-permute-start(bf16[64,2048]{1,0:T(8,128)(2,1)S(1)} %get-tuple-element.100.refs_0_), channel_id=1, source_target_pairs={{0,14},{1,15},{2,0},{3,1},{4,2},{5,3},{6,4},{7,5},{8,6},{9,7},{10,... | collective-permute-start | bytes 786440 | tf_op jit(solution)/shard_map/ppermute | solution.py:467
  91.4 11.2 %collective-permute-start.11 = (bf16[64,2048]{1,0:T(8,128)(2,1)S(1)}, bf16[64,2048]{1,0:T(8,128)(2,1)S(1)}, u32[]{:S(2)}, u32[]{:S(2)}) collective-permute-start(bf16[64,2048]{1,0:T(8,128)(2,1)S(1)} %collective-permute-done.10.refs_2_), channel_id=1, source_target_pairs={{0,2},{1,3},{2,4},{3,5},{4,6},{5,7},{6,8},{7,9},{8,10},{9,11},{10,... | collective-permute-start | bytes 786440 | tf_op jit(solution)/shard_map/ppermute | solution.py:464
  91.4 11.2 %collective-permute-start.20 = (bf16[64,2048]{1,0:T(8,128)(2,1)S(1)}, bf16[64,2048]{1,0:T(8,128)(2,1)S(1)}, u32[]{:S(2)}, u32[]{:S(2)}) collective-permute-start(bf16[64,2048]{1,0:T(8,128)(2,1)S(1)} %collective-permute-done.19.refs_5_), channel_id=1, source_target_pairs={{0,14},{1,15},{2,0},{3,1},{4,2},{5,3},{6,4},{7,5},{8,6},{9,7},{10,... | collective-permute-start | bytes 786440 | tf_op jit(solution)/shard_map/ppermute | solution.py:467
  97.0 11.2 %collective-permute-start.14 = (bf16[64,2048]{1,0:T(8,128)(2,1)S(1)}, bf16[64,2048]{1,0:T(8,128)(2,1)S(1)}, u32[]{:S(2)}, u32[]{:S(2)}) collective-permute-start(bf16[64,2048]{1,0:T(8,128)(2,1)S(1)} %collective-permute-done.13.refs_3_), channel_id=1, source_target_pairs={{0,2},{1,3},{2,4},{3,5},{4,6},{5,7},{6,8},{7,9},{8,10},{9,11},{10,... | collective-permute-start | bytes 786440 | tf_op jit(solution)/shard_map/ppermute | solution.py:464
  97.0 11.2 %collective-permute-start.17 = (bf16[64,2048]{1,0:T(8,128)(2,1)S(1)}, bf16[64,2048]{1,0:T(8,128)(2,1)S(1)}, u32[]{:S(2)}, u32[]{:S(2)}) collective-permute-start(bf16[64,2048]{1,0:T(8,128)(2,1)S(1)} %collective-permute-done.16.refs_4_), channel_id=1, source_target_pairs={{0,14},{1,15},{2,0},{3,1},{4,2},{5,3},{6,4},{7,5},{8,6},{9,7},{10,... | collective-permute-start | bytes 786440 | tf_op jit(solution)/shard_map/ppermute | solution.py:467
  102.6 11.2 %collective-permute-start.12 = (bf16[64,2048]{1,0:T(8,128)(2,1)S(1)}, bf16[64,2048]{1,0:T(8,128)(2,1)S(1)}, u32[]{:S(2)}, u32[]{:S(2)}) collective-permute-start(bf16[64,2048]{1,0:T(8,128)(2,1)S(1)} %collective-permute-done.11.refs_0_), channel_id=1, source_target_pairs={{0,2},{1,3},{2,4},{3,5},{4,6},{5,7},{6,8},{7,9},{8,10},{9,11},{10,... | collective-permute-start | bytes 786440 | tf_op jit(solution)/shard_map/ppermute | solution.py:464
  102.6 11.2 %collective-permute-start.21 = (bf16[64,2048]{1,0:T(8,128)(2,1)S(1)}, bf16[64,2048]{1,0:T(8,128)(2,1)S(1)}, u32[]{:S(2)}, u32[]{:S(2)}) collective-permute-start(bf16[64,2048]{1,0:T(8,128)(2,1)S(1)} %collective-permute-done.20.refs_3_), channel_id=1, source_target_pairs={{0,14},{1,15},{2,0},{3,1},{4,2},{5,3},{6,4},{7,5},{8,6},{9,7},{10,... | collective-permute-start | bytes 786440 | tf_op jit(solution)/shard_map/ppermute | solution.py:467
  108.2 11.2 %collective-permute-start.15 = (bf16[64,2048]{1,0:T(8,128)(2,1)S(1)}, bf16[64,2048]{1,0:T(8,128)(2,1)S(1)}, u32[]{:S(2)}, u32[]{:S(2)}) collective-permute-start(bf16[64,2048]{1,0:T(8,128)(2,1)S(1)} %collective-permute-done.14.refs_1_), channel_id=1, source_target_pairs={{0,2},{1,3},{2,4},{3,5},{4,6},{5,7},{6,8},{7,9},{8,10},{9,11},{10,... | collective-permute-start | bytes 786440 | tf_op jit(solution)/shard_map/ppermute | solution.py:464
  108.2 11.2 %collective-permute-start.18 = (bf16[64,2048]{1,0:T(8,128)(2,1)S(1)}, bf16[64,2048]{1,0:T(8,128)(2,1)S(1)}, u32[]{:S(2)}, u32[]{:S(2)}) collective-permute-start(bf16[64,2048]{1,0:T(8,128)(2,1)S(1)} %collective-permute-done.17.refs_2_), channel_id=1, source_target_pairs={{0,14},{1,15},{2,0},{3,1},{4,2},{5,3},{6,4},{7,5},{8,6},{9,7},{10,... | collective-permute-start | bytes 786440 | tf_op jit(solution)/shard_map/ppermute | solution.py:467
  113.8 10.5 %collective-permute-start.26 = (bf16[64,2048]{1,0:T(8,128)(2,1)S(1)}, bf16[64,2048]{1,0:T(8,128)(2,1)S(1)}, u32[]{:S(2)}, u32[]{:S(2)}) collective-permute-start(bf16[64,2048]{1,0:T(8,128)(2,1)S(1)} %collective-permute-done.12.refs_0_), channel_id=1, source_target_pairs={{0,2},{1,3},{2,4},{3,5},{4,6},{5,7},{6,8},{7,9},{8,10},{9,11},{10,... | collective-permute-start | bytes 786440 | tf_op jit(solution)/shard_map/ppermute | solution.py:464
  113.9 10.5 %collective-permute-start.27 = (bf16[64,2048]{1,0:T(8,128)(2,1)S(1)}, bf16[64,2048]{1,0:T(8,128)(2,1)S(1)}, u32[]{:S(2)}, u32[]{:S(2)}) collective-permute-start(bf16[64,2048]{1,0:T(8,128)(2,1)S(1)} %collective-permute-done.21.refs_3_), channel_id=1, source_target_pairs={{0,14},{1,15},{2,0},{3,1},{4,2},{5,3},{6,4},{7,5},{8,6},{9,7},{10,... | collective-permute-start | bytes 786440 | tf_op jit(solution)/shard_map/ppermute | solution.py:467
  121.9 14.8 %collective-permute-start.36 = (bf16[64,2048]{1,0:T(8,128)(2,1)S(1)}, bf16[64,2048]{1,0:T(8,128)(2,1)S(1)}, u32[]{:S(2)}, u32[]{:S(2)}) collective-permute-start(bf16[64,2048]{1,0:T(8,128)(2,1)S(1)} %get-tuple-element.94), channel_id=1, source_target_pairs={{0,2},{1,3},{2,4},{3,5},{4,6},{5,7},{6,8},{7,9},{8,10},{9,11},{10,... | collective-permute-start | bytes 786440 | tf_op jit(solution)/shard_map/ppermute | solution.py:464
  125.5 11.4 %collective-permute-start.32 = (bf16[64,2048]{1,0:T(8,128)(2,1)S(1)}, bf16[64,2048]{1,0:T(8,128)(2,1)S(1)}, u32[]{:S(2)}, u32[]{:S(2)}) collective-permute-start(bf16[64,2048]{1,0:T(8,128)(2,1)S(1)} %get-tuple-element.90), channel_id=1, source_target_pairs={{0,14},{1,15},{2,0},{3,1},{4,2},{5,3},{6,4},{7,5},{8,6},{9,7},{10,... | collective-permute-start | bytes 786440 | tf_op jit(solution)/shard_map/ppermute | solution.py:467
  127.5 12.7 %collective-permute-start.28 = (bf16[64,2048]{1,0:T(8,128)(2,1)S(1)}, bf16[64,2048]{1,0:T(8,128)(2,1)S(1)}, u32[]{:S(2)}, u32[]{:S(2)}) collective-permute-start(bf16[64,2048]{1,0:T(8,128)(2,1)S(1)} %get-tuple-element.85), channel_id=1, source_target_pairs={{0,2},{1,3},{2,4},{3,5},{4,6},{5,7},{6,8},{7,9},{8,10},{9,11},{10,... | collective-permute-start | bytes 786440 | tf_op jit(solution)/shard_map/ppermute | solution.py:464
  127.6 12.8 %collective-permute-start.23 = (bf16[64,2048]{1,0:T(8,128)(2,1)S(1)}, bf16[64,2048]{1,0:T(8,128)(2,1)S(1)}, u32[]{:S(2)}, u32[]{:S(2)}) collective-permute-start(bf16[64,2048]{1,0:T(8,128)(2,1)S(1)} %get-tuple-element.82), channel_id=1, source_target_pairs={{0,14},{1,15},{2,0},{3,1},{4,2},{5,3},{6,4},{7,5},{8,6},{9,7},{10,... | collective-permute-start | bytes 786440 | tf_op jit(solution)/shard_map/ppermute | solution.py:467
  136.8 10.5 %collective-permute-start.37 = (bf16[64,2048]{1,0:T(8,128)(2,1)S(1)}, bf16[64,2048]{1,0:T(8,128)(2,1)S(1)}, u32[]{:S(2)}, u32[]{:S(2)}) collective-permute-start(bf16[64,2048]{1,0:T(8,128)(2,1)S(1)} %add_convert_fusion.2), channel_id=1, source_target_pairs={{0,2},{1,3},{2,4},{3,5},{4,6},{5,7},{6,8},{7,9},{8,10},{9,11},{10,... | collective-permute-start | bytes 786440 | tf_op jit(solution)/shard_map/ppermute | solution.py:464
  136.9 10.5 %collective-permute-start.33 = (bf16[64,2048]{1,0:T(8,128)(2,1)S(1)}, bf16[64,2048]{1,0:T(8,128)(2,1)S(1)}, u32[]{:S(2)}, u32[]{:S(2)}) collective-permute-start(bf16[64,2048]{1,0:T(8,128)(2,1)S(1)} %add_convert_fusion.5), channel_id=1, source_target_pairs={{0,14},{1,15},{2,0},{3,1},{4,2},{5,3},{6,4},{7,5},{8,6},{9,7},{10,... | collective-permute-start | bytes 786440 | tf_op jit(solution)/shard_map/ppermute | solution.py:467
  140.3 12.6 %collective-permute-start.29 = (bf16[64,2048]{1,0:T(8,128)(2,1)S(1)}, bf16[64,2048]{1,0:T(8,128)(2,1)S(1)}, u32[]{:S(2)}, u32[]{:S(2)}) collective-permute-start(bf16[64,2048]{1,0:T(8,128)(2,1)S(1)} %add_convert_fusion.9), channel_id=1, source_target_pairs={{0,2},{1,3},{2,4},{3,5},{4,6},{5,7},{6,8},{7,9},{8,10},{9,11},{10,... | collective-permute-start | bytes 786440 | tf_op jit(solution)/shard_map/ppermute | solution.py:464
  140.5 12.5 %collective-permute-start.24 = (bf16[64,2048]{1,0:T(8,128)(2,1)S(1)}, bf16[64,2048]{1,0:T(8,128)(2,1)S(1)}, u32[]{:S(2)}, u32[]{:S(2)}) collective-permute-start(bf16[64,2048]{1,0:T(8,128)(2,1)S(1)} %add_convert_fusion.11), channel_id=1, source_target_pairs={{0,14},{1,15},{2,0},{3,1},{4,2},{5,3},{6,4},{7,5},{8,6},{9,7},{10,... | collective-permute-start | bytes 786440 | tf_op jit(solution)/shard_map/ppermute | solution.py:467
  147.3 14.9 %collective-permute-start.38 = (bf16[64,2048]{1,0:T(8,128)(2,1)S(1)}, bf16[64,2048]{1,0:T(8,128)(2,1)S(1)}, u32[]{:S(2)}, u32[]{:S(2)}) collective-permute-start(bf16[64,2048]{1,0:T(8,128)(2,1)S(1)} %add_convert_fusion.1), channel_id=1, source_target_pairs={{0,2},{1,3},{2,4},{3,5},{4,6},{5,7},{6,8},{7,9},{8,10},{9,11},{10,... | collective-permute-start | bytes 786440 | tf_op jit(solution)/shard_map/ppermute | solution.py:464
  147.5 10.7 %collective-permute-start.34 = (bf16[64,2048]{1,0:T(8,128)(2,1)S(1)}, bf16[64,2048]{1,0:T(8,128)(2,1)S(1)}, u32[]{:S(2)}, u32[]{:S(2)}) collective-permute-start(bf16[64,2048]{1,0:T(8,128)(2,1)S(1)} %add_convert_fusion.4), channel_id=1, source_target_pairs={{0,14},{1,15},{2,0},{3,1},{4,2},{5,3},{6,4},{7,5},{8,6},{9,7},{10,... | collective-permute-start | bytes 786440 | tf_op jit(solution)/shard_map/ppermute | solution.py:467
  152.9 9.1 %collective-permute-start.30 = (bf16[64,2048]{1,0:T(8,128)(2,1)S(1)}, bf16[64,2048]{1,0:T(8,128)(2,1)S(1)}, u32[]{:S(2)}, u32[]{:S(2)}) collective-permute-start(bf16[64,2048]{1,0:T(8,128)(2,1)S(1)} %add_convert_fusion.8), channel_id=1, source_target_pairs={{0,2},{1,3},{2,4},{3,5},{4,6},{5,7},{6,8},{7,9},{8,10},{9,11},{10,... | collective-permute-start | bytes 786440 | tf_op jit(solution)/shard_map/ppermute | solution.py:464
  153.1 12.9 %collective-permute-start.25 = (bf16[64,2048]{1,0:T(8,128)(2,1)S(1)}, bf16[64,2048]{1,0:T(8,128)(2,1)S(1)}, u32[]{:S(2)}, u32[]{:S(2)}) collective-permute-start(bf16[64,2048]{1,0:T(8,128)(2,1)S(1)} %add_convert_fusion.10), channel_id=1, source_target_pairs={{0,14},{1,15},{2,0},{3,1},{4,2},{5,3},{6,4},{7,5},{8,6},{9,7},{10,... | collective-permute-start | bytes 786440 | tf_op jit(solution)/shard_map/ppermute | solution.py:467
  158.2 7.7 %collective-permute-start.35 = (bf16[64,2048]{1,0:T(8,128)(2,1)S(1)}, bf16[64,2048]{1,0:T(8,128)(2,1)S(1)}, u32[]{:S(2)}, u32[]{:S(2)}) collective-permute-start(bf16[64,2048]{1,0:T(8,128)(2,1)S(1)} %add_convert_fusion.3), channel_id=1, source_target_pairs={{0,14},{1,15},{2,0},{3,1},{4,2},{5,3},{6,4},{7,5},{8,6},{9,7},{10,... | collective-permute-start | bytes 786440 | tf_op jit(solution)/shard_map/ppermute | solution.py:467
  162.1 7.7 %collective-permute-start.31 = (bf16[64,2048]{1,0:T(8,128)(2,1)S(1)}, bf16[64,2048]{1,0:T(8,128)(2,1)S(1)}, u32[]{:S(2)}, u32[]{:S(2)}) collective-permute-start(bf16[64,2048]{1,0:T(8,128)(2,1)S(1)} %add_convert_fusion.7), channel_id=1, source_target_pairs={{0,2},{1,3},{2,4},{3,5},{4,6},{5,7},{6,8},{7,9},{8,10},{9,11},{10,... | collective-permute-start | bytes 786440 | tf_op jit(solution)/shard_map/ppermute | solution.py:464

commit v3 on v2

--- a/solution.py
+++ b/solution.py
@@ -327,7 +327,7 @@
     )(*operands)
 
 
-def attention(queries, key_vectors, value_vectors, forget_totals, head_gain, weights):
+def attention(queries, key_vectors, value_vectors, forget_totals, head_gain):
     tok_count = queries.shape[0]
 
     def shift(array, dy, dx, needed):
@@ -361,10 +361,9 @@
     back2 = shift(part2, 2, 0, lambda y, x: y > 1)
     keys = [keys_own, low, high, far_a, far_b]
     (part1,) = attend(next_kernel, [pack1, *keys], [result], state + loaded(4), 4)
-    part1, own_pack, keys, weights = lax.optimization_barrier((part1, own_pack, keys, weights))
+    part1, own_pack, keys = lax.optimization_barrier((part1, own_pack, keys))
     back1 = shift(part1, 1, 0, lambda y, x: y > 0)
     own_state = attend(own_kernel, [own_pack, *keys], state, loaded(4), 4)
-    staged = stage_weights(*weights)
     (head_out,) = attend(
         merge_kernel,
         [back1, back2, back3, *own_state, head_gain.reshape(1, HD)],
@@ -372,7 +371,7 @@
         [],
         0,
     )
-    return head_out, staged
+    return head_out
 
 
 def staging_kernel(gate, up, down, out, sems):
@@ -477,17 +476,17 @@
     up_top.append(up(up_top[-1]))
     down_end.append(down(down_end[-1]))
     chains = (up_top, up_end, down_top, down_end)
-    made = []
-    for i in range(1, 4):
-        rows = [chain[i] for chain in chains]
-        made.append(expert_rows(([top, end] if i == 1 else []) + rows, weights))
-    mine, done = made[0][:2], [made[0][2:], made[1], made[2]]
+    rows = [top, end] + [chain[i] for i in (1, 2) for chain in chains]
+    near = expert_rows(rows, weights)
+    low_top, high_end = expert_rows([up_top[3], down_end[3]], weights)
+    low_end3, high_top3 = expert_rows([up_end[3], down_top[3]], weights)
     far_top, far_end = expert_rows([up_top[4], down_end[4]], weights)
-
-    low_top, high_end = down(done[2][0]), up(done[2][3])
+    mine, done = near[:2], [near[2:6], near[6:]]
+
+    low_top, high_end = down(low_top), up(high_end)
     high_top, low_end = up(far_top), down(far_end)
-    high_top = up(added(high_top, done[2][2]))
-    low_end = down(added(low_end, done[2][1]))
+    high_top = up(added(high_top, high_top3))
+    low_end = down(added(low_end, low_end3))
     for i in (1, 0):
         low_top = down(added(low_top, done[i][0]))
         high_end = up(added(high_end, done[i][3]))
@@ -610,15 +609,7 @@
     down_weight,
 ):
     sp_count = lax.axis_size("sp")
-    head_out, own_half = attention(
-        queries,
-        key_vectors,
-        value_vectors,
-        forget_totals,
-        head_gain,
-        (gate_weight[0], up_weight[0], down_weight[0]),
-    )
-    weights = own_half, lax.ppermute(own_half, "tp", core_swap)
+    head_out = attention(queries, key_vectors, value_vectors, forget_totals, head_gain)
     row_count, width = stream.shape
     capacity = max(2, 2 * TOP * row_count // sp_count)
     heads = head_out.reshape(-1, row_count, HD)
@@ -628,6 +619,10 @@
     )
     outgoing = outgoing.reshape(sp_count, capacity, width)
     arrived = lax.all_to_all(outgoing, "sp", split_axis=0, concat_axis=0, tiled=True)
+    own_weights = gate_weight[0], up_weight[0], down_weight[0]
+    arrived, own_weights = lax.optimization_barrier((arrived, own_weights))
+    own_half = stage_weights(*own_weights)
+    weights = own_half, lax.ppermute(own_half, "tp", core_swap)
     summed = expert_sum(arrived.reshape(-1, width), weights)
     expert_out = summed.reshape(sp_count, capacity, width)
     returned = lax.all_to_all(expert_out, "sp", split_axis=0, concat_axis=0, tiled=True)

time: 185 us -> 185 us (level)
    ppermute x14, waiting for transfers between devices: 27.4 us -> 29.5 us  [up(): return lax.ppermute(array, 'tp', z_perm(1))]
  transfers between devices with their start and end apart: 39 -> 39, of which waited for: 15 -> 15; matrix products, arithmetic and copies ran while one was open for 0% -> 0% of each run, Pallas kernels for 11% -> 9%
where the time goes in v3:
time: 185 us; the launch traced here: 184 us
  starting transfers between devices  69.5 us (38%)
  blocking collectives  49.9 us (27%)
  waiting for transfers between devices  36.3 us (20%)
  Pallas kernels  27 us (15%)
    ppermute x14, starting transfers between devices, down(): return lax.ppermute(array, 'tp', z_perm(-1))  44.4 us
    ppermute x14, waiting for transfers between devices, up(): return lax.ppermute(array, 'tp', z_perm(1))  29.5 us
    ppermute x10, starting transfers between devices, shift(): return lax.ppermute(array, 'sp', sp_perm(dy, dx, needed))  23.6 us
    all_to_all x1, blocking collectives, on_device(): lax.all_to_all(outgoing, 'sp', split_axis=0, concat_axis=0, tiled=True)  19.9 us
    all_to_all x1, blocking collectives, on_device(): heads = lax.all_to_all(heads, 'tp', split_axis=0, concat_axis=0, tiled=True)  17 us
    all_to_all x1, blocking collectives, on_device(): lax.all_to_all(expert_out, 'sp', split_axis=0, concat_axis=0, tiled=True)  13.1 us
    pallas_call x5, Pallas kernels, attend(): pl.pallas_call(kernel, out_shape=tuple((jax.ShapeDtypeStruct(*out) for ou...  10.9 us
    pallas_call x4, Pallas kernels, expert_rows(): pl.pallas_call(partial(expert_kernel, count=count), out_shape=tuple((jax....  9.34 us
  transfers between devices with their start and end apart: 39, of which 15 were waited for; matrix products, arithmetic and copies ran while one was open for 0% of the time, Pallas kernels for 9%

profile of v3, /device:TPU:2, one launch (start us, length us, event | category | flops | bytes accessed | tf_op | source)
XLA Modules:
  0.0 184.2 jit_solution(3830774717594405658)
XLA Ops:
  0.0 1.2 make_pieces.1
  1.2 3.4 %collective-permute-start.2 = (bf16[544,256]{1,0:T(8,128)(2,1)S(1)}, bf16[544,256]{1,0:T(8,128)(2,1)S(1)}, u32[]{:S(2)}, u32[]{:S(2)}) collective-permute-start(bf16[544,256]{1,0:T(8,128)(2,1)S(1)} %get-tuple-element.70.refs_2_.refs_1_), channel_id=1, source_target_pairs={{0,16},{16,32},{32,48},{48,0},{64,80},{80,96},{96,112},{112,64},{1... | collective-permute-start | bytes 835592 | tf_op jit(solution)/shard_map/ppermute | solution.py:334
  4.6 2.7 %collective-permute-start.4 = (bf16[544,256]{1,0:T(8,128)(2,1)S(1)}, bf16[544,256]{1,0:T(8,128)(2,1)S(1)}, u32[]{:S(2)}, u32[]{:S(2)}) collective-permute-start(bf16[544,256]{1,0:T(8,128)(2,1)S(1)} %get-tuple-element.70.refs_2_.refs_1_), channel_id=1, source_target_pairs={{0,48},{16,0},{32,16},{48,32},{64,112},{80,64},{96,80},{112,96},{1... | collective-permute-start | bytes 835592 | tf_op jit(solution)/shard_map/ppermute | solution.py:334
  7.3 1.3 collective-permute-start
  8.6 1.3 collective-permute-start.1
  9.9 1.3 collective-permute-start.6
  11.5 3.4 %collective-permute-start.3 = (bf16[272,256]{1,0:T(8,128)(2,1)S(1)}, bf16[272,256]{1,0:T(8,128)(2,1)S(1)}, u32[]{:S(2)}, u32[]{:S(2)}) collective-permute-start(bf16[272,256]{1,0:T(8,128)(2,1)S(1)} %slice.24), channel_id=1, source_target_pairs={{0,16},{16,32},{32,48},{48,0},{64,80},{80,96},{96,112},{112,64},{1... | collective-permute-start | bytes 417800 | tf_op jit(solution)/shard_map/ppermute | solution.py:334
  15.0 3.4 %collective-permute-start.5 = (bf16[272,256]{1,0:T(8,128)(2,1)S(1)}, bf16[272,256]{1,0:T(8,128)(2,1)S(1)}, u32[]{:S(2)}, u32[]{:S(2)}) collective-permute-start(bf16[272,256]{1,0:T(8,128)(2,1)S(1)} %slice.25), channel_id=1, source_target_pairs={{0,48},{16,0},{32,16},{48,32},{64,112},{80,64},{96,80},{112,96},{1... | collective-permute-start | bytes 417800 | tf_op jit(solution)/shard_map/ppermute | solution.py:334
  18.4 4.4 %shard_map.127 = (f32[16,512]{1,0:T(8,128)S(1)}, f32[16,512]{1,0:T(8,128)S(1)}, f32[256,512]{1,0:T(8,128)S(1)}) custom-call(bf16[144,512]{1,0:T(8,128)(2,1)S(1)} %collective-permute-done.refs_0_, bf16[144,512]{1,0:T(8,128)(2,1)S(1)} %collective-permute-done.1.refs_1_, bf16[544,256]{1,0:T(8,128)(2,1)S(1)} %get-tuple-element.70.refs_2_.refs_1_, ...), custom_call_target="tpu_custom_call" | custom-call | flops 1610612736 | bytes 1048576 | tf_op jit(solution)/shard_map/pallas_call | solution.py:315
  22.8 1.7 shard_map.128
  24.5 3.1 %shard_map.129 = bf16[144,512]{1,0:T(8,128)(2,1)S(1)} custom-call(bf16[144,512]{1,0:T(8,128)(2,1)S(1)} %collective-permute-done.6.refs_0_, bf16[544,256]{1,0:T(8,128)(2,1)S(1)} %get-tuple-element.70.refs_2_.refs_1_, bf16[544,256]{1,0:T(8,128)(2,1)S(1)} %collective-permute-done.2.refs_3_.refs_2_, bf16[544,256]{1,0:T(8,128)(2,1)S(1)} %collective-permute-done.4.refs_4_.refs_3_, ...), custom_call_target="tpu_custom_call" | custom-call | flops 1073741824 | bytes 1048576 | tf_op jit(solution)/shard_map/pallas_call | solution.py:315
  27.7 2.5 %collective-permute-start.7 = (bf16[144,512]{1,0:T(8,128)(2,1)S(1)}, bf16[144,512]{1,0:T(8,128)(2,1)S(1)}, u32[]{:S(2)}, u32[]{:S(2)}) collective-permute-start(bf16[144,512]{1,0:T(8,128)(2,1)S(1)} %shard_map.129), channel_id=1, source_target_pairs={{0,64},{16,80},{32,96},{48,112},{64,128},{80,144},{96,160},{112,17... | collective-permute-start | bytes 442376 | tf_op jit(solution)/shard_map/ppermute | solution.py:334
  30.2 3.2 %collective-permute-start.8 = (bf16[144,512]{1,0:T(8,128)(2,1)S(1)}, bf16[144,512]{1,0:T(8,128)(2,1)S(1)}, u32[]{:S(2)}, u32[]{:S(2)}) collective-permute-start(bf16[144,512]{1,0:T(8,128)(2,1)S(1)} %get-tuple-element.67), channel_id=1, source_target_pairs={{0,128},{16,144},{32,160},{48,176},{64,192},{80,208},{96,224},{112... | collective-permute-start | bytes 442376 | tf_op jit(solution)/shard_map/ppermute | solution.py:334
  33.3 1.3 collective-permute-start.9
  34.6 1.5 shard_map.130
  36.1 1.2 collective-permute-done.9.refs_2_
  37.7 17.0 %all_to_all.15.heads = bf16[16,32,128]{2,1,0:T(8,128)(2,1)S(1)} all-to-all(bf16[16,32,128]{2,1,0:T(8,128)(2,1)S(1)} %bitcast.21), channel_id=1, replica_groups=mesh['sp'=16,'tp'=16] {'tp'}, dimensions={0} | all-to-all | bytes 262144 | tf_op jit(solution)/shard_map/all_to_all | solution.py:616
  54.7 2.5 %project.1 = (f32[32,2048]{1,0:T(8,128)S(1)}, bf16[128,2048]{1,0:T(8,128)(2,1)S(1)}, f32[128,32]{1,0:T(8,128)S(1)}) custom-call(bf16[16,32,128]{2,1,0:T(8,128)(2,1)S(1)} %all_to_all.15.heads, bf16[2048,2048]{1,0:T(8,128)(2,1)S(1)} %bitcast.18, bf16[32,2048]{1,0:T(8,128)(2,1)S(1)} %copy-done, f32[1,2048]{1,0:T(1,128)S(1)} %bitcast.22, s32[2,32]{1,0:T(2,128)S(1)} %bitcast.23, ...), custom_call_target="tpu_custom_call" | custom-call | tf_op jit(solution)/shard_map/project/pallas_call | solution.py:554
  57.2 19.9 %all_to_all.16 = bf16[16,8,2048]{2,1,0:T(8,128)(2,1)S(1)} all-to-all(bf16[16,8,2048]{2,1,0:T(8,128)(2,1)S(1)} %bitcast.20), channel_id=1, replica_groups=mesh['sp'=16,'tp'=16] {'sp'}, dimensions={0} | all-to-all | bytes 1048576 | tf_op jit(solution)/shard_map/all_to_all | solution.py:621
  77.1 1.9 %stage_weights.1.refs_2_.refs_10_ = bf16[6144,256]{1,0:T(8,128)(2,1)S(1)} custom-call(bf16[2048,256]{1,0:T(8,128)(2,1)} %bitcast.26, bf16[2048,256]{1,0:T(8,128)(2,1)} %bitcast.27, bf16[256,2048]{1,0:T(8,128)(2,1)} %bitcast.28), custom_call_target="tpu_custom_call" | custom-call | tf_op jit(solution)/shard_map/stage_weights/pallas_call | solution.py:396
  79.8 2.7 %collective-permute-start.13 = (bf16[64,2048]{1,0:T(8,128)(2,1)S(1)}, bf16[64,2048]{1,0:T(8,128)(2,1)S(1)}, u32[]{:S(2)}, u32[]{:S(2)}) collective-permute-start(bf16[64,2048]{1,0:T(8,128)(2,1)S(1)} %get-tuple-element.101.refs_1_), channel_id=1, source_target_pairs={{0,14},{1,15},{2,0},{3,1},{4,2},{5,3},{6,4},{7,5},{8,6},{9,7},{10,... | collective-permute-start | bytes 786440 | tf_op jit(solution)/shard_map/ppermute | solution.py:466
  82.5 6.7 %collective-permute-done.10.refs_2_ = bf16[64,2048]{1,0:T(8,128)(2,1)S(1)} collective-permute-done((bf16[64,2048]{1,0:T(8,128)(2,1)S(1)}, bf16[64,2048]{1,0:T(8,128)(2,1)S(1)}, u32[]{:S(2)}, u32[]{:S(2)}) %collective-permute-start.10) | collective-permute-done | bytes 262176 | tf_op jit(solution)/shard_map/ppermute | solution.py:463
  89.2 3.2 %collective-permute-start.14 = (bf16[64,2048]{1,0:T(8,128)(2,1)S(1)}, bf16[64,2048]{1,0:T(8,128)(2,1)S(1)}, u32[]{:S(2)}, u32[]{:S(2)}) collective-permute-start(bf16[64,2048]{1,0:T(8,128)(2,1)S(1)} %collective-permute-done.13.refs_5_), channel_id=1, source_target_pairs={{0,14},{1,15},{2,0},{3,1},{4,2},{5,3},{6,4},{7,5},{8,6},{9,7},{10,... | collective-permute-start | bytes 786440 | tf_op jit(solution)/shard_map/ppermute | solution.py:466
  92.4 3.2 %collective-permute-start.19 = (bf16[64,2048]{1,0:T(8,128)(2,1)S(1)}, bf16[64,2048]{1,0:T(8,128)(2,1)S(1)}, u32[]{:S(2)}, u32[]{:S(2)}) collective-permute-start(bf16[64,2048]{1,0:T(8,128)(2,1)S(1)} %get-tuple-element.102.refs_0_), channel_id=1, source_target_pairs={{0,14},{1,15},{2,0},{3,1},{4,2},{5,3},{6,4},{7,5},{8,6},{9,7},{10,... | collective-permute-start | bytes 786440 | tf_op jit(solution)/shard_map/ppermute | solution.py:466
  95.6 3.9 %collective-permute-done.11.refs_6_ = bf16[64,2048]{1,0:T(8,128)(2,1)S(1)} collective-permute-done((bf16[64,2048]{1,0:T(8,128)(2,1)S(1)}, bf16[64,2048]{1,0:T(8,128)(2,1)S(1)}, u32[]{:S(2)}, u32[]{:S(2)}) %collective-permute-start.11) | collective-permute-done | bytes 262176 | tf_op jit(solution)/shard_map/ppermute | solution.py:463
  99.6 3.2 %collective-permute-start.15 = (bf16[64,2048]{1,0:T(8,128)(2,1)S(1)}, bf16[64,2048]{1,0:T(8,128)(2,1)S(1)}, u32[]{:S(2)}, u32[]{:S(2)}) collective-permute-start(bf16[64,2048]{1,0:T(8,128)(2,1)S(1)} %collective-permute-done.14.refs_9_), channel_id=1, source_target_pairs={{0,14},{1,15},{2,0},{3,1},{4,2},{5,3},{6,4},{7,5},{8,6},{9,7},{10,... | collective-permute-start | bytes 786440 | tf_op jit(solution)/shard_map/ppermute | solution.py:466
  102.8 2.4 %collective-permute-done.18.refs_3_ = bf16[64,2048]{1,0:T(8,128)(2,1)S(1)} collective-permute-done((bf16[64,2048]{1,0:T(8,128)(2,1)S(1)}, bf16[64,2048]{1,0:T(8,128)(2,1)S(1)}, u32[]{:S(2)}, u32[]{:S(2)}) %collective-permute-start.18) | collective-permute-done | bytes 262176 | tf_op jit(solution)/shard_map/ppermute | solution.py:463
  105.2 3.2 %collective-permute-start.21 = (bf16[64,2048]{1,0:T(8,128)(2,1)S(1)}, bf16[64,2048]{1,0:T(8,128)(2,1)S(1)}, u32[]{:S(2)}, u32[]{:S(2)}) collective-permute-start(bf16[64,2048]{1,0:T(8,128)(2,1)S(1)} %collective-permute-done.19.refs_4_), channel_id=1, source_target_pairs={{0,14},{1,15},{2,0},{3,1},{4,2},{5,3},{6,4},{7,5},{8,6},{9,7},{10,... | collective-permute-start | bytes 786440 | tf_op jit(solution)/shard_map/ppermute | solution.py:466
  108.4 2.4 %collective-permute-done.12.refs_0_ = bf16[64,2048]{1,0:T(8,128)(2,1)S(1)} collective-permute-done((bf16[64,2048]{1,0:T(8,128)(2,1)S(1)}, bf16[64,2048]{1,0:T(8,128)(2,1)S(1)}, u32[]{:S(2)}, u32[]{:S(2)}) %collective-permute-start.12) | collective-permute-done | bytes 262176 | tf_op jit(solution)/shard_map/ppermute | solution.py:463
  110.8 3.2 %collective-permute-start.25 = (bf16[64,2048]{1,0:T(8,128)(2,1)S(1)}, bf16[64,2048]{1,0:T(8,128)(2,1)S(1)}, u32[]{:S(2)}, u32[]{:S(2)}) collective-permute-start(bf16[64,2048]{1,0:T(8,128)(2,1)S(1)} %collective-permute-done.15.refs_1_), channel_id=1, source_target_pairs={{0,14},{1,15},{2,0},{3,1},{4,2},{5,3},{6,4},{7,5},{8,6},{9,7},{10,... | collective-permute-start | bytes 786440 | tf_op jit(solution)/shard_map/ppermute | solution.py:466
  114.0 2.4 %collective-permute-done.20.refs_7_ = bf16[64,2048]{1,0:T(8,128)(2,1)S(1)} collective-permute-done((bf16[64,2048]{1,0:T(8,128)(2,1)S(1)}, bf16[64,2048]{1,0:T(8,128)(2,1)S(1)}, u32[]{:S(2)}, u32[]{:S(2)}) %collective-permute-start.20) | collective-permute-done | bytes 262176 | tf_op jit(solution)/shard_map/ppermute | solution.py:463
  116.4 3.2 %collective-permute-start.28 = (bf16[64,2048]{1,0:T(8,128)(2,1)S(1)}, bf16[64,2048]{1,0:T(8,128)(2,1)S(1)}, u32[]{:S(2)}, u32[]{:S(2)}) collective-permute-start(bf16[64,2048]{1,0:T(8,128)(2,1)S(1)} %collective-permute-done.21.refs_8_), channel_id=1, source_target_pairs={{0,14},{1,15},{2,0},{3,1},{4,2},{5,3},{6,4},{7,5},{8,6},{9,7},{10,... | collective-permute-start | bytes 786440 | tf_op jit(solution)/shard_map/ppermute | solution.py:466
  120.9 1.1 collective-permute-done.24.refs_0_
  123.2 3.3 %collective-permute-start.32 = (bf16[64,2048]{1,0:T(8,128)(2,1)S(1)}, bf16[64,2048]{1,0:T(8,128)(2,1)S(1)}, u32[]{:S(2)}, u32[]{:S(2)}) collective-permute-start(bf16[64,2048]{1,0:T(8,128)(2,1)S(1)} %get-tuple-element.92), channel_id=1, source_target_pairs={{0,14},{1,15},{2,0},{3,1},{4,2},{5,3},{6,4},{7,5},{8,6},{9,7},{10,... | collective-permute-start | bytes 786440 | tf_op jit(solution)/shard_map/ppermute | solution.py:466
  126.5 1.2 collective-permute-done.27.refs_0_
  127.6 2.1 %collective-permute-start.17 = (bf16[64,2048]{1,0:T(8,128)(2,1)S(1)}, bf16[64,2048]{1,0:T(8,128)(2,1)S(1)}, u32[]{:S(2)}, u32[]{:S(2)}) collective-permute-start(bf16[64,2048]{1,0:T(8,128)(2,1)S(1)} %get-tuple-element.84), channel_id=1, source_target_pairs={{0,14},{1,15},{2,0},{3,1},{4,2},{5,3},{6,4},{7,5},{8,6},{9,7},{10,... | collective-permute-start | bytes 786440 | tf_op jit(solution)/shard_map/ppermute | solution.py:466
  130.9 6.0 %shard_map.133 = (bf16[64,2048]{1,0:T(8,128)(2,1)S(1)}, bf16[64,2048]{1,0:T(8,128)(2,1)S(1)}, bf16[64,2048]{1,0:T(8,128)(2,1)S(1)}, bf16[64,2048]{1,0:T(8,128)(2...) custom-call(bf16[64,2048]{1,0:T(8,128)(2,1)S(1)} %get-tuple-element., ...), custom_call_target="tpu_custom_call" | custom-call | flops 4026531840 | bytes 6291456 | tf_op jit(solution)/shard_map/pallas_call | solution.py:446
  137.3 3.3 %collective-permute-start.33 = (bf16[64,2048]{1,0:T(8,128)(2,1)S(1)}, bf16[64,2048]{1,0:T(8,128)(2,1)S(1)}, u32[]{:S(2)}, u32[]{:S(2)}) collective-permute-start(bf16[64,2048]{1,0:T(8,128)(2,1)S(1)} %add_convert_fusion.5), channel_id=1, source_target_pairs={{0,14},{1,15},{2,0},{3,1},{4,2},{5,3},{6,4},{7,5},{8,6},{9,7},{10,... | collective-permute-start | bytes 786440 | tf_op jit(solution)/shard_map/ppermute | solution.py:466
  140.8 3.3 %collective-permute-start.22 = (bf16[64,2048]{1,0:T(8,128)(2,1)S(1)}, bf16[64,2048]{1,0:T(8,128)(2,1)S(1)}, u32[]{:S(2)}, u32[]{:S(2)}) collective-permute-start(bf16[64,2048]{1,0:T(8,128)(2,1)S(1)} %add_convert_fusion.11), channel_id=1, source_target_pairs={{0,14},{1,15},{2,0},{3,1},{4,2},{5,3},{6,4},{7,5},{8,6},{9,7},{10,... | collective-permute-start | bytes 786440 | tf_op jit(solution)/shard_map/ppermute | solution.py:466
  144.1 3.5 %collective-permute-done.37 = bf16[64,2048]{1,0:T(8,128)(2,1)S(1)} collective-permute-done((bf16[64,2048]{1,0:T(8,128)(2,1)S(1)}, bf16[64,2048]{1,0:T(8,128)(2,1)S(1)}, u32[]{:S(2)}, u32[]{:S(2)}) %collective-permute-start.37) | collective-permute-done | bytes 262176 | tf_op jit(solution)/shard_map/ppermute | solution.py:463
  147.8 3.3 %collective-permute-start.34 = (bf16[64,2048]{1,0:T(8,128)(2,1)S(1)}, bf16[64,2048]{1,0:T(8,128)(2,1)S(1)}, u32[]{:S(2)}, u32[]{:S(2)}) collective-permute-start(bf16[64,2048]{1,0:T(8,128)(2,1)S(1)} %add_convert_fusion.4), channel_id=1, source_target_pairs={{0,14},{1,15},{2,0},{3,1},{4,2},{5,3},{6,4},{7,5},{8,6},{9,7},{10,... | collective-permute-start | bytes 786440 | tf_op jit(solution)/shard_map/ppermute | solution.py:466
  151.1 2.1 %collective-permute-done.29 = bf16[64,2048]{1,0:T(8,128)(2,1)S(1)} collective-permute-done((bf16[64,2048]{1,0:T(8,128)(2,1)S(1)}, bf16[64,2048]{1,0:T(8,128)(2,1)S(1)}, u32[]{:S(2)}, u32[]{:S(2)}) %collective-permute-start.29) | collective-permute-done | bytes 262176 | tf_op jit(solution)/shard_map/ppermute | solution.py:463
  153.5 3.3 %collective-permute-start.23 = (bf16[64,2048]{1,0:T(8,128)(2,1)S(1)}, bf16[64,2048]{1,0:T(8,128)(2,1)S(1)}, u32[]{:S(2)}, u32[]{:S(2)}) collective-permute-start(bf16[64,2048]{1,0:T(8,128)(2,1)S(1)} %add_convert_fusion.10), channel_id=1, source_target_pairs={{0,14},{1,15},{2,0},{3,1},{4,2},{5,3},{6,4},{7,5},{8,6},{9,7},{10,... | collective-permute-start | bytes 786440 | tf_op jit(solution)/shard_map/ppermute | solution.py:466
  156.7 1.6 collective-permute-done.34
  158.4 3.8 %collective-permute-start.35 = (bf16[64,2048]{1,0:T(8,128)(2,1)S(1)}, bf16[64,2048]{1,0:T(8,128)(2,1)S(1)}, u32[]{:S(2)}, u32[]{:S(2)}) collective-permute-start(bf16[64,2048]{1,0:T(8,128)(2,1)S(1)} %add_convert_fusion.3), channel_id=1, source_target_pairs={{0,14},{1,15},{2,0},{3,1},{4,2},{5,3},{6,4},{7,5},{8,6},{9,7},{10,... | collective-permute-start | bytes 786440 | tf_op jit(solution)/shard_map/ppermute | solution.py:466
  162.4 3.6 %collective-permute-done.35 = bf16[64,2048]{1,0:T(8,128)(2,1)S(1)} collective-permute-done((bf16[64,2048]{1,0:T(8,128)(2,1)S(1)}, bf16[64,2048]{1,0:T(8,128)(2,1)S(1)}, u32[]{:S(2)}, u32[]{:S(2)}) %collective-permute-start.35) | collective-permute-done | bytes 262176 | tf_op jit(solution)/shard_map/ppermute | solution.py:466
  166.2 3.8 %collective-permute-done.31 = bf16[64,2048]{1,0:T(8,128)(2,1)S(1)} collective-permute-done((bf16[64,2048]{1,0:T(8,128)(2,1)S(1)}, bf16[64,2048]{1,0:T(8,128)(2,1)S(1)}, u32[]{:S(2)}, u32[]{:S(2)}) %collective-permute-start.31) | collective-permute-done | bytes 262176 | tf_op jit(solution)/shard_map/ppermute | solution.py:463
  170.1 13.1 %all_to_all.17 = bf16[16,8,2048]{2,1,0:T(8,128)(2,1)S(1)} all-to-all(bf16[16,8,2048]{2,1,0:T(8,128)(2,1)S(1)} %maximum_bitcast_fusion), channel_id=1, replica_groups=mesh['sp'=16,'tp'=16] {'sp'}, dimensions={0} | all-to-all | bytes 1048576 | tf_op jit(solution)/shard_map/all_to_all | solution.py:628
  (77 shorter events, 7.7 us)
Async XLA Ops:
  1.2 10.3 %collective-permute-start.2 = (bf16[544,256]{1,0:T(8,128)(2,1)S(1)}, bf16[544,256]{1,0:T(8,128)(2,1)S(1)}, u32[]{:S(2)}, u32[]{:S(2)}) collective-permute-start(bf16[544,256]{1,0:T(8,128)(2,1)S(1)} %get-tuple-element.70.refs_2_.refs_1_), channel_id=1, source_target_pairs={{0,16},{16,32},{32,48},{48,0},{64,80},{80,96},{96,112},{112,64},{1... | collective-permute-start | bytes 835592 | tf_op jit(solution)/shard_map/ppermute | solution.py:334
  4.6 10.3 %collective-permute-start.4 = (bf16[544,256]{1,0:T(8,128)(2,1)S(1)}, bf16[544,256]{1,0:T(8,128)(2,1)S(1)}, u32[]{:S(2)}, u32[]{:S(2)}) collective-permute-start(bf16[544,256]{1,0:T(8,128)(2,1)S(1)} %get-tuple-element.70.refs_2_.refs_1_), channel_id=1, source_target_pairs={{0,48},{16,0},{32,16},{48,32},{64,112},{80,64},{96,80},{112,96},{1... | collective-permute-start | bytes 835592 | tf_op jit(solution)/shard_map/ppermute | solution.py:334
  7.3 11.1 %collective-permute-start = (bf16[144,512]{1,0:T(8,128)(2,1)S(1)}, bf16[144,512]{1,0:T(8,128)(2,1)S(1)}, u32[]{:S(2)}, u32[]{:S(2)}) collective-permute-start(bf16[144,512]{1,0:T(8,128)(2,1)S(1)} %get-tuple-element.69.refs_0_), channel_id=1, source_target_pairs={{192,0},{208,16},{224,32},{240,48},{193,1},{209,17},{225,33},{241,... | collective-permute-start | bytes 442376 | tf_op jit(solution)/shard_map/ppermute | solution.py:334
  8.6 9.8 %collective-permute-start.1 = (bf16[144,512]{1,0:T(8,128)(2,1)S(1)}, bf16[144,512]{1,0:T(8,128)(2,1)S(1)}, u32[]{:S(2)}, u32[]{:S(2)}) collective-permute-start(bf16[144,512]{1,0:T(8,128)(2,1)S(1)} %get-tuple-element.69.refs_0_), channel_id=1, source_target_pairs={{128,0},{144,16},{160,32},{176,48},{192,64},{208,80},{224,96},{240... | collective-permute-start | bytes 442376 | tf_op jit(solution)/shard_map/ppermute | solution.py:334
  9.9 14.6 %collective-permute-start.6 = (bf16[144,512]{1,0:T(8,128)(2,1)S(1)}, bf16[144,512]{1,0:T(8,128)(2,1)S(1)}, u32[]{:S(2)}, u32[]{:S(2)}) collective-permute-start(bf16[144,512]{1,0:T(8,128)(2,1)S(1)} %get-tuple-element.69.refs_0_), channel_id=1, source_target_pairs={{64,0},{80,16},{96,32},{112,48},{128,64},{144,80},{160,96},{176,11... | collective-permute-start | bytes 442376 | tf_op jit(solution)/shard_map/ppermute | solution.py:334
  11.5 11.3 %collective-permute-start.3 = (bf16[272,256]{1,0:T(8,128)(2,1)S(1)}, bf16[272,256]{1,0:T(8,128)(2,1)S(1)}, u32[]{:S(2)}, u32[]{:S(2)}) collective-permute-start(bf16[272,256]{1,0:T(8,128)(2,1)S(1)} %slice.24), channel_id=1, source_target_pairs={{0,16},{16,32},{32,48},{48,0},{64,80},{80,96},{96,112},{112,64},{1... | collective-permute-start | bytes 417800 | tf_op jit(solution)/shard_map/ppermute | solution.py:334
  15.0 7.8 %collective-permute-start.5 = (bf16[272,256]{1,0:T(8,128)(2,1)S(1)}, bf16[272,256]{1,0:T(8,128)(2,1)S(1)}, u32[]{:S(2)}, u32[]{:S(2)}) collective-permute-start(bf16[272,256]{1,0:T(8,128)(2,1)S(1)} %slice.25), channel_id=1, source_target_pairs={{0,48},{16,0},{32,16},{48,32},{64,112},{80,64},{96,80},{112,96},{1... | collective-permute-start | bytes 417800 | tf_op jit(solution)/shard_map/ppermute | solution.py:334
  18.4 36.2 %slice-start = ((s8[8388608]{0:T(1024)(128)(4,1)}), s8[4194304]{0:T(1024)(128)(4,1)S(1)}, s32[]{:S(2)}) async-start(s8[8388608]{0:T(1024)(128)(4,1)} %bitcast.17), calls=%async_computation.3 | async-start | bytes 8388608
  24.5 12.9 %copy-start.4 = (f32[128]{0:T(128)S(1)}, f32[128]{0:T(128)}, u32[]{:S(2)}) copy-start(f32[128]{0:T(128)} %param.17) | copy-start | bytes 1540
  24.5 30.1 %slice-start.1 = ((s8[8388608]{0:T(1024)(128)(4,1)}), s8[4194304]{0:T(1024)(128)(4,1)S(1)}, s32[]{:S(2)}) async-start(s8[8388608]{0:T(1024)(128)(4,1)} %bitcast.17), calls=%async_computation.4 | async-start | bytes 8388608
  27.6 27.0 %copy-start = (bf16[32,2048]{1,0:T(8,128)(2,1)S(1)}, bf16[32,2048]{1,0:T(8,128)(2,1)}, u32[]{:S(2)}) copy-start(bf16[32,2048]{1,0:T(8,128)(2,1)} %stream.1) | copy-start | bytes 393220
  27.7 27.0 %copy-start.1 = (f32[2048]{0:T(1024)S(1)}, f32[2048]{0:T(1024)}, u32[]{:S(2)}) copy-start(f32[2048]{0:T(1024)} %param.20) | copy-start | bytes 24580
  27.7 27.0 %copy-start.2 = (s32[32,2]{0,1:T(2,128)S(1)}, s32[32,2]{0,1:T(2,128)}, u32[]{:S(2)}) copy-start(s32[32,2]{0,1:T(2,128)} %param.21) | copy-start | bytes 772
  27.7 27.0 %copy-start.3 = (f32[32,2]{0,1:T(2,128)S(1)}, f32[32,2]{0,1:T(2,128)}, u32[]{:S(2)}) copy-start(f32[32,2]{0,1:T(2,128)} %param.22) | copy-start | bytes 772
  27.7 8.4 %collective-permute-start.7 = (bf16[144,512]{1,0:T(8,128)(2,1)S(1)}, bf16[144,512]{1,0:T(8,128)(2,1)S(1)}, u32[]{:S(2)}, u32[]{:S(2)}) collective-permute-start(bf16[144,512]{1,0:T(8,128)(2,1)S(1)} %shard_map.129), channel_id=1, source_target_pairs={{0,64},{16,80},{32,96},{48,112},{64,128},{80,144},{96,160},{112,17... | collective-permute-start | bytes 442376 | tf_op jit(solution)/shard_map/ppermute | solution.py:334
  30.2 6.0 %collective-permute-start.8 = (bf16[144,512]{1,0:T(8,128)(2,1)S(1)}, bf16[144,512]{1,0:T(8,128)(2,1)S(1)}, u32[]{:S(2)}, u32[]{:S(2)}) collective-permute-start(bf16[144,512]{1,0:T(8,128)(2,1)S(1)} %get-tuple-element.67), channel_id=1, source_target_pairs={{0,128},{16,144},{32,160},{48,176},{64,192},{80,208},{96,224},{112... | collective-permute-start | bytes 442376 | tf_op jit(solution)/shard_map/ppermute | solution.py:334
  33.3 4.0 %collective-permute-start.9 = (bf16[144,512]{1,0:T(8,128)(2,1)S(1)}, bf16[144,512]{1,0:T(8,128)(2,1)S(1)}, u32[]{:S(2)}, u32[]{:S(2)}) collective-permute-start(bf16[144,512]{1,0:T(8,128)(2,1)S(1)} %get-tuple-element.68), channel_id=1, source_target_pairs={{0,192},{16,208},{32,224},{48,240},{1,193},{17,209},{33,225},{49,2... | collective-permute-start | bytes 442376 | tf_op jit(solution)/shard_map/ppermute | solution.py:334
  79.0 40.6 %collective-permute-start.16 = (bf16[6144,256]{1,0:T(8,128)(2,1)S(1)}, bf16[6144,256]{1,0:T(8,128)(2,1)S(1)}, u32[]{:S(2)}, u32[]{:S(2)}) collective-permute-start(bf16[6144,256]{1,0:T(8,128)(2,1)S(1)} %stage_weights.1.refs_2_.refs_10_), channel_id=1, source_target_pairs={{0,1},{1,0},{2,3},{3,2},{4,5},{5,4},{6,7},{7,6},{8,9},{9,8},{10,11... | collective-permute-start | bytes 9437192 | tf_op jit(solution)/shard_map/ppermute | solution.py:625
  79.2 10.0 %collective-permute-start.10 = (bf16[64,2048]{1,0:T(8,128)(2,1)S(1)}, bf16[64,2048]{1,0:T(8,128)(2,1)S(1)}, u32[]{:S(2)}, u32[]{:S(2)}) collective-permute-start(bf16[64,2048]{1,0:T(8,128)(2,1)S(1)} %get-tuple-element.102.refs_0_), channel_id=1, source_target_pairs={{0,2},{1,3},{2,4},{3,5},{4,6},{5,7},{6,8},{7,9},{8,10},{9,11},{10,... | collective-permute-start | bytes 786440 | tf_op jit(solution)/shard_map/ppermute | solution.py:463
  79.8 9.4 %collective-permute-start.13 = (bf16[64,2048]{1,0:T(8,128)(2,1)S(1)}, bf16[64,2048]{1,0:T(8,128)(2,1)S(1)}, u32[]{:S(2)}, u32[]{:S(2)}) collective-permute-start(bf16[64,2048]{1,0:T(8,128)(2,1)S(1)} %get-tuple-element.101.refs_1_), channel_id=1, source_target_pairs={{0,14},{1,15},{2,0},{3,1},{4,2},{5,3},{6,4},{7,5},{8,6},{9,7},{10,... | collective-permute-start | bytes 786440 | tf_op jit(solution)/shard_map/ppermute | solution.py:466
  89.2 10.4 %collective-permute-start.11 = (bf16[64,2048]{1,0:T(8,128)(2,1)S(1)}, bf16[64,2048]{1,0:T(8,128)(2,1)S(1)}, u32[]{:S(2)}, u32[]{:S(2)}) collective-permute-start(bf16[64,2048]{1,0:T(8,128)(2,1)S(1)} %collective-permute-done.10.refs_2_), channel_id=1, source_target_pairs={{0,2},{1,3},{2,4},{3,5},{4,6},{5,7},{6,8},{7,9},{8,10},{9,11},{10,... | collective-permute-start | bytes 786440 | tf_op jit(solution)/shard_map/ppermute | solution.py:463
  89.2 10.4 %collective-permute-start.14 = (bf16[64,2048]{1,0:T(8,128)(2,1)S(1)}, bf16[64,2048]{1,0:T(8,128)(2,1)S(1)}, u32[]{:S(2)}, u32[]{:S(2)}) collective-permute-start(bf16[64,2048]{1,0:T(8,128)(2,1)S(1)} %collective-permute-done.13.refs_5_), channel_id=1, source_target_pairs={{0,14},{1,15},{2,0},{3,1},{4,2},{5,3},{6,4},{7,5},{8,6},{9,7},{10,... | collective-permute-start | bytes 786440 | tf_op jit(solution)/shard_map/ppermute | solution.py:466
  92.4 12.8 %collective-permute-start.18 = (bf16[64,2048]{1,0:T(8,128)(2,1)S(1)}, bf16[64,2048]{1,0:T(8,128)(2,1)S(1)}, u32[]{:S(2)}, u32[]{:S(2)}) collective-permute-start(bf16[64,2048]{1,0:T(8,128)(2,1)S(1)} %get-tuple-element.101.refs_1_), channel_id=1, source_target_pairs={{0,2},{1,3},{2,4},{3,5},{4,6},{5,7},{6,8},{7,9},{8,10},{9,11},{10,... | collective-permute-start | bytes 786440 | tf_op jit(solution)/shard_map/ppermute | solution.py:463
  92.4 12.8 %collective-permute-start.19 = (bf16[64,2048]{1,0:T(8,128)(2,1)S(1)}, bf16[64,2048]{1,0:T(8,128)(2,1)S(1)}, u32[]{:S(2)}, u32[]{:S(2)}) collective-permute-start(bf16[64,2048]{1,0:T(8,128)(2,1)S(1)} %get-tuple-element.102.refs_0_), channel_id=1, source_target_pairs={{0,14},{1,15},{2,0},{3,1},{4,2},{5,3},{6,4},{7,5},{8,6},{9,7},{10,... | collective-permute-start | bytes 786440 | tf_op jit(solution)/shard_map/ppermute | solution.py:466
  99.6 11.2 %collective-permute-start.12 = (bf16[64,2048]{1,0:T(8,128)(2,1)S(1)}, bf16[64,2048]{1,0:T(8,128)(2,1)S(1)}, u32[]{:S(2)}, u32[]{:S(2)}) collective-permute-start(bf16[64,2048]{1,0:T(8,128)(2,1)S(1)} %collective-permute-done.11.refs_6_), channel_id=1, source_target_pairs={{0,2},{1,3},{2,4},{3,5},{4,6},{5,7},{6,8},{7,9},{8,10},{9,11},{10,... | collective-permute-start | bytes 786440 | tf_op jit(solution)/shard_map/ppermute | solution.py:463
  99.6 11.2 %collective-permute-start.15 = (bf16[64,2048]{1,0:T(8,128)(2,1)S(1)}, bf16[64,2048]{1,0:T(8,128)(2,1)S(1)}, u32[]{:S(2)}, u32[]{:S(2)}) collective-permute-start(bf16[64,2048]{1,0:T(8,128)(2,1)S(1)} %collective-permute-done.14.refs_9_), channel_id=1, source_target_pairs={{0,14},{1,15},{2,0},{3,1},{4,2},{5,3},{6,4},{7,5},{8,6},{9,7},{10,... | collective-permute-start | bytes 786440 | tf_op jit(solution)/shard_map/ppermute | solution.py:466
  105.2 11.2 %collective-permute-start.20 = (bf16[64,2048]{1,0:T(8,128)(2,1)S(1)}, bf16[64,2048]{1,0:T(8,128)(2,1)S(1)}, u32[]{:S(2)}, u32[]{:S(2)}) collective-permute-start(bf16[64,2048]{1,0:T(8,128)(2,1)S(1)} %collective-permute-done.18.refs_3_), channel_id=1, source_target_pairs={{0,2},{1,3},{2,4},{3,5},{4,6},{5,7},{6,8},{7,9},{8,10},{9,11},{10,... | collective-permute-start | bytes 786440 | tf_op jit(solution)/shard_map/ppermute | solution.py:463
  105.2 11.2 %collective-permute-start.21 = (bf16[64,2048]{1,0:T(8,128)(2,1)S(1)}, bf16[64,2048]{1,0:T(8,128)(2,1)S(1)}, u32[]{:S(2)}, u32[]{:S(2)}) collective-permute-start(bf16[64,2048]{1,0:T(8,128)(2,1)S(1)} %collective-permute-done.19.refs_4_), channel_id=1, source_target_pairs={{0,14},{1,15},{2,0},{3,1},{4,2},{5,3},{6,4},{7,5},{8,6},{9,7},{10,... | collective-permute-start | bytes 786440 | tf_op jit(solution)/shard_map/ppermute | solution.py:466
  110.8 11.2 %collective-permute-start.24 = (bf16[64,2048]{1,0:T(8,128)(2,1)S(1)}, bf16[64,2048]{1,0:T(8,128)(2,1)S(1)}, u32[]{:S(2)}, u32[]{:S(2)}) collective-permute-start(bf16[64,2048]{1,0:T(8,128)(2,1)S(1)} %collective-permute-done.12.refs_0_), channel_id=1, source_target_pairs={{0,2},{1,3},{2,4},{3,5},{4,6},{5,7},{6,8},{7,9},{8,10},{9,11},{10,... | collective-permute-start | bytes 786440 | tf_op jit(solution)/shard_map/ppermute | solution.py:463
  110.8 11.2 %collective-permute-start.25 = (bf16[64,2048]{1,0:T(8,128)(2,1)S(1)}, bf16[64,2048]{1,0:T(8,128)(2,1)S(1)}, u32[]{:S(2)}, u32[]{:S(2)}) collective-permute-start(bf16[64,2048]{1,0:T(8,128)(2,1)S(1)} %collective-permute-done.15.refs_1_), channel_id=1, source_target_pairs={{0,14},{1,15},{2,0},{3,1},{4,2},{5,3},{6,4},{7,5},{8,6},{9,7},{10,... | collective-permute-start | bytes 786440 | tf_op jit(solution)/shard_map/ppermute | solution.py:466
  116.4 11.2 %collective-permute-start.27 = (bf16[64,2048]{1,0:T(8,128)(2,1)S(1)}, bf16[64,2048]{1,0:T(8,128)(2,1)S(1)}, u32[]{:S(2)}, u32[]{:S(2)}) collective-permute-start(bf16[64,2048]{1,0:T(8,128)(2,1)S(1)} %collective-permute-done.20.refs_7_), channel_id=1, source_target_pairs={{0,2},{1,3},{2,4},{3,5},{4,6},{5,7},{6,8},{7,9},{8,10},{9,11},{10,... | collective-permute-start | bytes 786440 | tf_op jit(solution)/shard_map/ppermute | solution.py:463
  116.4 13.3 %collective-permute-start.28 = (bf16[64,2048]{1,0:T(8,128)(2,1)S(1)}, bf16[64,2048]{1,0:T(8,128)(2,1)S(1)}, u32[]{:S(2)}, u32[]{:S(2)}) collective-permute-start(bf16[64,2048]{1,0:T(8,128)(2,1)S(1)} %collective-permute-done.21.refs_8_), channel_id=1, source_target_pairs={{0,14},{1,15},{2,0},{3,1},{4,2},{5,3},{6,4},{7,5},{8,6},{9,7},{10,... | collective-permute-start | bytes 786440 | tf_op jit(solution)/shard_map/ppermute | solution.py:466
  120.8 16.0 %collective-permute-start.36 = (bf16[64,2048]{1,0:T(8,128)(2,1)S(1)}, bf16[64,2048]{1,0:T(8,128)(2,1)S(1)}, u32[]{:S(2)}, u32[]{:S(2)}) collective-permute-start(bf16[64,2048]{1,0:T(8,128)(2,1)S(1)} %get-tuple-element.96), channel_id=1, source_target_pairs={{0,2},{1,3},{2,4},{3,5},{4,6},{5,7},{6,8},{7,9},{8,10},{9,11},{10,... | collective-permute-start | bytes 786440 | tf_op jit(solution)/shard_map/ppermute | solution.py:463
  123.2 14.1 %collective-permute-start.32 = (bf16[64,2048]{1,0:T(8,128)(2,1)S(1)}, bf16[64,2048]{1,0:T(8,128)(2,1)S(1)}, u32[]{:S(2)}, u32[]{:S(2)}) collective-permute-start(bf16[64,2048]{1,0:T(8,128)(2,1)S(1)} %get-tuple-element.92), channel_id=1, source_target_pairs={{0,14},{1,15},{2,0},{3,1},{4,2},{5,3},{6,4},{7,5},{8,6},{9,7},{10,... | collective-permute-start | bytes 786440 | tf_op jit(solution)/shard_map/ppermute | solution.py:466
  126.5 14.1 %collective-permute-start.26 = (bf16[64,2048]{1,0:T(8,128)(2,1)S(1)}, bf16[64,2048]{1,0:T(8,128)(2,1)S(1)}, u32[]{:S(2)}, u32[]{:S(2)}) collective-permute-start(bf16[64,2048]{1,0:T(8,128)(2,1)S(1)} %get-tuple-element.87), channel_id=1, source_target_pairs={{0,2},{1,3},{2,4},{3,5},{4,6},{5,7},{6,8},{7,9},{8,10},{9,11},{10,... | collective-permute-start | bytes 786440 | tf_op jit(solution)/shard_map/ppermute | solution.py:463
  127.6 13.1 %collective-permute-start.17 = (bf16[64,2048]{1,0:T(8,128)(2,1)S(1)}, bf16[64,2048]{1,0:T(8,128)(2,1)S(1)}, u32[]{:S(2)}, u32[]{:S(2)}) collective-permute-start(bf16[64,2048]{1,0:T(8,128)(2,1)S(1)} %get-tuple-element.84), channel_id=1, source_target_pairs={{0,14},{1,15},{2,0},{3,1},{4,2},{5,3},{6,4},{7,5},{8,6},{9,7},{10,... | collective-permute-start | bytes 786440 | tf_op jit(solution)/shard_map/ppermute | solution.py:466
  136.9 10.7 %collective-permute-start.37 = (bf16[64,2048]{1,0:T(8,128)(2,1)S(1)}, bf16[64,2048]{1,0:T(8,128)(2,1)S(1)}, u32[]{:S(2)}, u32[]{:S(2)}) collective-permute-start(bf16[64,2048]{1,0:T(8,128)(2,1)S(1)} %add_convert_fusion.2), channel_id=1, source_target_pairs={{0,2},{1,3},{2,4},{3,5},{4,6},{5,7},{6,8},{7,9},{8,10},{9,11},{10,... | collective-permute-start | bytes 786440 | tf_op jit(solution)/shard_map/ppermute | solution.py:463
  137.3 10.5 %collective-permute-start.33 = (bf16[64,2048]{1,0:T(8,128)(2,1)S(1)}, bf16[64,2048]{1,0:T(8,128)(2,1)S(1)}, u32[]{:S(2)}, u32[]{:S(2)}) collective-permute-start(bf16[64,2048]{1,0:T(8,128)(2,1)S(1)} %add_convert_fusion.5), channel_id=1, source_target_pairs={{0,14},{1,15},{2,0},{3,1},{4,2},{5,3},{6,4},{7,5},{8,6},{9,7},{10,... | collective-permute-start | bytes 786440 | tf_op jit(solution)/shard_map/ppermute | solution.py:466
  140.7 12.5 %collective-permute-start.29 = (bf16[64,2048]{1,0:T(8,128)(2,1)S(1)}, bf16[64,2048]{1,0:T(8,128)(2,1)S(1)}, u32[]{:S(2)}, u32[]{:S(2)}) collective-permute-start(bf16[64,2048]{1,0:T(8,128)(2,1)S(1)} %add_convert_fusion.9), channel_id=1, source_target_pairs={{0,2},{1,3},{2,4},{3,5},{4,6},{5,7},{6,8},{7,9},{8,10},{9,11},{10,... | collective-permute-start | bytes 786440 | tf_op jit(solution)/shard_map/ppermute | solution.py:463
  140.8 12.5 %collective-permute-start.22 = (bf16[64,2048]{1,0:T(8,128)(2,1)S(1)}, bf16[64,2048]{1,0:T(8,128)(2,1)S(1)}, u32[]{:S(2)}, u32[]{:S(2)}) collective-permute-start(bf16[64,2048]{1,0:T(8,128)(2,1)S(1)} %add_convert_fusion.11), channel_id=1, source_target_pairs={{0,14},{1,15},{2,0},{3,1},{4,2},{5,3},{6,4},{7,5},{8,6},{9,7},{10,... | collective-permute-start | bytes 786440 | tf_op jit(solution)/shard_map/ppermute | solution.py:466
  147.7 14.7 %collective-permute-start.38 = (bf16[64,2048]{1,0:T(8,128)(2,1)S(1)}, bf16[64,2048]{1,0:T(8,128)(2,1)S(1)}, u32[]{:S(2)}, u32[]{:S(2)}) collective-permute-start(bf16[64,2048]{1,0:T(8,128)(2,1)S(1)} %add_convert_fusion.1), channel_id=1, source_target_pairs={{0,2},{1,3},{2,4},{3,5},{4,6},{5,7},{6,8},{7,9},{8,10},{9,11},{10,... | collective-permute-start | bytes 786440 | tf_op jit(solution)/shard_map/ppermute | solution.py:463
  147.8 10.5 %collective-permute-start.34 = (bf16[64,2048]{1,0:T(8,128)(2,1)S(1)}, bf16[64,2048]{1,0:T(8,128)(2,1)S(1)}, u32[]{:S(2)}, u32[]{:S(2)}) collective-permute-start(bf16[64,2048]{1,0:T(8,128)(2,1)S(1)} %add_convert_fusion.4), channel_id=1, source_target_pairs={{0,14},{1,15},{2,0},{3,1},{4,2},{5,3},{6,4},{7,5},{8,6},{9,7},{10,... | collective-permute-start | bytes 786440 | tf_op jit(solution)/shard_map/ppermute | solution.py:466
  153.3 8.9 %collective-permute-start.30 = (bf16[64,2048]{1,0:T(8,128)(2,1)S(1)}, bf16[64,2048]{1,0:T(8,128)(2,1)S(1)}, u32[]{:S(2)}, u32[]{:S(2)}) collective-permute-start(bf16[64,2048]{1,0:T(8,128)(2,1)S(1)} %add_convert_fusion.8), channel_id=1, source_target_pairs={{0,2},{1,3},{2,4},{3,5},{4,6},{5,7},{6,8},{7,9},{8,10},{9,11},{10,... | collective-permute-start | bytes 786440 | tf_op jit(solution)/shard_map/ppermute | solution.py:463
  153.5 12.7 %collective-permute-start.23 = (bf16[64,2048]{1,0:T(8,128)(2,1)S(1)}, bf16[64,2048]{1,0:T(8,128)(2,1)S(1)}, u32[]{:S(2)}, u32[]{:S(2)}) collective-permute-start(bf16[64,2048]{1,0:T(8,128)(2,1)S(1)} %add_convert_fusion.10), channel_id=1, source_target_pairs={{0,14},{1,15},{2,0},{3,1},{4,2},{5,3},{6,4},{7,5},{8,6},{9,7},{10,... | collective-permute-start | bytes 786440 | tf_op jit(solution)/shard_map/ppermute | solution.py:466
  158.4 7.7 %collective-permute-start.35 = (bf16[64,2048]{1,0:T(8,128)(2,1)S(1)}, bf16[64,2048]{1,0:T(8,128)(2,1)S(1)}, u32[]{:S(2)}, u32[]{:S(2)}) collective-permute-start(bf16[64,2048]{1,0:T(8,128)(2,1)S(1)} %add_convert_fusion.3), channel_id=1, source_target_pairs={{0,14},{1,15},{2,0},{3,1},{4,2},{5,3},{6,4},{7,5},{8,6},{9,7},{10,... | collective-permute-start | bytes 786440 | tf_op jit(solution)/shard_map/ppermute | solution.py:466
  162.3 7.7 %collective-permute-start.31 = (bf16[64,2048]{1,0:T(8,128)(2,1)S(1)}, bf16[64,2048]{1,0:T(8,128)(2,1)S(1)}, u32[]{:S(2)}, u32[]{:S(2)}) collective-permute-start(bf16[64,2048]{1,0:T(8,128)(2,1)S(1)} %add_convert_fusion.7), channel_id=1, source_target_pairs={{0,2},{1,3},{2,4},{3,5},{4,6},{5,7},{6,8},{7,9},{8,10},{9,11},{10,... | collective-permute-start | bytes 786440 | tf_op jit(solution)/shard_map/ppermute | solution.py:463

commit v4 on v2

--- a/solution.py
+++ b/solution.py
@@ -155,7 +155,7 @@
 def nth_state(state, i):
     found = []
     for ref in state:
-        rows = ref.shape[0] // 2
+        rows = ref.shape[0] // 4
         found.append(ref.at[pl.ds(pl.multiple_of(i * rows, 8), rows)])
     return found
 
@@ -205,19 +205,17 @@
     out[HD:PACK, :] = block.astype(jnp.bfloat16)
 
 
-def distant_kernel(*refs):
-    packs, keys, states = refs[:2], refs[2:5], refs[5:8]
-    stack, keys_wide, query_wide = refs[8:]
-    own_y = lax.axis_index("sp") >> 2
-
-    @pl.when(own_y < 2)
-    def _():
-        load_blocks(stack, keys_wide, keys)
+def near_kernel(*refs):
+    packs, keys, states = refs[:4], refs[4:7], refs[7:10]
+    stack, keys_wide, query_wide = refs[10:]
+    own = lax.axis_index("sp")
+    own_y, own_x = own >> 2, own & 3
+    load_blocks(stack, keys_wide, keys)
 
     def each(i, carry):
         @pl.when(own_y <= i)
         def _():
-            for at, pack in enumerate(packs):
+            for at, pack in enumerate(packs[:3]):
                 pl.when(i == at)(partial(load_query, query_wide, pack))
             state = nth_state(states, i)
             clear(state)
@@ -225,61 +223,46 @@
 
         return carry
 
-    lax.fori_loop(0, 2, each, 0)
-
-
-def distant_end_kernel(*refs):
-    packs, far, states, outs = refs[:2], refs[2:4], refs[4:7], refs[7:9]
-    state, (stack, keys_wide, query_wide) = refs[9:12], refs[12:]
-    own_y = lax.axis_index("sp") >> 2
-
-    @pl.when(own_y < 2)
-    def _():
-        load_blocks(stack, keys_wide, far)
+    lax.fori_loop(0, 3, each, 0)
+    state = nth_state(states, 3)
+    load_query(query_wide, packs[3])
+    clear(state)
+    fold(query_wide, state, stack, keys_wide, 0, own_block=True)
+
+    def seen(i):
+        return ((own_x + jnp.where(i == 1, -1, 1)) & 3) < own_x
+
+    fold_blocks(query_wide, state, stack, keys_wide, 1, 2, seen)
+
+
+def end_kernel(*refs, first):
+    packs, far, states, outs = refs[:2], refs[2:4], refs[4:7], refs[7:-6]
+    state, (stack, keys_wide, query_wide) = refs[-6:-3], refs[-3:]
+    own = lax.axis_index("sp")
+    own_y, own_x = own >> 2, own & 3
+    load_blocks(stack, keys_wide, far)
 
     def each(i, carry):
-        @pl.when(own_y <= i)
+        needed = own_y <= first + i
+        if first == 2:
+            needed = jnp.where(i == 0, needed, ((own_x + 2) & 3) < own_x)
+        for into, came in zip(state, nth_state(states, first + i)):
+            into[...] = came[...]
+
+        @pl.when(needed)
         def _():
-            for into, came in zip(state, nth_state(states, i)):
-                into[...] = came[...]
             for at, pack in enumerate(packs):
                 pl.when(i == at)(partial(load_query, query_wide, pack))
             fold(query_wide, state, stack, keys_wide, 0)
-            for at, out in enumerate(outs):
-                pl.when(i == at)(partial(pack_result, state, out))
-
+
+        for at in range(1 if first == 2 else 2):
+            pl.when(jnp.logical_and(i == at, needed))(partial(pack_result, state, outs[at]))
         return carry
 
     lax.fori_loop(0, 2, each, 0)
-
-
-def next_kernel(*refs):
-    pack, keys, out, state = refs[0], refs[1:6], refs[6], refs[7:10]
-    stack, keys_wide, query_wide = refs[10:]
-
-    @pl.when(lax.axis_index("sp") < 12)
-    def _():
-        load_blocks(stack, keys_wide, keys)
-        load_query(query_wide, pack)
-        clear(state)
-        fold_blocks(query_wide, state, stack, keys_wide, 0, 4)
-        pack_result(state, out)
-
-
-def own_kernel(*refs):
-    pack, keys, state = refs[0], refs[1:6], refs[6:9]
-    stack, keys_wide, query_wide = refs[9:]
-    own_x = lax.axis_index("sp") & 3
-    load_blocks(stack, keys_wide, keys)
-    load_query(query_wide, pack)
-    clear(state)
-    fold(query_wide, state, stack, keys_wide, 0, own_block=True)
-
-    def seen(i):
-        move = jnp.where(i == 1, -1, jnp.where(i == 2, 1, 2))
-        return ((own_x + move) & 3) < own_x
-
-    fold_blocks(query_wide, state, stack, keys_wide, 1, 3, seen)
+    if first == 2:
+        for out, ref in zip(outs[1:], state):
+            out[...] = ref[...]
 
 
 def merge_kernel(*refs):
@@ -344,27 +327,28 @@
 
     narrow = ((8, tok_count), jnp.float32)
     state = [narrow, narrow, ((HD, tok_count), jnp.float32)]
-    both = [((2 * shape[0], tok_count), kind) for shape, kind in state]
+    all_states = [((4 * shape[0], tok_count), kind) for shape, kind in state]
     result = ((PACK, tok_count), jnp.bfloat16)
 
     def loaded(count):
         shapes = (count * BLOCK, 2 * HD), (count * 2 * KEYS, 2 * HD), (2 * HD, tok_count)
         return [(shape, jnp.bfloat16) for shape in shapes]
 
-    near = attend(distant_kernel, [pack3, pack2, keys_own, low, high], both, loaded(3), 6)
-    far_a, far_b, near = lax.optimization_barrier((far_a, far_b, near))
-    part3, part2 = attend(
-        distant_end_kernel, [pack3, pack2, far_a, far_b, *near], [result] * 2, state + loaded(1), 2
-    )
-    part3, part2, pack1 = lax.optimization_barrier((part3, part2, pack1))
+    packs = [pack3, pack2, pack1, own_pack]
+    near = attend(near_kernel, [*packs, keys_own, low, high], all_states, loaded(3), 12)
+    weights, near = lax.optimization_barrier((weights, near))
+    staged = stage_weights(*weights)
+
+    def end(first, outs):
+        operands = [*packs[first : first + 2], far_a, far_b, *near]
+        return attend(partial(end_kernel, first=first), operands, outs, state + loaded(1), 2)
+
+    part3, part2 = end(0, [result] * 2)
+    part3, part2, near = lax.optimization_barrier((part3, part2, near))
     back3 = shift(part3, -1, 0, lambda y, x: y == 3)
     back2 = shift(part2, 2, 0, lambda y, x: y > 1)
-    keys = [keys_own, low, high, far_a, far_b]
-    (part1,) = attend(next_kernel, [pack1, *keys], [result], state + loaded(4), 4)
-    part1, own_pack, keys, weights = lax.optimization_barrier((part1, own_pack, keys, weights))
+    part1, *own_state = end(2, [result] + state)
     back1 = shift(part1, 1, 0, lambda y, x: y > 0)
-    own_state = attend(own_kernel, [own_pack, *keys], state, loaded(4), 4)
-    staged = stage_weights(*weights)
     (head_out,) = attend(
         merge_kernel,
         [back1, back2, back3, *own_state, head_gain.reshape(1, HD)],

time: 185 us -> 196 us (1.059)
  waiting for transfers between devices: 36.1 us -> 50.6 us
  starting transfers between devices: 69.2 us -> 65.7 us
    ppermute x10, waiting for transfers between devices: 3.12 us -> 17.7 us  [shift(): return lax.ppermute(array, 'sp', sp_perm(dy, dx, needed))]
    ppermute x10, starting transfers between devices: 23.6 us -> 19.8 us  [shift(): return lax.ppermute(array, 'sp', sp_perm(dy, dx, needed))]
    pallas_call x5 -> x4, Pallas kernels: 10.9 us -> 10.8 us  [attend(): pl.pallas_call(kernel, out_shape=tuple((jax.ShapeDtypeStruct(*out) for ou...]
  transfers between devices with their start and end apart: 39 -> 39, of which waited for: 15 -> 18; matrix products, arithmetic and copies ran while one was open for 0% -> 0% of each run, Pallas kernels for 11% -> 8%
where the time goes in v4:
time: 196 us; the launch traced here: 195 us
  starting transfers between devices  65.7 us (34%)
  waiting for transfers between devices  50.6 us (26%)
  blocking collectives  50.4 us (26%)
  Pallas kernels  27.1 us (14%)
    ppermute x14, starting transfers between devices, down(): return lax.ppermute(array, 'tp', z_perm(-1))  44.2 us
    ppermute x14, waiting for transfers between devices, up(): return lax.ppermute(array, 'tp', z_perm(1))  27.4 us
    all_to_all x1, blocking collectives, on_device(): lax.all_to_all(outgoing, 'sp', split_axis=0, concat_axis=0, tiled=True)  19.9 us
    ppermute x10, starting transfers between devices, shift(): return lax.ppermute(array, 'sp', sp_perm(dy, dx, needed))  19.8 us
    ppermute x10, waiting for transfers between devices, shift(): return lax.ppermute(array, 'sp', sp_perm(dy, dx, needed))  17.7 us
    all_to_all x1, blocking collectives, on_device(): heads = lax.all_to_all(heads, 'tp', split_axis=0, concat_axis=0, tiled=True)  17 us
    all_to_all x1, blocking collectives, on_device(): lax.all_to_all(expert_out, 'sp', split_axis=0, concat_axis=0, tiled=True)  13.5 us
    pallas_call x4, Pallas kernels, attend(): pl.pallas_call(kernel, out_shape=tuple((jax.ShapeDtypeStruct(*out) for ou...  10.8 us
  transfers between devices with their start and end apart: 39, of which 18 were waited for; matrix products, arithmetic and copies ran while one was open for 0% of the time, Pallas kernels for 8%

profile of v4, /device:TPU:2, one launch (start us, length us, event | category | flops | bytes accessed | tf_op | source)
XLA Modules:
  0.0 195.2 jit_solution(9394720852197847670)
XLA Ops:
  1.2 3.4 %collective-permute-start.1 = (bf16[544,256]{1,0:T(8,128)(2,1)S(1)}, bf16[544,256]{1,0:T(8,128)(2,1)S(1)}, u32[]{:S(2)}, u32[]{:S(2)}) collective-permute-start(bf16[544,256]{1,0:T(8,128)(2,1)S(1)} %get-tuple-element.47.refs_4_), channel_id=1, source_target_pairs={{0,16},{16,32},{32,48},{48,0},{64,80},{80,96},{96,112},{112,64},{1... | collective-permute-start | bytes 835592 | tf_op jit(solution)/shard_map/ppermute | solution.py:317
  4.6 2.7 %collective-permute-start.3 = (bf16[544,256]{1,0:T(8,128)(2,1)S(1)}, bf16[544,256]{1,0:T(8,128)(2,1)S(1)}, u32[]{:S(2)}, u32[]{:S(2)}) collective-permute-start(bf16[544,256]{1,0:T(8,128)(2,1)S(1)} %get-tuple-element.47.refs_4_), channel_id=1, source_target_pairs={{0,48},{16,0},{32,16},{48,32},{64,112},{80,64},{96,80},{112,96},{1... | collective-permute-start | bytes 835592 | tf_op jit(solution)/shard_map/ppermute | solution.py:317
  11.2 3.1 %collective-permute-done.refs_2_.refs_0_ = bf16[144,512]{1,0:T(8,128)(2,1)S(1)} collective-permute-done((bf16[144,512]{1,0:T(8,128)(2,1)S(1)}, bf16[144,512]{1,0:T(8,128)(2,1)S(1)}, u32[]{:S(2)}, u32[]{:S(2)}) %collective-permute-start) | collective-permute-done | bytes 147488 | tf_op jit(solution)/shard_map/ppermute | solution.py:317
  14.3 5.9 %collective-permute-done.5.refs_0_ = bf16[144,512]{1,0:T(8,128)(2,1)S(1)} collective-permute-done((bf16[144,512]{1,0:T(8,128)(2,1)S(1)}, bf16[144,512]{1,0:T(8,128)(2,1)S(1)}, u32[]{:S(2)}, u32[]{:S(2)}) %collective-permute-start.5) | collective-permute-done | bytes 147488 | tf_op jit(solution)/shard_map/ppermute | solution.py:317
  20.2 7.8 %shard_map.127 = (f32[32,512]{1,0:T(8,128)S(1)}, f32[32,512]{1,0:T(8,128)S(1)}, f32[512,512]{1,0:T(8,128)S(1)}) custom-call(bf16[144,512]{1,0:T(8,128)(2,1)S(1)} %collective-permute-done.5.refs_0_, bf16[144,512]{1,0:T(8,128)(2,1)S(1)} %collective-permute-done.6.refs_1_, bf16[144,512]{1,0:T(8,128)(2,1)S(1)} %collective-permute-done.refs_2_.refs_0_, ...), custom_call_target="tpu_custom_call" | custom-call | flops 3221225472 | bytes 1048576 | tf_op jit(solution)/shard_map/pallas_call | solution.py:298
  28.1 2.1 %stage_weights.1.refs_4_.refs_6_.refs_2_ = bf16[6144,256]{1,0:T(8,128)(2,1)S(1)} custom-call(bf16[2048,256]{1,0:T(8,128)(2,1)} %bitcast.26, bf16[2048,256]{1,0:T(8,128)(2,1)} %bitcast.27, bf16[256,2048]{1,0:T(8,128)(2,1)} %bitcast.28), custom_call_target="tpu_custom_call" | custom-call | tf_op jit(solution)/shard_map/stage_weights/pallas_call | solution.py:381
  30.3 3.5 %collective-permute-start.2 = (bf16[272,256]{1,0:T(8,128)(2,1)S(1)}, bf16[272,256]{1,0:T(8,128)(2,1)S(1)}, u32[]{:S(2)}, u32[]{:S(2)}) collective-permute-start(bf16[272,256]{1,0:T(8,128)(2,1)S(1)} %slice.24), channel_id=1, source_target_pairs={{0,16},{16,32},{32,48},{48,0},{64,80},{80,96},{96,112},{112,64},{1... | collective-permute-start | bytes 417800 | tf_op jit(solution)/shard_map/ppermute | solution.py:317
  33.9 2.4 %collective-permute-start.4 = (bf16[272,256]{1,0:T(8,128)(2,1)S(1)}, bf16[272,256]{1,0:T(8,128)(2,1)S(1)}, u32[]{:S(2)}, u32[]{:S(2)}) collective-permute-start(bf16[272,256]{1,0:T(8,128)(2,1)S(1)} %slice.25), channel_id=1, source_target_pairs={{0,48},{16,0},{32,16},{48,32},{64,112},{80,64},{96,80},{112,96},{1... | collective-permute-start | bytes 417800 | tf_op jit(solution)/shard_map/ppermute | solution.py:317
  36.4 2.0 %collective-permute-done.2.refs_2_ = bf16[272,256]{1,0:T(8,128)(2,1)S(1)} collective-permute-done((bf16[272,256]{1,0:T(8,128)(2,1)S(1)}, bf16[272,256]{1,0:T(8,128)(2,1)S(1)}, u32[]{:S(2)}, u32[]{:S(2)}) %collective-permute-start.2) | collective-permute-done | bytes 139296 | tf_op jit(solution)/shard_map/ppermute | solution.py:317
  38.3 3.3 %collective-permute-done.4.refs_3_ = bf16[272,256]{1,0:T(8,128)(2,1)S(1)} collective-permute-done((bf16[272,256]{1,0:T(8,128)(2,1)S(1)}, bf16[272,256]{1,0:T(8,128)(2,1)S(1)}, u32[]{:S(2)}, u32[]{:S(2)}) %collective-permute-start.4) | collective-permute-done | bytes 139296 | tf_op jit(solution)/shard_map/ppermute | solution.py:317
  41.6 1.7 shard_map.128
  44.2 1.3 collective-permute-start.7
  45.5 1.3 collective-permute-start.8
  48.2 1.6 collective-permute-done.7.refs_0_
  49.8 1.8 collective-permute-done.8.refs_1_
  51.9 17.0 %all_to_all.15.heads = bf16[16,32,128]{2,1,0:T(8,128)(2,1)S(1)} all-to-all(bf16[16,32,128]{2,1,0:T(8,128)(2,1)S(1)} %bitcast.21), channel_id=1, replica_groups=mesh['sp'=16,'tp'=16] {'tp'}, dimensions={0} | all-to-all | bytes 262144 | tf_op jit(solution)/shard_map/all_to_all | solution.py:609
  69.0 2.5 %project.1 = (f32[32,2048]{1,0:T(8,128)S(1)}, bf16[128,2048]{1,0:T(8,128)(2,1)S(1)}, f32[128,32]{1,0:T(8,128)S(1)}) custom-call(bf16[16,32,128]{2,1,0:T(8,128)(2,1)S(1)} %all_to_all.15.heads, bf16[2048,2048]{1,0:T(8,128)(2,1)S(1)} %bitcast.18, bf16[32,2048]{1,0:T(8,128)(2,1)S(1)} %copy-done, f32[1,2048]{1,0:T(1,128)S(1)} %bitcast.22, s32[2,32]{1,0:T(2,128)S(1)} %bitcast.23, ...), custom_call_target="tpu_custom_call" | custom-call | tf_op jit(solution)/shard_map/project/pallas_call | solution.py:539
  71.5 19.9 %all_to_all.16 = bf16[16,8,2048]{2,1,0:T(8,128)(2,1)S(1)} all-to-all(bf16[16,8,2048]{2,1,0:T(8,128)(2,1)S(1)} %bitcast.20), channel_id=1, replica_groups=mesh['sp'=16,'tp'=16] {'sp'}, dimensions={0} | all-to-all | bytes 1048576 | tf_op jit(solution)/shard_map/all_to_all | solution.py:614
  92.1 2.7 %collective-permute-start.19 = (bf16[64,2048]{1,0:T(8,128)(2,1)S(1)}, bf16[64,2048]{1,0:T(8,128)(2,1)S(1)}, u32[]{:S(2)}, u32[]{:S(2)}) collective-permute-start(bf16[64,2048]{1,0:T(8,128)(2,1)S(1)} %get-tuple-element.87.refs_1_), channel_id=1, source_target_pairs={{0,14},{1,15},{2,0},{3,1},{4,2},{5,3},{6,4},{7,5},{8,6},{9,7},{10,... | collective-permute-start | bytes 786440 | tf_op jit(solution)/shard_map/ppermute | solution.py:451
  94.8 3.2 %collective-permute-start.16 = (bf16[64,2048]{1,0:T(8,128)(2,1)S(1)}, bf16[64,2048]{1,0:T(8,128)(2,1)S(1)}, u32[]{:S(2)}, u32[]{:S(2)}) collective-permute-start(bf16[64,2048]{1,0:T(8,128)(2,1)S(1)} %get-tuple-element.88.refs_0_), channel_id=1, source_target_pairs={{0,14},{1,15},{2,0},{3,1},{4,2},{5,3},{6,4},{7,5},{8,6},{9,7},{10,... | collective-permute-start | bytes 786440 | tf_op jit(solution)/shard_map/ppermute | solution.py:451
  98.0 3.9 %collective-permute-done.10.refs_2_ = bf16[64,2048]{1,0:T(8,128)(2,1)S(1)} collective-permute-done((bf16[64,2048]{1,0:T(8,128)(2,1)S(1)}, bf16[64,2048]{1,0:T(8,128)(2,1)S(1)}, u32[]{:S(2)}, u32[]{:S(2)}) %collective-permute-start.10) | collective-permute-done | bytes 262176 | tf_op jit(solution)/shard_map/ppermute | solution.py:448
  102.0 3.2 %collective-permute-start.20 = (bf16[64,2048]{1,0:T(8,128)(2,1)S(1)}, bf16[64,2048]{1,0:T(8,128)(2,1)S(1)}, u32[]{:S(2)}, u32[]{:S(2)}) collective-permute-start(bf16[64,2048]{1,0:T(8,128)(2,1)S(1)} %collective-permute-done.19.refs_5_), channel_id=1, source_target_pairs={{0,14},{1,15},{2,0},{3,1},{4,2},{5,3},{6,4},{7,5},{8,6},{9,7},{10,... | collective-permute-start | bytes 786440 | tf_op jit(solution)/shard_map/ppermute | solution.py:451
  105.2 2.4 %collective-permute-done.13.refs_3_ = bf16[64,2048]{1,0:T(8,128)(2,1)S(1)} collective-permute-done((bf16[64,2048]{1,0:T(8,128)(2,1)S(1)}, bf16[64,2048]{1,0:T(8,128)(2,1)S(1)}, u32[]{:S(2)}, u32[]{:S(2)}) %collective-permute-start.13) | collective-permute-done | bytes 262176 | tf_op jit(solution)/shard_map/ppermute | solution.py:448
  107.6 3.2 %collective-permute-start.17 = (bf16[64,2048]{1,0:T(8,128)(2,1)S(1)}, bf16[64,2048]{1,0:T(8,128)(2,1)S(1)}, u32[]{:S(2)}, u32[]{:S(2)}) collective-permute-start(bf16[64,2048]{1,0:T(8,128)(2,1)S(1)} %collective-permute-done.16.refs_4_), channel_id=1, source_target_pairs={{0,14},{1,15},{2,0},{3,1},{4,2},{5,3},{6,4},{7,5},{8,6},{9,7},{10,... | collective-permute-start | bytes 786440 | tf_op jit(solution)/shard_map/ppermute | solution.py:451
  110.8 2.4 %collective-permute-done.11.refs_0_ = bf16[64,2048]{1,0:T(8,128)(2,1)S(1)} collective-permute-done((bf16[64,2048]{1,0:T(8,128)(2,1)S(1)}, bf16[64,2048]{1,0:T(8,128)(2,1)S(1)}, u32[]{:S(2)}, u32[]{:S(2)}) %collective-permute-start.11) | collective-permute-done | bytes 262176 | tf_op jit(solution)/shard_map/ppermute | solution.py:448
  113.2 3.2 %collective-permute-start.21 = (bf16[64,2048]{1,0:T(8,128)(2,1)S(1)}, bf16[64,2048]{1,0:T(8,128)(2,1)S(1)}, u32[]{:S(2)}, u32[]{:S(2)}) collective-permute-start(bf16[64,2048]{1,0:T(8,128)(2,1)S(1)} %collective-permute-done.20.refs_3_), channel_id=1, source_target_pairs={{0,14},{1,15},{2,0},{3,1},{4,2},{5,3},{6,4},{7,5},{8,6},{9,7},{10,... | collective-permute-start | bytes 786440 | tf_op jit(solution)/shard_map/ppermute | solution.py:451
  116.4 2.4 %collective-permute-done.14.refs_1_ = bf16[64,2048]{1,0:T(8,128)(2,1)S(1)} collective-permute-done((bf16[64,2048]{1,0:T(8,128)(2,1)S(1)}, bf16[64,2048]{1,0:T(8,128)(2,1)S(1)}, u32[]{:S(2)}, u32[]{:S(2)}) %collective-permute-start.14) | collective-permute-done | bytes 262176 | tf_op jit(solution)/shard_map/ppermute | solution.py:448
  118.8 3.2 %collective-permute-start.18 = (bf16[64,2048]{1,0:T(8,128)(2,1)S(1)}, bf16[64,2048]{1,0:T(8,128)(2,1)S(1)}, u32[]{:S(2)}, u32[]{:S(2)}) collective-permute-start(bf16[64,2048]{1,0:T(8,128)(2,1)S(1)} %collective-permute-done.17.refs_2_), channel_id=1, source_target_pairs={{0,14},{1,15},{2,0},{3,1},{4,2},{5,3},{6,4},{7,5},{8,6},{9,7},{10,... | collective-permute-start | bytes 786440 | tf_op jit(solution)/shard_map/ppermute | solution.py:451
  122.1 2.4 %collective-permute-done.12.refs_0_ = bf16[64,2048]{1,0:T(8,128)(2,1)S(1)} collective-permute-done((bf16[64,2048]{1,0:T(8,128)(2,1)S(1)}, bf16[64,2048]{1,0:T(8,128)(2,1)S(1)}, u32[]{:S(2)}, u32[]{:S(2)}) %collective-permute-start.12) | collective-permute-done | bytes 262176 | tf_op jit(solution)/shard_map/ppermute | solution.py:448
  124.4 3.2 %collective-permute-start.27 = (bf16[64,2048]{1,0:T(8,128)(2,1)S(1)}, bf16[64,2048]{1,0:T(8,128)(2,1)S(1)}, u32[]{:S(2)}, u32[]{:S(2)}) collective-permute-start(bf16[64,2048]{1,0:T(8,128)(2,1)S(1)} %collective-permute-done.21.refs_3_), channel_id=1, source_target_pairs={{0,14},{1,15},{2,0},{3,1},{4,2},{5,3},{6,4},{7,5},{8,6},{9,7},{10,... | collective-permute-start | bytes 786440 | tf_op jit(solution)/shard_map/ppermute | solution.py:451
  127.7 2.4 %collective-permute-done.15.refs_1_ = bf16[64,2048]{1,0:T(8,128)(2,1)S(1)} collective-permute-done((bf16[64,2048]{1,0:T(8,128)(2,1)S(1)}, bf16[64,2048]{1,0:T(8,128)(2,1)S(1)}, u32[]{:S(2)}, u32[]{:S(2)}) %collective-permute-start.15) | collective-permute-done | bytes 262176 | tf_op jit(solution)/shard_map/ppermute | solution.py:448
  130.1 2.4 %shard_map.131 = (bf16[64,2048]{1,0:T(8,128)(2,1)S(1)}, bf16[64,2048]{1,0:T(8,128)(2,1)S(1)}, bf16[64,2048]{1,0:T(8,128)(2,1)S(1)}, bf16[64,2048]{1,0:T(8,128)(2,1)S(1)}) custom-call(bf16[64,2048]{1,0:T(8,128)(2,1)S(1)} %collective-permute-done.12.refs_0_, bf16[64,2048]{1,0:T(8,128)(2,1)S(1)} %collective-permute-done.15.refs_1_, ...), custom_call_target="tpu_custom_call" | custom-call | flops 1610612736 | bytes 6291456 | tf_op jit(solution)/shard_map/pallas_call | solution.py:431
  132.6 2.3 %collective-permute-done.26.refs_0_ = bf16[64,2048]{1,0:T(8,128)(2,1)S(1)} collective-permute-done((bf16[64,2048]{1,0:T(8,128)(2,1)S(1)}, bf16[64,2048]{1,0:T(8,128)(2,1)S(1)}, u32[]{:S(2)}, u32[]{:S(2)}) %collective-permute-start.26) | collective-permute-done | bytes 262176 | tf_op jit(solution)/shard_map/ppermute | solution.py:448
  136.0 2.1 %collective-permute-start.32 = (bf16[64,2048]{1,0:T(8,128)(2,1)S(1)}, bf16[64,2048]{1,0:T(8,128)(2,1)S(1)}, u32[]{:S(2)}, u32[]{:S(2)}) collective-permute-start(bf16[64,2048]{1,0:T(8,128)(2,1)S(1)} %get-tuple-element.78), channel_id=1, source_target_pairs={{0,14},{1,15},{2,0},{3,1},{4,2},{5,3},{6,4},{7,5},{8,6},{9,7},{10,... | collective-permute-start | bytes 786440 | tf_op jit(solution)/shard_map/ppermute | solution.py:451
  138.1 3.2 %collective-permute-start.23 = (bf16[64,2048]{1,0:T(8,128)(2,1)S(1)}, bf16[64,2048]{1,0:T(8,128)(2,1)S(1)}, u32[]{:S(2)}, u32[]{:S(2)}) collective-permute-start(bf16[64,2048]{1,0:T(8,128)(2,1)S(1)} %get-tuple-element.70), channel_id=1, source_target_pairs={{0,14},{1,15},{2,0},{3,1},{4,2},{5,3},{6,4},{7,5},{8,6},{9,7},{10,... | collective-permute-start | bytes 786440 | tf_op jit(solution)/shard_map/ppermute | solution.py:451
  141.3 2.4 %shard_map.132 = (bf16[64,2048]{1,0:T(8,128)(2,1)S(1)}, bf16[64,2048]{1,0:T(8,128)(2,1)S(1)}, bf16[64,2048]{1,0:T(8,128)(2,1)S(1)}, bf16[64,2048]{1,0:T(8,128)(2,1)S(1)}) custom-call(bf16[64,2048]{1,0:T(8,128)(2,1)S(1)} %collective-permute-done.11.refs_0_, bf16[64,2048]{1,0:T(8,128)(2,1)S(1)} %collective-permute-done.14.refs_1_, ...), custom_call_target="tpu_custom_call" | custom-call | flops 1610612736 | bytes 6291456 | tf_op jit(solution)/shard_map/pallas_call | solution.py:431
  143.7 3.6 %shard_map.133 = (bf16[64,2048]{1,0:T(8,128)(2,1)S(1)}, bf16[64,2048]{1,0:T(8,128)(2,1)S(1)}, bf16[64,2048]{1,0:T(8,128)(2,1)S(1)}, bf16[64,2048]{1,0:T(8,128)(2...) custom-call(bf16[64,2048]{1,0:T(8,128)(2,1)S(1)} %get-tuple-element.88.refs_0_, ...), custom_call_target="tpu_custom_call" | custom-call | flops 2415919104 | bytes 6291456 | tf_op jit(solution)/shard_map/pallas_call | solution.py:431
  147.8 3.3 %collective-permute-start.33 = (bf16[64,2048]{1,0:T(8,128)(2,1)S(1)}, bf16[64,2048]{1,0:T(8,128)(2,1)S(1)}, u32[]{:S(2)}, u32[]{:S(2)}) collective-permute-start(bf16[64,2048]{1,0:T(8,128)(2,1)S(1)} %add_convert_fusion.5), channel_id=1, source_target_pairs={{0,14},{1,15},{2,0},{3,1},{4,2},{5,3},{6,4},{7,5},{8,6},{9,7},{10,... | collective-permute-start | bytes 786440 | tf_op jit(solution)/shard_map/ppermute | solution.py:451
  151.3 3.3 %collective-permute-start.24 = (bf16[64,2048]{1,0:T(8,128)(2,1)S(1)}, bf16[64,2048]{1,0:T(8,128)(2,1)S(1)}, u32[]{:S(2)}, u32[]{:S(2)}) collective-permute-start(bf16[64,2048]{1,0:T(8,128)(2,1)S(1)} %add_convert_fusion.11), channel_id=1, source_target_pairs={{0,14},{1,15},{2,0},{3,1},{4,2},{5,3},{6,4},{7,5},{8,6},{9,7},{10,... | collective-permute-start | bytes 786440 | tf_op jit(solution)/shard_map/ppermute | solution.py:451
  154.6 3.5 %collective-permute-done.37 = bf16[64,2048]{1,0:T(8,128)(2,1)S(1)} collective-permute-done((bf16[64,2048]{1,0:T(8,128)(2,1)S(1)}, bf16[64,2048]{1,0:T(8,128)(2,1)S(1)}, u32[]{:S(2)}, u32[]{:S(2)}) %collective-permute-start.37) | collective-permute-done | bytes 262176 | tf_op jit(solution)/shard_map/ppermute | solution.py:448
  158.3 3.3 %collective-permute-start.34 = (bf16[64,2048]{1,0:T(8,128)(2,1)S(1)}, bf16[64,2048]{1,0:T(8,128)(2,1)S(1)}, u32[]{:S(2)}, u32[]{:S(2)}) collective-permute-start(bf16[64,2048]{1,0:T(8,128)(2,1)S(1)} %add_convert_fusion.4), channel_id=1, source_target_pairs={{0,14},{1,15},{2,0},{3,1},{4,2},{5,3},{6,4},{7,5},{8,6},{9,7},{10,... | collective-permute-start | bytes 786440 | tf_op jit(solution)/shard_map/ppermute | solution.py:451
  161.6 2.1 %collective-permute-done.29 = bf16[64,2048]{1,0:T(8,128)(2,1)S(1)} collective-permute-done((bf16[64,2048]{1,0:T(8,128)(2,1)S(1)}, bf16[64,2048]{1,0:T(8,128)(2,1)S(1)}, u32[]{:S(2)}, u32[]{:S(2)}) %collective-permute-start.29) | collective-permute-done | bytes 262176 | tf_op jit(solution)/shard_map/ppermute | solution.py:448
  163.9 3.3 %collective-permute-start.25 = (bf16[64,2048]{1,0:T(8,128)(2,1)S(1)}, bf16[64,2048]{1,0:T(8,128)(2,1)S(1)}, u32[]{:S(2)}, u32[]{:S(2)}) collective-permute-start(bf16[64,2048]{1,0:T(8,128)(2,1)S(1)} %add_convert_fusion.10), channel_id=1, source_target_pairs={{0,14},{1,15},{2,0},{3,1},{4,2},{5,3},{6,4},{7,5},{8,6},{9,7},{10,... | collective-permute-start | bytes 786440 | tf_op jit(solution)/shard_map/ppermute | solution.py:451
  167.2 1.8 collective-permute-done.34
  169.0 3.8 %collective-permute-start.35 = (bf16[64,2048]{1,0:T(8,128)(2,1)S(1)}, bf16[64,2048]{1,0:T(8,128)(2,1)S(1)}, u32[]{:S(2)}, u32[]{:S(2)}) collective-permute-start(bf16[64,2048]{1,0:T(8,128)(2,1)S(1)} %add_convert_fusion.3), channel_id=1, source_target_pairs={{0,14},{1,15},{2,0},{3,1},{4,2},{5,3},{6,4},{7,5},{8,6},{9,7},{10,... | collective-permute-start | bytes 786440 | tf_op jit(solution)/shard_map/ppermute | solution.py:451
  173.0 3.7 %collective-permute-done.35 = bf16[64,2048]{1,0:T(8,128)(2,1)S(1)} collective-permute-done((bf16[64,2048]{1,0:T(8,128)(2,1)S(1)}, bf16[64,2048]{1,0:T(8,128)(2,1)S(1)}, u32[]{:S(2)}, u32[]{:S(2)}) %collective-permute-start.35) | collective-permute-done | bytes 262176 | tf_op jit(solution)/shard_map/ppermute | solution.py:451
  176.8 3.7 %collective-permute-done.31 = bf16[64,2048]{1,0:T(8,128)(2,1)S(1)} collective-permute-done((bf16[64,2048]{1,0:T(8,128)(2,1)S(1)}, bf16[64,2048]{1,0:T(8,128)(2,1)S(1)}, u32[]{:S(2)}, u32[]{:S(2)}) %collective-permute-start.31) | collective-permute-done | bytes 262176 | tf_op jit(solution)/shard_map/ppermute | solution.py:448
  180.7 13.5 %all_to_all.17 = bf16[16,8,2048]{2,1,0:T(8,128)(2,1)S(1)} all-to-all(bf16[16,8,2048]{2,1,0:T(8,128)(2,1)S(1)} %maximum_bitcast_fusion), channel_id=1, replica_groups=mesh['sp'=16,'tp'=16] {'sp'}, dimensions={0} | all-to-all | bytes 1048576 | tf_op jit(solution)/shard_map/all_to_all | solution.py:617
  (76 shorter events, 12.5 us)
Async XLA Ops:
  1.2 19.0 %collective-permute-start.1 = (bf16[544,256]{1,0:T(8,128)(2,1)S(1)}, bf16[544,256]{1,0:T(8,128)(2,1)S(1)}, u32[]{:S(2)}, u32[]{:S(2)}) collective-permute-start(bf16[544,256]{1,0:T(8,128)(2,1)S(1)} %get-tuple-element.47.refs_4_), channel_id=1, source_target_pairs={{0,16},{16,32},{32,48},{48,0},{64,80},{80,96},{96,112},{112,64},{1... | collective-permute-start | bytes 835592 | tf_op jit(solution)/shard_map/ppermute | solution.py:317
  4.6 15.6 %collective-permute-start.3 = (bf16[544,256]{1,0:T(8,128)(2,1)S(1)}, bf16[544,256]{1,0:T(8,128)(2,1)S(1)}, u32[]{:S(2)}, u32[]{:S(2)}) collective-permute-start(bf16[544,256]{1,0:T(8,128)(2,1)S(1)} %get-tuple-element.47.refs_4_), channel_id=1, source_target_pairs={{0,48},{16,0},{32,16},{48,32},{64,112},{80,64},{96,80},{112,96},{1... | collective-permute-start | bytes 835592 | tf_op jit(solution)/shard_map/ppermute | solution.py:317
  7.3 7.0 %collective-permute-start = (bf16[144,512]{1,0:T(8,128)(2,1)S(1)}, bf16[144,512]{1,0:T(8,128)(2,1)S(1)}, u32[]{:S(2)}, u32[]{:S(2)}) collective-permute-start(bf16[144,512]{1,0:T(8,128)(2,1)S(1)} %get-tuple-element.46.refs_3_.refs_1_), channel_id=1, source_target_pairs={{64,0},{80,16},{96,32},{112,48},{128,64},{144,80},{160,96},{176,11... | collective-permute-start | bytes 442376 | tf_op jit(solution)/shard_map/ppermute | solution.py:317
  8.6 11.6 %collective-permute-start.5 = (bf16[144,512]{1,0:T(8,128)(2,1)S(1)}, bf16[144,512]{1,0:T(8,128)(2,1)S(1)}, u32[]{:S(2)}, u32[]{:S(2)}) collective-permute-start(bf16[144,512]{1,0:T(8,128)(2,1)S(1)} %get-tuple-element.46.refs_3_.refs_1_), channel_id=1, source_target_pairs={{192,0},{208,16},{224,32},{240,48},{193,1},{209,17},{225,33},{241,... | collective-permute-start | bytes 442376 | tf_op jit(solution)/shard_map/ppermute | solution.py:317
  9.9 10.3 %collective-permute-start.6 = (bf16[144,512]{1,0:T(8,128)(2,1)S(1)}, bf16[144,512]{1,0:T(8,128)(2,1)S(1)}, u32[]{:S(2)}, u32[]{:S(2)}) collective-permute-start(bf16[144,512]{1,0:T(8,128)(2,1)S(1)} %get-tuple-element.46.refs_3_.refs_1_), channel_id=1, source_target_pairs={{128,0},{144,16},{160,32},{176,48},{192,64},{208,80},{224,96},{240... | collective-permute-start | bytes 442376 | tf_op jit(solution)/shard_map/ppermute | solution.py:317
  20.2 48.7 %slice-start = ((s8[8388608]{0:T(1024)(128)(4,1)}), s8[4194304]{0:T(1024)(128)(4,1)S(1)}, s32[]{:S(2)}) async-start(s8[8388608]{0:T(1024)(128)(4,1)} %bitcast.17), calls=%async_computation.3 | async-start | bytes 8388608
  28.1 40.9 %slice-start.1 = ((s8[8388608]{0:T(1024)(128)(4,1)}), s8[4194304]{0:T(1024)(128)(4,1)S(1)}, s32[]{:S(2)}) async-start(s8[8388608]{0:T(1024)(128)(4,1)} %bitcast.17), calls=%async_computation.4 | async-start | bytes 8388608
  30.2 21.4 %copy-start.4 = (f32[128]{0:T(128)S(1)}, f32[128]{0:T(128)}, u32[]{:S(2)}) copy-start(f32[128]{0:T(128)} %param.17) | copy-start | bytes 1540
  30.2 38.8 %copy-start = (bf16[32,2048]{1,0:T(8,128)(2,1)S(1)}, bf16[32,2048]{1,0:T(8,128)(2,1)}, u32[]{:S(2)}) copy-start(bf16[32,2048]{1,0:T(8,128)(2,1)} %stream.1) | copy-start | bytes 393220
  30.2 38.8 %copy-start.1 = (f32[2048]{0:T(1024)S(1)}, f32[2048]{0:T(1024)}, u32[]{:S(2)}) copy-start(f32[2048]{0:T(1024)} %param.20) | copy-start | bytes 24580
  30.2 38.8 %copy-start.2 = (s32[32,2]{0,1:T(2,128)S(1)}, s32[32,2]{0,1:T(2,128)}, u32[]{:S(2)}) copy-start(s32[32,2]{0,1:T(2,128)} %param.21) | copy-start | bytes 772
  30.2 38.8 %copy-start.3 = (f32[32,2]{0,1:T(2,128)S(1)}, f32[32,2]{0,1:T(2,128)}, u32[]{:S(2)}) copy-start(f32[32,2]{0,1:T(2,128)} %param.22) | copy-start | bytes 772
  30.2 99.8 %collective-permute-start.22 = (bf16[6144,256]{1,0:T(8,128)(2,1)S(1)}, bf16[6144,256]{1,0:T(8,128)(2,1)S(1)}, u32[]{:S(2)}, u32[]{:S(2)}) collective-permute-start(bf16[6144,256]{1,0:T(8,128)(2,1)S(1)} %stage_weights.1.refs_4_.refs_6_.refs_2_), channel_id=1, source_target_pairs={{0,1},{1,0},{2,3},{3,2},{4,5},{5,4},{6,7},{7,6},{8,9},{9,8},{10,11... | collective-permute-start | bytes 9437192 | tf_op jit(solution)/shard_map/ppermute | solution.py:605
  30.3 8.0 %collective-permute-start.2 = (bf16[272,256]{1,0:T(8,128)(2,1)S(1)}, bf16[272,256]{1,0:T(8,128)(2,1)S(1)}, u32[]{:S(2)}, u32[]{:S(2)}) collective-permute-start(bf16[272,256]{1,0:T(8,128)(2,1)S(1)} %slice.24), channel_id=1, source_target_pairs={{0,16},{16,32},{32,48},{48,0},{64,80},{80,96},{96,112},{112,64},{1... | collective-permute-start | bytes 417800 | tf_op jit(solution)/shard_map/ppermute | solution.py:317
  33.9 7.7 %collective-permute-start.4 = (bf16[272,256]{1,0:T(8,128)(2,1)S(1)}, bf16[272,256]{1,0:T(8,128)(2,1)S(1)}, u32[]{:S(2)}, u32[]{:S(2)}) collective-permute-start(bf16[272,256]{1,0:T(8,128)(2,1)S(1)} %slice.25), channel_id=1, source_target_pairs={{0,48},{16,0},{32,16},{48,32},{64,112},{80,64},{96,80},{112,96},{1... | collective-permute-start | bytes 417800 | tf_op jit(solution)/shard_map/ppermute | solution.py:317
  44.2 5.5 %collective-permute-start.7 = (bf16[144,512]{1,0:T(8,128)(2,1)S(1)}, bf16[144,512]{1,0:T(8,128)(2,1)S(1)}, u32[]{:S(2)}, u32[]{:S(2)}) collective-permute-start(bf16[144,512]{1,0:T(8,128)(2,1)S(1)} %get-tuple-element.59), channel_id=1, source_target_pairs={{0,64},{16,80},{32,96},{48,112},{64,128},{80,144},{96,160},{112,17... | collective-permute-start | bytes 442376 | tf_op jit(solution)/shard_map/ppermute | solution.py:317
  45.5 6.0 %collective-permute-start.8 = (bf16[144,512]{1,0:T(8,128)(2,1)S(1)}, bf16[144,512]{1,0:T(8,128)(2,1)S(1)}, u32[]{:S(2)}, u32[]{:S(2)}) collective-permute-start(bf16[144,512]{1,0:T(8,128)(2,1)S(1)} %get-tuple-element.60), channel_id=1, source_target_pairs={{0,128},{16,144},{32,160},{48,176},{64,192},{80,208},{96,224},{112... | collective-permute-start | bytes 442376 | tf_op jit(solution)/shard_map/ppermute | solution.py:317
  46.9 4.7 %collective-permute-start.9 = (bf16[144,512]{1,0:T(8,128)(2,1)S(1)}, bf16[144,512]{1,0:T(8,128)(2,1)S(1)}, u32[]{:S(2)}, u32[]{:S(2)}) collective-permute-start(bf16[144,512]{1,0:T(8,128)(2,1)S(1)} %get-tuple-element.61), channel_id=1, source_target_pairs={{0,192},{16,208},{32,224},{48,240},{1,193},{17,209},{33,225},{49,2... | collective-permute-start | bytes 442376 | tf_op jit(solution)/shard_map/ppermute | solution.py:317
  91.5 10.5 %collective-permute-start.10 = (bf16[64,2048]{1,0:T(8,128)(2,1)S(1)}, bf16[64,2048]{1,0:T(8,128)(2,1)S(1)}, u32[]{:S(2)}, u32[]{:S(2)}) collective-permute-start(bf16[64,2048]{1,0:T(8,128)(2,1)S(1)} %get-tuple-element.88.refs_0_), channel_id=1, source_target_pairs={{0,2},{1,3},{2,4},{3,5},{4,6},{5,7},{6,8},{7,9},{8,10},{9,11},{10,... | collective-permute-start | bytes 786440 | tf_op jit(solution)/shard_map/ppermute | solution.py:448
  92.1 9.8 %collective-permute-start.19 = (bf16[64,2048]{1,0:T(8,128)(2,1)S(1)}, bf16[64,2048]{1,0:T(8,128)(2,1)S(1)}, u32[]{:S(2)}, u32[]{:S(2)}) collective-permute-start(bf16[64,2048]{1,0:T(8,128)(2,1)S(1)} %get-tuple-element.87.refs_1_), channel_id=1, source_target_pairs={{0,14},{1,15},{2,0},{3,1},{4,2},{5,3},{6,4},{7,5},{8,6},{9,7},{10,... | collective-permute-start | bytes 786440 | tf_op jit(solution)/shard_map/ppermute | solution.py:451
  94.8 12.8 %collective-permute-start.13 = (bf16[64,2048]{1,0:T(8,128)(2,1)S(1)}, bf16[64,2048]{1,0:T(8,128)(2,1)S(1)}, u32[]{:S(2)}, u32[]{:S(2)}) collective-permute-start(bf16[64,2048]{1,0:T(8,128)(2,1)S(1)} %get-tuple-element.87.refs_1_), channel_id=1, source_target_pairs={{0,2},{1,3},{2,4},{3,5},{4,6},{5,7},{6,8},{7,9},{8,10},{9,11},{10,... | collective-permute-start | bytes 786440 | tf_op jit(solution)/shard_map/ppermute | solution.py:448
  94.8 12.8 %collective-permute-start.16 = (bf16[64,2048]{1,0:T(8,128)(2,1)S(1)}, bf16[64,2048]{1,0:T(8,128)(2,1)S(1)}, u32[]{:S(2)}, u32[]{:S(2)}) collective-permute-start(bf16[64,2048]{1,0:T(8,128)(2,1)S(1)} %get-tuple-element.88.refs_0_), channel_id=1, source_target_pairs={{0,14},{1,15},{2,0},{3,1},{4,2},{5,3},{6,4},{7,5},{8,6},{9,7},{10,... | collective-permute-start | bytes 786440 | tf_op jit(solution)/shard_map/ppermute | solution.py:451
  102.0 11.2 %collective-permute-start.11 = (bf16[64,2048]{1,0:T(8,128)(2,1)S(1)}, bf16[64,2048]{1,0:T(8,128)(2,1)S(1)}, u32[]{:S(2)}, u32[]{:S(2)}) collective-permute-start(bf16[64,2048]{1,0:T(8,128)(2,1)S(1)} %collective-permute-done.10.refs_2_), channel_id=1, source_target_pairs={{0,2},{1,3},{2,4},{3,5},{4,6},{5,7},{6,8},{7,9},{8,10},{9,11},{10,... | collective-permute-start | bytes 786440 | tf_op jit(solution)/shard_map/ppermute | solution.py:448
  102.0 11.2 %collective-permute-start.20 = (bf16[64,2048]{1,0:T(8,128)(2,1)S(1)}, bf16[64,2048]{1,0:T(8,128)(2,1)S(1)}, u32[]{:S(2)}, u32[]{:S(2)}) collective-permute-start(bf16[64,2048]{1,0:T(8,128)(2,1)S(1)} %collective-permute-done.19.refs_5_), channel_id=1, source_target_pairs={{0,14},{1,15},{2,0},{3,1},{4,2},{5,3},{6,4},{7,5},{8,6},{9,7},{10,... | collective-permute-start | bytes 786440 | tf_op jit(solution)/shard_map/ppermute | solution.py:451
  107.6 11.2 %collective-permute-start.14 = (bf16[64,2048]{1,0:T(8,128)(2,1)S(1)}, bf16[64,2048]{1,0:T(8,128)(2,1)S(1)}, u32[]{:S(2)}, u32[]{:S(2)}) collective-permute-start(bf16[64,2048]{1,0:T(8,128)(2,1)S(1)} %collective-permute-done.13.refs_3_), channel_id=1, source_target_pairs={{0,2},{1,3},{2,4},{3,5},{4,6},{5,7},{6,8},{7,9},{8,10},{9,11},{10,... | collective-permute-start | bytes 786440 | tf_op jit(solution)/shard_map/ppermute | solution.py:448
  107.6 11.2 %collective-permute-start.17 = (bf16[64,2048]{1,0:T(8,128)(2,1)S(1)}, bf16[64,2048]{1,0:T(8,128)(2,1)S(1)}, u32[]{:S(2)}, u32[]{:S(2)}) collective-permute-start(bf16[64,2048]{1,0:T(8,128)(2,1)S(1)} %collective-permute-done.16.refs_4_), channel_id=1, source_target_pairs={{0,14},{1,15},{2,0},{3,1},{4,2},{5,3},{6,4},{7,5},{8,6},{9,7},{10,... | collective-permute-start | bytes 786440 | tf_op jit(solution)/shard_map/ppermute | solution.py:451
  113.2 11.2 %collective-permute-start.12 = (bf16[64,2048]{1,0:T(8,128)(2,1)S(1)}, bf16[64,2048]{1,0:T(8,128)(2,1)S(1)}, u32[]{:S(2)}, u32[]{:S(2)}) collective-permute-start(bf16[64,2048]{1,0:T(8,128)(2,1)S(1)} %collective-permute-done.11.refs_0_), channel_id=1, source_target_pairs={{0,2},{1,3},{2,4},{3,5},{4,6},{5,7},{6,8},{7,9},{8,10},{9,11},{10,... | collective-permute-start | bytes 786440 | tf_op jit(solution)/shard_map/ppermute | solution.py:448
  113.2 11.2 %collective-permute-start.21 = (bf16[64,2048]{1,0:T(8,128)(2,1)S(1)}, bf16[64,2048]{1,0:T(8,128)(2,1)S(1)}, u32[]{:S(2)}, u32[]{:S(2)}) collective-permute-start(bf16[64,2048]{1,0:T(8,128)(2,1)S(1)} %collective-permute-done.20.refs_3_), channel_id=1, source_target_pairs={{0,14},{1,15},{2,0},{3,1},{4,2},{5,3},{6,4},{7,5},{8,6},{9,7},{10,... | collective-permute-start | bytes 786440 | tf_op jit(solution)/shard_map/ppermute | solution.py:451
  118.8 11.2 %collective-permute-start.15 = (bf16[64,2048]{1,0:T(8,128)(2,1)S(1)}, bf16[64,2048]{1,0:T(8,128)(2,1)S(1)}, u32[]{:S(2)}, u32[]{:S(2)}) collective-permute-start(bf16[64,2048]{1,0:T(8,128)(2,1)S(1)} %collective-permute-done.14.refs_1_), channel_id=1, source_target_pairs={{0,2},{1,3},{2,4},{3,5},{4,6},{5,7},{6,8},{7,9},{8,10},{9,11},{10,... | collective-permute-start | bytes 786440 | tf_op jit(solution)/shard_map/ppermute | solution.py:448
  118.8 11.2 %collective-permute-start.18 = (bf16[64,2048]{1,0:T(8,128)(2,1)S(1)}, bf16[64,2048]{1,0:T(8,128)(2,1)S(1)}, u32[]{:S(2)}, u32[]{:S(2)}) collective-permute-start(bf16[64,2048]{1,0:T(8,128)(2,1)S(1)} %collective-permute-done.17.refs_2_), channel_id=1, source_target_pairs={{0,14},{1,15},{2,0},{3,1},{4,2},{5,3},{6,4},{7,5},{8,6},{9,7},{10,... | collective-permute-start | bytes 786440 | tf_op jit(solution)/shard_map/ppermute | solution.py:451
  124.4 10.5 %collective-permute-start.26 = (bf16[64,2048]{1,0:T(8,128)(2,1)S(1)}, bf16[64,2048]{1,0:T(8,128)(2,1)S(1)}, u32[]{:S(2)}, u32[]{:S(2)}) collective-permute-start(bf16[64,2048]{1,0:T(8,128)(2,1)S(1)} %collective-permute-done.12.refs_0_), channel_id=1, source_target_pairs={{0,2},{1,3},{2,4},{3,5},{4,6},{5,7},{6,8},{7,9},{8,10},{9,11},{10,... | collective-permute-start | bytes 786440 | tf_op jit(solution)/shard_map/ppermute | solution.py:448
  124.4 10.5 %collective-permute-start.27 = (bf16[64,2048]{1,0:T(8,128)(2,1)S(1)}, bf16[64,2048]{1,0:T(8,128)(2,1)S(1)}, u32[]{:S(2)}, u32[]{:S(2)}) collective-permute-start(bf16[64,2048]{1,0:T(8,128)(2,1)S(1)} %collective-permute-done.21.refs_3_), channel_id=1, source_target_pairs={{0,14},{1,15},{2,0},{3,1},{4,2},{5,3},{6,4},{7,5},{8,6},{9,7},{10,... | collective-permute-start | bytes 786440 | tf_op jit(solution)/shard_map/ppermute | solution.py:451
  132.4 14.8 %collective-permute-start.36 = (bf16[64,2048]{1,0:T(8,128)(2,1)S(1)}, bf16[64,2048]{1,0:T(8,128)(2,1)S(1)}, u32[]{:S(2)}, u32[]{:S(2)}) collective-permute-start(bf16[64,2048]{1,0:T(8,128)(2,1)S(1)} %get-tuple-element.82), channel_id=1, source_target_pairs={{0,2},{1,3},{2,4},{3,5},{4,6},{5,7},{6,8},{7,9},{8,10},{9,11},{10,... | collective-permute-start | bytes 786440 | tf_op jit(solution)/shard_map/ppermute | solution.py:448
  136.0 11.7 %collective-permute-start.32 = (bf16[64,2048]{1,0:T(8,128)(2,1)S(1)}, bf16[64,2048]{1,0:T(8,128)(2,1)S(1)}, u32[]{:S(2)}, u32[]{:S(2)}) collective-permute-start(bf16[64,2048]{1,0:T(8,128)(2,1)S(1)} %get-tuple-element.78), channel_id=1, source_target_pairs={{0,14},{1,15},{2,0},{3,1},{4,2},{5,3},{6,4},{7,5},{8,6},{9,7},{10,... | collective-permute-start | bytes 786440 | tf_op jit(solution)/shard_map/ppermute | solution.py:451
  138.1 13.0 %collective-permute-start.28 = (bf16[64,2048]{1,0:T(8,128)(2,1)S(1)}, bf16[64,2048]{1,0:T(8,128)(2,1)S(1)}, u32[]{:S(2)}, u32[]{:S(2)}) collective-permute-start(bf16[64,2048]{1,0:T(8,128)(2,1)S(1)} %get-tuple-element.73), channel_id=1, source_target_pairs={{0,2},{1,3},{2,4},{3,5},{4,6},{5,7},{6,8},{7,9},{8,10},{9,11},{10,... | collective-permute-start | bytes 786440 | tf_op jit(solution)/shard_map/ppermute | solution.py:448
  138.1 13.1 %collective-permute-start.23 = (bf16[64,2048]{1,0:T(8,128)(2,1)S(1)}, bf16[64,2048]{1,0:T(8,128)(2,1)S(1)}, u32[]{:S(2)}, u32[]{:S(2)}) collective-permute-start(bf16[64,2048]{1,0:T(8,128)(2,1)S(1)} %get-tuple-element.70), channel_id=1, source_target_pairs={{0,14},{1,15},{2,0},{3,1},{4,2},{5,3},{6,4},{7,5},{8,6},{9,7},{10,... | collective-permute-start | bytes 786440 | tf_op jit(solution)/shard_map/ppermute | solution.py:451
  147.4 10.7 %collective-permute-start.37 = (bf16[64,2048]{1,0:T(8,128)(2,1)S(1)}, bf16[64,2048]{1,0:T(8,128)(2,1)S(1)}, u32[]{:S(2)}, u32[]{:S(2)}) collective-permute-start(bf16[64,2048]{1,0:T(8,128)(2,1)S(1)} %add_convert_fusion.2), channel_id=1, source_target_pairs={{0,2},{1,3},{2,4},{3,5},{4,6},{5,7},{6,8},{7,9},{8,10},{9,11},{10,... | collective-permute-start | bytes 786440 | tf_op jit(solution)/shard_map/ppermute | solution.py:448
  147.8 10.5 %collective-permute-start.33 = (bf16[64,2048]{1,0:T(8,128)(2,1)S(1)}, bf16[64,2048]{1,0:T(8,128)(2,1)S(1)}, u32[]{:S(2)}, u32[]{:S(2)}) collective-permute-start(bf16[64,2048]{1,0:T(8,128)(2,1)S(1)} %add_convert_fusion.5), channel_id=1, source_target_pairs={{0,14},{1,15},{2,0},{3,1},{4,2},{5,3},{6,4},{7,5},{8,6},{9,7},{10,... | collective-permute-start | bytes 786440 | tf_op jit(solution)/shard_map/ppermute | solution.py:451
  151.1 12.6 %collective-permute-start.29 = (bf16[64,2048]{1,0:T(8,128)(2,1)S(1)}, bf16[64,2048]{1,0:T(8,128)(2,1)S(1)}, u32[]{:S(2)}, u32[]{:S(2)}) collective-permute-start(bf16[64,2048]{1,0:T(8,128)(2,1)S(1)} %add_convert_fusion.9), channel_id=1, source_target_pairs={{0,2},{1,3},{2,4},{3,5},{4,6},{5,7},{6,8},{7,9},{8,10},{9,11},{10,... | collective-permute-start | bytes 786440 | tf_op jit(solution)/shard_map/ppermute | solution.py:448
  151.3 12.5 %collective-permute-start.24 = (bf16[64,2048]{1,0:T(8,128)(2,1)S(1)}, bf16[64,2048]{1,0:T(8,128)(2,1)S(1)}, u32[]{:S(2)}, u32[]{:S(2)}) collective-permute-start(bf16[64,2048]{1,0:T(8,128)(2,1)S(1)} %add_convert_fusion.11), channel_id=1, source_target_pairs={{0,14},{1,15},{2,0},{3,1},{4,2},{5,3},{6,4},{7,5},{8,6},{9,7},{10,... | collective-permute-start | bytes 786440 | tf_op jit(solution)/shard_map/ppermute | solution.py:451
  158.1 14.9 %collective-permute-start.38 = (bf16[64,2048]{1,0:T(8,128)(2,1)S(1)}, bf16[64,2048]{1,0:T(8,128)(2,1)S(1)}, u32[]{:S(2)}, u32[]{:S(2)}) collective-permute-start(bf16[64,2048]{1,0:T(8,128)(2,1)S(1)} %add_convert_fusion.1), channel_id=1, source_target_pairs={{0,2},{1,3},{2,4},{3,5},{4,6},{5,7},{6,8},{7,9},{8,10},{9,11},{10,... | collective-permute-start | bytes 786440 | tf_op jit(solution)/shard_map/ppermute | solution.py:448
  158.3 10.7 %collective-permute-start.34 = (bf16[64,2048]{1,0:T(8,128)(2,1)S(1)}, bf16[64,2048]{1,0:T(8,128)(2,1)S(1)}, u32[]{:S(2)}, u32[]{:S(2)}) collective-permute-start(bf16[64,2048]{1,0:T(8,128)(2,1)S(1)} %add_convert_fusion.4), channel_id=1, source_target_pairs={{0,14},{1,15},{2,0},{3,1},{4,2},{5,3},{6,4},{7,5},{8,6},{9,7},{10,... | collective-permute-start | bytes 786440 | tf_op jit(solution)/shard_map/ppermute | solution.py:451
  163.7 9.1 %collective-permute-start.30 = (bf16[64,2048]{1,0:T(8,128)(2,1)S(1)}, bf16[64,2048]{1,0:T(8,128)(2,1)S(1)}, u32[]{:S(2)}, u32[]{:S(2)}) collective-permute-start(bf16[64,2048]{1,0:T(8,128)(2,1)S(1)} %add_convert_fusion.8), channel_id=1, source_target_pairs={{0,2},{1,3},{2,4},{3,5},{4,6},{5,7},{6,8},{7,9},{8,10},{9,11},{10,... | collective-permute-start | bytes 786440 | tf_op jit(solution)/shard_map/ppermute | solution.py:448
  163.9 12.9 %collective-permute-start.25 = (bf16[64,2048]{1,0:T(8,128)(2,1)S(1)}, bf16[64,2048]{1,0:T(8,128)(2,1)S(1)}, u32[]{:S(2)}, u32[]{:S(2)}) collective-permute-start(bf16[64,2048]{1,0:T(8,128)(2,1)S(1)} %add_convert_fusion.10), channel_id=1, source_target_pairs={{0,14},{1,15},{2,0},{3,1},{4,2},{5,3},{6,4},{7,5},{8,6},{9,7},{10,... | collective-permute-start | bytes 786440 | tf_op jit(solution)/shard_map/ppermute | solution.py:451
  169.0 7.7 %collective-permute-start.35 = (bf16[64,2048]{1,0:T(8,128)(2,1)S(1)}, bf16[64,2048]{1,0:T(8,128)(2,1)S(1)}, u32[]{:S(2)}, u32[]{:S(2)}) collective-permute-start(bf16[64,2048]{1,0:T(8,128)(2,1)S(1)} %add_convert_fusion.3), channel_id=1, source_target_pairs={{0,14},{1,15},{2,0},{3,1},{4,2},{5,3},{6,4},{7,5},{8,6},{9,7},{10,... | collective-permute-start | bytes 786440 | tf_op jit(solution)/shard_map/ppermute | solution.py:451
  172.9 7.7 %collective-permute-start.31 = (bf16[64,2048]{1,0:T(8,128)(2,1)S(1)}, bf16[64,2048]{1,0:T(8,128)(2,1)S(1)}, u32[]{:S(2)}, u32[]{:S(2)}) collective-permute-start(bf16[64,2048]{1,0:T(8,128)(2,1)S(1)} %add_convert_fusion.7), channel_id=1, source_target_pairs={{0,2},{1,3},{2,4},{3,5},{4,6},{5,7},{6,8},{7,9},{8,10},{9,11},{10,... | collective-permute-start | bytes 786440 | tf_op jit(solution)/shard_map/ppermute | solution.py:448

commit v5 on v2

--- a/solution.py
+++ b/solution.py
@@ -155,7 +155,7 @@
 def nth_state(state, i):
     found = []
     for ref in state:
-        rows = ref.shape[0] // 2
+        rows = ref.shape[0] // 3
         found.append(ref.at[pl.ds(pl.multiple_of(i * rows, 8), rows)])
     return found
 
@@ -205,12 +205,12 @@
     out[HD:PACK, :] = block.astype(jnp.bfloat16)
 
 
-def distant_kernel(*refs):
-    packs, keys, states = refs[:2], refs[2:5], refs[5:8]
-    stack, keys_wide, query_wide = refs[8:]
+def near_kernel(*refs):
+    packs, keys, states = refs[:3], refs[3:6], refs[6:9]
+    stack, keys_wide, query_wide = refs[9:]
     own_y = lax.axis_index("sp") >> 2
 
-    @pl.when(own_y < 2)
+    @pl.when(own_y < 3)
     def _():
         load_blocks(stack, keys_wide, keys)
 
@@ -225,22 +225,23 @@
 
         return carry
 
-    lax.fori_loop(0, 2, each, 0)
-
-
-def distant_end_kernel(*refs):
-    packs, far, states, outs = refs[:2], refs[2:4], refs[4:7], refs[7:9]
-    state, (stack, keys_wide, query_wide) = refs[9:12], refs[12:]
+    lax.fori_loop(0, 3, each, 0)
+
+
+def end_kernel(*refs, first, count):
+    packs, far, states = refs[:count], refs[count : count + 2], refs[count + 2 : count + 5]
+    outs = refs[count + 5 : 2 * count + 5]
+    state, (stack, keys_wide, query_wide) = refs[-6:-3], refs[-3:]
     own_y = lax.axis_index("sp") >> 2
 
-    @pl.when(own_y < 2)
+    @pl.when(own_y < first + count)
     def _():
         load_blocks(stack, keys_wide, far)
 
     def each(i, carry):
-        @pl.when(own_y <= i)
+        @pl.when(own_y <= first + i)
         def _():
-            for into, came in zip(state, nth_state(states, i)):
+            for into, came in zip(state, nth_state(states, first + i)):
                 into[...] = came[...]
             for at, pack in enumerate(packs):
                 pl.when(i == at)(partial(load_query, query_wide, pack))
@@ -250,20 +251,7 @@
 
         return carry
 
-    lax.fori_loop(0, 2, each, 0)
-
-
-def next_kernel(*refs):
-    pack, keys, out, state = refs[0], refs[1:6], refs[6], refs[7:10]
-    stack, keys_wide, query_wide = refs[10:]
-
-    @pl.when(lax.axis_index("sp") < 12)
-    def _():
-        load_blocks(stack, keys_wide, keys)
-        load_query(query_wide, pack)
-        clear(state)
-        fold_blocks(query_wide, state, stack, keys_wide, 0, 4)
-        pack_result(state, out)
+    lax.fori_loop(0, count, each, 0)
 
 
 def own_kernel(*refs):
@@ -344,23 +332,27 @@
 
     narrow = ((8, tok_count), jnp.float32)
     state = [narrow, narrow, ((HD, tok_count), jnp.float32)]
-    both = [((2 * shape[0], tok_count), kind) for shape, kind in state]
+    all_states = [((3 * shape[0], tok_count), kind) for shape, kind in state]
     result = ((PACK, tok_count), jnp.bfloat16)
 
     def loaded(count):
         shapes = (count * BLOCK, 2 * HD), (count * 2 * KEYS, 2 * HD), (2 * HD, tok_count)
         return [(shape, jnp.bfloat16) for shape in shapes]
 
-    near = attend(distant_kernel, [pack3, pack2, keys_own, low, high], both, loaded(3), 6)
-    far_a, far_b, near = lax.optimization_barrier((far_a, far_b, near))
-    part3, part2 = attend(
-        distant_end_kernel, [pack3, pack2, far_a, far_b, *near], [result] * 2, state + loaded(1), 2
-    )
-    part3, part2, pack1 = lax.optimization_barrier((part3, part2, pack1))
+    packs = [pack3, pack2, pack1]
+    near = attend(near_kernel, [*packs, keys_own, low, high], all_states, loaded(3), 9)
+
+    def end(first, count):
+        operands = [*packs[first : first + count], far_a, far_b, *near]
+        kernel = partial(end_kernel, first=first, count=count)
+        return attend(kernel, operands, [result] * count, state + loaded(1), count)
+
+    part3, part2 = end(0, 2)
+    part3, part2, near = lax.optimization_barrier((part3, part2, near))
     back3 = shift(part3, -1, 0, lambda y, x: y == 3)
     back2 = shift(part2, 2, 0, lambda y, x: y > 1)
+    (part1,) = end(2, 1)
     keys = [keys_own, low, high, far_a, far_b]
-    (part1,) = attend(next_kernel, [pack1, *keys], [result], state + loaded(4), 4)
     part1, own_pack, keys, weights = lax.optimization_barrier((part1, own_pack, keys, weights))
     back1 = shift(part1, 1, 0, lambda y, x: y > 0)
     own_state = attend(own_kernel, [own_pack, *keys], state, loaded(4), 4)

time: 185 us -> 183 us (0.989)
  starting transfers between devices: 69.2 us -> 66.4 us
  waiting for transfers between devices: 36.1 us -> 38.2 us
    ppermute x10, starting transfers between devices: 23.6 us -> 20.6 us  [shift(): return lax.ppermute(array, 'sp', sp_perm(dy, dx, needed))]
    ppermute x10, waiting for transfers between devices: 3.12 us -> 5.25 us  [shift(): return lax.ppermute(array, 'sp', sp_perm(dy, dx, needed))]
  transfers between devices with their start and end apart: 39 -> 39, of which waited for: 15 -> 16; matrix products, arithmetic and copies ran while one was open for 0% -> 0% of each run, Pallas kernels for 11% -> 11%
where the time goes in v5:
time: 183 us
  starting transfers between devices  66.4 us (36%)
  blocking collectives  49.5 us (27%)
  waiting for transfers between devices  38.2 us (21%)
  Pallas kernels  27.3 us (15%)
    ppermute x14, starting transfers between devices, down(): return lax.ppermute(array, 'tp', z_perm(-1))  44.2 us
    ppermute x14, waiting for transfers between devices, up(): return lax.ppermute(array, 'tp', z_perm(1))  27.4 us
    ppermute x10, starting transfers between devices, shift(): return lax.ppermute(array, 'sp', sp_perm(dy, dx, needed))  20.6 us
    all_to_all x1, blocking collectives, on_device(): lax.all_to_all(outgoing, 'sp', split_axis=0, concat_axis=0, tiled=True)  19 us
    all_to_all x1, blocking collectives, on_device(): heads = lax.all_to_all(heads, 'tp', split_axis=0, concat_axis=0, tiled=True)  17 us
    all_to_all x1, blocking collectives, on_device(): lax.all_to_all(expert_out, 'sp', split_axis=0, concat_axis=0, tiled=True)  13.5 us
    pallas_call x5, Pallas kernels, attend(): pl.pallas_call(kernel, out_shape=tuple((jax.ShapeDtypeStruct(*out) for ou...  10.7 us
    pallas_call x4, Pallas kernels, expert_rows(): pl.pallas_call(partial(expert_kernel, count=count), out_shape=tuple((jax....  9.44 us
  transfers between devices with their start and end apart: 39, of which 16 were waited for; matrix products, arithmetic and copies ran while one was open for 0% of the time, Pallas kernels for 11%

profile of v5, /device:TPU:2, one launch (start us, length us, event | category | flops | bytes accessed | tf_op | source)
XLA Modules:
  0.0 182.9 jit_solution(4790841468836493213)
XLA Ops:
  1.2 3.4 %collective-permute-start.1 = (bf16[544,256]{1,0:T(8,128)(2,1)S(1)}, bf16[544,256]{1,0:T(8,128)(2,1)S(1)}, u32[]{:S(2)}, u32[]{:S(2)}) collective-permute-start(bf16[544,256]{1,0:T(8,128)(2,1)S(1)} %get-tuple-element.63.refs_3_.refs_1_), channel_id=1, source_target_pairs={{0,16},{16,32},{32,48},{48,0},{64,80},{80,96},{96,112},{112,64},{1... | collective-permute-start | bytes 835592 | tf_op jit(solution)/shard_map/ppermute | solution.py:322
  4.6 2.7 %collective-permute-start.3 = (bf16[544,256]{1,0:T(8,128)(2,1)S(1)}, bf16[544,256]{1,0:T(8,128)(2,1)S(1)}, u32[]{:S(2)}, u32[]{:S(2)}) collective-permute-start(bf16[544,256]{1,0:T(8,128)(2,1)S(1)} %get-tuple-element.63.refs_3_.refs_1_), channel_id=1, source_target_pairs={{0,48},{16,0},{32,16},{48,32},{64,112},{80,64},{96,80},{112,96},{1... | collective-permute-start | bytes 835592 | tf_op jit(solution)/shard_map/ppermute | solution.py:322
  7.3 1.3 collective-permute-start
  8.6 1.3 collective-permute-start.5
  11.5 3.4 %collective-permute-start.2 = (bf16[272,256]{1,0:T(8,128)(2,1)S(1)}, bf16[272,256]{1,0:T(8,128)(2,1)S(1)}, u32[]{:S(2)}, u32[]{:S(2)}) collective-permute-start(bf16[272,256]{1,0:T(8,128)(2,1)S(1)} %slice.24), channel_id=1, source_target_pairs={{0,16},{16,32},{32,48},{48,0},{64,80},{80,96},{96,112},{112,64},{1... | collective-permute-start | bytes 417800 | tf_op jit(solution)/shard_map/ppermute | solution.py:322
  15.0 3.4 %collective-permute-start.4 = (bf16[272,256]{1,0:T(8,128)(2,1)S(1)}, bf16[272,256]{1,0:T(8,128)(2,1)S(1)}, u32[]{:S(2)}, u32[]{:S(2)}) collective-permute-start(bf16[272,256]{1,0:T(8,128)(2,1)S(1)} %slice.25), channel_id=1, source_target_pairs={{0,48},{16,0},{32,16},{48,32},{64,112},{80,64},{96,80},{112,96},{1... | collective-permute-start | bytes 417800 | tf_op jit(solution)/shard_map/ppermute | solution.py:322
  18.3 1.9 %collective-permute-done.5.refs_0_ = bf16[144,512]{1,0:T(8,128)(2,1)S(1)} collective-permute-done((bf16[144,512]{1,0:T(8,128)(2,1)S(1)}, bf16[144,512]{1,0:T(8,128)(2,1)S(1)}, u32[]{:S(2)}, u32[]{:S(2)}) %collective-permute-start.5) | collective-permute-done | bytes 147488 | tf_op jit(solution)/shard_map/ppermute | solution.py:322
  20.2 6.5 %shard_map.127 = (f32[24,512]{1,0:T(8,128)S(1)}, f32[24,512]{1,0:T(8,128)S(1)}, f32[384,512]{1,0:T(8,128)S(1)}) custom-call(bf16[144,512]{1,0:T(8,128)(2,1)S(1)} %collective-permute-done.5.refs_0_, bf16[144,512]{1,0:T(8,128)(2,1)S(1)} %collective-permute-done.6.refs_1_, bf16[144,512]{1,0:T(8,128)(2,1)S(1)} %collective-permute-done.refs_2_.refs_0_, ...), custom_call_target="tpu_custom_call" | custom-call | flops 2415919104 | bytes 1048576 | tf_op jit(solution)/shard_map/pallas_call | solution.py:303
  26.7 1.7 shard_map.128
  29.2 2.3 %stage_weights.1.refs_4_.refs_6_.refs_2_ = bf16[6144,256]{1,0:T(8,128)(2,1)S(1)} custom-call(bf16[2048,256]{1,0:T(8,128)(2,1)} %bitcast.26, bf16[2048,256]{1,0:T(8,128)(2,1)} %bitcast.27, bf16[256,2048]{1,0:T(8,128)(2,1)} %bitcast.28), custom_call_target="tpu_custom_call" | custom-call | tf_op jit(solution)/shard_map/stage_weights/pallas_call | solution.py:389
  31.7 1.3 collective-permute-start.7
  33.0 1.3 collective-permute-start.8
  34.3 1.3 collective-permute-start.9
  35.7 1.5 shard_map.130
  37.3 3.0 %collective-permute-done.8.refs_1_ = bf16[144,512]{1,0:T(8,128)(2,1)S(1)} collective-permute-done((bf16[144,512]{1,0:T(8,128)(2,1)S(1)}, bf16[144,512]{1,0:T(8,128)(2,1)S(1)}, u32[]{:S(2)}, u32[]{:S(2)}) %collective-permute-start.8) | collective-permute-done | bytes 147488 | tf_op jit(solution)/shard_map/ppermute | solution.py:322
  40.5 17.0 %all_to_all.15.heads = bf16[16,32,128]{2,1,0:T(8,128)(2,1)S(1)} all-to-all(bf16[16,32,128]{2,1,0:T(8,128)(2,1)S(1)} %bitcast.21), channel_id=1, replica_groups=mesh['sp'=16,'tp'=16] {'tp'}, dimensions={0} | all-to-all | bytes 262144 | tf_op jit(solution)/shard_map/all_to_all | solution.py:617
  57.6 2.5 %project.1 = (f32[32,2048]{1,0:T(8,128)S(1)}, bf16[128,2048]{1,0:T(8,128)(2,1)S(1)}, f32[128,32]{1,0:T(8,128)S(1)}) custom-call(bf16[16,32,128]{2,1,0:T(8,128)(2,1)S(1)} %all_to_all.15.heads, bf16[2048,2048]{1,0:T(8,128)(2,1)S(1)} %bitcast.18, bf16[32,2048]{1,0:T(8,128)(2,1)S(1)} %copy-done, f32[1,2048]{1,0:T(1,128)S(1)} %bitcast.22, s32[2,32]{1,0:T(2,128)S(1)} %bitcast.23, ...), custom_call_target="tpu_custom_call" | custom-call | tf_op jit(solution)/shard_map/project/pallas_call | solution.py:547
  60.1 19.0 %all_to_all.16 = bf16[16,8,2048]{2,1,0:T(8,128)(2,1)S(1)} all-to-all(bf16[16,8,2048]{2,1,0:T(8,128)(2,1)S(1)} %bitcast.20), channel_id=1, replica_groups=mesh['sp'=16,'tp'=16] {'sp'}, dimensions={0} | all-to-all | bytes 1048576 | tf_op jit(solution)/shard_map/all_to_all | solution.py:622
  79.8 2.7 %collective-permute-start.19 = (bf16[64,2048]{1,0:T(8,128)(2,1)S(1)}, bf16[64,2048]{1,0:T(8,128)(2,1)S(1)}, u32[]{:S(2)}, u32[]{:S(2)}) collective-permute-start(bf16[64,2048]{1,0:T(8,128)(2,1)S(1)} %get-tuple-element.93.refs_1_), channel_id=1, source_target_pairs={{0,14},{1,15},{2,0},{3,1},{4,2},{5,3},{6,4},{7,5},{8,6},{9,7},{10,... | collective-permute-start | bytes 786440 | tf_op jit(solution)/shard_map/ppermute | solution.py:459
  82.5 3.2 %collective-permute-start.16 = (bf16[64,2048]{1,0:T(8,128)(2,1)S(1)}, bf16[64,2048]{1,0:T(8,128)(2,1)S(1)}, u32[]{:S(2)}, u32[]{:S(2)}) collective-permute-start(bf16[64,2048]{1,0:T(8,128)(2,1)S(1)} %get-tuple-element.94.refs_0_), channel_id=1, source_target_pairs={{0,14},{1,15},{2,0},{3,1},{4,2},{5,3},{6,4},{7,5},{8,6},{9,7},{10,... | collective-permute-start | bytes 786440 | tf_op jit(solution)/shard_map/ppermute | solution.py:459
  85.7 3.9 %collective-permute-done.10.refs_2_ = bf16[64,2048]{1,0:T(8,128)(2,1)S(1)} collective-permute-done((bf16[64,2048]{1,0:T(8,128)(2,1)S(1)}, bf16[64,2048]{1,0:T(8,128)(2,1)S(1)}, u32[]{:S(2)}, u32[]{:S(2)}) %collective-permute-start.10) | collective-permute-done | bytes 262176 | tf_op jit(solution)/shard_map/ppermute | solution.py:456
  89.7 3.2 %collective-permute-start.20 = (bf16[64,2048]{1,0:T(8,128)(2,1)S(1)}, bf16[64,2048]{1,0:T(8,128)(2,1)S(1)}, u32[]{:S(2)}, u32[]{:S(2)}) collective-permute-start(bf16[64,2048]{1,0:T(8,128)(2,1)S(1)} %collective-permute-done.19.refs_5_), channel_id=1, source_target_pairs={{0,14},{1,15},{2,0},{3,1},{4,2},{5,3},{6,4},{7,5},{8,6},{9,7},{10,... | collective-permute-start | bytes 786440 | tf_op jit(solution)/shard_map/ppermute | solution.py:459
  92.9 2.4 %collective-permute-done.13.refs_3_ = bf16[64,2048]{1,0:T(8,128)(2,1)S(1)} collective-permute-done((bf16[64,2048]{1,0:T(8,128)(2,1)S(1)}, bf16[64,2048]{1,0:T(8,128)(2,1)S(1)}, u32[]{:S(2)}, u32[]{:S(2)}) %collective-permute-start.13) | collective-permute-done | bytes 262176 | tf_op jit(solution)/shard_map/ppermute | solution.py:456
  95.3 3.2 %collective-permute-start.17 = (bf16[64,2048]{1,0:T(8,128)(2,1)S(1)}, bf16[64,2048]{1,0:T(8,128)(2,1)S(1)}, u32[]{:S(2)}, u32[]{:S(2)}) collective-permute-start(bf16[64,2048]{1,0:T(8,128)(2,1)S(1)} %collective-permute-done.16.refs_4_), channel_id=1, source_target_pairs={{0,14},{1,15},{2,0},{3,1},{4,2},{5,3},{6,4},{7,5},{8,6},{9,7},{10,... | collective-permute-start | bytes 786440 | tf_op jit(solution)/shard_map/ppermute | solution.py:459
  98.5 2.4 %collective-permute-done.11.refs_0_ = bf16[64,2048]{1,0:T(8,128)(2,1)S(1)} collective-permute-done((bf16[64,2048]{1,0:T(8,128)(2,1)S(1)}, bf16[64,2048]{1,0:T(8,128)(2,1)S(1)}, u32[]{:S(2)}, u32[]{:S(2)}) %collective-permute-start.11) | collective-permute-done | bytes 262176 | tf_op jit(solution)/shard_map/ppermute | solution.py:456
  100.9 3.2 %collective-permute-start.21 = (bf16[64,2048]{1,0:T(8,128)(2,1)S(1)}, bf16[64,2048]{1,0:T(8,128)(2,1)S(1)}, u32[]{:S(2)}, u32[]{:S(2)}) collective-permute-start(bf16[64,2048]{1,0:T(8,128)(2,1)S(1)} %collective-permute-done.20.refs_3_), channel_id=1, source_target_pairs={{0,14},{1,15},{2,0},{3,1},{4,2},{5,3},{6,4},{7,5},{8,6},{9,7},{10,... | collective-permute-start | bytes 786440 | tf_op jit(solution)/shard_map/ppermute | solution.py:459
  104.1 2.4 %collective-permute-done.14.refs_1_ = bf16[64,2048]{1,0:T(8,128)(2,1)S(1)} collective-permute-done((bf16[64,2048]{1,0:T(8,128)(2,1)S(1)}, bf16[64,2048]{1,0:T(8,128)(2,1)S(1)}, u32[]{:S(2)}, u32[]{:S(2)}) %collective-permute-start.14) | collective-permute-done | bytes 262176 | tf_op jit(solution)/shard_map/ppermute | solution.py:456
  106.5 3.2 %collective-permute-start.18 = (bf16[64,2048]{1,0:T(8,128)(2,1)S(1)}, bf16[64,2048]{1,0:T(8,128)(2,1)S(1)}, u32[]{:S(2)}, u32[]{:S(2)}) collective-permute-start(bf16[64,2048]{1,0:T(8,128)(2,1)S(1)} %collective-permute-done.17.refs_2_), channel_id=1, source_target_pairs={{0,14},{1,15},{2,0},{3,1},{4,2},{5,3},{6,4},{7,5},{8,6},{9,7},{10,... | collective-permute-start | bytes 786440 | tf_op jit(solution)/shard_map/ppermute | solution.py:459
  109.7 2.4 %collective-permute-done.12.refs_0_ = bf16[64,2048]{1,0:T(8,128)(2,1)S(1)} collective-permute-done((bf16[64,2048]{1,0:T(8,128)(2,1)S(1)}, bf16[64,2048]{1,0:T(8,128)(2,1)S(1)}, u32[]{:S(2)}, u32[]{:S(2)}) %collective-permute-start.12) | collective-permute-done | bytes 262176 | tf_op jit(solution)/shard_map/ppermute | solution.py:456
  112.1 3.2 %collective-permute-start.27 = (bf16[64,2048]{1,0:T(8,128)(2,1)S(1)}, bf16[64,2048]{1,0:T(8,128)(2,1)S(1)}, u32[]{:S(2)}, u32[]{:S(2)}) collective-permute-start(bf16[64,2048]{1,0:T(8,128)(2,1)S(1)} %collective-permute-done.21.refs_3_), channel_id=1, source_target_pairs={{0,14},{1,15},{2,0},{3,1},{4,2},{5,3},{6,4},{7,5},{8,6},{9,7},{10,... | collective-permute-start | bytes 786440 | tf_op jit(solution)/shard_map/ppermute | solution.py:459
  115.4 2.4 %collective-permute-done.15.refs_1_ = bf16[64,2048]{1,0:T(8,128)(2,1)S(1)} collective-permute-done((bf16[64,2048]{1,0:T(8,128)(2,1)S(1)}, bf16[64,2048]{1,0:T(8,128)(2,1)S(1)}, u32[]{:S(2)}, u32[]{:S(2)}) %collective-permute-start.15) | collective-permute-done | bytes 262176 | tf_op jit(solution)/shard_map/ppermute | solution.py:456
  117.7 2.4 %shard_map.132 = (bf16[64,2048]{1,0:T(8,128)(2,1)S(1)}, bf16[64,2048]{1,0:T(8,128)(2,1)S(1)}, bf16[64,2048]{1,0:T(8,128)(2,1)S(1)}, bf16[64,2048]{1,0:T(8,128)(2,1)S(1)}) custom-call(bf16[64,2048]{1,0:T(8,128)(2,1)S(1)} %collective-permute-done.12.refs_0_, bf16[64,2048]{1,0:T(8,128)(2,1)S(1)} %collective-permute-done.15.refs_1_, ...), custom_call_target="tpu_custom_call" | custom-call | flops 1610612736 | bytes 6291456 | tf_op jit(solution)/shard_map/pallas_call | solution.py:439
  120.3 2.3 %collective-permute-done.26.refs_0_ = bf16[64,2048]{1,0:T(8,128)(2,1)S(1)} collective-permute-done((bf16[64,2048]{1,0:T(8,128)(2,1)S(1)}, bf16[64,2048]{1,0:T(8,128)(2,1)S(1)}, u32[]{:S(2)}, u32[]{:S(2)}) %collective-permute-start.26) | collective-permute-done | bytes 262176 | tf_op jit(solution)/shard_map/ppermute | solution.py:456
  123.7 2.0 %collective-permute-start.32 = (bf16[64,2048]{1,0:T(8,128)(2,1)S(1)}, bf16[64,2048]{1,0:T(8,128)(2,1)S(1)}, u32[]{:S(2)}, u32[]{:S(2)}) collective-permute-start(bf16[64,2048]{1,0:T(8,128)(2,1)S(1)} %get-tuple-element.84), channel_id=1, source_target_pairs={{0,14},{1,15},{2,0},{3,1},{4,2},{5,3},{6,4},{7,5},{8,6},{9,7},{10,... | collective-permute-start | bytes 786440 | tf_op jit(solution)/shard_map/ppermute | solution.py:459
  125.8 3.2 %collective-permute-start.23 = (bf16[64,2048]{1,0:T(8,128)(2,1)S(1)}, bf16[64,2048]{1,0:T(8,128)(2,1)S(1)}, u32[]{:S(2)}, u32[]{:S(2)}) collective-permute-start(bf16[64,2048]{1,0:T(8,128)(2,1)S(1)} %get-tuple-element.76), channel_id=1, source_target_pairs={{0,14},{1,15},{2,0},{3,1},{4,2},{5,3},{6,4},{7,5},{8,6},{9,7},{10,... | collective-permute-start | bytes 786440 | tf_op jit(solution)/shard_map/ppermute | solution.py:459
  129.0 2.4 %shard_map.133 = (bf16[64,2048]{1,0:T(8,128)(2,1)S(1)}, bf16[64,2048]{1,0:T(8,128)(2,1)S(1)}, bf16[64,2048]{1,0:T(8,128)(2,1)S(1)}, bf16[64,2048]{1,0:T(8,128)(2,1)S(1)}) custom-call(bf16[64,2048]{1,0:T(8,128)(2,1)S(1)} %collective-permute-done.11.refs_0_, bf16[64,2048]{1,0:T(8,128)(2,1)S(1)} %collective-permute-done.14.refs_1_, ...), custom_call_target="tpu_custom_call" | custom-call | flops 1610612736 | bytes 6291456 | tf_op jit(solution)/shard_map/pallas_call | solution.py:439
  131.4 3.6 %shard_map.134 = (bf16[64,2048]{1,0:T(8,128)(2,1)S(1)}, bf16[64,2048]{1,0:T(8,128)(2,1)S(1)}, bf16[64,2048]{1,0:T(8,128)(2,1)S(1)}, bf16[64,2048]{1,0:T(8,128)(2...) custom-call(bf16[64,2048]{1,0:T(8,128)(2,1)S(1)} %get-tuple-element.94.refs_0_, ...), custom_call_target="tpu_custom_call" | custom-call | flops 2415919104 | bytes 6291456 | tf_op jit(solution)/shard_map/pallas_call | solution.py:439
  135.4 3.3 %collective-permute-start.33 = (bf16[64,2048]{1,0:T(8,128)(2,1)S(1)}, bf16[64,2048]{1,0:T(8,128)(2,1)S(1)}, u32[]{:S(2)}, u32[]{:S(2)}) collective-permute-start(bf16[64,2048]{1,0:T(8,128)(2,1)S(1)} %add_convert_fusion.5), channel_id=1, source_target_pairs={{0,14},{1,15},{2,0},{3,1},{4,2},{5,3},{6,4},{7,5},{8,6},{9,7},{10,... | collective-permute-start | bytes 786440 | tf_op jit(solution)/shard_map/ppermute | solution.py:459
  139.0 3.3 %collective-permute-start.24 = (bf16[64,2048]{1,0:T(8,128)(2,1)S(1)}, bf16[64,2048]{1,0:T(8,128)(2,1)S(1)}, u32[]{:S(2)}, u32[]{:S(2)}) collective-permute-start(bf16[64,2048]{1,0:T(8,128)(2,1)S(1)} %add_convert_fusion.11), channel_id=1, source_target_pairs={{0,14},{1,15},{2,0},{3,1},{4,2},{5,3},{6,4},{7,5},{8,6},{9,7},{10,... | collective-permute-start | bytes 786440 | tf_op jit(solution)/shard_map/ppermute | solution.py:459
  142.3 3.5 %collective-permute-done.37 = bf16[64,2048]{1,0:T(8,128)(2,1)S(1)} collective-permute-done((bf16[64,2048]{1,0:T(8,128)(2,1)S(1)}, bf16[64,2048]{1,0:T(8,128)(2,1)S(1)}, u32[]{:S(2)}, u32[]{:S(2)}) %collective-permute-start.37) | collective-permute-done | bytes 262176 | tf_op jit(solution)/shard_map/ppermute | solution.py:456
  146.0 3.3 %collective-permute-start.34 = (bf16[64,2048]{1,0:T(8,128)(2,1)S(1)}, bf16[64,2048]{1,0:T(8,128)(2,1)S(1)}, u32[]{:S(2)}, u32[]{:S(2)}) collective-permute-start(bf16[64,2048]{1,0:T(8,128)(2,1)S(1)} %add_convert_fusion.4), channel_id=1, source_target_pairs={{0,14},{1,15},{2,0},{3,1},{4,2},{5,3},{6,4},{7,5},{8,6},{9,7},{10,... | collective-permute-start | bytes 786440 | tf_op jit(solution)/shard_map/ppermute | solution.py:459
  149.3 2.1 %collective-permute-done.29 = bf16[64,2048]{1,0:T(8,128)(2,1)S(1)} collective-permute-done((bf16[64,2048]{1,0:T(8,128)(2,1)S(1)}, bf16[64,2048]{1,0:T(8,128)(2,1)S(1)}, u32[]{:S(2)}, u32[]{:S(2)}) %collective-permute-start.29) | collective-permute-done | bytes 262176 | tf_op jit(solution)/shard_map/ppermute | solution.py:456
  151.6 3.3 %collective-permute-start.25 = (bf16[64,2048]{1,0:T(8,128)(2,1)S(1)}, bf16[64,2048]{1,0:T(8,128)(2,1)S(1)}, u32[]{:S(2)}, u32[]{:S(2)}) collective-permute-start(bf16[64,2048]{1,0:T(8,128)(2,1)S(1)} %add_convert_fusion.10), channel_id=1, source_target_pairs={{0,14},{1,15},{2,0},{3,1},{4,2},{5,3},{6,4},{7,5},{8,6},{9,7},{10,... | collective-permute-start | bytes 786440 | tf_op jit(solution)/shard_map/ppermute | solution.py:459
  154.9 1.8 collective-permute-done.34
  156.7 3.8 %collective-permute-start.35 = (bf16[64,2048]{1,0:T(8,128)(2,1)S(1)}, bf16[64,2048]{1,0:T(8,128)(2,1)S(1)}, u32[]{:S(2)}, u32[]{:S(2)}) collective-permute-start(bf16[64,2048]{1,0:T(8,128)(2,1)S(1)} %add_convert_fusion.3), channel_id=1, source_target_pairs={{0,14},{1,15},{2,0},{3,1},{4,2},{5,3},{6,4},{7,5},{8,6},{9,7},{10,... | collective-permute-start | bytes 786440 | tf_op jit(solution)/shard_map/ppermute | solution.py:459
  160.7 3.7 %collective-permute-done.35 = bf16[64,2048]{1,0:T(8,128)(2,1)S(1)} collective-permute-done((bf16[64,2048]{1,0:T(8,128)(2,1)S(1)}, bf16[64,2048]{1,0:T(8,128)(2,1)S(1)}, u32[]{:S(2)}, u32[]{:S(2)}) %collective-permute-start.35) | collective-permute-done | bytes 262176 | tf_op jit(solution)/shard_map/ppermute | solution.py:459
  164.5 3.7 %collective-permute-done.31 = bf16[64,2048]{1,0:T(8,128)(2,1)S(1)} collective-permute-done((bf16[64,2048]{1,0:T(8,128)(2,1)S(1)}, bf16[64,2048]{1,0:T(8,128)(2,1)S(1)}, u32[]{:S(2)}, u32[]{:S(2)}) %collective-permute-start.31) | collective-permute-done | bytes 262176 | tf_op jit(solution)/shard_map/ppermute | solution.py:456
  168.4 13.5 %all_to_all.17 = bf16[16,8,2048]{2,1,0:T(8,128)(2,1)S(1)} all-to-all(bf16[16,8,2048]{2,1,0:T(8,128)(2,1)S(1)} %maximum_bitcast_fusion), channel_id=1, replica_groups=mesh['sp'=16,'tp'=16] {'sp'}, dimensions={0} | all-to-all | bytes 1048576 | tf_op jit(solution)/shard_map/all_to_all | solution.py:625
  (77 shorter events, 8.8 us)
Async XLA Ops:
  1.2 10.3 %collective-permute-start.1 = (bf16[544,256]{1,0:T(8,128)(2,1)S(1)}, bf16[544,256]{1,0:T(8,128)(2,1)S(1)}, u32[]{:S(2)}, u32[]{:S(2)}) collective-permute-start(bf16[544,256]{1,0:T(8,128)(2,1)S(1)} %get-tuple-element.63.refs_3_.refs_1_), channel_id=1, source_target_pairs={{0,16},{16,32},{32,48},{48,0},{64,80},{80,96},{96,112},{112,64},{1... | collective-permute-start | bytes 835592 | tf_op jit(solution)/shard_map/ppermute | solution.py:322
  4.6 10.3 %collective-permute-start.3 = (bf16[544,256]{1,0:T(8,128)(2,1)S(1)}, bf16[544,256]{1,0:T(8,128)(2,1)S(1)}, u32[]{:S(2)}, u32[]{:S(2)}) collective-permute-start(bf16[544,256]{1,0:T(8,128)(2,1)S(1)} %get-tuple-element.63.refs_3_.refs_1_), channel_id=1, source_target_pairs={{0,48},{16,0},{32,16},{48,32},{64,112},{80,64},{96,80},{112,96},{1... | collective-permute-start | bytes 835592 | tf_op jit(solution)/shard_map/ppermute | solution.py:322
  7.3 11.0 %collective-permute-start = (bf16[144,512]{1,0:T(8,128)(2,1)S(1)}, bf16[144,512]{1,0:T(8,128)(2,1)S(1)}, u32[]{:S(2)}, u32[]{:S(2)}) collective-permute-start(bf16[144,512]{1,0:T(8,128)(2,1)S(1)} %get-tuple-element.62.refs_0_), channel_id=1, source_target_pairs={{64,0},{80,16},{96,32},{112,48},{128,64},{144,80},{160,96},{176,11... | collective-permute-start | bytes 442376 | tf_op jit(solution)/shard_map/ppermute | solution.py:322
  8.6 11.6 %collective-permute-start.5 = (bf16[144,512]{1,0:T(8,128)(2,1)S(1)}, bf16[144,512]{1,0:T(8,128)(2,1)S(1)}, u32[]{:S(2)}, u32[]{:S(2)}) collective-permute-start(bf16[144,512]{1,0:T(8,128)(2,1)S(1)} %get-tuple-element.62.refs_0_), channel_id=1, source_target_pairs={{192,0},{208,16},{224,32},{240,48},{193,1},{209,17},{225,33},{241,... | collective-permute-start | bytes 442376 | tf_op jit(solution)/shard_map/ppermute | solution.py:322
  9.9 10.3 %collective-permute-start.6 = (bf16[144,512]{1,0:T(8,128)(2,1)S(1)}, bf16[144,512]{1,0:T(8,128)(2,1)S(1)}, u32[]{:S(2)}, u32[]{:S(2)}) collective-permute-start(bf16[144,512]{1,0:T(8,128)(2,1)S(1)} %get-tuple-element.62.refs_0_), channel_id=1, source_target_pairs={{128,0},{144,16},{160,32},{176,48},{192,64},{208,80},{224,96},{240... | collective-permute-start | bytes 442376 | tf_op jit(solution)/shard_map/ppermute | solution.py:322
  11.5 15.2 %collective-permute-start.2 = (bf16[272,256]{1,0:T(8,128)(2,1)S(1)}, bf16[272,256]{1,0:T(8,128)(2,1)S(1)}, u32[]{:S(2)}, u32[]{:S(2)}) collective-permute-start(bf16[272,256]{1,0:T(8,128)(2,1)S(1)} %slice.24), channel_id=1, source_target_pairs={{0,16},{16,32},{32,48},{48,0},{64,80},{80,96},{96,112},{112,64},{1... | collective-permute-start | bytes 417800 | tf_op jit(solution)/shard_map/ppermute | solution.py:322
  15.0 11.8 %collective-permute-start.4 = (bf16[272,256]{1,0:T(8,128)(2,1)S(1)}, bf16[272,256]{1,0:T(8,128)(2,1)S(1)}, u32[]{:S(2)}, u32[]{:S(2)}) collective-permute-start(bf16[272,256]{1,0:T(8,128)(2,1)S(1)} %slice.25), channel_id=1, source_target_pairs={{0,48},{16,0},{32,16},{48,32},{64,112},{80,64},{96,80},{112,96},{1... | collective-permute-start | bytes 417800 | tf_op jit(solution)/shard_map/ppermute | solution.py:322
  20.2 37.3 %slice-start = ((s8[8388608]{0:T(1024)(128)(4,1)}), s8[4194304]{0:T(1024)(128)(4,1)S(1)}, s32[]{:S(2)}) async-start(s8[8388608]{0:T(1024)(128)(4,1)} %bitcast.17), calls=%async_computation.3 | async-start | bytes 8388608
  28.4 29.1 %slice-start.1 = ((s8[8388608]{0:T(1024)(128)(4,1)}), s8[4194304]{0:T(1024)(128)(4,1)S(1)}, s32[]{:S(2)}) async-start(s8[8388608]{0:T(1024)(128)(4,1)} %bitcast.17), calls=%async_computation.4 | async-start | bytes 8388608
  31.6 8.6 %copy-start.4 = (f32[128]{0:T(128)S(1)}, f32[128]{0:T(128)}, u32[]{:S(2)}) copy-start(f32[128]{0:T(128)} %param.17) | copy-start | bytes 1540
  31.6 26.0 %copy-start = (bf16[32,2048]{1,0:T(8,128)(2,1)S(1)}, bf16[32,2048]{1,0:T(8,128)(2,1)}, u32[]{:S(2)}) copy-start(bf16[32,2048]{1,0:T(8,128)(2,1)} %stream.1) | copy-start | bytes 393220
  31.6 26.0 %copy-start.1 = (f32[2048]{0:T(1024)S(1)}, f32[2048]{0:T(1024)}, u32[]{:S(2)}) copy-start(f32[2048]{0:T(1024)} %param.20) | copy-start | bytes 24580
  31.6 26.0 %copy-start.2 = (s32[32,2]{0,1:T(2,128)S(1)}, s32[32,2]{0,1:T(2,128)}, u32[]{:S(2)}) copy-start(s32[32,2]{0,1:T(2,128)} %param.21) | copy-start | bytes 772
  31.6 25.9 %copy-start.3 = (f32[32,2]{0,1:T(2,128)S(1)}, f32[32,2]{0,1:T(2,128)}, u32[]{:S(2)}) copy-start(f32[32,2]{0,1:T(2,128)} %param.22) | copy-start | bytes 772
  31.6 86.1 %collective-permute-start.22 = (bf16[6144,256]{1,0:T(8,128)(2,1)S(1)}, bf16[6144,256]{1,0:T(8,128)(2,1)S(1)}, u32[]{:S(2)}, u32[]{:S(2)}) collective-permute-start(bf16[6144,256]{1,0:T(8,128)(2,1)S(1)} %stage_weights.1.refs_4_.refs_6_.refs_2_), channel_id=1, source_target_pairs={{0,1},{1,0},{2,3},{3,2},{4,5},{5,4},{6,7},{7,6},{8,9},{9,8},{10,11... | collective-permute-start | bytes 9437192 | tf_op jit(solution)/shard_map/ppermute | solution.py:613
  31.7 5.5 %collective-permute-start.7 = (bf16[144,512]{1,0:T(8,128)(2,1)S(1)}, bf16[144,512]{1,0:T(8,128)(2,1)S(1)}, u32[]{:S(2)}, u32[]{:S(2)}) collective-permute-start(bf16[144,512]{1,0:T(8,128)(2,1)S(1)} %shard_map.129), channel_id=1, source_target_pairs={{0,64},{16,80},{32,96},{48,112},{64,128},{80,144},{96,160},{112,17... | collective-permute-start | bytes 442376 | tf_op jit(solution)/shard_map/ppermute | solution.py:322
  33.0 7.2 %collective-permute-start.8 = (bf16[144,512]{1,0:T(8,128)(2,1)S(1)}, bf16[144,512]{1,0:T(8,128)(2,1)S(1)}, u32[]{:S(2)}, u32[]{:S(2)}) collective-permute-start(bf16[144,512]{1,0:T(8,128)(2,1)S(1)} %get-tuple-element.60), channel_id=1, source_target_pairs={{0,128},{16,144},{32,160},{48,176},{64,192},{80,208},{96,224},{112... | collective-permute-start | bytes 442376 | tf_op jit(solution)/shard_map/ppermute | solution.py:322
  34.3 5.9 %collective-permute-start.9 = (bf16[144,512]{1,0:T(8,128)(2,1)S(1)}, bf16[144,512]{1,0:T(8,128)(2,1)S(1)}, u32[]{:S(2)}, u32[]{:S(2)}) collective-permute-start(bf16[144,512]{1,0:T(8,128)(2,1)S(1)} %get-tuple-element.61), channel_id=1, source_target_pairs={{0,192},{16,208},{32,224},{48,240},{1,193},{17,209},{33,225},{49,2... | collective-permute-start | bytes 442376 | tf_op jit(solution)/shard_map/ppermute | solution.py:322
  79.2 10.5 %collective-permute-start.10 = (bf16[64,2048]{1,0:T(8,128)(2,1)S(1)}, bf16[64,2048]{1,0:T(8,128)(2,1)S(1)}, u32[]{:S(2)}, u32[]{:S(2)}) collective-permute-start(bf16[64,2048]{1,0:T(8,128)(2,1)S(1)} %get-tuple-element.94.refs_0_), channel_id=1, source_target_pairs={{0,2},{1,3},{2,4},{3,5},{4,6},{5,7},{6,8},{7,9},{8,10},{9,11},{10,... | collective-permute-start | bytes 786440 | tf_op jit(solution)/shard_map/ppermute | solution.py:456
  79.8 9.8 %collective-permute-start.19 = (bf16[64,2048]{1,0:T(8,128)(2,1)S(1)}, bf16[64,2048]{1,0:T(8,128)(2,1)S(1)}, u32[]{:S(2)}, u32[]{:S(2)}) collective-permute-start(bf16[64,2048]{1,0:T(8,128)(2,1)S(1)} %get-tuple-element.93.refs_1_), channel_id=1, source_target_pairs={{0,14},{1,15},{2,0},{3,1},{4,2},{5,3},{6,4},{7,5},{8,6},{9,7},{10,... | collective-permute-start | bytes 786440 | tf_op jit(solution)/shard_map/ppermute | solution.py:459
  82.5 12.8 %collective-permute-start.13 = (bf16[64,2048]{1,0:T(8,128)(2,1)S(1)}, bf16[64,2048]{1,0:T(8,128)(2,1)S(1)}, u32[]{:S(2)}, u32[]{:S(2)}) collective-permute-start(bf16[64,2048]{1,0:T(8,128)(2,1)S(1)} %get-tuple-element.93.refs_1_), channel_id=1, source_target_pairs={{0,2},{1,3},{2,4},{3,5},{4,6},{5,7},{6,8},{7,9},{8,10},{9,11},{10,... | collective-permute-start | bytes 786440 | tf_op jit(solution)/shard_map/ppermute | solution.py:456
  82.5 12.8 %collective-permute-start.16 = (bf16[64,2048]{1,0:T(8,128)(2,1)S(1)}, bf16[64,2048]{1,0:T(8,128)(2,1)S(1)}, u32[]{:S(2)}, u32[]{:S(2)}) collective-permute-start(bf16[64,2048]{1,0:T(8,128)(2,1)S(1)} %get-tuple-element.94.refs_0_), channel_id=1, source_target_pairs={{0,14},{1,15},{2,0},{3,1},{4,2},{5,3},{6,4},{7,5},{8,6},{9,7},{10,... | collective-permute-start | bytes 786440 | tf_op jit(solution)/shard_map/ppermute | solution.py:459
  89.7 11.2 %collective-permute-start.11 = (bf16[64,2048]{1,0:T(8,128)(2,1)S(1)}, bf16[64,2048]{1,0:T(8,128)(2,1)S(1)}, u32[]{:S(2)}, u32[]{:S(2)}) collective-permute-start(bf16[64,2048]{1,0:T(8,128)(2,1)S(1)} %collective-permute-done.10.refs_2_), channel_id=1, source_target_pairs={{0,2},{1,3},{2,4},{3,5},{4,6},{5,7},{6,8},{7,9},{8,10},{9,11},{10,... | collective-permute-start | bytes 786440 | tf_op jit(solution)/shard_map/ppermute | solution.py:456
  89.7 11.2 %collective-permute-start.20 = (bf16[64,2048]{1,0:T(8,128)(2,1)S(1)}, bf16[64,2048]{1,0:T(8,128)(2,1)S(1)}, u32[]{:S(2)}, u32[]{:S(2)}) collective-permute-start(bf16[64,2048]{1,0:T(8,128)(2,1)S(1)} %collective-permute-done.19.refs_5_), channel_id=1, source_target_pairs={{0,14},{1,15},{2,0},{3,1},{4,2},{5,3},{6,4},{7,5},{8,6},{9,7},{10,... | collective-permute-start | bytes 786440 | tf_op jit(solution)/shard_map/ppermute | solution.py:459
  95.3 11.2 %collective-permute-start.14 = (bf16[64,2048]{1,0:T(8,128)(2,1)S(1)}, bf16[64,2048]{1,0:T(8,128)(2,1)S(1)}, u32[]{:S(2)}, u32[]{:S(2)}) collective-permute-start(bf16[64,2048]{1,0:T(8,128)(2,1)S(1)} %collective-permute-done.13.refs_3_), channel_id=1, source_target_pairs={{0,2},{1,3},{2,4},{3,5},{4,6},{5,7},{6,8},{7,9},{8,10},{9,11},{10,... | collective-permute-start | bytes 786440 | tf_op jit(solution)/shard_map/ppermute | solution.py:456
  95.3 11.2 %collective-permute-start.17 = (bf16[64,2048]{1,0:T(8,128)(2,1)S(1)}, bf16[64,2048]{1,0:T(8,128)(2,1)S(1)}, u32[]{:S(2)}, u32[]{:S(2)}) collective-permute-start(bf16[64,2048]{1,0:T(8,128)(2,1)S(1)} %collective-permute-done.16.refs_4_), channel_id=1, source_target_pairs={{0,14},{1,15},{2,0},{3,1},{4,2},{5,3},{6,4},{7,5},{8,6},{9,7},{10,... | collective-permute-start | bytes 786440 | tf_op jit(solution)/shard_map/ppermute | solution.py:459
  100.9 11.2 %collective-permute-start.12 = (bf16[64,2048]{1,0:T(8,128)(2,1)S(1)}, bf16[64,2048]{1,0:T(8,128)(2,1)S(1)}, u32[]{:S(2)}, u32[]{:S(2)}) collective-permute-start(bf16[64,2048]{1,0:T(8,128)(2,1)S(1)} %collective-permute-done.11.refs_0_), channel_id=1, source_target_pairs={{0,2},{1,3},{2,4},{3,5},{4,6},{5,7},{6,8},{7,9},{8,10},{9,11},{10,... | collective-permute-start | bytes 786440 | tf_op jit(solution)/shard_map/ppermute | solution.py:456
  100.9 11.2 %collective-permute-start.21 = (bf16[64,2048]{1,0:T(8,128)(2,1)S(1)}, bf16[64,2048]{1,0:T(8,128)(2,1)S(1)}, u32[]{:S(2)}, u32[]{:S(2)}) collective-permute-start(bf16[64,2048]{1,0:T(8,128)(2,1)S(1)} %collective-permute-done.20.refs_3_), channel_id=1, source_target_pairs={{0,14},{1,15},{2,0},{3,1},{4,2},{5,3},{6,4},{7,5},{8,6},{9,7},{10,... | collective-permute-start | bytes 786440 | tf_op jit(solution)/shard_map/ppermute | solution.py:459
  106.5 11.2 %collective-permute-start.15 = (bf16[64,2048]{1,0:T(8,128)(2,1)S(1)}, bf16[64,2048]{1,0:T(8,128)(2,1)S(1)}, u32[]{:S(2)}, u32[]{:S(2)}) collective-permute-start(bf16[64,2048]{1,0:T(8,128)(2,1)S(1)} %collective-permute-done.14.refs_1_), channel_id=1, source_target_pairs={{0,2},{1,3},{2,4},{3,5},{4,6},{5,7},{6,8},{7,9},{8,10},{9,11},{10,... | collective-permute-start | bytes 786440 | tf_op jit(solution)/shard_map/ppermute | solution.py:456
  106.5 11.2 %collective-permute-start.18 = (bf16[64,2048]{1,0:T(8,128)(2,1)S(1)}, bf16[64,2048]{1,0:T(8,128)(2,1)S(1)}, u32[]{:S(2)}, u32[]{:S(2)}) collective-permute-start(bf16[64,2048]{1,0:T(8,128)(2,1)S(1)} %collective-permute-done.17.refs_2_), channel_id=1, source_target_pairs={{0,14},{1,15},{2,0},{3,1},{4,2},{5,3},{6,4},{7,5},{8,6},{9,7},{10,... | collective-permute-start | bytes 786440 | tf_op jit(solution)/shard_map/ppermute | solution.py:459
  112.1 10.5 %collective-permute-start.26 = (bf16[64,2048]{1,0:T(8,128)(2,1)S(1)}, bf16[64,2048]{1,0:T(8,128)(2,1)S(1)}, u32[]{:S(2)}, u32[]{:S(2)}) collective-permute-start(bf16[64,2048]{1,0:T(8,128)(2,1)S(1)} %collective-permute-done.12.refs_0_), channel_id=1, source_target_pairs={{0,2},{1,3},{2,4},{3,5},{4,6},{5,7},{6,8},{7,9},{8,10},{9,11},{10,... | collective-permute-start | bytes 786440 | tf_op jit(solution)/shard_map/ppermute | solution.py:456
  112.1 10.5 %collective-permute-start.27 = (bf16[64,2048]{1,0:T(8,128)(2,1)S(1)}, bf16[64,2048]{1,0:T(8,128)(2,1)S(1)}, u32[]{:S(2)}, u32[]{:S(2)}) collective-permute-start(bf16[64,2048]{1,0:T(8,128)(2,1)S(1)} %collective-permute-done.21.refs_3_), channel_id=1, source_target_pairs={{0,14},{1,15},{2,0},{3,1},{4,2},{5,3},{6,4},{7,5},{8,6},{9,7},{10,... | collective-permute-start | bytes 786440 | tf_op jit(solution)/shard_map/ppermute | solution.py:459
  120.1 14.8 %collective-permute-start.36 = (bf16[64,2048]{1,0:T(8,128)(2,1)S(1)}, bf16[64,2048]{1,0:T(8,128)(2,1)S(1)}, u32[]{:S(2)}, u32[]{:S(2)}) collective-permute-start(bf16[64,2048]{1,0:T(8,128)(2,1)S(1)} %get-tuple-element.88), channel_id=1, source_target_pairs={{0,2},{1,3},{2,4},{3,5},{4,6},{5,7},{6,8},{7,9},{8,10},{9,11},{10,... | collective-permute-start | bytes 786440 | tf_op jit(solution)/shard_map/ppermute | solution.py:456
  123.7 11.6 %collective-permute-start.32 = (bf16[64,2048]{1,0:T(8,128)(2,1)S(1)}, bf16[64,2048]{1,0:T(8,128)(2,1)S(1)}, u32[]{:S(2)}, u32[]{:S(2)}) collective-permute-start(bf16[64,2048]{1,0:T(8,128)(2,1)S(1)} %get-tuple-element.84), channel_id=1, source_target_pairs={{0,14},{1,15},{2,0},{3,1},{4,2},{5,3},{6,4},{7,5},{8,6},{9,7},{10,... | collective-permute-start | bytes 786440 | tf_op jit(solution)/shard_map/ppermute | solution.py:459
  125.8 13.0 %collective-permute-start.28 = (bf16[64,2048]{1,0:T(8,128)(2,1)S(1)}, bf16[64,2048]{1,0:T(8,128)(2,1)S(1)}, u32[]{:S(2)}, u32[]{:S(2)}) collective-permute-start(bf16[64,2048]{1,0:T(8,128)(2,1)S(1)} %get-tuple-element.79), channel_id=1, source_target_pairs={{0,2},{1,3},{2,4},{3,5},{4,6},{5,7},{6,8},{7,9},{8,10},{9,11},{10,... | collective-permute-start | bytes 786440 | tf_op jit(solution)/shard_map/ppermute | solution.py:456
  125.8 13.1 %collective-permute-start.23 = (bf16[64,2048]{1,0:T(8,128)(2,1)S(1)}, bf16[64,2048]{1,0:T(8,128)(2,1)S(1)}, u32[]{:S(2)}, u32[]{:S(2)}) collective-permute-start(bf16[64,2048]{1,0:T(8,128)(2,1)S(1)} %get-tuple-element.76), channel_id=1, source_target_pairs={{0,14},{1,15},{2,0},{3,1},{4,2},{5,3},{6,4},{7,5},{8,6},{9,7},{10,... | collective-permute-start | bytes 786440 | tf_op jit(solution)/shard_map/ppermute | solution.py:459
  135.0 10.7 %collective-permute-start.37 = (bf16[64,2048]{1,0:T(8,128)(2,1)S(1)}, bf16[64,2048]{1,0:T(8,128)(2,1)S(1)}, u32[]{:S(2)}, u32[]{:S(2)}) collective-permute-start(bf16[64,2048]{1,0:T(8,128)(2,1)S(1)} %add_convert_fusion.2), channel_id=1, source_target_pairs={{0,2},{1,3},{2,4},{3,5},{4,6},{5,7},{6,8},{7,9},{8,10},{9,11},{10,... | collective-permute-start | bytes 786440 | tf_op jit(solution)/shard_map/ppermute | solution.py:456
  135.4 10.5 %collective-permute-start.33 = (bf16[64,2048]{1,0:T(8,128)(2,1)S(1)}, bf16[64,2048]{1,0:T(8,128)(2,1)S(1)}, u32[]{:S(2)}, u32[]{:S(2)}) collective-permute-start(bf16[64,2048]{1,0:T(8,128)(2,1)S(1)} %add_convert_fusion.5), channel_id=1, source_target_pairs={{0,14},{1,15},{2,0},{3,1},{4,2},{5,3},{6,4},{7,5},{8,6},{9,7},{10,... | collective-permute-start | bytes 786440 | tf_op jit(solution)/shard_map/ppermute | solution.py:459
  138.8 12.5 %collective-permute-start.29 = (bf16[64,2048]{1,0:T(8,128)(2,1)S(1)}, bf16[64,2048]{1,0:T(8,128)(2,1)S(1)}, u32[]{:S(2)}, u32[]{:S(2)}) collective-permute-start(bf16[64,2048]{1,0:T(8,128)(2,1)S(1)} %add_convert_fusion.9), channel_id=1, source_target_pairs={{0,2},{1,3},{2,4},{3,5},{4,6},{5,7},{6,8},{7,9},{8,10},{9,11},{10,... | collective-permute-start | bytes 786440 | tf_op jit(solution)/shard_map/ppermute | solution.py:456
  139.0 12.5 %collective-permute-start.24 = (bf16[64,2048]{1,0:T(8,128)(2,1)S(1)}, bf16[64,2048]{1,0:T(8,128)(2,1)S(1)}, u32[]{:S(2)}, u32[]{:S(2)}) collective-permute-start(bf16[64,2048]{1,0:T(8,128)(2,1)S(1)} %add_convert_fusion.11), channel_id=1, source_target_pairs={{0,14},{1,15},{2,0},{3,1},{4,2},{5,3},{6,4},{7,5},{8,6},{9,7},{10,... | collective-permute-start | bytes 786440 | tf_op jit(solution)/shard_map/ppermute | solution.py:459
  145.8 14.9 %collective-permute-start.38 = (bf16[64,2048]{1,0:T(8,128)(2,1)S(1)}, bf16[64,2048]{1,0:T(8,128)(2,1)S(1)}, u32[]{:S(2)}, u32[]{:S(2)}) collective-permute-start(bf16[64,2048]{1,0:T(8,128)(2,1)S(1)} %add_convert_fusion.1), channel_id=1, source_target_pairs={{0,2},{1,3},{2,4},{3,5},{4,6},{5,7},{6,8},{7,9},{8,10},{9,11},{10,... | collective-permute-start | bytes 786440 | tf_op jit(solution)/shard_map/ppermute | solution.py:456
  146.0 10.7 %collective-permute-start.34 = (bf16[64,2048]{1,0:T(8,128)(2,1)S(1)}, bf16[64,2048]{1,0:T(8,128)(2,1)S(1)}, u32[]{:S(2)}, u32[]{:S(2)}) collective-permute-start(bf16[64,2048]{1,0:T(8,128)(2,1)S(1)} %add_convert_fusion.4), channel_id=1, source_target_pairs={{0,14},{1,15},{2,0},{3,1},{4,2},{5,3},{6,4},{7,5},{8,6},{9,7},{10,... | collective-permute-start | bytes 786440 | tf_op jit(solution)/shard_map/ppermute | solution.py:459
  151.4 9.1 %collective-permute-start.30 = (bf16[64,2048]{1,0:T(8,128)(2,1)S(1)}, bf16[64,2048]{1,0:T(8,128)(2,1)S(1)}, u32[]{:S(2)}, u32[]{:S(2)}) collective-permute-start(bf16[64,2048]{1,0:T(8,128)(2,1)S(1)} %add_convert_fusion.8), channel_id=1, source_target_pairs={{0,2},{1,3},{2,4},{3,5},{4,6},{5,7},{6,8},{7,9},{8,10},{9,11},{10,... | collective-permute-start | bytes 786440 | tf_op jit(solution)/shard_map/ppermute | solution.py:456
  151.6 12.9 %collective-permute-start.25 = (bf16[64,2048]{1,0:T(8,128)(2,1)S(1)}, bf16[64,2048]{1,0:T(8,128)(2,1)S(1)}, u32[]{:S(2)}, u32[]{:S(2)}) collective-permute-start(bf16[64,2048]{1,0:T(8,128)(2,1)S(1)} %add_convert_fusion.10), channel_id=1, source_target_pairs={{0,14},{1,15},{2,0},{3,1},{4,2},{5,3},{6,4},{7,5},{8,6},{9,7},{10,... | collective-permute-start | bytes 786440 | tf_op jit(solution)/shard_map/ppermute | solution.py:459
  156.7 7.7 %collective-permute-start.35 = (bf16[64,2048]{1,0:T(8,128)(2,1)S(1)}, bf16[64,2048]{1,0:T(8,128)(2,1)S(1)}, u32[]{:S(2)}, u32[]{:S(2)}) collective-permute-start(bf16[64,2048]{1,0:T(8,128)(2,1)S(1)} %add_convert_fusion.3), channel_id=1, source_target_pairs={{0,14},{1,15},{2,0},{3,1},{4,2},{5,3},{6,4},{7,5},{8,6},{9,7},{10,... | collective-permute-start | bytes 786440 | tf_op jit(solution)/shard_map/ppermute | solution.py:459
  160.6 7.7 %collective-permute-start.31 = (bf16[64,2048]{1,0:T(8,128)(2,1)S(1)}, bf16[64,2048]{1,0:T(8,128)(2,1)S(1)}, u32[]{:S(2)}, u32[]{:S(2)}) collective-permute-start(bf16[64,2048]{1,0:T(8,128)(2,1)S(1)} %add_convert_fusion.7), channel_id=1, source_target_pairs={{0,2},{1,3},{2,4},{3,5},{4,6},{5,7},{6,8},{7,9},{8,10},{9,11},{10,... | collective-permute-start | bytes 786440 | tf_op jit(solution)/shard_map/ppermute | solution.py:456

commit v6 on v5

--- a/solution.py
+++ b/solution.py
@@ -228,20 +228,19 @@
     lax.fori_loop(0, 3, each, 0)
 
 
-def end_kernel(*refs, first, count):
-    packs, far, states = refs[:count], refs[count : count + 2], refs[count + 2 : count + 5]
-    outs = refs[count + 5 : 2 * count + 5]
-    state, (stack, keys_wide, query_wide) = refs[-6:-3], refs[-3:]
+def end_kernel(*refs):
+    packs, far, states, outs = refs[:3], refs[3:5], refs[5:8], refs[8:11]
+    state, (stack, keys_wide, query_wide) = refs[11:14], refs[14:]
     own_y = lax.axis_index("sp") >> 2
 
-    @pl.when(own_y < first + count)
+    @pl.when(own_y < 3)
     def _():
         load_blocks(stack, keys_wide, far)
 
     def each(i, carry):
-        @pl.when(own_y <= first + i)
+        @pl.when(own_y <= i)
         def _():
-            for into, came in zip(state, nth_state(states, first + i)):
+            for into, came in zip(state, nth_state(states, i)):
                 into[...] = came[...]
             for at, pack in enumerate(packs):
                 pl.when(i == at)(partial(load_query, query_wide, pack))
@@ -251,7 +250,7 @@
 
         return carry
 
-    lax.fori_loop(0, count, each, 0)
+    lax.fori_loop(0, 3, each, 0)
 
 
 def own_kernel(*refs):
@@ -341,19 +340,15 @@
 
     packs = [pack3, pack2, pack1]
     near = attend(near_kernel, [*packs, keys_own, low, high], all_states, loaded(3), 9)
-
-    def end(first, count):
-        operands = [*packs[first : first + count], far_a, far_b, *near]
-        kernel = partial(end_kernel, first=first, count=count)
-        return attend(kernel, operands, [result] * count, state + loaded(1), count)
-
-    part3, part2 = end(0, 2)
-    part3, part2, near = lax.optimization_barrier((part3, part2, near))
+    part3, part2, part1 = attend(
+        end_kernel, [*packs, far_a, far_b, *near], [result] * 3, state + loaded(1), 3
+    )
+    keys = [keys_own, low, high, far_a, far_b]
+    part3, part2, part1, own_pack, keys, weights = lax.optimization_barrier(
+        (part3, part2, part1, own_pack, keys, weights)
+    )
     back3 = shift(part3, -1, 0, lambda y, x: y == 3)
     back2 = shift(part2, 2, 0, lambda y, x: y > 1)
-    (part1,) = end(2, 1)
-    keys = [keys_own, low, high, far_a, far_b]
-    part1, own_pack, keys, weights = lax.optimization_barrier((part1, own_pack, keys, weights))
     back1 = shift(part1, 1, 0, lambda y, x: y > 0)
     own_state = attend(own_kernel, [own_pack, *keys], state, loaded(4), 4)
     staged = stage_weights(*weights)

time: 183 us -> 183 us (level)
  waiting for transfers between devices: 38.2 us -> 36.3 us
    ppermute x10, waiting for transfers between devices: 5.25 us -> 3.36 us  [shift(): return lax.ppermute(array, 'sp', sp_perm(dy, dx, needed))]
    pallas_call x5 -> x4, Pallas kernels: 10.7 us -> 10.7 us  [attend(): pl.pallas_call(kernel, out_shape=tuple((jax.ShapeDtypeStruct(*out) for ou...]
  transfers between devices with their start and end apart: 39 -> 39, of which waited for: 16 -> 15; matrix products, arithmetic and copies ran while one was open for 0% -> 0% of each run, Pallas kernels for 11% -> 11%
where the time goes in v6:
time: 183 us
  starting transfers between devices  67.7 us (37%)
  blocking collectives  50.3 us (27%)
  waiting for transfers between devices  36.3 us (20%)
  Pallas kernels  26.9 us (15%)
    ppermute x14, starting transfers between devices, down(): return lax.ppermute(array, 'tp', z_perm(-1))  44.2 us
    ppermute x14, waiting for transfers between devices, up(): return lax.ppermute(array, 'tp', z_perm(1))  27.4 us
    ppermute x10, starting transfers between devices, shift(): return lax.ppermute(array, 'sp', sp_perm(dy, dx, needed))  21.9 us
    all_to_all x1, blocking collectives, on_device(): lax.all_to_all(outgoing, 'sp', split_axis=0, concat_axis=0, tiled=True)  19.9 us
    all_to_all x1, blocking collectives, on_device(): heads = lax.all_to_all(heads, 'tp', split_axis=0, concat_axis=0, tiled=True)  16.9 us
    all_to_all x1, blocking collectives, on_device(): lax.all_to_all(expert_out, 'sp', split_axis=0, concat_axis=0, tiled=True)  13.5 us
    pallas_call x4, Pallas kernels, attend(): pl.pallas_call(kernel, out_shape=tuple((jax.ShapeDtypeStruct(*out) for ou...  10.7 us
    pallas_call x4, Pallas kernels, expert_rows(): pl.pallas_call(partial(expert_kernel, count=count), out_shape=tuple((jax....  9.43 us
  transfers between devices with their start and end apart: 39, of which 15 were waited for; matrix products, arithmetic and copies ran while one was open for 0% of the time, Pallas kernels for 11%

profile of v6, /device:TPU:2, one launch (start us, length us, event | category | flops | bytes accessed | tf_op | source)
XLA Modules:
  0.0 182.6 jit_solution(581136660191339450)
XLA Ops:
  1.2 3.4 %collective-permute-start.3 = (bf16[544,256]{1,0:T(8,128)(2,1)S(1)}, bf16[544,256]{1,0:T(8,128)(2,1)S(1)}, u32[]{:S(2)}, u32[]{:S(2)}) collective-permute-start(bf16[544,256]{1,0:T(8,128)(2,1)S(1)} %get-tuple-element.59.refs_3_.refs_1_), channel_id=1, source_target_pairs={{0,16},{16,32},{32,48},{48,0},{64,80},{80,96},{96,112},{112,64},{1... | collective-permute-start | bytes 835592 | tf_op jit(solution)/shard_map/ppermute | solution.py:321
  4.6 2.7 %collective-permute-start.5 = (bf16[544,256]{1,0:T(8,128)(2,1)S(1)}, bf16[544,256]{1,0:T(8,128)(2,1)S(1)}, u32[]{:S(2)}, u32[]{:S(2)}) collective-permute-start(bf16[544,256]{1,0:T(8,128)(2,1)S(1)} %get-tuple-element.59.refs_3_.refs_1_), channel_id=1, source_target_pairs={{0,48},{16,0},{32,16},{48,32},{64,112},{80,64},{96,80},{112,96},{1... | collective-permute-start | bytes 835592 | tf_op jit(solution)/shard_map/ppermute | solution.py:321
  7.3 1.3 collective-permute-start
  8.6 1.3 collective-permute-start.1
  9.9 1.3 collective-permute-start.2
  11.5 3.4 %collective-permute-start.4 = (bf16[272,256]{1,0:T(8,128)(2,1)S(1)}, bf16[272,256]{1,0:T(8,128)(2,1)S(1)}, u32[]{:S(2)}, u32[]{:S(2)}) collective-permute-start(bf16[272,256]{1,0:T(8,128)(2,1)S(1)} %slice.24), channel_id=1, source_target_pairs={{0,16},{16,32},{32,48},{48,0},{64,80},{80,96},{96,112},{112,64},{1... | collective-permute-start | bytes 417800 | tf_op jit(solution)/shard_map/ppermute | solution.py:321
  15.0 3.4 %collective-permute-start.6 = (bf16[272,256]{1,0:T(8,128)(2,1)S(1)}, bf16[272,256]{1,0:T(8,128)(2,1)S(1)}, u32[]{:S(2)}, u32[]{:S(2)}) collective-permute-start(bf16[272,256]{1,0:T(8,128)(2,1)S(1)} %slice.25), channel_id=1, source_target_pairs={{0,48},{16,0},{32,16},{48,32},{64,112},{80,64},{96,80},{112,96},{1... | collective-permute-start | bytes 417800 | tf_op jit(solution)/shard_map/ppermute | solution.py:321
  18.4 6.5 %shard_map.127 = (f32[24,512]{1,0:T(8,128)S(1)}, f32[24,512]{1,0:T(8,128)S(1)}, f32[384,512]{1,0:T(8,128)S(1)}) custom-call(bf16[144,512]{1,0:T(8,128)(2,1)S(1)} %collective-permute-done.refs_0_, bf16[144,512]{1,0:T(8,128)(2,1)S(1)} %collective-permute-done.1.refs_1_, bf16[144,512]{1,0:T(8,128)(2,1)S(1)} %collective-permute-done.2.refs_2_, ...), custom_call_target="tpu_custom_call" | custom-call | flops 2415919104 | bytes 1048576 | tf_op jit(solution)/shard_map/pallas_call | solution.py:302
  25.0 2.4 %shard_map.128 = (bf16[144,512]{1,0:T(8,128)(2,1)S(1)}, bf16[144,512]{1,0:T(8,128)(2,1)S(1)}, bf16[144,512]{1,0:T(8,128)(2,1)S(1)}) custom-call(bf16[144,512]{1,0:T(8,128)(2,1)S(1)} %collective-permute-done.refs_0_, bf16[144,512]{1,0:T(8,128)(2,1)S(1)} %collective-permute-done.1.refs_1_, bf16[144,512]{1,0:T(8,128)(2,1)S(1)} %collective-permute-done.2.refs_2_, ...), custom_call_target="tpu_custom_call" | custom-call | flops 805306368 | bytes 1048576 | tf_op jit(solution)/shard_map/pallas_call | solution.py:302
  27.4 1.9 %stage_weights.1.refs_4_.refs_6_.refs_2_ = bf16[6144,256]{1,0:T(8,128)(2,1)S(1)} custom-call(bf16[2048,256]{1,0:T(8,128)(2,1)} %bitcast.26, bf16[2048,256]{1,0:T(8,128)(2,1)} %bitcast.27, bf16[256,2048]{1,0:T(8,128)(2,1)} %bitcast.28), custom_call_target="tpu_custom_call" | custom-call | tf_op jit(solution)/shard_map/stage_weights/pallas_call | solution.py:384
  29.5 1.7 collective-permute-start.7
  31.2 2.2 %collective-permute-start.8 = (bf16[144,512]{1,0:T(8,128)(2,1)S(1)}, bf16[144,512]{1,0:T(8,128)(2,1)S(1)}, u32[]{:S(2)}, u32[]{:S(2)}) collective-permute-start(bf16[144,512]{1,0:T(8,128)(2,1)S(1)} %get-tuple-element.56), channel_id=1, source_target_pairs={{0,128},{16,144},{32,160},{48,176},{64,192},{80,208},{96,224},{112... | collective-permute-start | bytes 442376 | tf_op jit(solution)/shard_map/ppermute | solution.py:321
  33.4 1.3 collective-permute-start.9
  34.7 1.5 shard_map.129
  36.2 1.9 %collective-permute-done.8.refs_1_ = bf16[144,512]{1,0:T(8,128)(2,1)S(1)} collective-permute-done((bf16[144,512]{1,0:T(8,128)(2,1)S(1)}, bf16[144,512]{1,0:T(8,128)(2,1)S(1)}, u32[]{:S(2)}, u32[]{:S(2)}) %collective-permute-start.8) | collective-permute-done | bytes 147488 | tf_op jit(solution)/shard_map/ppermute | solution.py:321
  39.5 16.9 %all_to_all.15.heads = bf16[16,32,128]{2,1,0:T(8,128)(2,1)S(1)} all-to-all(bf16[16,32,128]{2,1,0:T(8,128)(2,1)S(1)} %bitcast.21), channel_id=1, replica_groups=mesh['sp'=16,'tp'=16] {'tp'}, dimensions={0} | all-to-all | bytes 262144 | tf_op jit(solution)/shard_map/all_to_all | solution.py:612
  56.4 2.5 %project.1 = (f32[32,2048]{1,0:T(8,128)S(1)}, bf16[128,2048]{1,0:T(8,128)(2,1)S(1)}, f32[128,32]{1,0:T(8,128)S(1)}) custom-call(bf16[16,32,128]{2,1,0:T(8,128)(2,1)S(1)} %all_to_all.15.heads, bf16[2048,2048]{1,0:T(8,128)(2,1)S(1)} %bitcast.18, bf16[32,2048]{1,0:T(8,128)(2,1)S(1)} %copy-done, f32[1,2048]{1,0:T(1,128)S(1)} %bitcast.22, s32[2,32]{1,0:T(2,128)S(1)} %bitcast.23, ...), custom_call_target="tpu_custom_call" | custom-call | tf_op jit(solution)/shard_map/project/pallas_call | solution.py:542
  59.0 19.9 %all_to_all.16 = bf16[16,8,2048]{2,1,0:T(8,128)(2,1)S(1)} all-to-all(bf16[16,8,2048]{2,1,0:T(8,128)(2,1)S(1)} %bitcast.20), channel_id=1, replica_groups=mesh['sp'=16,'tp'=16] {'sp'}, dimensions={0} | all-to-all | bytes 1048576 | tf_op jit(solution)/shard_map/all_to_all | solution.py:617
  79.5 2.7 %collective-permute-start.19 = (bf16[64,2048]{1,0:T(8,128)(2,1)S(1)}, bf16[64,2048]{1,0:T(8,128)(2,1)S(1)}, u32[]{:S(2)}, u32[]{:S(2)}) collective-permute-start(bf16[64,2048]{1,0:T(8,128)(2,1)S(1)} %get-tuple-element.89.refs_1_), channel_id=1, source_target_pairs={{0,14},{1,15},{2,0},{3,1},{4,2},{5,3},{6,4},{7,5},{8,6},{9,7},{10,... | collective-permute-start | bytes 786440 | tf_op jit(solution)/shard_map/ppermute | solution.py:454
  82.2 3.2 %collective-permute-start.16 = (bf16[64,2048]{1,0:T(8,128)(2,1)S(1)}, bf16[64,2048]{1,0:T(8,128)(2,1)S(1)}, u32[]{:S(2)}, u32[]{:S(2)}) collective-permute-start(bf16[64,2048]{1,0:T(8,128)(2,1)S(1)} %get-tuple-element.90.refs_0_), channel_id=1, source_target_pairs={{0,14},{1,15},{2,0},{3,1},{4,2},{5,3},{6,4},{7,5},{8,6},{9,7},{10,... | collective-permute-start | bytes 786440 | tf_op jit(solution)/shard_map/ppermute | solution.py:454
  85.4 3.9 %collective-permute-done.10.refs_2_ = bf16[64,2048]{1,0:T(8,128)(2,1)S(1)} collective-permute-done((bf16[64,2048]{1,0:T(8,128)(2,1)S(1)}, bf16[64,2048]{1,0:T(8,128)(2,1)S(1)}, u32[]{:S(2)}, u32[]{:S(2)}) %collective-permute-start.10) | collective-permute-done | bytes 262176 | tf_op jit(solution)/shard_map/ppermute | solution.py:451
  89.4 3.2 %collective-permute-start.20 = (bf16[64,2048]{1,0:T(8,128)(2,1)S(1)}, bf16[64,2048]{1,0:T(8,128)(2,1)S(1)}, u32[]{:S(2)}, u32[]{:S(2)}) collective-permute-start(bf16[64,2048]{1,0:T(8,128)(2,1)S(1)} %collective-permute-done.19.refs_5_), channel_id=1, source_target_pairs={{0,14},{1,15},{2,0},{3,1},{4,2},{5,3},{6,4},{7,5},{8,6},{9,7},{10,... | collective-permute-start | bytes 786440 | tf_op jit(solution)/shard_map/ppermute | solution.py:454
  92.6 2.4 %collective-permute-done.13.refs_3_ = bf16[64,2048]{1,0:T(8,128)(2,1)S(1)} collective-permute-done((bf16[64,2048]{1,0:T(8,128)(2,1)S(1)}, bf16[64,2048]{1,0:T(8,128)(2,1)S(1)}, u32[]{:S(2)}, u32[]{:S(2)}) %collective-permute-start.13) | collective-permute-done | bytes 262176 | tf_op jit(solution)/shard_map/ppermute | solution.py:451
  95.0 3.2 %collective-permute-start.17 = (bf16[64,2048]{1,0:T(8,128)(2,1)S(1)}, bf16[64,2048]{1,0:T(8,128)(2,1)S(1)}, u32[]{:S(2)}, u32[]{:S(2)}) collective-permute-start(bf16[64,2048]{1,0:T(8,128)(2,1)S(1)} %collective-permute-done.16.refs_4_), channel_id=1, source_target_pairs={{0,14},{1,15},{2,0},{3,1},{4,2},{5,3},{6,4},{7,5},{8,6},{9,7},{10,... | collective-permute-start | bytes 786440 | tf_op jit(solution)/shard_map/ppermute | solution.py:454
  98.2 2.4 %collective-permute-done.11.refs_0_ = bf16[64,2048]{1,0:T(8,128)(2,1)S(1)} collective-permute-done((bf16[64,2048]{1,0:T(8,128)(2,1)S(1)}, bf16[64,2048]{1,0:T(8,128)(2,1)S(1)}, u32[]{:S(2)}, u32[]{:S(2)}) %collective-permute-start.11) | collective-permute-done | bytes 262176 | tf_op jit(solution)/shard_map/ppermute | solution.py:451
  100.6 3.2 %collective-permute-start.21 = (bf16[64,2048]{1,0:T(8,128)(2,1)S(1)}, bf16[64,2048]{1,0:T(8,128)(2,1)S(1)}, u32[]{:S(2)}, u32[]{:S(2)}) collective-permute-start(bf16[64,2048]{1,0:T(8,128)(2,1)S(1)} %collective-permute-done.20.refs_3_), channel_id=1, source_target_pairs={{0,14},{1,15},{2,0},{3,1},{4,2},{5,3},{6,4},{7,5},{8,6},{9,7},{10,... | collective-permute-start | bytes 786440 | tf_op jit(solution)/shard_map/ppermute | solution.py:454
  103.8 2.4 %collective-permute-done.14.refs_1_ = bf16[64,2048]{1,0:T(8,128)(2,1)S(1)} collective-permute-done((bf16[64,2048]{1,0:T(8,128)(2,1)S(1)}, bf16[64,2048]{1,0:T(8,128)(2,1)S(1)}, u32[]{:S(2)}, u32[]{:S(2)}) %collective-permute-start.14) | collective-permute-done | bytes 262176 | tf_op jit(solution)/shard_map/ppermute | solution.py:451
  106.2 3.2 %collective-permute-start.18 = (bf16[64,2048]{1,0:T(8,128)(2,1)S(1)}, bf16[64,2048]{1,0:T(8,128)(2,1)S(1)}, u32[]{:S(2)}, u32[]{:S(2)}) collective-permute-start(bf16[64,2048]{1,0:T(8,128)(2,1)S(1)} %collective-permute-done.17.refs_2_), channel_id=1, source_target_pairs={{0,14},{1,15},{2,0},{3,1},{4,2},{5,3},{6,4},{7,5},{8,6},{9,7},{10,... | collective-permute-start | bytes 786440 | tf_op jit(solution)/shard_map/ppermute | solution.py:454
  109.4 2.4 %collective-permute-done.12.refs_0_ = bf16[64,2048]{1,0:T(8,128)(2,1)S(1)} collective-permute-done((bf16[64,2048]{1,0:T(8,128)(2,1)S(1)}, bf16[64,2048]{1,0:T(8,128)(2,1)S(1)}, u32[]{:S(2)}, u32[]{:S(2)}) %collective-permute-start.12) | collective-permute-done | bytes 262176 | tf_op jit(solution)/shard_map/ppermute | solution.py:451
  111.8 3.2 %collective-permute-start.27 = (bf16[64,2048]{1,0:T(8,128)(2,1)S(1)}, bf16[64,2048]{1,0:T(8,128)(2,1)S(1)}, u32[]{:S(2)}, u32[]{:S(2)}) collective-permute-start(bf16[64,2048]{1,0:T(8,128)(2,1)S(1)} %collective-permute-done.21.refs_3_), channel_id=1, source_target_pairs={{0,14},{1,15},{2,0},{3,1},{4,2},{5,3},{6,4},{7,5},{8,6},{9,7},{10,... | collective-permute-start | bytes 786440 | tf_op jit(solution)/shard_map/ppermute | solution.py:454
  115.1 2.4 %collective-permute-done.15.refs_1_ = bf16[64,2048]{1,0:T(8,128)(2,1)S(1)} collective-permute-done((bf16[64,2048]{1,0:T(8,128)(2,1)S(1)}, bf16[64,2048]{1,0:T(8,128)(2,1)S(1)}, u32[]{:S(2)}, u32[]{:S(2)}) %collective-permute-start.15) | collective-permute-done | bytes 262176 | tf_op jit(solution)/shard_map/ppermute | solution.py:451
  117.4 2.4 %shard_map.131 = (bf16[64,2048]{1,0:T(8,128)(2,1)S(1)}, bf16[64,2048]{1,0:T(8,128)(2,1)S(1)}, bf16[64,2048]{1,0:T(8,128)(2,1)S(1)}, bf16[64,2048]{1,0:T(8,128)(2,1)S(1)}) custom-call(bf16[64,2048]{1,0:T(8,128)(2,1)S(1)} %collective-permute-done.12.refs_0_, bf16[64,2048]{1,0:T(8,128)(2,1)S(1)} %collective-permute-done.15.refs_1_, ...), custom_call_target="tpu_custom_call" | custom-call | flops 1610612736 | bytes 6291456 | tf_op jit(solution)/shard_map/pallas_call | solution.py:434
  120.0 2.3 %collective-permute-done.26.refs_0_ = bf16[64,2048]{1,0:T(8,128)(2,1)S(1)} collective-permute-done((bf16[64,2048]{1,0:T(8,128)(2,1)S(1)}, bf16[64,2048]{1,0:T(8,128)(2,1)S(1)}, u32[]{:S(2)}, u32[]{:S(2)}) %collective-permute-start.26) | collective-permute-done | bytes 262176 | tf_op jit(solution)/shard_map/ppermute | solution.py:451
  123.4 2.0 %collective-permute-start.32 = (bf16[64,2048]{1,0:T(8,128)(2,1)S(1)}, bf16[64,2048]{1,0:T(8,128)(2,1)S(1)}, u32[]{:S(2)}, u32[]{:S(2)}) collective-permute-start(bf16[64,2048]{1,0:T(8,128)(2,1)S(1)} %get-tuple-element.80), channel_id=1, source_target_pairs={{0,14},{1,15},{2,0},{3,1},{4,2},{5,3},{6,4},{7,5},{8,6},{9,7},{10,... | collective-permute-start | bytes 786440 | tf_op jit(solution)/shard_map/ppermute | solution.py:454
  125.5 3.2 %collective-permute-start.23 = (bf16[64,2048]{1,0:T(8,128)(2,1)S(1)}, bf16[64,2048]{1,0:T(8,128)(2,1)S(1)}, u32[]{:S(2)}, u32[]{:S(2)}) collective-permute-start(bf16[64,2048]{1,0:T(8,128)(2,1)S(1)} %get-tuple-element.72), channel_id=1, source_target_pairs={{0,14},{1,15},{2,0},{3,1},{4,2},{5,3},{6,4},{7,5},{8,6},{9,7},{10,... | collective-permute-start | bytes 786440 | tf_op jit(solution)/shard_map/ppermute | solution.py:454
  128.7 2.4 %shard_map.132 = (bf16[64,2048]{1,0:T(8,128)(2,1)S(1)}, bf16[64,2048]{1,0:T(8,128)(2,1)S(1)}, bf16[64,2048]{1,0:T(8,128)(2,1)S(1)}, bf16[64,2048]{1,0:T(8,128)(2,1)S(1)}) custom-call(bf16[64,2048]{1,0:T(8,128)(2,1)S(1)} %collective-permute-done.11.refs_0_, bf16[64,2048]{1,0:T(8,128)(2,1)S(1)} %collective-permute-done.14.refs_1_, ...), custom_call_target="tpu_custom_call" | custom-call | flops 1610612736 | bytes 6291456 | tf_op jit(solution)/shard_map/pallas_call | solution.py:434
  131.1 3.6 %shard_map.133 = (bf16[64,2048]{1,0:T(8,128)(2,1)S(1)}, bf16[64,2048]{1,0:T(8,128)(2,1)S(1)}, bf16[64,2048]{1,0:T(8,128)(2,1)S(1)}, bf16[64,2048]{1,0:T(8,128)(2...) custom-call(bf16[64,2048]{1,0:T(8,128)(2,1)S(1)} %get-tuple-element.90.refs_0_, ...), custom_call_target="tpu_custom_call" | custom-call | flops 2415919104 | bytes 6291456 | tf_op jit(solution)/shard_map/pallas_call | solution.py:434
  135.1 3.3 %collective-permute-start.33 = (bf16[64,2048]{1,0:T(8,128)(2,1)S(1)}, bf16[64,2048]{1,0:T(8,128)(2,1)S(1)}, u32[]{:S(2)}, u32[]{:S(2)}) collective-permute-start(bf16[64,2048]{1,0:T(8,128)(2,1)S(1)} %add_convert_fusion.5), channel_id=1, source_target_pairs={{0,14},{1,15},{2,0},{3,1},{4,2},{5,3},{6,4},{7,5},{8,6},{9,7},{10,... | collective-permute-start | bytes 786440 | tf_op jit(solution)/shard_map/ppermute | solution.py:454
  138.7 3.3 %collective-permute-start.24 = (bf16[64,2048]{1,0:T(8,128)(2,1)S(1)}, bf16[64,2048]{1,0:T(8,128)(2,1)S(1)}, u32[]{:S(2)}, u32[]{:S(2)}) collective-permute-start(bf16[64,2048]{1,0:T(8,128)(2,1)S(1)} %add_convert_fusion.11), channel_id=1, source_target_pairs={{0,14},{1,15},{2,0},{3,1},{4,2},{5,3},{6,4},{7,5},{8,6},{9,7},{10,... | collective-permute-start | bytes 786440 | tf_op jit(solution)/shard_map/ppermute | solution.py:454
  142.0 3.5 %collective-permute-done.37 = bf16[64,2048]{1,0:T(8,128)(2,1)S(1)} collective-permute-done((bf16[64,2048]{1,0:T(8,128)(2,1)S(1)}, bf16[64,2048]{1,0:T(8,128)(2,1)S(1)}, u32[]{:S(2)}, u32[]{:S(2)}) %collective-permute-start.37) | collective-permute-done | bytes 262176 | tf_op jit(solution)/shard_map/ppermute | solution.py:451
  145.7 3.3 %collective-permute-start.34 = (bf16[64,2048]{1,0:T(8,128)(2,1)S(1)}, bf16[64,2048]{1,0:T(8,128)(2,1)S(1)}, u32[]{:S(2)}, u32[]{:S(2)}) collective-permute-start(bf16[64,2048]{1,0:T(8,128)(2,1)S(1)} %add_convert_fusion.4), channel_id=1, source_target_pairs={{0,14},{1,15},{2,0},{3,1},{4,2},{5,3},{6,4},{7,5},{8,6},{9,7},{10,... | collective-permute-start | bytes 786440 | tf_op jit(solution)/shard_map/ppermute | solution.py:454
  149.0 2.1 %collective-permute-done.29 = bf16[64,2048]{1,0:T(8,128)(2,1)S(1)} collective-permute-done((bf16[64,2048]{1,0:T(8,128)(2,1)S(1)}, bf16[64,2048]{1,0:T(8,128)(2,1)S(1)}, u32[]{:S(2)}, u32[]{:S(2)}) %collective-permute-start.29) | collective-permute-done | bytes 262176 | tf_op jit(solution)/shard_map/ppermute | solution.py:451
  151.3 3.3 %collective-permute-start.25 = (bf16[64,2048]{1,0:T(8,128)(2,1)S(1)}, bf16[64,2048]{1,0:T(8,128)(2,1)S(1)}, u32[]{:S(2)}, u32[]{:S(2)}) collective-permute-start(bf16[64,2048]{1,0:T(8,128)(2,1)S(1)} %add_convert_fusion.10), channel_id=1, source_target_pairs={{0,14},{1,15},{2,0},{3,1},{4,2},{5,3},{6,4},{7,5},{8,6},{9,7},{10,... | collective-permute-start | bytes 786440 | tf_op jit(solution)/shard_map/ppermute | solution.py:454
  154.6 1.8 collective-permute-done.34
  156.4 3.8 %collective-permute-start.35 = (bf16[64,2048]{1,0:T(8,128)(2,1)S(1)}, bf16[64,2048]{1,0:T(8,128)(2,1)S(1)}, u32[]{:S(2)}, u32[]{:S(2)}) collective-permute-start(bf16[64,2048]{1,0:T(8,128)(2,1)S(1)} %add_convert_fusion.3), channel_id=1, source_target_pairs={{0,14},{1,15},{2,0},{3,1},{4,2},{5,3},{6,4},{7,5},{8,6},{9,7},{10,... | collective-permute-start | bytes 786440 | tf_op jit(solution)/shard_map/ppermute | solution.py:454
  160.4 3.7 %collective-permute-done.35 = bf16[64,2048]{1,0:T(8,128)(2,1)S(1)} collective-permute-done((bf16[64,2048]{1,0:T(8,128)(2,1)S(1)}, bf16[64,2048]{1,0:T(8,128)(2,1)S(1)}, u32[]{:S(2)}, u32[]{:S(2)}) %collective-permute-start.35) | collective-permute-done | bytes 262176 | tf_op jit(solution)/shard_map/ppermute | solution.py:454
  164.2 3.7 %collective-permute-done.31 = bf16[64,2048]{1,0:T(8,128)(2,1)S(1)} collective-permute-done((bf16[64,2048]{1,0:T(8,128)(2,1)S(1)}, bf16[64,2048]{1,0:T(8,128)(2,1)S(1)}, u32[]{:S(2)}, u32[]{:S(2)}) %collective-permute-start.31) | collective-permute-done | bytes 262176 | tf_op jit(solution)/shard_map/ppermute | solution.py:451
  168.1 13.5 %all_to_all.17 = bf16[16,8,2048]{2,1,0:T(8,128)(2,1)S(1)} all-to-all(bf16[16,8,2048]{2,1,0:T(8,128)(2,1)S(1)} %maximum_bitcast_fusion), channel_id=1, replica_groups=mesh['sp'=16,'tp'=16] {'sp'}, dimensions={0} | all-to-all | bytes 1048576 | tf_op jit(solution)/shard_map/all_to_all | solution.py:620
  (76 shorter events, 7.7 us)
Async XLA Ops:
  1.2 10.3 %collective-permute-start.3 = (bf16[544,256]{1,0:T(8,128)(2,1)S(1)}, bf16[544,256]{1,0:T(8,128)(2,1)S(1)}, u32[]{:S(2)}, u32[]{:S(2)}) collective-permute-start(bf16[544,256]{1,0:T(8,128)(2,1)S(1)} %get-tuple-element.59.refs_3_.refs_1_), channel_id=1, source_target_pairs={{0,16},{16,32},{32,48},{48,0},{64,80},{80,96},{96,112},{112,64},{1... | collective-permute-start | bytes 835592 | tf_op jit(solution)/shard_map/ppermute | solution.py:321
  4.6 10.3 %collective-permute-start.5 = (bf16[544,256]{1,0:T(8,128)(2,1)S(1)}, bf16[544,256]{1,0:T(8,128)(2,1)S(1)}, u32[]{:S(2)}, u32[]{:S(2)}) collective-permute-start(bf16[544,256]{1,0:T(8,128)(2,1)S(1)} %get-tuple-element.59.refs_3_.refs_1_), channel_id=1, source_target_pairs={{0,48},{16,0},{32,16},{48,32},{64,112},{80,64},{96,80},{112,96},{1... | collective-permute-start | bytes 835592 | tf_op jit(solution)/shard_map/ppermute | solution.py:321
  7.3 11.1 %collective-permute-start = (bf16[144,512]{1,0:T(8,128)(2,1)S(1)}, bf16[144,512]{1,0:T(8,128)(2,1)S(1)}, u32[]{:S(2)}, u32[]{:S(2)}) collective-permute-start(bf16[144,512]{1,0:T(8,128)(2,1)S(1)} %get-tuple-element.58.refs_0_), channel_id=1, source_target_pairs={{192,0},{208,16},{224,32},{240,48},{193,1},{209,17},{225,33},{241,... | collective-permute-start | bytes 442376 | tf_op jit(solution)/shard_map/ppermute | solution.py:321
  8.6 9.8 %collective-permute-start.1 = (bf16[144,512]{1,0:T(8,128)(2,1)S(1)}, bf16[144,512]{1,0:T(8,128)(2,1)S(1)}, u32[]{:S(2)}, u32[]{:S(2)}) collective-permute-start(bf16[144,512]{1,0:T(8,128)(2,1)S(1)} %get-tuple-element.58.refs_0_), channel_id=1, source_target_pairs={{128,0},{144,16},{160,32},{176,48},{192,64},{208,80},{224,96},{240... | collective-permute-start | bytes 442376 | tf_op jit(solution)/shard_map/ppermute | solution.py:321
  9.9 8.5 %collective-permute-start.2 = (bf16[144,512]{1,0:T(8,128)(2,1)S(1)}, bf16[144,512]{1,0:T(8,128)(2,1)S(1)}, u32[]{:S(2)}, u32[]{:S(2)}) collective-permute-start(bf16[144,512]{1,0:T(8,128)(2,1)S(1)} %get-tuple-element.58.refs_0_), channel_id=1, source_target_pairs={{64,0},{80,16},{96,32},{112,48},{128,64},{144,80},{160,96},{176,11... | collective-permute-start | bytes 442376 | tf_op jit(solution)/shard_map/ppermute | solution.py:321
  11.5 13.4 %collective-permute-start.4 = (bf16[272,256]{1,0:T(8,128)(2,1)S(1)}, bf16[272,256]{1,0:T(8,128)(2,1)S(1)}, u32[]{:S(2)}, u32[]{:S(2)}) collective-permute-start(bf16[272,256]{1,0:T(8,128)(2,1)S(1)} %slice.24), channel_id=1, source_target_pairs={{0,16},{16,32},{32,48},{48,0},{64,80},{80,96},{96,112},{112,64},{1... | collective-permute-start | bytes 417800 | tf_op jit(solution)/shard_map/ppermute | solution.py:321
  15.0 10.0 %collective-permute-start.6 = (bf16[272,256]{1,0:T(8,128)(2,1)S(1)}, bf16[272,256]{1,0:T(8,128)(2,1)S(1)}, u32[]{:S(2)}, u32[]{:S(2)}) collective-permute-start(bf16[272,256]{1,0:T(8,128)(2,1)S(1)} %slice.25), channel_id=1, source_target_pairs={{0,48},{16,0},{32,16},{48,32},{64,112},{80,64},{96,80},{112,96},{1... | collective-permute-start | bytes 417800 | tf_op jit(solution)/shard_map/ppermute | solution.py:321
  18.4 38.0 %slice-start = ((s8[8388608]{0:T(1024)(128)(4,1)}), s8[4194304]{0:T(1024)(128)(4,1)S(1)}, s32[]{:S(2)}) async-start(s8[8388608]{0:T(1024)(128)(4,1)} %bitcast.17), calls=%async_computation.3 | async-start | bytes 8388608
  25.0 31.4 %slice-start.1 = ((s8[8388608]{0:T(1024)(128)(4,1)}), s8[4194304]{0:T(1024)(128)(4,1)S(1)}, s32[]{:S(2)}) async-start(s8[8388608]{0:T(1024)(128)(4,1)} %bitcast.17), calls=%async_computation.4 | async-start | bytes 8388608
  29.4 9.8 %copy-start.4 = (f32[128]{0:T(128)S(1)}, f32[128]{0:T(128)}, u32[]{:S(2)}) copy-start(f32[128]{0:T(128)} %param.17) | copy-start | bytes 1540
  29.4 27.0 %copy-start = (bf16[32,2048]{1,0:T(8,128)(2,1)S(1)}, bf16[32,2048]{1,0:T(8,128)(2,1)}, u32[]{:S(2)}) copy-start(bf16[32,2048]{1,0:T(8,128)(2,1)} %stream.1) | copy-start | bytes 393220
  29.4 27.0 %copy-start.1 = (f32[2048]{0:T(1024)S(1)}, f32[2048]{0:T(1024)}, u32[]{:S(2)}) copy-start(f32[2048]{0:T(1024)} %param.20) | copy-start | bytes 24580
  29.4 27.0 %copy-start.2 = (s32[32,2]{0,1:T(2,128)S(1)}, s32[32,2]{0,1:T(2,128)}, u32[]{:S(2)}) copy-start(s32[32,2]{0,1:T(2,128)} %param.21) | copy-start | bytes 772
  29.4 27.0 %copy-start.3 = (f32[32,2]{0,1:T(2,128)S(1)}, f32[32,2]{0,1:T(2,128)}, u32[]{:S(2)}) copy-start(f32[32,2]{0,1:T(2,128)} %param.22) | copy-start | bytes 772
  29.4 88.0 %collective-permute-start.22 = (bf16[6144,256]{1,0:T(8,128)(2,1)S(1)}, bf16[6144,256]{1,0:T(8,128)(2,1)S(1)}, u32[]{:S(2)}, u32[]{:S(2)}) collective-permute-start(bf16[6144,256]{1,0:T(8,128)(2,1)S(1)} %stage_weights.1.refs_4_.refs_6_.refs_2_), channel_id=1, source_target_pairs={{0,1},{1,0},{2,3},{3,2},{4,5},{5,4},{6,7},{7,6},{8,9},{9,8},{10,11... | collective-permute-start | bytes 9437192 | tf_op jit(solution)/shard_map/ppermute | solution.py:608
  29.5 6.6 %collective-permute-start.7 = (bf16[144,512]{1,0:T(8,128)(2,1)S(1)}, bf16[144,512]{1,0:T(8,128)(2,1)S(1)}, u32[]{:S(2)}, u32[]{:S(2)}) collective-permute-start(bf16[144,512]{1,0:T(8,128)(2,1)S(1)} %get-tuple-element.55), channel_id=1, source_target_pairs={{0,64},{16,80},{32,96},{48,112},{64,128},{80,144},{96,160},{112,17... | collective-permute-start | bytes 442376 | tf_op jit(solution)/shard_map/ppermute | solution.py:321
  31.2 6.9 %collective-permute-start.8 = (bf16[144,512]{1,0:T(8,128)(2,1)S(1)}, bf16[144,512]{1,0:T(8,128)(2,1)S(1)}, u32[]{:S(2)}, u32[]{:S(2)}) collective-permute-start(bf16[144,512]{1,0:T(8,128)(2,1)S(1)} %get-tuple-element.56), channel_id=1, source_target_pairs={{0,128},{16,144},{32,160},{48,176},{64,192},{80,208},{96,224},{112... | collective-permute-start | bytes 442376 | tf_op jit(solution)/shard_map/ppermute | solution.py:321
  33.4 5.8 %collective-permute-start.9 = (bf16[144,512]{1,0:T(8,128)(2,1)S(1)}, bf16[144,512]{1,0:T(8,128)(2,1)S(1)}, u32[]{:S(2)}, u32[]{:S(2)}) collective-permute-start(bf16[144,512]{1,0:T(8,128)(2,1)S(1)} %get-tuple-element.57), channel_id=1, source_target_pairs={{0,192},{16,208},{32,224},{48,240},{1,193},{17,209},{33,225},{49,2... | collective-permute-start | bytes 442376 | tf_op jit(solution)/shard_map/ppermute | solution.py:321
  78.9 10.5 %collective-permute-start.10 = (bf16[64,2048]{1,0:T(8,128)(2,1)S(1)}, bf16[64,2048]{1,0:T(8,128)(2,1)S(1)}, u32[]{:S(2)}, u32[]{:S(2)}) collective-permute-start(bf16[64,2048]{1,0:T(8,128)(2,1)S(1)} %get-tuple-element.90.refs_0_), channel_id=1, source_target_pairs={{0,2},{1,3},{2,4},{3,5},{4,6},{5,7},{6,8},{7,9},{8,10},{9,11},{10,... | collective-permute-start | bytes 786440 | tf_op jit(solution)/shard_map/ppermute | solution.py:451
  79.5 9.8 %collective-permute-start.19 = (bf16[64,2048]{1,0:T(8,128)(2,1)S(1)}, bf16[64,2048]{1,0:T(8,128)(2,1)S(1)}, u32[]{:S(2)}, u32[]{:S(2)}) collective-permute-start(bf16[64,2048]{1,0:T(8,128)(2,1)S(1)} %get-tuple-element.89.refs_1_), channel_id=1, source_target_pairs={{0,14},{1,15},{2,0},{3,1},{4,2},{5,3},{6,4},{7,5},{8,6},{9,7},{10,... | collective-permute-start | bytes 786440 | tf_op jit(solution)/shard_map/ppermute | solution.py:454
  82.2 12.8 %collective-permute-start.13 = (bf16[64,2048]{1,0:T(8,128)(2,1)S(1)}, bf16[64,2048]{1,0:T(8,128)(2,1)S(1)}, u32[]{:S(2)}, u32[]{:S(2)}) collective-permute-start(bf16[64,2048]{1,0:T(8,128)(2,1)S(1)} %get-tuple-element.89.refs_1_), channel_id=1, source_target_pairs={{0,2},{1,3},{2,4},{3,5},{4,6},{5,7},{6,8},{7,9},{8,10},{9,11},{10,... | collective-permute-start | bytes 786440 | tf_op jit(solution)/shard_map/ppermute | solution.py:451
  82.2 12.8 %collective-permute-start.16 = (bf16[64,2048]{1,0:T(8,128)(2,1)S(1)}, bf16[64,2048]{1,0:T(8,128)(2,1)S(1)}, u32[]{:S(2)}, u32[]{:S(2)}) collective-permute-start(bf16[64,2048]{1,0:T(8,128)(2,1)S(1)} %get-tuple-element.90.refs_0_), channel_id=1, source_target_pairs={{0,14},{1,15},{2,0},{3,1},{4,2},{5,3},{6,4},{7,5},{8,6},{9,7},{10,... | collective-permute-start | bytes 786440 | tf_op jit(solution)/shard_map/ppermute | solution.py:454
  89.4 11.2 %collective-permute-start.11 = (bf16[64,2048]{1,0:T(8,128)(2,1)S(1)}, bf16[64,2048]{1,0:T(8,128)(2,1)S(1)}, u32[]{:S(2)}, u32[]{:S(2)}) collective-permute-start(bf16[64,2048]{1,0:T(8,128)(2,1)S(1)} %collective-permute-done.10.refs_2_), channel_id=1, source_target_pairs={{0,2},{1,3},{2,4},{3,5},{4,6},{5,7},{6,8},{7,9},{8,10},{9,11},{10,... | collective-permute-start | bytes 786440 | tf_op jit(solution)/shard_map/ppermute | solution.py:451
  89.4 11.2 %collective-permute-start.20 = (bf16[64,2048]{1,0:T(8,128)(2,1)S(1)}, bf16[64,2048]{1,0:T(8,128)(2,1)S(1)}, u32[]{:S(2)}, u32[]{:S(2)}) collective-permute-start(bf16[64,2048]{1,0:T(8,128)(2,1)S(1)} %collective-permute-done.19.refs_5_), channel_id=1, source_target_pairs={{0,14},{1,15},{2,0},{3,1},{4,2},{5,3},{6,4},{7,5},{8,6},{9,7},{10,... | collective-permute-start | bytes 786440 | tf_op jit(solution)/shard_map/ppermute | solution.py:454
  95.0 11.2 %collective-permute-start.14 = (bf16[64,2048]{1,0:T(8,128)(2,1)S(1)}, bf16[64,2048]{1,0:T(8,128)(2,1)S(1)}, u32[]{:S(2)}, u32[]{:S(2)}) collective-permute-start(bf16[64,2048]{1,0:T(8,128)(2,1)S(1)} %collective-permute-done.13.refs_3_), channel_id=1, source_target_pairs={{0,2},{1,3},{2,4},{3,5},{4,6},{5,7},{6,8},{7,9},{8,10},{9,11},{10,... | collective-permute-start | bytes 786440 | tf_op jit(solution)/shard_map/ppermute | solution.py:451
  95.0 11.2 %collective-permute-start.17 = (bf16[64,2048]{1,0:T(8,128)(2,1)S(1)}, bf16[64,2048]{1,0:T(8,128)(2,1)S(1)}, u32[]{:S(2)}, u32[]{:S(2)}) collective-permute-start(bf16[64,2048]{1,0:T(8,128)(2,1)S(1)} %collective-permute-done.16.refs_4_), channel_id=1, source_target_pairs={{0,14},{1,15},{2,0},{3,1},{4,2},{5,3},{6,4},{7,5},{8,6},{9,7},{10,... | collective-permute-start | bytes 786440 | tf_op jit(solution)/shard_map/ppermute | solution.py:454
  100.6 11.2 %collective-permute-start.12 = (bf16[64,2048]{1,0:T(8,128)(2,1)S(1)}, bf16[64,2048]{1,0:T(8,128)(2,1)S(1)}, u32[]{:S(2)}, u32[]{:S(2)}) collective-permute-start(bf16[64,2048]{1,0:T(8,128)(2,1)S(1)} %collective-permute-done.11.refs_0_), channel_id=1, source_target_pairs={{0,2},{1,3},{2,4},{3,5},{4,6},{5,7},{6,8},{7,9},{8,10},{9,11},{10,... | collective-permute-start | bytes 786440 | tf_op jit(solution)/shard_map/ppermute | solution.py:451
  100.6 11.2 %collective-permute-start.21 = (bf16[64,2048]{1,0:T(8,128)(2,1)S(1)}, bf16[64,2048]{1,0:T(8,128)(2,1)S(1)}, u32[]{:S(2)}, u32[]{:S(2)}) collective-permute-start(bf16[64,2048]{1,0:T(8,128)(2,1)S(1)} %collective-permute-done.20.refs_3_), channel_id=1, source_target_pairs={{0,14},{1,15},{2,0},{3,1},{4,2},{5,3},{6,4},{7,5},{8,6},{9,7},{10,... | collective-permute-start | bytes 786440 | tf_op jit(solution)/shard_map/ppermute | solution.py:454
  106.2 11.2 %collective-permute-start.15 = (bf16[64,2048]{1,0:T(8,128)(2,1)S(1)}, bf16[64,2048]{1,0:T(8,128)(2,1)S(1)}, u32[]{:S(2)}, u32[]{:S(2)}) collective-permute-start(bf16[64,2048]{1,0:T(8,128)(2,1)S(1)} %collective-permute-done.14.refs_1_), channel_id=1, source_target_pairs={{0,2},{1,3},{2,4},{3,5},{4,6},{5,7},{6,8},{7,9},{8,10},{9,11},{10,... | collective-permute-start | bytes 786440 | tf_op jit(solution)/shard_map/ppermute | solution.py:451
  106.2 11.2 %collective-permute-start.18 = (bf16[64,2048]{1,0:T(8,128)(2,1)S(1)}, bf16[64,2048]{1,0:T(8,128)(2,1)S(1)}, u32[]{:S(2)}, u32[]{:S(2)}) collective-permute-start(bf16[64,2048]{1,0:T(8,128)(2,1)S(1)} %collective-permute-done.17.refs_2_), channel_id=1, source_target_pairs={{0,14},{1,15},{2,0},{3,1},{4,2},{5,3},{6,4},{7,5},{8,6},{9,7},{10,... | collective-permute-start | bytes 786440 | tf_op jit(solution)/shard_map/ppermute | solution.py:454
  111.8 10.5 %collective-permute-start.26 = (bf16[64,2048]{1,0:T(8,128)(2,1)S(1)}, bf16[64,2048]{1,0:T(8,128)(2,1)S(1)}, u32[]{:S(2)}, u32[]{:S(2)}) collective-permute-start(bf16[64,2048]{1,0:T(8,128)(2,1)S(1)} %collective-permute-done.12.refs_0_), channel_id=1, source_target_pairs={{0,2},{1,3},{2,4},{3,5},{4,6},{5,7},{6,8},{7,9},{8,10},{9,11},{10,... | collective-permute-start | bytes 786440 | tf_op jit(solution)/shard_map/ppermute | solution.py:451
  111.8 10.5 %collective-permute-start.27 = (bf16[64,2048]{1,0:T(8,128)(2,1)S(1)}, bf16[64,2048]{1,0:T(8,128)(2,1)S(1)}, u32[]{:S(2)}, u32[]{:S(2)}) collective-permute-start(bf16[64,2048]{1,0:T(8,128)(2,1)S(1)} %collective-permute-done.21.refs_3_), channel_id=1, source_target_pairs={{0,14},{1,15},{2,0},{3,1},{4,2},{5,3},{6,4},{7,5},{8,6},{9,7},{10,... | collective-permute-start | bytes 786440 | tf_op jit(solution)/shard_map/ppermute | solution.py:454
  119.8 14.8 %collective-permute-start.36 = (bf16[64,2048]{1,0:T(8,128)(2,1)S(1)}, bf16[64,2048]{1,0:T(8,128)(2,1)S(1)}, u32[]{:S(2)}, u32[]{:S(2)}) collective-permute-start(bf16[64,2048]{1,0:T(8,128)(2,1)S(1)} %get-tuple-element.84), channel_id=1, source_target_pairs={{0,2},{1,3},{2,4},{3,5},{4,6},{5,7},{6,8},{7,9},{8,10},{9,11},{10,... | collective-permute-start | bytes 786440 | tf_op jit(solution)/shard_map/ppermute | solution.py:451
  123.4 11.6 %collective-permute-start.32 = (bf16[64,2048]{1,0:T(8,128)(2,1)S(1)}, bf16[64,2048]{1,0:T(8,128)(2,1)S(1)}, u32[]{:S(2)}, u32[]{:S(2)}) collective-permute-start(bf16[64,2048]{1,0:T(8,128)(2,1)S(1)} %get-tuple-element.80), channel_id=1, source_target_pairs={{0,14},{1,15},{2,0},{3,1},{4,2},{5,3},{6,4},{7,5},{8,6},{9,7},{10,... | collective-permute-start | bytes 786440 | tf_op jit(solution)/shard_map/ppermute | solution.py:454
  125.5 13.0 %collective-permute-start.28 = (bf16[64,2048]{1,0:T(8,128)(2,1)S(1)}, bf16[64,2048]{1,0:T(8,128)(2,1)S(1)}, u32[]{:S(2)}, u32[]{:S(2)}) collective-permute-start(bf16[64,2048]{1,0:T(8,128)(2,1)S(1)} %get-tuple-element.75), channel_id=1, source_target_pairs={{0,2},{1,3},{2,4},{3,5},{4,6},{5,7},{6,8},{7,9},{8,10},{9,11},{10,... | collective-permute-start | bytes 786440 | tf_op jit(solution)/shard_map/ppermute | solution.py:451
  125.5 13.1 %collective-permute-start.23 = (bf16[64,2048]{1,0:T(8,128)(2,1)S(1)}, bf16[64,2048]{1,0:T(8,128)(2,1)S(1)}, u32[]{:S(2)}, u32[]{:S(2)}) collective-permute-start(bf16[64,2048]{1,0:T(8,128)(2,1)S(1)} %get-tuple-element.72), channel_id=1, source_target_pairs={{0,14},{1,15},{2,0},{3,1},{4,2},{5,3},{6,4},{7,5},{8,6},{9,7},{10,... | collective-permute-start | bytes 786440 | tf_op jit(solution)/shard_map/ppermute | solution.py:454
  134.7 10.7 %collective-permute-start.37 = (bf16[64,2048]{1,0:T(8,128)(2,1)S(1)}, bf16[64,2048]{1,0:T(8,128)(2,1)S(1)}, u32[]{:S(2)}, u32[]{:S(2)}) collective-permute-start(bf16[64,2048]{1,0:T(8,128)(2,1)S(1)} %add_convert_fusion.2), channel_id=1, source_target_pairs={{0,2},{1,3},{2,4},{3,5},{4,6},{5,7},{6,8},{7,9},{8,10},{9,11},{10,... | collective-permute-start | bytes 786440 | tf_op jit(solution)/shard_map/ppermute | solution.py:451
  135.1 10.5 %collective-permute-start.33 = (bf16[64,2048]{1,0:T(8,128)(2,1)S(1)}, bf16[64,2048]{1,0:T(8,128)(2,1)S(1)}, u32[]{:S(2)}, u32[]{:S(2)}) collective-permute-start(bf16[64,2048]{1,0:T(8,128)(2,1)S(1)} %add_convert_fusion.5), channel_id=1, source_target_pairs={{0,14},{1,15},{2,0},{3,1},{4,2},{5,3},{6,4},{7,5},{8,6},{9,7},{10,... | collective-permute-start | bytes 786440 | tf_op jit(solution)/shard_map/ppermute | solution.py:454
  138.5 12.6 %collective-permute-start.29 = (bf16[64,2048]{1,0:T(8,128)(2,1)S(1)}, bf16[64,2048]{1,0:T(8,128)(2,1)S(1)}, u32[]{:S(2)}, u32[]{:S(2)}) collective-permute-start(bf16[64,2048]{1,0:T(8,128)(2,1)S(1)} %add_convert_fusion.9), channel_id=1, source_target_pairs={{0,2},{1,3},{2,4},{3,5},{4,6},{5,7},{6,8},{7,9},{8,10},{9,11},{10,... | collective-permute-start | bytes 786440 | tf_op jit(solution)/shard_map/ppermute | solution.py:451
  138.7 12.5 %collective-permute-start.24 = (bf16[64,2048]{1,0:T(8,128)(2,1)S(1)}, bf16[64,2048]{1,0:T(8,128)(2,1)S(1)}, u32[]{:S(2)}, u32[]{:S(2)}) collective-permute-start(bf16[64,2048]{1,0:T(8,128)(2,1)S(1)} %add_convert_fusion.11), channel_id=1, source_target_pairs={{0,14},{1,15},{2,0},{3,1},{4,2},{5,3},{6,4},{7,5},{8,6},{9,7},{10,... | collective-permute-start | bytes 786440 | tf_op jit(solution)/shard_map/ppermute | solution.py:454
  145.5 14.9 %collective-permute-start.38 = (bf16[64,2048]{1,0:T(8,128)(2,1)S(1)}, bf16[64,2048]{1,0:T(8,128)(2,1)S(1)}, u32[]{:S(2)}, u32[]{:S(2)}) collective-permute-start(bf16[64,2048]{1,0:T(8,128)(2,1)S(1)} %add_convert_fusion.1), channel_id=1, source_target_pairs={{0,2},{1,3},{2,4},{3,5},{4,6},{5,7},{6,8},{7,9},{8,10},{9,11},{10,... | collective-permute-start | bytes 786440 | tf_op jit(solution)/shard_map/ppermute | solution.py:451
  145.7 10.7 %collective-permute-start.34 = (bf16[64,2048]{1,0:T(8,128)(2,1)S(1)}, bf16[64,2048]{1,0:T(8,128)(2,1)S(1)}, u32[]{:S(2)}, u32[]{:S(2)}) collective-permute-start(bf16[64,2048]{1,0:T(8,128)(2,1)S(1)} %add_convert_fusion.4), channel_id=1, source_target_pairs={{0,14},{1,15},{2,0},{3,1},{4,2},{5,3},{6,4},{7,5},{8,6},{9,7},{10,... | collective-permute-start | bytes 786440 | tf_op jit(solution)/shard_map/ppermute | solution.py:454
  151.1 9.1 %collective-permute-start.30 = (bf16[64,2048]{1,0:T(8,128)(2,1)S(1)}, bf16[64,2048]{1,0:T(8,128)(2,1)S(1)}, u32[]{:S(2)}, u32[]{:S(2)}) collective-permute-start(bf16[64,2048]{1,0:T(8,128)(2,1)S(1)} %add_convert_fusion.8), channel_id=1, source_target_pairs={{0,2},{1,3},{2,4},{3,5},{4,6},{5,7},{6,8},{7,9},{8,10},{9,11},{10,... | collective-permute-start | bytes 786440 | tf_op jit(solution)/shard_map/ppermute | solution.py:451
  151.3 12.9 %collective-permute-start.25 = (bf16[64,2048]{1,0:T(8,128)(2,1)S(1)}, bf16[64,2048]{1,0:T(8,128)(2,1)S(1)}, u32[]{:S(2)}, u32[]{:S(2)}) collective-permute-start(bf16[64,2048]{1,0:T(8,128)(2,1)S(1)} %add_convert_fusion.10), channel_id=1, source_target_pairs={{0,14},{1,15},{2,0},{3,1},{4,2},{5,3},{6,4},{7,5},{8,6},{9,7},{10,... | collective-permute-start | bytes 786440 | tf_op jit(solution)/shard_map/ppermute | solution.py:454
  156.4 7.7 %collective-permute-start.35 = (bf16[64,2048]{1,0:T(8,128)(2,1)S(1)}, bf16[64,2048]{1,0:T(8,128)(2,1)S(1)}, u32[]{:S(2)}, u32[]{:S(2)}) collective-permute-start(bf16[64,2048]{1,0:T(8,128)(2,1)S(1)} %add_convert_fusion.3), channel_id=1, source_target_pairs={{0,14},{1,15},{2,0},{3,1},{4,2},{5,3},{6,4},{7,5},{8,6},{9,7},{10,... | collective-permute-start | bytes 786440 | tf_op jit(solution)/shard_map/ppermute | solution.py:454
  160.3 7.7 %collective-permute-start.31 = (bf16[64,2048]{1,0:T(8,128)(2,1)S(1)}, bf16[64,2048]{1,0:T(8,128)(2,1)S(1)}, u32[]{:S(2)}, u32[]{:S(2)}) collective-permute-start(bf16[64,2048]{1,0:T(8,128)(2,1)S(1)} %add_convert_fusion.7), channel_id=1, source_target_pairs={{0,2},{1,3},{2,4},{3,5},{4,6},{5,7},{6,8},{7,9},{8,10},{9,11},{10,... | collective-permute-start | bytes 786440 | tf_op jit(solution)/shard_map/ppermute | solution.py:451
